TPU v7x, 256 devices: a whole 4x4x8 slice. The times are simulated.
256 devices in a mesh: sp: 32 (over z, x), tp: 8 (over y, core).
Axes of the slice: x: 4, y: 4, z: 8, core: 2. Of those that a mesh axis runs over, the one named last changes fastest.
Arguments:
- upstream: bfloat16 [8192, 2048], P('sp'), may hold values from -6 to 6
- stream: bfloat16 [8192, 2048], P('sp'), may hold values from -10 to 10
- routes: int32 [8192, 2], P('sp'), may hold values from 0 to 31, all different within a row; in each aligned block of 256 rows (0 to 255, 256 to 511, ...) at most 32 rows name the same one
- route_weights: float32 [8192, 2], P('sp'), may hold values from 0.1 to 1
- glu_value: bfloat16 [8192, 512], P('sp', 'tp'), may hold values from -6 to 6
- glu_gate: bfloat16 [8192, 512], P('sp', 'tp'), may hold values from -10 to 10
- conv_taps: float32 [31, 512], P(None, 'tp'), may hold values from -1 to 1
- conv_saved: bfloat16 [8192, 512], P('sp', 'tp'), may hold values from -600 to 600
- out_proj: bfloat16 [2048, 512], P(None, 'tp'), may hold values from -0.25 to 0.25
- expert_gate: bfloat16 [32, 2048, 2048], P('sp', None, 'tp'), may hold values from -0.125 to 0.125
- expert_up: bfloat16 [32, 2048, 2048], P('sp', None, 'tp'), may hold values from -0.125 to 0.125
- expert_down: bfloat16 [32, 2048, 2048], P('sp', 'tp'), may hold values from -0.125 to 0.125
Outputs:
- grad_stream: bfloat16 [8192, 2048], P('sp', 'tp')
- grad_value: bfloat16 [8192, 512], P('sp', 'tp')
- grad_gate: bfloat16 [8192, 512], P('sp', 'tp')
- grad_out_proj: float32 [2048, 512], P('sp', 'tp')
- grad_expert_gate: float32 [32, 2048, 2048], P('sp', None, 'tp')
- grad_expert_up: float32 [32, 2048, 2048], P('sp', None, 'tp')
- grad_expert_down: float32 [32, 2048, 2048], P('sp', 'tp')
Inputs may be any that keep to these rules, and one draw needn't show every extreme that they name: `routes`: each row names 2 different experts; among the 256 rows of one index of sp no expert is named more than 32 times, a bound that some block reaches.
All inputs are finite; a program needn't handle non-finite values.
Results may differ from a plain program's by a relative error of at most 0.014.
Values may be sent and summed in bfloat16 or wider, within the bound.
No kernel may reach another device: no remote copies, remote signals or barrier semaphores. Data moves between devices by JAX's collectives and lax.ppermute only.
A program may use at most 128 MiB of HBM per device.

v0:
```python
import jax
import jax.numpy as jnp
from jax import lax
from jax.experimental import pallas as pl
from jax.experimental.pallas import tpu as pltpu
from jax.sharding import PartitionSpec as P

CLAMP = 7.0
ALPHA = 1.702
EPS = 1e-05
CW = 512
CAP = 32
HALF = 16
SP = 32
TP = 8
TOK = 256
ROWS = SP * HALF
BF = jnp.bfloat16
F32 = jnp.float32
MIB = 1 << 20


def dot(a, b, ca=1, cb=0):
    return lax.dot_general(a, b, (((ca,), (cb,)), ((), ())), preferred_element_type=F32)


def flag(mask):
    return jnp.where(mask, 1.0, 0.0)


def iota(shape, dim):
    return lax.broadcasted_iota(jnp.int32, shape, dim)


class Later:
    def __init__(self, source, buffer, sem):
        self.copy, self.buffer, self.waiting = pltpu.make_async_copy(source, buffer, sem), buffer, True
        self.copy.start()

    def now(self):
        if self.waiting:
            self.copy.wait()
            self.waiting = False
        return self.buffer


def now(x):
    return x.now() if isinstance(x, Later) else x


def call(body, outs, tp, args, staged=(), cuts=None, scratch=(), flops=0, limit=40):
    cuts = cuts or {}
    single = not isinstance(outs, tuple)
    outs = (outs,) if single else outs
    n_in, n_out, n_scr = len(args), len(outs), len(scratch)

    def kernel(t_ref, *refs):
        ins, rest = list(refs[:n_in]), refs[n_in:]
        made, scr, buffers = rest[:n_out], rest[n_out : n_out + n_scr], rest[n_out + n_scr :]
        for n, i in enumerate(staged):
            source = ins[i].at[cuts[i][1](t_ref[0])] if i in cuts else ins[i]
            ins[i] = Later(source, buffers[n], buffers[-1].at[n])
        body(t_ref[0], ins, made, scr)
        for i in staged:
            now(ins[i])

    extra = [
        pltpu.VMEM(cuts[i][0] if i in cuts else args[i].shape, args[i].dtype) for i in staged
    ]
    if staged:
        extra.append(pltpu.SemaphoreType.DMA((len(staged),)))
    args = tuple(
        pltpu.with_memory_space_constraint(x, pltpu.HBM) if i in staged else x
        for i, x in enumerate(args)
    )
    made = pl.pallas_call(
        kernel,
        out_shape=outs,
        in_specs=[SMEM] + [HBM if i in staged else VMEM for i in range(n_in)],
        out_specs=(VMEM,) * n_out,
        scratch_shapes=list(scratch) + extra,
        compiler_params=pltpu.CompilerParams(vmem_limit_bytes=limit * MIB),
        cost_estimate=pl.CostEstimate(flops=flops, bytes_accessed=MIB, transcendentals=0),
    )(tp, *args)
    return made[0] if single else made


def shape(dims, dtype):
    return jax.ShapeDtypeStruct(dims, dtype)


SMEM = pl.BlockSpec(memory_space=pltpu.SMEM)
VMEM = pl.BlockSpec(memory_space=pltpu.VMEM)
HBM = pl.BlockSpec(memory_space=pltpu.HBM)


def columns_of(width, which):
    return lambda t: (slice(None), pl.ds(pl.multiple_of(which(t) * width, width), width))


def pick_rows_body(t, ins, outs, scr):
    core = t % 2
    r = ins[0][...]
    r0, r1 = r[0:1, :], r[1:2, :]
    expert = iota((SP, TOK), 0)
    named0, named1 = expert == r0, expert == r1
    both = (flag(named0) + flag(named1)).astype(BF)
    before = flag(iota((TOK, TOK), 0) < iota((TOK, TOK), 1)).astype(BF)
    earlier = dot(both, before)
    slot0 = jnp.sum(jnp.where(named0, earlier, 0.0), axis=0, keepdims=True).astype(jnp.int32)
    slot1 = jnp.sum(jnp.where(named1, earlier, 0.0), axis=0, keepdims=True).astype(jnp.int32)
    l0 = jnp.where(slot0 // HALF == core, r0 * HALF + slot0 - HALF * core, -1)
    l1 = jnp.where(slot1 // HALF == core, r1 * HALF + slot1 - HALF * core, -1)
    b0 = r0 * CAP + (slot0 + HALF * core) % CAP
    b1 = r1 * CAP + (slot1 + HALF * core) % CAP
    outs[1][...] = jnp.concatenate([l0, l1, b0, b1, l0, l1, b0, b1], axis=0)
    place = iota((ROWS, TOK), 0)
    pick = flag((place == l0) | (place == l1)).astype(BF)
    outs[0][...] = dot(pick, now(ins[1])[...]).astype(BF)


def pick_rows(tp, routes, stream):
    return call(
        pick_rows_body,
        (pltpu.HBM((ROWS, 512), BF), shape((8, TOK), jnp.int32)),
        tp,
        (routes, stream),
        staged=(1,),
        cuts={1: ((TOK, 512), columns_of(512, lambda t: t // 2))},
        flops=10**9,
    )


def pick_cot_body(t, ins, outs, scr):
    tgt, w = ins[0][...], ins[1][...]
    table = jnp.concatenate([tgt[2:4, :].astype(F32), w, tgt[2:4, :].astype(F32), w], axis=0)
    columns = jnp.transpose(jnp.concatenate([table] * 16, axis=0))
    up = now(ins[2])[...].astype(F32)
    cot0 = (columns[:, 2:3] * up).astype(BF)
    cot1 = (columns[:, 3:4] * up).astype(BF)
    place = iota((ROWS, TOK), 0)
    cot = dot(flag(place == tgt[0:1, :]).astype(BF), cot0)
    cot = cot + dot(flag(place == tgt[1:2, :]).astype(BF), cot1)
    outs[0][...] = cot.astype(BF)
    b0 = columns[:, 0:1].astype(jnp.int32)
    b1 = columns[:, 1:2].astype(jnp.int32)
    spot = iota((TOK, SP * CAP), 1)
    outs[1][...] = flag((spot == b0) | (spot == b1)).astype(BF)


def pick_cot(tp, target, weights, upstream):
    return call(
        pick_cot_body,
        (pltpu.HBM((ROWS, 512), BF), pltpu.HBM((TOK, SP * CAP), BF)),
        tp,
        (target, weights, upstream),
        staged=(2,),
        cuts={2: ((TOK, 512), columns_of(512, lambda t: t // 2))},
        flops=10**9,
    )


def quarters(t):
    y = t // 2
    return y, (y + 3) % 4, (y + 1) % 4, (y + 2) % 4


def joined(refs):
    own, left, right, top, bottom = [now(r) for r in refs]
    return (
        own[...],
        left[...],
        right[...],
        jnp.concatenate([top[...], bottom[...]], axis=0),
    )


def forward_body(t, ins, outs, scr):
    act_ref, a1_ref, a2_ref = outs
    pg, pu = scr
    q = quarters(t)
    x = joined(ins[0:5])
    for j in range(2):
        cols = slice(256 * j, 256 * j + 256)
        g = now(ins[5 + j])
        pg[:, cols] = sum(dot(x[i], g[q[i]]) for i in range(4))
        u = now(ins[7 + j])
        pu[:, cols] = sum(dot(x[i], u[q[i]]) for i in range(4))

    @pl.loop(0, ROWS // 32)
    def _(i):
        at = pl.ds(pl.multiple_of(i * 32, 32), 32)
        gate_pre, up_pre = pg[at, :], pu[at, :]
        capped = jnp.minimum(gate_pre, CLAMP)
        clipped = jnp.clip(up_pre, -CLAMP, CLAMP)
        sig = jax.nn.sigmoid(ALPHA * capped)
        gated = capped * sig
        act_ref[at, :] = (gated * (clipped + 1.0)).astype(BF)
        slope = sig + ALPHA * gated * (1.0 - sig)
        a1_ref[at, :] = jnp.where(gate_pre < CLAMP, (clipped + 1.0) * slope, 0.0)
        a2_ref[at, :] = jnp.where(jnp.abs(up_pre) < CLAMP, gated, 0.0)


def forward(tp, blocks, weights):
    return call(
        forward_body,
        (shape((ROWS, 512), BF), shape((ROWS, 512), F32), shape((ROWS, 512), F32)),
        tp,
        (*blocks, *weights),
        staged=(5, 7, 6, 8),
        scratch=[pltpu.VMEM((ROWS, 512), F32)] * 2,
        flops=2 * 10**9,
    )


def partial_of(g, u, weights, piece):
    g0, g1, u0, u1 = weights
    return (
        dot(g[:, 0:256], g0[piece], 1, 1)
        + dot(g[:, 256:512], g1[piece], 1, 1)
        + dot(u[:, 0:256], u0[piece], 1, 1)
        + dot(u[:, 256:512], u1[piece], 1, 1)
    )


def backward_body(t, ins, outs, scr):
    top_ref, bottom_ref, gg_ref, gu_ref = outs
    ga = scr[0]
    a1, a2 = ins[7], ins[8]
    q = quarters(t)
    x = joined(ins[0:5])
    for j in range(2):
        d = now(ins[5 + j])
        ga[:, 256 * j : 256 * j + 256] = sum(
            dot(x[i], d[:, pl.ds(pl.multiple_of(q[i] * 512, 512), 512)], 1, 1) for i in range(4)
        )

    @pl.loop(0, ROWS // 32)
    def _(i):
        at = pl.ds(pl.multiple_of(i * 32, 32), 32)
        grad = ga[at, :]
        gg_ref[at, :] = (grad * a1[at, :]).astype(BF)
        gu_ref[at, :] = (grad * a2[at, :]).astype(BF)

    g, u = gg_ref[...], gu_ref[...]
    weights = [now(w) for w in ins[9:13]]
    for half in range(2):
        part = partial_of(g, u, weights, half).astype(BF)
        top_ref[half] = part[0:256]
        bottom_ref[half] = part[256:512]


def backward(tp, blocks, downs, a1, a2, weights):
    far = ((2, 256, 256), lambda t: (pl.ds(2 * ((t // 2 + 2) % 4), 2),))
    return call(
        backward_body,
        (
            shape((2, 256, 256), BF),
            shape((2, 256, 256), BF),
            shape((ROWS, 512), BF),
            shape((ROWS, 512), BF),
        ),
        tp,
        (*blocks, *downs, a1, a2, *weights),
        staged=(5, 6, 9, 10, 11, 12),
        cuts={9: far, 10: far, 11: far, 12: far},
        scratch=[pltpu.VMEM((ROWS, 512), F32)],
        flops=2 * 10**9,
    )


def near_body(t, ins, outs, scr):
    g, u = ins[0][...], ins[1][...]
    weights = [now(w) for w in ins[2:6]]
    right, left = (t + 2) % 8, (t + 6) % 8
    swap = 1 - 2 * (t % 2)
    pieces = (right, right + swap, left, left + swap, t, t + swap)
    for ref, piece in zip(outs, pieces):
        ref[...] = partial_of(g, u, weights, piece).astype(BF)


def near(tp, gg, gu, weights):
    return call(
        near_body,
        (shape((ROWS, 256), BF),) * 6,
        tp,
        (gg, gu, *weights),
        staged=(2, 3, 4, 5),
        flops=3 * 10**9,
    )


def merge_body(t, ins, outs, scr):
    core = t % 2
    top, bottom = ins[0:2]
    for src, dst, got, first in (
        (ins[2], outs[0], top[core], True),
        (ins[3], outs[1], top[1 - core], True),
        (ins[4], outs[2], bottom[core], False),
        (ins[5], outs[3], bottom[1 - core], False),
    ):
        hit, other = (slice(0, 256), slice(256, 512)) if first else (slice(256, 512), slice(0, 256))
        dst[hit, :] = (src[hit, :].astype(F32) + got.astype(F32)).astype(BF)
        dst[other, :] = src[other, :]


def merge(tp, top, bottom, parts):
    return call(
        merge_body, (shape((ROWS, 256), BF),) * 4, tp, (top, bottom, *parts), flops=10**7, limit=16
    )


def settle_body(t, ins, outs, scr):
    a0, a1, a2, b0, b1, b2 = [x[...].astype(F32) for x in ins]
    outs[0][:, 0:HALF, :] = (a0 + a1 + a2).astype(BF).reshape(SP, HALF, 256)
    outs[0][:, HALF:CAP, :] = (b0 + b1 + b2).astype(BF).reshape(SP, HALF, 256)


def settle(tp, parts):
    return call(settle_body, pltpu.HBM((SP, CAP, 256), BF), tp, parts, flops=10**7, limit=16)


def weights_of(t, ins, cols):
    q = quarters(t)
    xs, cs = joined(ins[0:5]), joined(ins[5:10])
    gg, gu, act = [now(x) for x in ins[10:13]]
    gu_cols = jnp.concatenate([gg[:, cols], gu[:, cols]], axis=1)
    act_cols = act[:, cols]
    for i in range(4):
        both = dot(xs[i], gu_cols, 0, 0)
        yield q[i], both[:, 0:256], both[:, 256:512], dot(act_cols, cs[i], 0, 0)


def lend_body(t, ins, outs, scr):
    for q, a, b, d in weights_of(t, ins, slice(256, 512)):
        outs[0][q] = a.astype(BF)
        outs[0][4 + q] = b.astype(BF)
        outs[0][8 + q, 0:256, :] = d[:, 0:256].astype(BF)
        outs[0][8 + q, 256:512, :] = d[:, 256:512].astype(BF)


def lend(tp, xs, cs, gg, gu, act):
    return call(
        lend_body,
        shape((12, 512, 256), BF),
        tp,
        (*xs, *cs, gg, gu, act),
        staged=tuple(range(13)),
        flops=2 * 10**9,
    )


def keep_body(t, ins, outs, scr):
    gate_ref, up_ref, down_ref = outs
    lent = now(ins[13])
    for q, a, b, d in weights_of(t, ins, slice(0, 256)):
        gate_ref[q] = a + lent[q].astype(F32)
        up_ref[q] = b + lent[4 + q].astype(F32)
        for half in range(2):
            cols = slice(256 * half, 256 * half + 256)
            at = pl.ds(pl.multiple_of(q * 512 + 256 * half, 256), 256)
            down_ref[:, at] = d[:, cols] + lent[8 + q, cols, :].astype(F32)


def keep(tp, xs, cs, gg, gu, act, lent):
    return call(
        keep_body,
        (shape((4, 512, 256), F32), shape((4, 512, 256), F32), shape((256, 2048), F32)),
        tp,
        (*xs, *cs, gg, gu, act, lent),
        staged=tuple(range(14)),
        flops=2 * 10**9,
    )


def hand_out_body(t, ins, outs, scr):
    proj = now(ins[0])
    for d in range(4):
        other = lax.bitwise_xor(t, 2 * d + 1)
        outs[0][d] = proj[:, pl.ds(pl.multiple_of(other * 256, 256), 256)]
    outs[0][4] = ins[1][...]


def hand_out(tp, proj, saved):
    return call(
        hand_out_body, shape((5, 64, TOK), BF), tp, (proj, saved), staged=(0,), limit=16
    )


def hand_on_body(t, ins, outs, scr):
    proj = now(ins[0])
    for d in range(1, 4):
        other = lax.bitwise_xor(t, 2 * d)
        outs[d - 1][0] = proj[:, pl.ds(pl.multiple_of(other * 256, 256), 256)]
        outs[d - 1][1] = ins[2][d]
        outs[d - 1][2] = ins[1][...]
        outs[d - 1][3] = ins[2][4]


def hand_on(tp, proj, saved, got):
    return call(
        hand_on_body,
        (shape((4, 64, TOK), BF),) * 3,
        tp,
        (proj, saved, got),
        staged=(0,),
        limit=16,
    )


def prepare_body(t, ins, outs, scr):
    proj_ref, mixed_ref, slope_ref, slope_n_ref, stat_ref = outs
    all_saved = scr[0]

    def at(d):
        return pl.ds(pl.multiple_of(lax.bitwise_xor(t, d) * 64, 64), 64)

    proj_ref[at(0), :] = now(ins[0])[...]
    all_saved[at(0), :] = ins[1][...]
    proj_ref[at(1), :] = ins[2][0]
    all_saved[at(1), :] = ins[2][4]
    for d in range(1, 4):
        for other in range(2):
            proj_ref[at(2 * d + other), :] = ins[2 + d][other]
            all_saved[at(2 * d + other), :] = ins[2 + d][2 + other]
    saved = all_saved[...].astype(F32)
    mean = jnp.sum(saved, axis=0, keepdims=True) / CW
    var = jnp.sum(saved * saved, axis=0, keepdims=True) / CW - mean * mean
    inv = lax.rsqrt(var + EPS)
    normed = (saved - mean) * inv
    sig = jax.nn.sigmoid(normed)
    mixed_ref[...] = (normed * sig).astype(BF)
    slope = sig * (1.0 + normed * (1.0 - sig))
    slope_ref[...] = slope
    slope_n_ref[...] = slope * normed
    stat_ref[...] = jnp.concatenate([mean, inv, mean, inv, mean, inv, mean, inv], axis=0)


def prepare(tp, proj, saved, got):
    return call(
        prepare_body,
        (
            pltpu.HBM((CW, TOK), BF),
            pltpu.HBM((CW, TOK), BF),
            pltpu.HBM((CW, TOK), F32),
            pltpu.HBM((CW, TOK), F32),
            shape((8, TOK), F32),
        ),
        tp,
        (proj, saved, *got),
        staged=(0,),
        cuts={0: ((64, TOK), columns_of(256, lambda t: t))},
        scratch=[pltpu.VMEM((CW, TOK), BF)],
        flops=10**8,
    )


def tokens_body(t, ins, outs, scr):
    gs_ref, outer_ref, own_ref, lent_ref = outs
    routed = dot(now(ins[0])[...], ins[2][...])
    gs = (now(ins[1])[...].astype(F32) + routed).astype(BF)
    gs_ref[...] = gs
    outer = dot(gs, now(ins[4])[...], 0, 1)
    lane = iota((64, 128), 1) < 64
    for u in range(4):
        for i in range(4):
            block = outer[64 * i : 64 * i + 64, 128 * u : 128 * u + 128]
            turned = pltpu.roll(block, 64, 1)
            even = jnp.where(lane[0:32], block[0:32], turned[32:64])
            odd = jnp.where(lane[0:32], turned[0:32], block[32:64])
            outer_ref[8 * i + 2 * u] = even.astype(BF)
            outer_ref[8 * i + 2 * u + 1] = odd.astype(BF)
    part_all = scr[0]
    part = dot(now(ins[3])[...], gs, 1, 1)
    part_all[...] = part
    first = jnp.sum(part * now(ins[5])[...], axis=0, keepdims=True)
    second = jnp.sum(part * now(ins[6])[...], axis=0, keepdims=True)
    sums = jnp.concatenate([first, second], axis=0)
    parted = split_sums(sums)

    def at(d):
        return pl.ds(pl.multiple_of(lax.bitwise_xor(t, d) * 64, 64), 64)

    for d in range(4):
        own_ref[d, 0:64, :] = part_all[at(2 * d), :]
        lent_ref[d, 0:64, :] = part_all[at(2 * d + 1), :].astype(BF)
        lent_ref[d, 64:72, :] = parted
    own_ref[0, 64:72, :] = jnp.concatenate([sums] * 4, axis=0)


def split_sums(sums):
    high = sums.astype(BF).astype(F32)
    low = sums - high
    return jnp.concatenate([high, low, high, low], axis=0).astype(BF)


def fold_body(t, ins, outs, scr):
    own, got = ins
    sums = own[0, 64:66, :] + got[0, 64:66, :].astype(F32) + got[0, 66:68, :].astype(F32)
    outs[0][0:64, :] = own[0, 0:64, :] + got[0, 0:64, :].astype(F32)
    outs[0][64:72, :] = jnp.concatenate([sums] * 4, axis=0)
    parted = split_sums(sums)
    for d in range(1, 4):
        outs[d][0:64, :] = (own[d, 0:64, :] + got[d, 0:64, :].astype(F32)).astype(BF)
        outs[d][64:72, :] = parted


def fold(tp, own, got):
    return call(
        fold_body,
        (shape((72, TOK), F32),) + (shape((72, TOK), BF),) * 3,
        tp,
        (own, got),
        flops=10**7,
        limit=16,
    )


def tokens(tp, back, upstream, ret, proj, mixed, slope, slope_n):
    return call(
        tokens_body,
        (
            shape((TOK, 256), BF),
            pltpu.HBM((SP, 32, 128), BF),
            shape((4, 72, TOK), F32),
            shape((4, 72, TOK), BF),
        ),
        tp,
        (back, upstream, ret, proj, mixed, slope, slope_n),
        staged=(0, 1, 4, 3, 5, 6),
        cuts={1: ((TOK, 256), columns_of(256, lambda t: t))},
        scratch=[pltpu.VMEM((CW, TOK), F32)],
        flops=10**9,
    )


def norm_body(t, ins, outs, scr):
    own, saved, stat = ins[0], ins[4], ins[5]
    mixed, sums = own[0:64, :], own[64:66, :]
    for got in ins[1:4]:
        mixed = mixed + got[0:64, :].astype(F32)
        sums = sums + got[64:66, :].astype(F32) + got[66:68, :].astype(F32)
    first, second = sums[0:1] / CW, sums[1:2] / CW
    mean, inv = stat[0:1, :], stat[1:2, :]
    normed = (saved[...].astype(F32) - mean) * inv
    sig = jax.nn.sigmoid(normed)
    grad = mixed * sig * (1.0 + normed * (1.0 - sig))
    conv_grad = inv * (grad - first - normed * second)
    outs[0][...] = conv_grad
    outs[1][...] = conv_grad[:, 0:128]


def norm(tp, own, got, saved, stat):
    return call(
        norm_body,
        (shape((64, TOK), F32), shape((64, 128), F32)),
        tp,
        (own, *got, saved, stat),
        flops=10**7,
        limit=16,
    )


def tap_sum(padded, taps):
    total = jnp.zeros((64, TOK), F32)
    width = padded.shape[1]
    for j in range(taps.shape[1]):
        turned = padded if j == 0 else pltpu.roll(padded, width - j, 1)
        total = total + taps[:, j : j + 1] * turned[:, 0:TOK]
    return total


def conv_own_body(t, ins, outs, scr):
    grad, taps = ins
    outs[0][...] = tap_sum(jnp.concatenate([grad[...], jnp.zeros((64, 128), F32)], axis=1), taps)


def conv_own(tp, grad, taps):
    return call(conv_own_body, shape((64, TOK), F32), tp, (grad, taps), flops=10**8, limit=16)


def conv_rim_body(t, ins, outs, scr):
    own, rim, taps, value, gate = ins
    dv_ref, dg_ref = outs
    both = jnp.concatenate([jnp.zeros((64, 128), F32), rim[...]], axis=1)
    reach = jnp.zeros((64, 128), F32)
    for j in range(1, taps.shape[1]):
        reach = reach + taps[:, j : j + 1] * pltpu.roll(both, TOK - j, 1)[:, 0:128]
    total = jnp.concatenate([own[:, 0:128], own[:, 128:256] + reach], axis=1)
    sig = jax.nn.sigmoid(gate[...].astype(F32))
    dv_ref[...] = (total * sig).astype(BF)
    dg_ref[...] = (total * value[...].astype(F32) * sig * (1.0 - sig)).astype(BF)


def conv_rim(tp, own, rim, taps, value, gate):
    return call(
        conv_rim_body,
        (shape((64, TOK), BF), shape((64, TOK), BF)),
        tp,
        (own, rim, taps, value, gate),
        flops=10**8,
        limit=16,
    )


def total_body(t, ins, outs, scr):
    whole = jnp.sum(ins[0][...].astype(F32), axis=0)
    outs[0][0:32, :] = whole[:, 0:64]
    outs[0][32:64, :] = whole[:, 64:128]


def total(tp, got):
    return call(total_body, shape((64, 64), F32), tp, (got,), flops=10**7, limit=16)


def moved(x, by):
    return lax.ppermute(x, "tp", [(i, (i + by) % TP) for i in range(TP)])


def swapped(x, by):
    return lax.ppermute(x, "tp", [(i, i ^ by) for i in range(TP)])


def across_moved(x, by):
    return lax.ppermute(x, "tp", [(i, ((i + by) % TP) ^ 1) for i in range(TP)])


def around(block, hold=None):
    left, right = moved(block, 2), moved(block, -2)
    if hold is not None:
        left, right, _ = lax.optimization_barrier((left, right, hold))
    top, bottom = moved(left[:256], 2), moved(right[256:], -2)
    return block, left, right, top, bottom


def exchange(x):
    return lax.all_to_all(x, "sp", 0, 0, tiled=True)


def after(x, *others):
    return lax.optimization_barrier((x, *others))[0]


def step(
    upstream, stream, routes, route_weights, glu_value, glu_gate, conv_taps, conv_saved,
    out_proj, expert_gate, expert_up, expert_down,
):
    tp = lax.axis_index("tp").reshape(1)
    rows_out, target = pick_rows(tp, routes.T, stream)
    rows_in = exchange(rows_out.reshape(SP, HALF, 512)).reshape(ROWS, 512)

    saved, proj = conv_saved.T, out_proj.T
    near_early = swapped(hand_out(tp, proj, saved), 1)
    far_early = hand_on(tp, proj, saved, near_early)
    early = (near_early, *(swapped(x, 2 * d + 2) for d, x in enumerate(far_early)))
    gate_own, up_own, down_own = expert_gate[0], expert_up[0], expert_down[0]
    gate_par, up_par, down_par = (swapped(w, 1) for w in (gate_own, up_own, down_own))

    cot_out, back = pick_cot(tp, target, route_weights.T, upstream)
    cot_out = after(cot_out, *early)
    cot_in = exchange(cot_out.reshape(SP, HALF, 512)).reshape(ROWS, 512)
    proj_all, mixed, slope, slope_n, stat = prepare(tp, proj, saved, early)

    xs = around(rows_in)
    by_quarter = [w.reshape(4, 512, 256) for w in (gate_own, gate_par, up_own, up_par)]
    by_piece = [w.reshape(8, 256, 256) for w in (gate_own, gate_par, up_own, up_par)]
    act, a1, a2 = forward(tp, xs, by_quarter)

    cs = around(cot_in, act)
    far_top, far_bottom, gg, gu = backward(tp, cs, (down_own, down_par), a1, a2, by_piece)
    got_top, got_bottom = moved(far_top, 2), moved(far_bottom, -2)
    parts = near(tp, gg, gu, by_piece)
    rs, rc, ls, lc = merge(tp, got_top, got_bottom, parts[:4])
    lent = lend(tp, xs, cs, gg, gu, after(act, rs))
    came = (moved(rs, 2), moved(ls, -2), across_moved(rc, 2), across_moved(lc, -2))
    own_cross = swapped(parts[5], 1)
    summed = settle(
        tp, (after(parts[4], lent), came[0], came[1], own_cross, came[2], came[3])
    )
    returned = exchange(summed).reshape(SP * CAP, 256)
    grads = keep(tp, xs, cs, gg, gu, act, swapped(lent, 1))
    grad_gate_w, grad_up_w, grad_down_w = grads
    back = after(back, grad_down_w)

    made = tokens(tp, back, upstream, returned, proj_all, mixed, slope, slope_n)
    grad_stream, outer, own_part, lent_part = made
    outer_in = exchange(outer)
    folded = fold(tp, own_part, swapped(lent_part, 1))
    own_part = folded[0]
    part_in = tuple(swapped(x, 2 * d + 2) for d, x in enumerate(folded[1:]))
    grad_conv, rim = norm(tp, own_part, part_in, saved, stat)
    rim_in = lax.ppermute(rim, "sp", [(i, i - 1) for i in range(1, SP)])
    taps = conv_taps.T
    grad_glu = conv_own(tp, grad_conv, taps)
    grad_value, grad_gate = conv_rim(tp, grad_glu, rim_in, taps, glu_value.T, glu_gate.T)
    grad_out_proj = lax.ppermute(
        total(tp, outer_in),
        ("sp", "tp"),
        [
            ((i * 8 + u) * TP + t, (4 * t + i) * TP + u)
            for i in range(4)
            for u in range(TP)
            for t in range(TP)
        ],
    )
    return (
        grad_stream,
        grad_value.T,
        grad_gate.T,
        grad_out_proj,
        grad_gate_w.reshape(1, 2048, 256),
        grad_up_w.reshape(1, 2048, 256),
        grad_down_w[None],
    )


def solution(mesh):
    in_specs = (
        P("sp", None),
        P("sp", None),
        P("sp", None),
        P("sp", None),
        P("sp", "tp"),
        P("sp", "tp"),
        P(None, "tp"),
        P("sp", "tp"),
        P(None, "tp"),
        P("sp", None, "tp"),
        P("sp", None, "tp"),
        P("sp", "tp", None),
    )
    out_specs = (
        P("sp", "tp"),
        P("sp", "tp"),
        P("sp", "tp"),
        P("sp", "tp"),
        P("sp", None, "tp"),
        P("sp", None, "tp"),
        P("sp", "tp", None),
    )
    return jax.shard_map(step, mesh=mesh, in_specs=in_specs, out_specs=out_specs, check_vma=False)
```

profile of v0, /device:TPU:128, one launch (start us, length us, event | category | flops | bytes accessed | tf_op | source)
XLA Modules:
  0.0 191.8 jit_solution(10932116650514459133)
XLA Ops:
  1.3 2.1 %shard_map.171 = (bf16[512,512]{1,0:T(8,128)(2,1)}, s32[8,256]{1,0:T(8,128)S(1)}) custom-call(s32[1]{0:T(128)} %bitcast.t_ref, s32[2,256]{1,0:T(2,128)S(1)} %bitcast.47, bf16[256,2048]{1,0:T(8,128)(2,1)} %refs_1_.2), custom_call_target="tpu_custom_call" | custom-call | flops 1000000000 | bytes 1048576 | tf_op jit(solution)/shard_map/pallas_call | solution.py:76
  3.4 9.9 %all-to-all-start = ((bf16[32,16,512]{2,1,0:T(8,128)(2,1)}), bf16[32,16,512]{2,1,0:T(8,128)(2,1)S(1)}, u32[]{:S(2)}, u32[]{:S(2)}) async-start(bf16[32,16,512]{2,1,0:T(8,128)(2,1)} %bitcast.62), calls=%async_computation | async-start | bytes 1048576 | tf_op jit(solution)/shard_map/all_to_all | solution.py:637
  13.3 1.0 shard_map.173
  14.4 1.4 collective-permute-done.4.refs_2_
  15.8 1.0 shard_map.174
  17.4 1.6 collective-permute-start.5
  19.0 2.9 %collective-permute-start.6 = (bf16[4,64,256]{2,1,0:T(8,128)(2,1)S(1)}, bf16[4,64,256]{2,1,0:T(8,128)(2,1)S(1)}, u32[]{:S(2)}, u32[]{:S(2)}) collective-permute-start(bf16[4,64,256]{2,1,0:T(8,128)(2,1)S(1)} %get-tuple-element.62), channel_id=1, source_target_pairs={{0,4},{1,5},{2,6},{3,7},{4,0},{5,1},{6,2},{7,3},{8,12},{9,13},{10,... | collective-permute-start | bytes 393224 | tf_op jit(solution)/shard_map/ppermute | solution.py:621
  22.1 2.6 %shard_map.172 = (bf16[512,512]{1,0:T(8,128)(2,1)}, bf16[256,1024]{1,0:T(8,128)(2,1)}) custom-call(s32[1]{0:T(128)} %bitcast.t_ref, s32[8,256]{1,0:T(8,128)S(1)} %get-tuple-element.57.refs_0_, f32[2,256]{1,0:T(2,128)S(1)} %bitcast.48, bf16[256,2048]{1,0:T(8,128)(2,1)} %refs_1_.3), custom_call_target="tpu_custom_call" | custom-call | flops 1000000000 | bytes 1048576 | tf_op jit(solution)/shard_map/pallas_call | solution.py:76
  24.7 3.6 %collective-permute-done.6.refs_4_ = bf16[4,64,256]{2,1,0:T(8,128)(2,1)S(1)} collective-permute-done((bf16[4,64,256]{2,1,0:T(8,128)(2,1)S(1)}, bf16[4,64,256]{2,1,0:T(8,128)(2,1)S(1)}, u32[]{:S(2)}, u32[]{:S(2)}) %collective-permute-start.6) | collective-permute-done | bytes 131104 | tf_op jit(solution)/shard_map/ppermute | solution.py:621
  28.3 2.2 %collective-permute-done.7.refs_5_ = bf16[4,64,256]{2,1,0:T(8,128)(2,1)S(1)} collective-permute-done((bf16[4,64,256]{2,1,0:T(8,128)(2,1)S(1)}, bf16[4,64,256]{2,1,0:T(8,128)(2,1)S(1)}, u32[]{:S(2)}, u32[]{:S(2)}) %collective-permute-start.7) | collective-permute-done | bytes 131104 | tf_op jit(solution)/shard_map/ppermute | solution.py:621
  30.6 9.8 %all-to-all-start.1 = ((bf16[32,16,512]{2,1,0:T(8,128)(2,1)}), bf16[32,16,512]{2,1,0:T(8,128)(2,1)S(1)}, u32[]{:S(2)}, u32[]{:S(2)}) async-start(bf16[32,16,512]{2,1,0:T(8,128)(2,1)} %bitcast.63), calls=%async_computation.1 | async-start | bytes 1048576 | tf_op jit(solution)/shard_map/all_to_all | solution.py:637
  41.1 3.2 %collective-permute-start.1 = (bf16[512,512]{1,0:T(8,128)(2,1)S(1)}, bf16[512,512]{1,0:T(8,128)(2,1)S(1)}, u32[]{:S(2)}, u32[]{:S(2)}) collective-permute-start(bf16[512,512]{1,0:T(8,128)(2,1)S(1)} %bitcast.35), channel_id=1, source_target_pairs={{0,6},{1,7},{2,0},{3,1},{4,2},{5,3},{6,4},{7,5},{8,14},{9,15},{10,... | collective-permute-start | bytes 1572872 | tf_op jit(solution)/shard_map/ppermute | solution.py:617
  44.3 9.6 %all-to-all-done.1 = bf16[32,16,512]{2,1,0:T(8,128)(2,1)S(1)} async-done(((bf16[32,16,512]{2,1,0:T(8,128)(2,1)}), bf16[32,16,512]{2,1,0:T(8,128)(2,1)S(1)}, u32[]{:S(2)}, u32[]{:S(2)}) %all-to-all-start.1) | async-done | bytes 524320 | tf_op jit(solution)/shard_map/all_to_all | solution.py:637
  53.9 2.3 %collective-permute-done.refs_1_ = bf16[512,512]{1,0:T(8,128)(2,1)S(1)} collective-permute-done((bf16[512,512]{1,0:T(8,128)(2,1)S(1)}, bf16[512,512]{1,0:T(8,128)(2,1)S(1)}, u32[]{:S(2)}, u32[]{:S(2)}) %collective-permute-start) | collective-permute-done | bytes 524320 | tf_op jit(solution)/shard_map/ppermute | solution.py:617
  56.2 3.2 %collective-permute-start.9 = (bf16[512,512]{1,0:T(8,128)(2,1)S(1)}, bf16[512,512]{1,0:T(8,128)(2,1)S(1)}, u32[]{:S(2)}, u32[]{:S(2)}) collective-permute-start(bf16[512,512]{1,0:T(8,128)(2,1)S(1)} %bitcast.30), channel_id=1, source_target_pairs={{0,6},{1,7},{2,0},{3,1},{4,2},{5,3},{6,4},{7,5},{8,14},{9,15},{10,... | collective-permute-start | bytes 1572872 | tf_op jit(solution)/shard_map/ppermute | solution.py:617
  59.6 3.2 %collective-permute-start.3 = (bf16[256,512]{1,0:T(8,128)(2,1)S(1)}, bf16[256,512]{1,0:T(8,128)(2,1)S(1)}, u32[]{:S(2)}, u32[]{:S(2)}) collective-permute-start(bf16[256,512]{1,0:T(8,128)(2,1)S(1)} %slice.17), channel_id=1, source_target_pairs={{0,6},{1,7},{2,0},{3,1},{4,2},{5,3},{6,4},{7,5},{8,14},{9,15},{10,... | collective-permute-start | bytes 786440 | tf_op jit(solution)/shard_map/ppermute | solution.py:617
  62.8 13.3 %collective-permute-done.2.refs_3_ = bf16[256,512]{1,0:T(8,128)(2,1)S(1)} collective-permute-done((bf16[256,512]{1,0:T(8,128)(2,1)S(1)}, bf16[256,512]{1,0:T(8,128)(2,1)S(1)}, u32[]{:S(2)}, u32[]{:S(2)}) %collective-permute-start.2) | collective-permute-done | bytes 262176 | tf_op jit(solution)/shard_map/ppermute | solution.py:617
  76.1 7.2 %shard_map.175 = (bf16[512,512]{1,0:T(8,128)(2,1)S(1)}, f32[512,512]{1,0:T(8,128)S(1)}, f32[512,512]{1,0:T(8,128)S(1)}) custom-call(s32[1]{0:T(128)} %bitcast.t_ref, bf16[512,512]{1,0:T(8,128)(2,1)S(1)} %bitcast.36, bf16[512,512]{1,0:T(8,128)(2,1)S(1)} %collective-permute-done.refs_1_, bf16[512,512]{1,0:T(8,128)(2,1)S(1)} %collective-permute-done.1.refs_2_, ...), custom_call_target="tpu_custom_call" | custom-call | flops 2000000000 | bytes 1048576 | tf_op jit(solution)/shard_map/pallas_call | solution.py:76
  83.6 3.3 %collective-permute-start.13 = (bf16[256,512]{1,0:T(8,128)(2,1)S(1)}, bf16[256,512]{1,0:T(8,128)(2,1)S(1)}, u32[]{:S(2)}, u32[]{:S(2)}) collective-permute-start(bf16[256,512]{1,0:T(8,128)(2,1)S(1)} %slice.15), channel_id=1, source_target_pairs={{0,6},{1,7},{2,0},{3,1},{4,2},{5,3},{6,4},{7,5},{8,14},{9,15},{10,... | collective-permute-start | bytes 786440 | tf_op jit(solution)/shard_map/ppermute | solution.py:617
  86.9 4.5 %collective-permute-done.12.refs_3_.refs_8_ = bf16[256,512]{1,0:T(8,128)(2,1)S(1)} collective-permute-done((bf16[256,512]{1,0:T(8,128)(2,1)S(1)}, bf16[256,512]{1,0:T(8,128)(2,1)S(1)}, u32[]{:S(2)}, u32[]{:S(2)}) %collective-permute-start.12) | collective-permute-done | bytes 262176 | tf_op jit(solution)/shard_map/ppermute | solution.py:617
  91.3 5.0 %shard_map.176 = (bf16[2,256,256]{2,1,0:T(8,128)(2,1)S(1)}, bf16[2,256,256]{2,1,0:T(8,128)(2,1)S(1)}, bf16[512,512]{1,0:T(8,128)(2,1)S(1)}, bf16[512,512]{1,0:T(8,128)(2,1)S(1)}) custom-call(s32[1]{0:T(128)} %bitcast.t_ref, bf16[512,512]{1,0:T(8,128)(2,1)S(1)} %bitcast.31, bf16[512,512]{1,0:T(8,128)(2,1)S(1)} %collective-permute-done.8.refs_1_.refs_6_, ...), custom_call_target="tpu_custom_call" | custom-call | flops 2000000000 | bytes 1048576 | tf_op jit(solution)/shard_map/pallas_call | solution.py:76
  97.3 2.4 %collective-permute-start.16 = (bf16[2,256,256]{2,1,0:T(8,128)(2,1)S(1)}, bf16[2,256,256]{2,1,0:T(8,128)(2,1)S(1)}, u32[]{:S(2)}, u32[]{:S(2)}) collective-permute-start(bf16[2,256,256]{2,1,0:T(8,128)(2,1)S(1)} %get-tuple-element.73), channel_id=1, source_target_pairs={{0,6},{1,7},{2,0},{3,1},{4,2},{5,3},{6,4},{7,5},{8,14},{9,15},{10,... | collective-permute-start | bytes 786440 | tf_op jit(solution)/shard_map/ppermute | solution.py:617
  99.8 4.0 %shard_map.177 = (bf16[512,256]{1,0:T(8,128)(2,1)S(1)}, bf16[512,256]{1,0:T(8,128)(2,1)S(1)}, bf16[512,256]{1,0:T(8,128)(2,1)S(1)}, bf16[512,256]{1,0:T(8,128)(2...) custom-call(s32[1]{0:T(128)} %bitcast.t_ref, ...), custom_call_target="tpu_custom_call" | custom-call | flops 3000000000 | bytes 1048576 | tf_op jit(solution)/shard_map/pallas_call | solution.py:76
  104.3 4.6 %shard_map.179 = bf16[12,512,256]{2,1,0:T(8,128)(2,1)S(1)} custom-call(s32[1]{0:T(128)} %bitcast.t_ref, bf16[512,512]{1,0:T(8,128)(2,1)} %bitcast.37, bf16[512,512]{1,0:T(8,128)(2,1)} %copy-done.4, bf16[512,512]{1,0:T(8,128)(2,1)} %copy-done.5, bf16[256,512]{1,0:T(8,128)(2,1)} %copy-done.11, bf16[256,512]{1,0:T(8,128)(2,1)} %copy-done.12, ...), custom_call_target="tpu_custom_call" | custom-call | flops 2000000000 | bytes 1048576 | tf_op jit(solution)/shard_map/pallas_call | solution.py:76
  109.4 1.6 collective-permute-start.18
  111.1 1.6 collective-permute-start.19
  112.7 2.3 %collective-permute-done.20.refs_3_ = bf16[512,256]{1,0:T(8,128)(2,1)S(1)} collective-permute-done((bf16[512,256]{1,0:T(8,128)(2,1)S(1)}, bf16[512,256]{1,0:T(8,128)(2,1)S(1)}, u32[]{:S(2)}, u32[]{:S(2)}) %collective-permute-start.20) | collective-permute-done | bytes 262176 | tf_op jit(solution)/shard_map/ppermute | solution.py:621
  115.0 3.0 %collective-permute-start.22 = (bf16[512,256]{1,0:T(8,128)(2,1)S(1)}, bf16[512,256]{1,0:T(8,128)(2,1)S(1)}, u32[]{:S(2)}, u32[]{:S(2)}) collective-permute-start(bf16[512,256]{1,0:T(8,128)(2,1)S(1)} %get-tuple-element.87), channel_id=1, source_target_pairs={{0,7},{1,6},{2,1},{3,0},{4,3},{5,2},{6,5},{7,4},{8,15},{9,14},{10,... | collective-permute-start | bytes 786440 | tf_op jit(solution)/shard_map/ppermute | solution.py:625
  117.9 1.9 collective-permute-done.18.refs_1_
  120.2 4.1 %collective-permute-done.21.refs_4_ = bf16[512,256]{1,0:T(8,128)(2,1)S(1)} collective-permute-done((bf16[512,256]{1,0:T(8,128)(2,1)S(1)}, bf16[512,256]{1,0:T(8,128)(2,1)S(1)}, u32[]{:S(2)}, u32[]{:S(2)}) %collective-permute-start.21) | collective-permute-done | bytes 262176 | tf_op jit(solution)/shard_map/ppermute | solution.py:625
  124.3 1.0 shard_map.181
  125.3 9.8 %all-to-all-start.2 = ((bf16[32,32,256]{2,1,0:T(8,128)(2,1)}), bf16[32,32,256]{2,1,0:T(8,128)(2,1)}, u32[]{:S(2)}, u32[]{:S(2)}) async-start(bf16[32,32,256]{2,1,0:T(8,128)(2,1)} %shard_map.181), calls=%async_computation.2 | async-start | bytes 1048576 | tf_op jit(solution)/shard_map/all_to_all | solution.py:637
  137.0 0.9 copy-done.21
  137.9 2.2 %shard_map.182 = (bf16[512,256]{1,0:T(8,128)(2,1)}, bf16[512,256]{1,0:T(8,128)(2,1)}, f32[512,256]{1,0:T(8,128)}, f32[512,256]{1,0:T(8,128)}, f32[8,256]{1,0:T(8,128)S(1)}) custom-call(s32[1]{0:T(128)} %bitcast.t_ref, bf16[64,2048]{1,0:T(8,128)(2,1)} %bitcast.51, bf16[64,256]{1,0:T(8,128)(2,1)S(1)} %bitcast.41, bf16[5,64,256]{2,1,0:T(8,128)(2,1)S(1)} %copy-done.14, ...), custom_call_target="tpu_custom_call" | custom-call | flops 100000000 | bytes 1048576 | tf_op jit(solution)/shard_map/pallas_call | solution.py:76
  140.1 8.5 %shard_map.180 = (f32[4,512,256]{2,1,0:T(8,128)}, f32[4,512,256]{2,1,0:T(8,128)}, f32[256,2048]{1,0:T(8,128)}) custom-call(s32[1]{0:T(128)} %bitcast.t_ref, bf16[512,512]{1,0:T(8,128)(2,1)} %bitcast.38, bf16[512,512]{1,0:T(8,128)(2,1)} %copy-done.4, bf16[512,512]{1,0:T(8,128)(2,1)} %copy-done.5, bf16[256,512]{1,0:T(8,128)(2,1)} %copy-done.11, ...), custom_call_target="tpu_custom_call" | custom-call | flops 2000000000 | bytes 1048576 | tf_op jit(solution)/shard_map/pallas_call | solution.py:76
  148.6 0.9 all-to-all-done.2
  149.6 4.1 %shard_map.183 = (bf16[256,256]{1,0:T(8,128)(2,1)}, bf16[32,32,128]{2,1,0:T(8,128)(2,1)}, f32[4,72,256]{2,1,0:T(8,128)S(1)}, bf16[4,72,256]{2,1,0:T(8,128)(2,1)S(1)}) custom-call(s32[1]{0:T(128)} %bitcast.t_ref, bf16[256,1024]{1,0:T(8,128)(2,1)} %get-tuple-element.81.refs_0_, bf16[256,2048]{1,0:T(8,128)(2,1)} %refs_1_.3, bf16[1024,256]{1,0:T(8,128)(2,1)} %bitcast.20.refs_2_, ...), custom_call_target="tpu_custom_call" | custom-call | flops 1000000000 | bytes 1048576 | tf_op jit(solution)/shard_map/pallas_call | solution.py:76
  153.7 8.9 %all-to-all-start.3 = ((bf16[32,32,128]{2,1,0:T(8,128)(2,1)}), bf16[32,32,128]{2,1,0:T(8,128)(2,1)S(1)}, u32[]{:S(2)}, u32[]{:S(2)}) async-start(bf16[32,32,128]{2,1,0:T(8,128)(2,1)} %get-tuple-element.104), calls=%async_computation.3 | async-start | bytes 524288 | tf_op jit(solution)/shard_map/all_to_all | solution.py:637
  162.7 1.4 collective-permute-done.23.refs_1_
  164.1 1.2 collective-permute-start.24
  165.3 3.7 %collective-permute-start.25 = (bf16[72,256]{1,0:T(8,128)(2,1)S(1)}, bf16[72,256]{1,0:T(8,128)(2,1)S(1)}, u32[]{:S(2)}, u32[]{:S(2)}) collective-permute-start(bf16[72,256]{1,0:T(8,128)(2,1)S(1)} %get-tuple-element.97), channel_id=1, source_target_pairs={{0,4},{1,5},{2,6},{3,7},{4,0},{5,1},{6,2},{7,3},{8,12},{9,13},{10,... | collective-permute-start | bytes 110600 | tf_op jit(solution)/shard_map/ppermute | solution.py:621
  169.0 2.3 %collective-permute-done.25.refs_2_ = bf16[72,256]{1,0:T(8,128)(2,1)S(1)} collective-permute-done((bf16[72,256]{1,0:T(8,128)(2,1)S(1)}, bf16[72,256]{1,0:T(8,128)(2,1)S(1)}, u32[]{:S(2)}, u32[]{:S(2)}) %collective-permute-start.25) | collective-permute-done | bytes 36896 | tf_op jit(solution)/shard_map/ppermute | solution.py:621
  171.4 2.8 %collective-permute-done.26.refs_3_ = bf16[72,256]{1,0:T(8,128)(2,1)S(1)} collective-permute-done((bf16[72,256]{1,0:T(8,128)(2,1)S(1)}, bf16[72,256]{1,0:T(8,128)(2,1)S(1)}, u32[]{:S(2)}, u32[]{:S(2)}) %collective-permute-start.26) | collective-permute-done | bytes 36896 | tf_op jit(solution)/shard_map/ppermute | solution.py:621
  174.3 4.6 %collective-permute-start.27 = (f32[64,128]{1,0:T(8,128)S(1)}, f32[64,128]{1,0:T(8,128)S(1)}, u32[]{:S(2)}, u32[]{:S(2)}) collective-permute-start(f32[64,128]{1,0:T(8,128)S(1)} %get-tuple-element.101), channel_id=1, source_target_pairs={{8,0},{16,8},{24,16},{32,24},{40,32},{48,40},{56,48},{64,56},{72,6... | collective-permute-start | bytes 98312 | tf_op jit(solution)/shard_map/ppermute | solution.py:692
  179.1 2.7 %collective-permute-start.28 = (f32[64,64]{1,0:T(8,128)S(1)}, f32[64,64]{1,0:T(8,128)S(1)}, u32[]{:S(2)}, u32[]{:S(2)}) collective-permute-start(f32[64,64]{1,0:T(8,128)S(1)} %shard_map.188), channel_id=1, source_target_pairs={{0,0},{1,32},{2,64},{3,96},{4,128},{5,160},{6,192},{7,224},{8,1},{... | collective-permute-start | bytes 49160 | tf_op jit(solution)/shard_map/ppermute | solution.py:696
  181.8 1.0 shard_map.186.refs_0_
  182.8 1.4 shard_map.187
  184.2 7.0 %collective-permute-done.28 = f32[64,64]{1,0:T(8,128)S(1)} collective-permute-done((f32[64,64]{1,0:T(8,128)S(1)}, f32[64,64]{1,0:T(8,128)S(1)}, u32[]{:S(2)}, u32[]{:S(2)}) %collective-permute-start.28) | collective-permute-done | bytes 16416 | tf_op jit(solution)/shard_map/ppermute | solution.py:696
  (98 shorter events, 7.8 us)
Async XLA Ops:
  1.3 20.8 %copy-start.25 = (f32[256,2]{0,1:T(2,128)S(1)}, f32[256,2]{0,1:T(2,128)}, u32[]{:S(2)}) copy-start(f32[256,2]{0,1:T(2,128)} %param.15) | copy-start | bytes 6148
  3.4 27.1 %all-to-all-start = ((bf16[32,16,512]{2,1,0:T(8,128)(2,1)}), bf16[32,16,512]{2,1,0:T(8,128)(2,1)S(1)}, u32[]{:S(2)}, u32[]{:S(2)}) async-start(bf16[32,16,512]{2,1,0:T(8,128)(2,1)} %bitcast.62), calls=%async_computation | async-start | bytes 1048576 | tf_op jit(solution)/shard_map/all_to_all | solution.py:637
  14.3 1.5 collective-permute-start.4
  17.4 7.3 %collective-permute-start.5 = (bf16[4,64,256]{2,1,0:T(8,128)(2,1)S(1)}, bf16[4,64,256]{2,1,0:T(8,128)(2,1)S(1)}, u32[]{:S(2)}, u32[]{:S(2)}) collective-permute-start(bf16[4,64,256]{2,1,0:T(8,128)(2,1)S(1)} %get-tuple-element.61), channel_id=1, source_target_pairs={{0,2},{1,3},{2,0},{3,1},{4,6},{5,7},{6,4},{7,5},{8,10},{9,11},{10,... | collective-permute-start | bytes 393224 | tf_op jit(solution)/shard_map/ppermute | solution.py:621
  19.0 9.3 %collective-permute-start.6 = (bf16[4,64,256]{2,1,0:T(8,128)(2,1)S(1)}, bf16[4,64,256]{2,1,0:T(8,128)(2,1)S(1)}, u32[]{:S(2)}, u32[]{:S(2)}) collective-permute-start(bf16[4,64,256]{2,1,0:T(8,128)(2,1)S(1)} %get-tuple-element.62), channel_id=1, source_target_pairs={{0,4},{1,5},{2,6},{3,7},{4,0},{5,1},{6,2},{7,3},{8,12},{9,13},{10,... | collective-permute-start | bytes 393224 | tf_op jit(solution)/shard_map/ppermute | solution.py:621
  21.9 8.7 %collective-permute-start.7 = (bf16[4,64,256]{2,1,0:T(8,128)(2,1)S(1)}, bf16[4,64,256]{2,1,0:T(8,128)(2,1)S(1)}, u32[]{:S(2)}, u32[]{:S(2)}) collective-permute-start(bf16[4,64,256]{2,1,0:T(8,128)(2,1)S(1)} %get-tuple-element.63), channel_id=1, source_target_pairs={{0,6},{1,7},{2,4},{3,5},{4,2},{5,3},{6,0},{7,1},{8,14},{9,15},{10,... | collective-permute-start | bytes 393224 | tf_op jit(solution)/shard_map/ppermute | solution.py:621
  22.1 22.2 %copy-start.26 = (bf16[1,256,2048]{2,1,0:T(8,128)(2,1)S(1)}, bf16[1,256,2048]{2,1,0:T(8,128)(2,1)}, u32[]{:S(2)}) copy-start(bf16[1,256,2048]{2,1,0:T(8,128)(2,1)} %param.23) | copy-start | bytes 3145732
  24.7 16.2 %copy-start.16 = (bf16[4,64,256]{2,1,0:T(8,128)(2,1)}, bf16[4,64,256]{2,1,0:T(8,128)(2,1)S(1)}, u32[]{:S(2)}) copy-start(bf16[4,64,256]{2,1,0:T(8,128)(2,1)S(1)} %collective-permute-done.5.refs_3_) | copy-start | bytes 393220
  28.3 12.6 %copy-start.18 = (bf16[4,64,256]{2,1,0:T(8,128)(2,1)}, bf16[4,64,256]{2,1,0:T(8,128)(2,1)S(1)}, u32[]{:S(2)}) copy-start(bf16[4,64,256]{2,1,0:T(8,128)(2,1)S(1)} %collective-permute-done.6.refs_4_) | copy-start | bytes 393220
  30.6 52.7 %copy-start.3 = (bf16[32,16,512]{2,1,0:T(8,128)(2,1)}, bf16[32,16,512]{2,1,0:T(8,128)(2,1)S(1)}, u32[]{:S(2)}) copy-start(bf16[32,16,512]{2,1,0:T(8,128)(2,1)S(1)} %all-to-all-done) | copy-start | bytes 1572868
  30.6 23.3 %all-to-all-start.1 = ((bf16[32,16,512]{2,1,0:T(8,128)(2,1)}), bf16[32,16,512]{2,1,0:T(8,128)(2,1)S(1)}, u32[]{:S(2)}, u32[]{:S(2)}) async-start(bf16[32,16,512]{2,1,0:T(8,128)(2,1)} %bitcast.63), calls=%async_computation.1 | async-start | bytes 1048576 | tf_op jit(solution)/shard_map/all_to_all | solution.py:637
  40.4 19.1 %collective-permute-start.10 = (bf16[2048,256]{1,0:T(8,128)(2,1)}, bf16[2048,256]{1,0:T(8,128)(2,1)}, u32[]{:S(2)}, u32[]{:S(2)}) collective-permute-start(bf16[2048,256]{1,0:T(8,128)(2,1)} %bitcast.54), channel_id=1, source_target_pairs={{0,1},{1,0},{2,3},{3,2},{4,5},{5,4},{6,7},{7,6},{8,9},{9,8},{10,11... | collective-permute-start | bytes 3145736 | tf_op jit(solution)/shard_map/ppermute | solution.py:621
  40.5 19.1 %collective-permute-start.11 = (bf16[2048,256]{1,0:T(8,128)(2,1)}, bf16[2048,256]{1,0:T(8,128)(2,1)}, u32[]{:S(2)}, u32[]{:S(2)}) collective-permute-start(bf16[2048,256]{1,0:T(8,128)(2,1)} %bitcast.58), channel_id=1, source_target_pairs={{0,1},{1,0},{2,3},{3,2},{4,5},{5,4},{6,7},{7,6},{8,9},{9,8},{10,11... | collective-permute-start | bytes 3145736 | tf_op jit(solution)/shard_map/ppermute | solution.py:621
  41.0 15.2 %collective-permute-start = (bf16[512,512]{1,0:T(8,128)(2,1)S(1)}, bf16[512,512]{1,0:T(8,128)(2,1)S(1)}, u32[]{:S(2)}, u32[]{:S(2)}) collective-permute-start(bf16[512,512]{1,0:T(8,128)(2,1)S(1)} %bitcast.34), channel_id=1, source_target_pairs={{0,2},{1,3},{2,4},{3,5},{4,6},{5,7},{6,0},{7,1},{8,10},{9,11},{10,... | collective-permute-start | bytes 1572872 | tf_op jit(solution)/shard_map/ppermute | solution.py:617
  41.1 15.1 %collective-permute-start.1 = (bf16[512,512]{1,0:T(8,128)(2,1)S(1)}, bf16[512,512]{1,0:T(8,128)(2,1)S(1)}, u32[]{:S(2)}, u32[]{:S(2)}) collective-permute-start(bf16[512,512]{1,0:T(8,128)(2,1)S(1)} %bitcast.35), channel_id=1, source_target_pairs={{0,6},{1,7},{2,0},{3,1},{4,2},{5,3},{6,4},{7,5},{8,14},{9,15},{10,... | collective-permute-start | bytes 1572872 | tf_op jit(solution)/shard_map/ppermute | solution.py:617
  44.3 42.6 %collective-permute-start.14 = (bf16[256,2048]{1,0:T(8,128)(2,1)S(1)}, bf16[256,2048]{1,0:T(8,128)(2,1)}, u32[]{:S(2)}, u32[]{:S(2)}) collective-permute-start(bf16[256,2048]{1,0:T(8,128)(2,1)S(1)} %bitcast.53), channel_id=1, source_target_pairs={{0,1},{1,0},{2,3},{3,2},{4,5},{5,4},{6,7},{7,6},{8,9},{9,8},{10,11... | collective-permute-start | bytes 3145736 | tf_op jit(solution)/shard_map/ppermute | solution.py:621
  53.9 37.4 %copy-start = (bf16[32,16,512]{2,1,0:T(8,128)(2,1)}, bf16[32,16,512]{2,1,0:T(8,128)(2,1)S(1)}, u32[]{:S(2)}) copy-start(bf16[32,16,512]{2,1,0:T(8,128)(2,1)S(1)} %all-to-all-done.1) | copy-start | bytes 1572868
  56.2 27.1 %copy-start.4 = (bf16[512,512]{1,0:T(8,128)(2,1)}, bf16[512,512]{1,0:T(8,128)(2,1)S(1)}, u32[]{:S(2)}) copy-start(bf16[512,512]{1,0:T(8,128)(2,1)S(1)} %collective-permute-done.refs_1_) | copy-start | bytes 1572868
  56.2 27.2 %collective-permute-start.8 = (bf16[512,512]{1,0:T(8,128)(2,1)S(1)}, bf16[512,512]{1,0:T(8,128)(2,1)S(1)}, u32[]{:S(2)}, u32[]{:S(2)}) collective-permute-start(bf16[512,512]{1,0:T(8,128)(2,1)S(1)} %bitcast.29), channel_id=1, source_target_pairs={{0,2},{1,3},{2,4},{3,5},{4,6},{5,7},{6,0},{7,1},{8,10},{9,11},{10,... | collective-permute-start | bytes 1572872 | tf_op jit(solution)/shard_map/ppermute | solution.py:617
  56.2 27.1 %copy-start.5 = (bf16[512,512]{1,0:T(8,128)(2,1)}, bf16[512,512]{1,0:T(8,128)(2,1)S(1)}, u32[]{:S(2)}) copy-start(bf16[512,512]{1,0:T(8,128)(2,1)S(1)} %collective-permute-done.1.refs_2_) | copy-start | bytes 1572868
  56.2 27.2 %collective-permute-start.9 = (bf16[512,512]{1,0:T(8,128)(2,1)S(1)}, bf16[512,512]{1,0:T(8,128)(2,1)S(1)}, u32[]{:S(2)}, u32[]{:S(2)}) collective-permute-start(bf16[512,512]{1,0:T(8,128)(2,1)S(1)} %bitcast.30), channel_id=1, source_target_pairs={{0,6},{1,7},{2,0},{3,1},{4,2},{5,3},{6,4},{7,5},{8,14},{9,15},{10,... | collective-permute-start | bytes 1572872 | tf_op jit(solution)/shard_map/ppermute | solution.py:617
  59.5 16.6 %collective-permute-start.2 = (bf16[256,512]{1,0:T(8,128)(2,1)S(1)}, bf16[256,512]{1,0:T(8,128)(2,1)S(1)}, u32[]{:S(2)}, u32[]{:S(2)}) collective-permute-start(bf16[256,512]{1,0:T(8,128)(2,1)S(1)} %slice.16), channel_id=1, source_target_pairs={{0,2},{1,3},{2,4},{3,5},{4,6},{5,7},{6,0},{7,1},{8,10},{9,11},{10,... | collective-permute-start | bytes 786440 | tf_op jit(solution)/shard_map/ppermute | solution.py:617
  59.6 16.5 %collective-permute-start.3 = (bf16[256,512]{1,0:T(8,128)(2,1)S(1)}, bf16[256,512]{1,0:T(8,128)(2,1)S(1)}, u32[]{:S(2)}, u32[]{:S(2)}) collective-permute-start(bf16[256,512]{1,0:T(8,128)(2,1)S(1)} %slice.17), channel_id=1, source_target_pairs={{0,6},{1,7},{2,0},{3,1},{4,2},{5,3},{6,4},{7,5},{8,14},{9,15},{10,... | collective-permute-start | bytes 786440 | tf_op jit(solution)/shard_map/ppermute | solution.py:617
  83.4 13.0 %copy-start.8 = (bf16[512,512]{1,0:T(8,128)(2,1)}, bf16[512,512]{1,0:T(8,128)(2,1)S(1)}, u32[]{:S(2)}) copy-start(bf16[512,512]{1,0:T(8,128)(2,1)S(1)} %get-tuple-element.79.refs_12_) | copy-start | bytes 1572868
  83.4 13.0 %copy-start.1 = (bf16[512,512]{1,0:T(8,128)(2,1)}, bf16[512,512]{1,0:T(8,128)(2,1)S(1)}, u32[]{:S(2)}) copy-start(bf16[512,512]{1,0:T(8,128)(2,1)S(1)} %collective-permute-done.8.refs_1_.refs_6_) | copy-start | bytes 1572868
  83.4 13.0 %copy-start.2 = (bf16[512,512]{1,0:T(8,128)(2,1)}, bf16[512,512]{1,0:T(8,128)(2,1)S(1)}, u32[]{:S(2)}) copy-start(bf16[512,512]{1,0:T(8,128)(2,1)S(1)} %collective-permute-done.9.refs_2_.refs_7_) | copy-start | bytes 1572868
  83.4 7.9 %collective-permute-start.12 = (bf16[256,512]{1,0:T(8,128)(2,1)S(1)}, bf16[256,512]{1,0:T(8,128)(2,1)S(1)}, u32[]{:S(2)}, u32[]{:S(2)}) collective-permute-start(bf16[256,512]{1,0:T(8,128)(2,1)S(1)} %slice.14), channel_id=1, source_target_pairs={{0,2},{1,3},{2,4},{3,5},{4,6},{5,7},{6,0},{7,1},{8,10},{9,11},{10,... | collective-permute-start | bytes 786440 | tf_op jit(solution)/shard_map/ppermute | solution.py:617
  83.6 7.8 %collective-permute-start.13 = (bf16[256,512]{1,0:T(8,128)(2,1)S(1)}, bf16[256,512]{1,0:T(8,128)(2,1)S(1)}, u32[]{:S(2)}, u32[]{:S(2)}) collective-permute-start(bf16[256,512]{1,0:T(8,128)(2,1)S(1)} %slice.15), channel_id=1, source_target_pairs={{0,6},{1,7},{2,0},{3,1},{4,2},{5,3},{6,4},{7,5},{8,14},{9,15},{10,... | collective-permute-start | bytes 786440 | tf_op jit(solution)/shard_map/ppermute | solution.py:617
  96.5 7.7 %collective-permute-start.15 = (bf16[2,256,256]{2,1,0:T(8,128)(2,1)S(1)}, bf16[2,256,256]{2,1,0:T(8,128)(2,1)S(1)}, u32[]{:S(2)}, u32[]{:S(2)}) collective-permute-start(bf16[2,256,256]{2,1,0:T(8,128)(2,1)S(1)} %get-tuple-element.72), channel_id=1, source_target_pairs={{0,2},{1,3},{2,4},{3,5},{4,6},{5,7},{6,0},{7,1},{8,10},{9,11},{10,... | collective-permute-start | bytes 786440 | tf_op jit(solution)/shard_map/ppermute | solution.py:617
  97.3 6.8 %collective-permute-start.16 = (bf16[2,256,256]{2,1,0:T(8,128)(2,1)S(1)}, bf16[2,256,256]{2,1,0:T(8,128)(2,1)S(1)}, u32[]{:S(2)}, u32[]{:S(2)}) collective-permute-start(bf16[2,256,256]{2,1,0:T(8,128)(2,1)S(1)} %get-tuple-element.73), channel_id=1, source_target_pairs={{0,6},{1,7},{2,0},{3,1},{4,2},{5,3},{6,4},{7,5},{8,14},{9,15},{10,... | collective-permute-start | bytes 786440 | tf_op jit(solution)/shard_map/ppermute | solution.py:617
  108.8 26.3 %copy-start.14 = (bf16[5,64,256]{2,1,0:T(8,128)(2,1)S(1)}, bf16[5,64,256]{2,1,0:T(8,128)(2,1)}, u32[]{:S(2)}) copy-start(bf16[5,64,256]{2,1,0:T(8,128)(2,1)} %copy-done.13) | copy-start | bytes 491524
  108.8 31.2 %collective-permute-start.17 = (bf16[12,512,256]{2,1,0:T(8,128)(2,1)S(1)}, bf16[12,512,256]{2,1,0:T(8,128)(2,1)}, u32[]{:S(2)}, u32[]{:S(2)}) collective-permute-start(bf16[12,512,256]{2,1,0:T(8,128)(2,1)S(1)} %shard_map.179), channel_id=1, source_target_pairs={{0,1},{1,0},{2,3},{3,2},{4,5},{5,4},{6,7},{7,6},{8,9},{9,8},{10,11... | collective-permute-start | bytes 9437192 | tf_op jit(solution)/shard_map/ppermute | solution.py:621
  108.9 6.0 %collective-permute-start.20 = (bf16[512,256]{1,0:T(8,128)(2,1)S(1)}, bf16[512,256]{1,0:T(8,128)(2,1)S(1)}, u32[]{:S(2)}, u32[]{:S(2)}) collective-permute-start(bf16[512,256]{1,0:T(8,128)(2,1)S(1)} %get-tuple-element.85), channel_id=1, source_target_pairs={{0,1},{1,0},{2,3},{3,2},{4,5},{5,4},{6,7},{7,6},{8,9},{9,8},{10,11... | collective-permute-start | bytes 786440 | tf_op jit(solution)/shard_map/ppermute | solution.py:621
  109.4 10.4 %collective-permute-start.18 = (bf16[512,256]{1,0:T(8,128)(2,1)S(1)}, bf16[512,256]{1,0:T(8,128)(2,1)S(1)}, u32[]{:S(2)}, u32[]{:S(2)}) collective-permute-start(bf16[512,256]{1,0:T(8,128)(2,1)S(1)} %get-tuple-element.78), channel_id=1, source_target_pairs={{0,2},{1,3},{2,4},{3,5},{4,6},{5,7},{6,0},{7,1},{8,10},{9,11},{10,... | collective-permute-start | bytes 786440 | tf_op jit(solution)/shard_map/ppermute | solution.py:617
  111.1 9.2 %collective-permute-start.19 = (bf16[512,256]{1,0:T(8,128)(2,1)S(1)}, bf16[512,256]{1,0:T(8,128)(2,1)S(1)}, u32[]{:S(2)}, u32[]{:S(2)}) collective-permute-start(bf16[512,256]{1,0:T(8,128)(2,1)S(1)} %get-tuple-element.84), channel_id=1, source_target_pairs={{0,6},{1,7},{2,0},{3,1},{4,2},{5,3},{6,4},{7,5},{8,14},{9,15},{10,... | collective-permute-start | bytes 786440 | tf_op jit(solution)/shard_map/ppermute | solution.py:617
  112.7 11.6 %collective-permute-start.21 = (bf16[512,256]{1,0:T(8,128)(2,1)S(1)}, bf16[512,256]{1,0:T(8,128)(2,1)S(1)}, u32[]{:S(2)}, u32[]{:S(2)}) collective-permute-start(bf16[512,256]{1,0:T(8,128)(2,1)S(1)} %get-tuple-element.86), channel_id=1, source_target_pairs={{0,3},{1,2},{2,5},{3,4},{4,7},{5,6},{6,1},{7,0},{8,11},{9,10},{10,... | collective-permute-start | bytes 786440 | tf_op jit(solution)/shard_map/ppermute | solution.py:625
  115.0 9.4 %collective-permute-start.22 = (bf16[512,256]{1,0:T(8,128)(2,1)S(1)}, bf16[512,256]{1,0:T(8,128)(2,1)S(1)}, u32[]{:S(2)}, u32[]{:S(2)}) collective-permute-start(bf16[512,256]{1,0:T(8,128)(2,1)S(1)} %get-tuple-element.87), channel_id=1, source_target_pairs={{0,7},{1,6},{2,1},{3,0},{4,3},{5,2},{6,5},{7,4},{8,15},{9,14},{10,... | collective-permute-start | bytes 786440 | tf_op jit(solution)/shard_map/ppermute | solution.py:625
  125.3 24.2 %all-to-all-start.2 = ((bf16[32,32,256]{2,1,0:T(8,128)(2,1)}), bf16[32,32,256]{2,1,0:T(8,128)(2,1)}, u32[]{:S(2)}, u32[]{:S(2)}) async-start(bf16[32,32,256]{2,1,0:T(8,128)(2,1)} %shard_map.181), calls=%async_computation.2 | async-start | bytes 1048576 | tf_op jit(solution)/shard_map/all_to_all | solution.py:637
  149.6 29.3 %copy-start.27 = (f32[31,64]{1,0:T(8,128)S(1)}, f32[31,64]{1,0:T(8,128)}, u32[]{:S(2)}) copy-start(f32[31,64]{1,0:T(8,128)} %param.18) | copy-start | bytes 23812
  149.6 33.3 %copy-start.22 = (bf16[256,64]{0,1:T(8,128)(2,1)S(1)}, bf16[256,64]{0,1:T(8,128)(2,1)}, u32[]{:S(2)}) copy-start(bf16[256,64]{0,1:T(8,128)(2,1)} %param.16) | copy-start | bytes 98308
  149.6 33.3 %copy-start.23 = (bf16[256,64]{0,1:T(8,128)(2,1)S(1)}, bf16[256,64]{0,1:T(8,128)(2,1)}, u32[]{:S(2)}) copy-start(bf16[256,64]{0,1:T(8,128)(2,1)} %param.17) | copy-start | bytes 98308
  153.7 25.3 %all-to-all-start.3 = ((bf16[32,32,128]{2,1,0:T(8,128)(2,1)}), bf16[32,32,128]{2,1,0:T(8,128)(2,1)S(1)}, u32[]{:S(2)}, u32[]{:S(2)}) async-start(bf16[32,32,128]{2,1,0:T(8,128)(2,1)} %get-tuple-element.104), calls=%async_computation.3 | async-start | bytes 524288 | tf_op jit(solution)/shard_map/all_to_all | solution.py:637
  162.6 1.5 collective-permute-start.23
  164.1 5.0 %collective-permute-start.24 = (bf16[72,256]{1,0:T(8,128)(2,1)S(1)}, bf16[72,256]{1,0:T(8,128)(2,1)S(1)}, u32[]{:S(2)}, u32[]{:S(2)}) collective-permute-start(bf16[72,256]{1,0:T(8,128)(2,1)S(1)} %get-tuple-element.96), channel_id=1, source_target_pairs={{0,2},{1,3},{2,0},{3,1},{4,6},{5,7},{6,4},{7,5},{8,10},{9,11},{10,... | collective-permute-start | bytes 110600 | tf_op jit(solution)/shard_map/ppermute | solution.py:621
  165.3 6.1 %collective-permute-start.25 = (bf16[72,256]{1,0:T(8,128)(2,1)S(1)}, bf16[72,256]{1,0:T(8,128)(2,1)S(1)}, u32[]{:S(2)}, u32[]{:S(2)}) collective-permute-start(bf16[72,256]{1,0:T(8,128)(2,1)S(1)} %get-tuple-element.97), channel_id=1, source_target_pairs={{0,4},{1,5},{2,6},{3,7},{4,0},{5,1},{6,2},{7,3},{8,12},{9,13},{10,... | collective-permute-start | bytes 110600 | tf_op jit(solution)/shard_map/ppermute | solution.py:621
  169.0 5.2 %collective-permute-start.26 = (bf16[72,256]{1,0:T(8,128)(2,1)S(1)}, bf16[72,256]{1,0:T(8,128)(2,1)S(1)}, u32[]{:S(2)}, u32[]{:S(2)}) collective-permute-start(bf16[72,256]{1,0:T(8,128)(2,1)S(1)} %get-tuple-element.98), channel_id=1, source_target_pairs={{0,6},{1,7},{2,4},{3,5},{4,2},{5,3},{6,0},{7,1},{8,14},{9,15},{10,... | collective-permute-start | bytes 110600 | tf_op jit(solution)/shard_map/ppermute | solution.py:621
  174.3 8.6 %collective-permute-start.27 = (f32[64,128]{1,0:T(8,128)S(1)}, f32[64,128]{1,0:T(8,128)S(1)}, u32[]{:S(2)}, u32[]{:S(2)}) collective-permute-start(f32[64,128]{1,0:T(8,128)S(1)} %get-tuple-element.101), channel_id=1, source_target_pairs={{8,0},{16,8},{24,16},{32,24},{40,32},{48,40},{56,48},{64,56},{72,6... | collective-permute-start | bytes 98312 | tf_op jit(solution)/shard_map/ppermute | solution.py:692
  179.1 12.1 %collective-permute-start.28 = (f32[64,64]{1,0:T(8,128)S(1)}, f32[64,64]{1,0:T(8,128)S(1)}, u32[]{:S(2)}, u32[]{:S(2)}) collective-permute-start(f32[64,64]{1,0:T(8,128)S(1)} %shard_map.188), channel_id=1, source_target_pairs={{0,0},{1,32},{2,64},{3,96},{4,128},{5,160},{6,192},{7,224},{8,1},{... | collective-permute-start | bytes 49160 | tf_op jit(solution)/shard_map/ppermute | solution.py:696
  (13 other events, 65.9 us)
where the time goes:
time: 193 us; the launch traced here: 192 us
  starting transfers between devices  79.4 us (41%)
  waiting for transfers between devices  60.3 us (31%)
  Pallas kernels  46 us (24%)
  local copies, waits for them, and re-layouts  4.92 us (3%)
    pallas_call x18, Pallas kernels, call(): pl.pallas_call(kernel, out_shape=outs, in_specs=[SMEM] + [HBM if i in sta...  46 us
    all_to_all x4, starting transfers between devices, exchange(): return lax.all_to_all(x, 'sp', 0, 0, tiled=True)  38.3 us
    ppermute x12, waiting for transfers between devices, moved(): return lax.ppermute(x, 'tp', [(i, (i + by) % TP) for i in range(TP)])  22.6 us
    ppermute x12, starting transfers between devices, moved(): return lax.ppermute(x, 'tp', [(i, (i + by) % TP) for i in range(TP)])  19.8 us
    ppermute x13, waiting for transfers between devices, swapped(): return lax.ppermute(x, 'tp', [(i, i ^ by) for i in range(TP)])  16 us
    ppermute x13, starting transfers between devices, swapped(): return lax.ppermute(x, 'tp', [(i, i ^ by) for i in range(TP)])  11 us
    all_to_all x4, waiting for transfers between devices, exchange(): return lax.all_to_all(x, 'sp', 0, 0, tiled=True)  10.6 us
    ppermute x1, waiting for transfers between devices, step(): lax.ppermute(total(tp, outer_in), ('sp', 'tp'), [((i * 8 + u) * TP + t, (...  6.97 us
  transfers between devices with their start and end apart: 33, of which 18 were waited for; matrix products, arithmetic and copies ran while one was open for 0% of the time, Pallas kernels for 16%

commit v1 on v0

--- a/solution.py
+++ b/solution.py
@@ -48,8 +48,9 @@
     return x.now() if isinstance(x, Later) else x
 
 
-def call(body, outs, tp, args, staged=(), cuts=None, scratch=(), flops=0, limit=40):
-    cuts = cuts or {}
+def call(body, outs, tp, args, staged=(), cuts=None, into=None, scratch=(), flops=0, limit=40):
+    cuts, into = cuts or {}, into or {}
+    own = tuple(i for i in staged if i not in into)
     single = not isinstance(outs, tuple)
     outs = (outs,) if single else outs
     n_in, n_out, n_scr = len(args), len(outs), len(scratch)
@@ -59,13 +60,17 @@
         made, scr, buffers = rest[:n_out], rest[n_out : n_out + n_scr], rest[n_out + n_scr :]
         for n, i in enumerate(staged):
             source = ins[i].at[cuts[i][1](t_ref[0])] if i in cuts else ins[i]
-            ins[i] = Later(source, buffers[n], buffers[-1].at[n])
+            if i in into:
+                target = scr[into[i][0]].at[into[i][1](t_ref[0])]
+            else:
+                target = buffers[own.index(i)]
+            ins[i] = Later(source, target, buffers[-1].at[n])
         body(t_ref[0], ins, made, scr)
         for i in staged:
             now(ins[i])
 
     extra = [
-        pltpu.VMEM(cuts[i][0] if i in cuts else args[i].shape, args[i].dtype) for i in staged
+        pltpu.VMEM(cuts[i][0] if i in cuts else args[i].shape, args[i].dtype) for i in own
     ]
     if staged:
         extra.append(pltpu.SemaphoreType.DMA((len(staged),)))
@@ -166,13 +171,11 @@
 
 
 def joined(refs):
-    own, left, right, top, bottom = [now(r) for r in refs]
-    return (
-        own[...],
-        left[...],
-        right[...],
-        jnp.concatenate([top[...], bottom[...]], axis=0),
-    )
+    refs = [now(r)[...] for r in refs]
+    own, sides, far = refs[0], refs[1:-2], jnp.concatenate(refs[-2:], axis=0)
+    if len(sides) == 4:
+        sides = [jnp.concatenate(sides[0:2], axis=0), jnp.concatenate(sides[2:4], axis=0)]
+    return own, *sides, far
 
 
 def forward_body(t, ins, outs, scr):
@@ -226,11 +229,11 @@
 def backward_body(t, ins, outs, scr):
     top_ref, bottom_ref, gg_ref, gu_ref = outs
     ga = scr[0]
-    a1, a2 = ins[7], ins[8]
+    a1, a2 = ins[9], ins[10]
     q = quarters(t)
-    x = joined(ins[0:5])
+    x = joined(ins[0:7])
     for j in range(2):
-        d = now(ins[5 + j])
+        d = now(ins[7 + j])
         ga[:, 256 * j : 256 * j + 256] = sum(
             dot(x[i], d[:, pl.ds(pl.multiple_of(q[i] * 512, 512), 512)], 1, 1) for i in range(4)
         )
@@ -243,7 +246,7 @@
         gu_ref[at, :] = (grad * a2[at, :]).astype(BF)
 
     g, u = gg_ref[...], gu_ref[...]
-    weights = [now(w) for w in ins[9:13]]
+    weights = [now(w) for w in ins[11:15]]
     for half in range(2):
         part = partial_of(g, u, weights, half).astype(BF)
         top_ref[half] = part[0:256]
@@ -262,8 +265,8 @@
         ),
         tp,
         (*blocks, *downs, a1, a2, *weights),
-        staged=(5, 6, 9, 10, 11, 12),
-        cuts={9: far, 10: far, 11: far, 12: far},
+        staged=(7, 8, 11, 12, 13, 14),
+        cuts={11: far, 12: far, 13: far, 14: far},
         scratch=[pltpu.VMEM((ROWS, 512), F32)],
         flops=2 * 10**9,
     )
@@ -320,56 +323,77 @@
     return call(settle_body, pltpu.HBM((SP, CAP, 256), BF), tp, parts, flops=10**7, limit=16)
 
 
-def weights_of(t, ins, cols):
-    q = quarters(t)
-    xs, cs = joined(ins[0:5]), joined(ins[5:10])
-    gg, gu, act = [now(x) for x in ins[10:13]]
+def by_column(scr_index, first, halves):
+    whole, upper, lower = slice(None), slice(0, 256), slice(256, 512)
+    sides = ((3, upper), (3, lower), (1, upper), (1, lower)) if halves else ((3, whole), (1, whole))
+    places = ((0, whole), *sides, (2, upper), (2, lower))
+    return {
+        first + n: (scr_index, lambda t, by=by, rows=rows: ((t // 2 + by) % 4, rows))
+        for n, (by, rows) in enumerate(places)
+    }
+
+
+def weights_call(body, outs, tp, args):
+    return call(
+        body,
+        outs,
+        tp,
+        args,
+        staged=tuple(range(len(args))),
+        into=by_column(0, 0, False) | by_column(1, 5, True),
+        scratch=[pltpu.VMEM((4, ROWS, 512), BF)] * 2,
+        flops=2 * 10**9,
+    )
+
+
+def each_quarter(ins, scr, cols, store):
+    ins = [now(x) for x in ins]
+    gg, gu, act = ins[12:15]
     gu_cols = jnp.concatenate([gg[:, cols], gu[:, cols]], axis=1)
     act_cols = act[:, cols]
-    for i in range(4):
-        both = dot(xs[i], gu_cols, 0, 0)
-        yield q[i], both[:, 0:256], both[:, 256:512], dot(act_cols, cs[i], 0, 0)
+
+    @pl.loop(0, 4)
+    def _(q):
+        store(q, dot(scr[0][q], gu_cols, 0, 0), dot(act_cols, scr[1][q], 0, 0))
 
 
 def lend_body(t, ins, outs, scr):
-    for q, a, b, d in weights_of(t, ins, slice(256, 512)):
-        outs[0][q] = a.astype(BF)
-        outs[0][4 + q] = b.astype(BF)
-        outs[0][8 + q, 0:256, :] = d[:, 0:256].astype(BF)
-        outs[0][8 + q, 256:512, :] = d[:, 256:512].astype(BF)
+    def store(q, both, down):
+        outs[0][q] = both[:, 0:256].astype(BF)
+        outs[0][4 + q] = both[:, 256:512].astype(BF)
+        outs[0][8 + q, 0:256, :] = down[:, 0:256].astype(BF)
+        outs[0][8 + q, 256:512, :] = down[:, 256:512].astype(BF)
+
+    each_quarter(ins, scr, slice(256, 512), store)
 
 
 def lend(tp, xs, cs, gg, gu, act):
-    return call(
-        lend_body,
-        shape((12, 512, 256), BF),
-        tp,
-        (*xs, *cs, gg, gu, act),
-        staged=tuple(range(13)),
-        flops=2 * 10**9,
+    return weights_call(
+        lend_body, shape((12, 512, 256), BF), tp, (*xs, *cs, gg, gu, act)
     )
 
 
 def keep_body(t, ins, outs, scr):
     gate_ref, up_ref, down_ref = outs
-    lent = now(ins[13])
-    for q, a, b, d in weights_of(t, ins, slice(0, 256)):
-        gate_ref[q] = a + lent[q].astype(F32)
-        up_ref[q] = b + lent[4 + q].astype(F32)
+
+    def store(q, both, down):
+        lent = now(ins[15])
+        gate_ref[q] = both[:, 0:256] + lent[q].astype(F32)
+        up_ref[q] = both[:, 256:512] + lent[4 + q].astype(F32)
         for half in range(2):
             cols = slice(256 * half, 256 * half + 256)
             at = pl.ds(pl.multiple_of(q * 512 + 256 * half, 256), 256)
-            down_ref[:, at] = d[:, cols] + lent[8 + q, cols, :].astype(F32)
+            down_ref[:, at] = down[:, cols] + lent[8 + q, cols, :].astype(F32)
+
+    each_quarter(ins, scr, slice(0, 256), store)
 
 
 def keep(tp, xs, cs, gg, gu, act, lent):
-    return call(
+    return weights_call(
         keep_body,
         (shape((4, 512, 256), F32), shape((4, 512, 256), F32), shape((256, 2048), F32)),
         tp,
         (*xs, *cs, gg, gu, act, lent),
-        staged=tuple(range(14)),
-        flops=2 * 10**9,
     )
 
 
@@ -468,8 +492,8 @@
             turned = pltpu.roll(block, 64, 1)
             even = jnp.where(lane[0:32], block[0:32], turned[32:64])
             odd = jnp.where(lane[0:32], turned[0:32], block[32:64])
-            outer_ref[8 * i + 2 * u] = even.astype(BF)
-            outer_ref[8 * i + 2 * u + 1] = odd.astype(BF)
+            outer_ref[8 * u + i] = even.astype(BF)
+            outer_ref[8 * u + 4 + i] = odd.astype(BF)
     part_all = scr[0]
     part = dot(now(ins[3])[...], gs, 1, 1)
     part_all[...] = part
@@ -625,12 +649,18 @@
     return lax.ppermute(x, "tp", [(i, ((i + by) % TP) ^ 1) for i in range(TP)])
 
 
-def around(block, hold=None):
+def around(block):
     left, right = moved(block, 2), moved(block, -2)
-    if hold is not None:
-        left, right, _ = lax.optimization_barrier((left, right, hold))
     top, bottom = moved(left[:256], 2), moved(right[256:], -2)
     return block, left, right, top, bottom
+
+
+def around_in_halves(block):
+    upper, lower = block[:256], block[256:]
+    left_upper, right_lower = moved(upper, 2), moved(lower, -2)
+    left_lower, right_upper = moved(lower, 2), moved(upper, -2)
+    top, bottom = moved(left_upper, 2), moved(right_lower, -2)
+    return block, left_upper, left_lower, right_upper, right_lower, top, bottom
 
 
 def exchange(x):
@@ -658,7 +688,8 @@
 
     cot_out, back = pick_cot(tp, target, route_weights.T, upstream)
     cot_out = after(cot_out, *early)
-    cot_in = exchange(cot_out.reshape(SP, HALF, 512)).reshape(ROWS, 512)
+    cot_in = exchange(cot_out.reshape(SP, HALF, 512))
+    cot_in = cot_in.reshape(ROWS, 512)
     proj_all, mixed, slope, slope_n, stat = prepare(tp, proj, saved, early)
 
     xs = around(rows_in)
@@ -666,7 +697,7 @@
     by_piece = [w.reshape(8, 256, 256) for w in (gate_own, gate_par, up_own, up_par)]
     act, a1, a2 = forward(tp, xs, by_quarter)
 
-    cs = around(cot_in, act)
+    cs = around_in_halves(cot_in)
     far_top, far_bottom, gg, gu = backward(tp, cs, (down_own, down_par), a1, a2, by_piece)
     got_top, got_bottom = moved(far_top, 2), moved(far_bottom, -2)
     parts = near(tp, gg, gu, by_piece)
@@ -685,7 +716,8 @@
     made = tokens(tp, back, upstream, returned, proj_all, mixed, slope, slope_n)
     grad_stream, outer, own_part, lent_part = made
     outer_in = exchange(outer)
-    folded = fold(tp, own_part, swapped(lent_part, 1))
+    lent_in = swapped(lent_part, 1)
+    folded = fold(tp, own_part, lent_in)
     own_part = folded[0]
     part_in = tuple(swapped(x, 2 * d + 2) for d, x in enumerate(folded[1:]))
     grad_conv, rim = norm(tp, own_part, part_in, saved, stat)
@@ -697,7 +729,7 @@
         total(tp, outer_in),
         ("sp", "tp"),
         [
-            ((i * 8 + u) * TP + t, (4 * t + i) * TP + u)
+            ((4 * u + i) * TP + t, (4 * t + i) * TP + u)
             for i in range(4)
             for u in range(TP)
             for t in range(TP)

time: 193 us -> 185 us (0.959)
  waiting for transfers between devices: 60.3 us -> 50.2 us
    ppermute x12 -> x14, waiting for transfers between devices: 22.6 us -> 11.7 us  [moved(): return lax.ppermute(x, 'tp', [(i, (i + by) % TP) for i in range(TP)])]
    ppermute x12 -> x14, starting transfers between devices: 19.8 us -> 21.8 us  [moved(): return lax.ppermute(x, 'tp', [(i, (i + by) % TP) for i in range(TP)])]
    unnamed x58 -> x62, local copies, waits for them, and re-layouts: 4.84 us -> 4.85 us
  transfers between devices with their start and end apart: 33 -> 35, of which waited for: 18 -> 17; matrix products, arithmetic and copies ran while one was open for 0% -> 0% of each run, Pallas kernels for 16% -> 16%
where the time goes in v1:
time: 185 us; the launch traced here: 184 us
  starting transfers between devices  81 us (44%)
  waiting for transfers between devices  50.2 us (27%)
  Pallas kernels  47.1 us (25%)
  local copies, waits for them, and re-layouts  4.92 us (3%)
    pallas_call x18, Pallas kernels, call(): pl.pallas_call(kernel, out_shape=outs, in_specs=[SMEM] + [HBM if i in sta...  47.1 us
    all_to_all x4, starting transfers between devices, exchange(): return lax.all_to_all(x, 'sp', 0, 0, tiled=True)  38.7 us
    ppermute x14, starting transfers between devices, moved(): return lax.ppermute(x, 'tp', [(i, (i + by) % TP) for i in range(TP)])  21.8 us
    ppermute x13, waiting for transfers between devices, swapped(): return lax.ppermute(x, 'tp', [(i, i ^ by) for i in range(TP)])  16 us
    ppermute x14, waiting for transfers between devices, moved(): return lax.ppermute(x, 'tp', [(i, (i + by) % TP) for i in range(TP)])  11.7 us
    ppermute x13, starting transfers between devices, swapped(): return lax.ppermute(x, 'tp', [(i, i ^ by) for i in range(TP)])  11 us
    all_to_all x4, waiting for transfers between devices, exchange(): return lax.all_to_all(x, 'sp', 0, 0, tiled=True)  10.2 us
    ppermute x1, waiting for transfers between devices, step(): lax.ppermute(total(tp, outer_in), ('sp', 'tp'), [((4 * u + i) * TP + t, (...  7.81 us
  transfers between devices with their start and end apart: 35, of which 17 were waited for; matrix products, arithmetic and copies ran while one was open for 0% of the time, Pallas kernels for 16%

profile of v1, /device:TPU:128, one launch (start us, length us, event | category | flops | bytes accessed | tf_op | source)
XLA Modules:
  0.0 184.5 jit_solution(7487810487349551626)
XLA Ops:
  1.3 2.1 %shard_map.171 = (bf16[512,512]{1,0:T(8,128)(2,1)}, s32[8,256]{1,0:T(8,128)S(1)}) custom-call(s32[1]{0:T(128)} %bitcast.t_ref, s32[2,256]{1,0:T(2,128)S(1)} %bitcast.47, bf16[256,2048]{1,0:T(8,128)(2,1)} %refs_1_.2), custom_call_target="tpu_custom_call" | custom-call | flops 1000000000 | bytes 1048576 | tf_op jit(solution)/shard_map/pallas_call | solution.py:81
  3.4 9.9 %all-to-all-start = ((bf16[32,16,512]{2,1,0:T(8,128)(2,1)}), bf16[32,16,512]{2,1,0:T(8,128)(2,1)S(1)}, u32[]{:S(2)}, u32[]{:S(2)}) async-start(bf16[32,16,512]{2,1,0:T(8,128)(2,1)} %bitcast.62), calls=%async_computation | async-start | bytes 1048576 | tf_op jit(solution)/shard_map/all_to_all | solution.py:667
  13.3 1.0 shard_map.173
  14.4 1.4 collective-permute-done.4.refs_2_
  15.8 1.0 shard_map.174
  17.4 1.6 collective-permute-start.5
  19.0 2.9 %collective-permute-start.6 = (bf16[4,64,256]{2,1,0:T(8,128)(2,1)S(1)}, bf16[4,64,256]{2,1,0:T(8,128)(2,1)S(1)}, u32[]{:S(2)}, u32[]{:S(2)}) collective-permute-start(bf16[4,64,256]{2,1,0:T(8,128)(2,1)S(1)} %get-tuple-element.60), channel_id=1, source_target_pairs={{0,4},{1,5},{2,6},{3,7},{4,0},{5,1},{6,2},{7,3},{8,12},{9,13},{10,... | collective-permute-start | bytes 393224 | tf_op jit(solution)/shard_map/ppermute | solution.py:645
  22.1 2.6 %shard_map.172 = (bf16[512,512]{1,0:T(8,128)(2,1)}, bf16[256,1024]{1,0:T(8,128)(2,1)}) custom-call(s32[1]{0:T(128)} %bitcast.t_ref, s32[8,256]{1,0:T(8,128)S(1)} %get-tuple-element.55.refs_0_, f32[2,256]{1,0:T(2,128)S(1)} %bitcast.48, bf16[256,2048]{1,0:T(8,128)(2,1)} %refs_1_.3), custom_call_target="tpu_custom_call" | custom-call | flops 1000000000 | bytes 1048576 | tf_op jit(solution)/shard_map/pallas_call | solution.py:81
  24.7 3.6 %collective-permute-done.6.refs_4_ = bf16[4,64,256]{2,1,0:T(8,128)(2,1)S(1)} collective-permute-done((bf16[4,64,256]{2,1,0:T(8,128)(2,1)S(1)}, bf16[4,64,256]{2,1,0:T(8,128)(2,1)S(1)}, u32[]{:S(2)}, u32[]{:S(2)}) %collective-permute-start.6) | collective-permute-done | bytes 131104 | tf_op jit(solution)/shard_map/ppermute | solution.py:645
  28.3 2.2 %collective-permute-done.7.refs_5_ = bf16[4,64,256]{2,1,0:T(8,128)(2,1)S(1)} collective-permute-done((bf16[4,64,256]{2,1,0:T(8,128)(2,1)S(1)}, bf16[4,64,256]{2,1,0:T(8,128)(2,1)S(1)}, u32[]{:S(2)}, u32[]{:S(2)}) %collective-permute-start.7) | collective-permute-done | bytes 131104 | tf_op jit(solution)/shard_map/ppermute | solution.py:645
  30.6 9.8 %all-to-all-start.1 = ((bf16[32,16,512]{2,1,0:T(8,128)(2,1)}), bf16[32,16,512]{2,1,0:T(8,128)(2,1)S(1)}, u32[]{:S(2)}, u32[]{:S(2)}) async-start(bf16[32,16,512]{2,1,0:T(8,128)(2,1)} %bitcast.63), calls=%async_computation.1 | async-start | bytes 1048576 | tf_op jit(solution)/shard_map/all_to_all | solution.py:667
  41.1 3.2 %collective-permute-start.1 = (bf16[512,512]{1,0:T(8,128)(2,1)S(1)}, bf16[512,512]{1,0:T(8,128)(2,1)S(1)}, u32[]{:S(2)}, u32[]{:S(2)}) collective-permute-start(bf16[512,512]{1,0:T(8,128)(2,1)S(1)} %bitcast.35), channel_id=1, source_target_pairs={{0,6},{1,7},{2,0},{3,1},{4,2},{5,3},{6,4},{7,5},{8,14},{9,15},{10,... | collective-permute-start | bytes 1572872 | tf_op jit(solution)/shard_map/ppermute | solution.py:641
  44.3 9.6 %all-to-all-done.1 = bf16[32,16,512]{2,1,0:T(8,128)(2,1)S(1)} async-done(((bf16[32,16,512]{2,1,0:T(8,128)(2,1)}), bf16[32,16,512]{2,1,0:T(8,128)(2,1)S(1)}, u32[]{:S(2)}, u32[]{:S(2)}) %all-to-all-start.1) | async-done | bytes 524320 | tf_op jit(solution)/shard_map/all_to_all | solution.py:667
  54.0 2.2 %collective-permute-done.refs_1_ = bf16[512,512]{1,0:T(8,128)(2,1)S(1)} collective-permute-done((bf16[512,512]{1,0:T(8,128)(2,1)S(1)}, bf16[512,512]{1,0:T(8,128)(2,1)S(1)}, u32[]{:S(2)}, u32[]{:S(2)}) %collective-permute-start) | collective-permute-done | bytes 524320 | tf_op jit(solution)/shard_map/ppermute | solution.py:641
  56.2 3.3 %collective-permute-start.11 = (bf16[256,512]{1,0:T(8,128)(2,1)S(1)}, bf16[256,512]{1,0:T(8,128)(2,1)S(1)}, u32[]{:S(2)}, u32[]{:S(2)}) collective-permute-start(bf16[256,512]{1,0:T(8,128)(2,1)S(1)} %bitcast.64), channel_id=1, source_target_pairs={{0,6},{1,7},{2,0},{3,1},{4,2},{5,3},{6,4},{7,5},{8,14},{9,15},{10,... | collective-permute-start | bytes 786440 | tf_op jit(solution)/shard_map/ppermute | solution.py:641
  59.7 3.2 %collective-permute-start.3 = (bf16[256,512]{1,0:T(8,128)(2,1)S(1)}, bf16[256,512]{1,0:T(8,128)(2,1)S(1)}, u32[]{:S(2)}, u32[]{:S(2)}) collective-permute-start(bf16[256,512]{1,0:T(8,128)(2,1)S(1)} %slice.25), channel_id=1, source_target_pairs={{0,6},{1,7},{2,0},{3,1},{4,2},{5,3},{6,4},{7,5},{8,14},{9,15},{10,... | collective-permute-start | bytes 786440 | tf_op jit(solution)/shard_map/ppermute | solution.py:641
  62.9 3.7 %collective-permute-done.8.refs_1_.refs_6_ = bf16[256,512]{1,0:T(8,128)(2,1)S(1)} collective-permute-done((bf16[256,512]{1,0:T(8,128)(2,1)S(1)}, bf16[256,512]{1,0:T(8,128)(2,1)S(1)}, u32[]{:S(2)}, u32[]{:S(2)}) %collective-permute-start.8) | collective-permute-done | bytes 262176 | tf_op jit(solution)/shard_map/ppermute | solution.py:641
  66.6 2.0 %collective-permute-start.9 = (bf16[256,512]{1,0:T(8,128)(2,1)S(1)}, bf16[256,512]{1,0:T(8,128)(2,1)S(1)}, u32[]{:S(2)}, u32[]{:S(2)}) collective-permute-start(bf16[256,512]{1,0:T(8,128)(2,1)S(1)} %bitcast.65), channel_id=1, source_target_pairs={{0,2},{1,3},{2,4},{3,5},{4,6},{5,7},{6,0},{7,1},{8,10},{9,11},{10,... | collective-permute-start | bytes 786440 | tf_op jit(solution)/shard_map/ppermute | solution.py:641
  68.6 3.6 %collective-permute-done.2.refs_3_ = bf16[256,512]{1,0:T(8,128)(2,1)S(1)} collective-permute-done((bf16[256,512]{1,0:T(8,128)(2,1)S(1)}, bf16[256,512]{1,0:T(8,128)(2,1)S(1)}, u32[]{:S(2)}, u32[]{:S(2)}) %collective-permute-start.2) | collective-permute-done | bytes 262176 | tf_op jit(solution)/shard_map/ppermute | solution.py:641
  72.2 3.3 %collective-permute-start.13 = (bf16[256,512]{1,0:T(8,128)(2,1)S(1)}, bf16[256,512]{1,0:T(8,128)(2,1)S(1)}, u32[]{:S(2)}, u32[]{:S(2)}) collective-permute-start(bf16[256,512]{1,0:T(8,128)(2,1)S(1)} %collective-permute-done.11.refs_4_.refs_9_), channel_id=1, source_target_pairs={{0,6},{1,7},{2,0},{3,1},{4,2},{5,3},{6,4},{7,5},{8,14},{9,15},{10,... | collective-permute-start | bytes 786440 | tf_op jit(solution)/shard_map/ppermute | solution.py:641
  75.6 7.0 %shard_map.175 = (bf16[512,512]{1,0:T(8,128)(2,1)S(1)}, f32[512,512]{1,0:T(8,128)S(1)}, f32[512,512]{1,0:T(8,128)S(1)}) custom-call(s32[1]{0:T(128)} %bitcast.t_ref, bf16[512,512]{1,0:T(8,128)(2,1)S(1)} %bitcast.36, bf16[512,512]{1,0:T(8,128)(2,1)S(1)} %collective-permute-done.refs_1_, bf16[512,512]{1,0:T(8,128)(2,1)S(1)} %collective-permute-done.1.refs_2_, ...), custom_call_target="tpu_custom_call" | custom-call | flops 2000000000 | bytes 1048576 | tf_op jit(solution)/shard_map/pallas_call | solution.py:81
  82.8 5.3 %shard_map.176 = (bf16[2,256,256]{2,1,0:T(8,128)(2,1)S(1)}, bf16[2,256,256]{2,1,0:T(8,128)(2,1)S(1)}, bf16[512,512]{1,0:T(8,128)(2,1)S(1)}, bf16[512,512]{1,0:T(8,128)(2,1)S(1)}) custom-call(s32[1]{0:T(128)} %bitcast.t_ref, bf16[512,512]{1,0:T(8,128)(2,1)S(1)} %bitcast.31, bf16[256,512]{1,0:T(8,128)(2,1)S(1)} %collective-permute-done.8.refs_1_.refs_6_, ...), custom_call_target="tpu_custom_call" | custom-call | flops 2000000000 | bytes 1048576 | tf_op jit(solution)/shard_map/pallas_call | solution.py:81
  88.2 3.2 %collective-permute-start.18 = (bf16[2,256,256]{2,1,0:T(8,128)(2,1)S(1)}, bf16[2,256,256]{2,1,0:T(8,128)(2,1)S(1)}, u32[]{:S(2)}, u32[]{:S(2)}) collective-permute-start(bf16[2,256,256]{2,1,0:T(8,128)(2,1)S(1)} %get-tuple-element.69), channel_id=1, source_target_pairs={{0,6},{1,7},{2,0},{3,1},{4,2},{5,3},{6,4},{7,5},{8,14},{9,15},{10,... | collective-permute-start | bytes 786440 | tf_op jit(solution)/shard_map/ppermute | solution.py:641
  91.4 4.0 %shard_map.177 = (bf16[512,256]{1,0:T(8,128)(2,1)S(1)}, bf16[512,256]{1,0:T(8,128)(2,1)S(1)}, bf16[512,256]{1,0:T(8,128)(2,1)S(1)}, bf16[512,256]{1,0:T(8,128)(2...) custom-call(s32[1]{0:T(128)} %bitcast.t_ref, ...), custom_call_target="tpu_custom_call" | custom-call | flops 3000000000 | bytes 1048576 | tf_op jit(solution)/shard_map/pallas_call | solution.py:81
  95.9 5.2 %shard_map.179 = bf16[12,512,256]{2,1,0:T(8,128)(2,1)S(1)} custom-call(s32[1]{0:T(128)} %bitcast.t_ref, bf16[512,512]{1,0:T(8,128)(2,1)} %bitcast.37, bf16[512,512]{1,0:T(8,128)(2,1)} %copy-done.2, bf16[512,512]{1,0:T(8,128)(2,1)} %copy-done.3, bf16[256,512]{1,0:T(8,128)(2,1)} %copy-done.13, bf16[256,512]{1,0:T(8,128)(2,1)} %copy-done.14, ...), custom_call_target="tpu_custom_call" | custom-call | flops 2000000000 | bytes 1048576 | tf_op jit(solution)/shard_map/pallas_call | solution.py:81
  101.8 3.2 %collective-permute-start.21 = (bf16[512,256]{1,0:T(8,128)(2,1)S(1)}, bf16[512,256]{1,0:T(8,128)(2,1)S(1)}, u32[]{:S(2)}, u32[]{:S(2)}) collective-permute-start(bf16[512,256]{1,0:T(8,128)(2,1)S(1)} %get-tuple-element.80), channel_id=1, source_target_pairs={{0,6},{1,7},{2,0},{3,1},{4,2},{5,3},{6,4},{7,5},{8,14},{9,15},{10,... | collective-permute-start | bytes 786440 | tf_op jit(solution)/shard_map/ppermute | solution.py:641
  105.0 2.3 %collective-permute-done.22.refs_3_ = bf16[512,256]{1,0:T(8,128)(2,1)S(1)} collective-permute-done((bf16[512,256]{1,0:T(8,128)(2,1)S(1)}, bf16[512,256]{1,0:T(8,128)(2,1)S(1)}, u32[]{:S(2)}, u32[]{:S(2)}) %collective-permute-start.22) | collective-permute-done | bytes 262176 | tf_op jit(solution)/shard_map/ppermute | solution.py:645
  107.3 3.0 %collective-permute-start.24 = (bf16[512,256]{1,0:T(8,128)(2,1)S(1)}, bf16[512,256]{1,0:T(8,128)(2,1)S(1)}, u32[]{:S(2)}, u32[]{:S(2)}) collective-permute-start(bf16[512,256]{1,0:T(8,128)(2,1)S(1)} %get-tuple-element.83), channel_id=1, source_target_pairs={{0,7},{1,6},{2,1},{3,0},{4,3},{5,2},{6,5},{7,4},{8,15},{9,14},{10,... | collective-permute-start | bytes 786440 | tf_op jit(solution)/shard_map/ppermute | solution.py:649
  110.3 1.9 %collective-permute-done.20.refs_1_ = bf16[512,256]{1,0:T(8,128)(2,1)S(1)} collective-permute-done((bf16[512,256]{1,0:T(8,128)(2,1)S(1)}, bf16[512,256]{1,0:T(8,128)(2,1)S(1)}, u32[]{:S(2)}, u32[]{:S(2)}) %collective-permute-start.20) | collective-permute-done | bytes 262176 | tf_op jit(solution)/shard_map/ppermute | solution.py:641
  112.2 4.4 %collective-permute-done.23.refs_4_ = bf16[512,256]{1,0:T(8,128)(2,1)S(1)} collective-permute-done((bf16[512,256]{1,0:T(8,128)(2,1)S(1)}, bf16[512,256]{1,0:T(8,128)(2,1)S(1)}, u32[]{:S(2)}, u32[]{:S(2)}) %collective-permute-start.23) | collective-permute-done | bytes 262176 | tf_op jit(solution)/shard_map/ppermute | solution.py:649
  116.6 1.0 shard_map.181
  117.6 9.8 %all-to-all-start.2 = ((bf16[32,32,256]{2,1,0:T(8,128)(2,1)}), bf16[32,32,256]{2,1,0:T(8,128)(2,1)}, u32[]{:S(2)}, u32[]{:S(2)}) async-start(bf16[32,32,256]{2,1,0:T(8,128)(2,1)} %shard_map.181), calls=%async_computation.2 | async-start | bytes 1048576 | tf_op jit(solution)/shard_map/all_to_all | solution.py:667
  128.4 0.9 copy-done.21
  129.3 0.9 copy-done.23
  130.2 2.2 %shard_map.182 = (bf16[512,256]{1,0:T(8,128)(2,1)}, bf16[512,256]{1,0:T(8,128)(2,1)}, f32[512,256]{1,0:T(8,128)}, f32[512,256]{1,0:T(8,128)}, f32[8,256]{1,0:T(8,128)S(1)}) custom-call(s32[1]{0:T(128)} %bitcast.t_ref, bf16[64,2048]{1,0:T(8,128)(2,1)} %bitcast.51, bf16[64,256]{1,0:T(8,128)(2,1)S(1)} %bitcast.41, bf16[5,64,256]{2,1,0:T(8,128)(2,1)S(1)} %copy-done.16, ...), custom_call_target="tpu_custom_call" | custom-call | flops 100000000 | bytes 1048576 | tf_op jit(solution)/shard_map/pallas_call | solution.py:81
  132.4 8.9 %shard_map.180 = (f32[4,512,256]{2,1,0:T(8,128)}, f32[4,512,256]{2,1,0:T(8,128)}, f32[256,2048]{1,0:T(8,128)}) custom-call(s32[1]{0:T(128)} %bitcast.t_ref, bf16[512,512]{1,0:T(8,128)(2,1)} %bitcast.38, bf16[512,512]{1,0:T(8,128)(2,1)} %copy-done.2, bf16[512,512]{1,0:T(8,128)(2,1)} %copy-done.3, bf16[256,512]{1,0:T(8,128)(2,1)} %copy-done.13, ...), custom_call_target="tpu_custom_call" | custom-call | flops 2000000000 | bytes 1048576 | tf_op jit(solution)/shard_map/pallas_call | solution.py:81
  141.9 4.2 %shard_map.183 = (bf16[256,256]{1,0:T(8,128)(2,1)}, bf16[32,32,128]{2,1,0:T(8,128)(2,1)}, f32[4,72,256]{2,1,0:T(8,128)S(1)}, bf16[4,72,256]{2,1,0:T(8,128)(2,1)S(1)}) custom-call(s32[1]{0:T(128)} %bitcast.t_ref, bf16[256,1024]{1,0:T(8,128)(2,1)} %get-tuple-element.77.refs_0_, bf16[256,2048]{1,0:T(8,128)(2,1)} %refs_1_.3, bf16[1024,256]{1,0:T(8,128)(2,1)} %bitcast.22.refs_2_, ...), custom_call_target="tpu_custom_call" | custom-call | flops 1000000000 | bytes 1048576 | tf_op jit(solution)/shard_map/pallas_call | solution.py:81
  146.1 9.2 %all-to-all-start.3 = ((bf16[32,32,128]{2,1,0:T(8,128)(2,1)}), bf16[32,32,128]{2,1,0:T(8,128)(2,1)S(1)}, u32[]{:S(2)}, u32[]{:S(2)}) async-start(bf16[32,32,128]{2,1,0:T(8,128)(2,1)} %get-tuple-element.100), calls=%async_computation.3 | async-start | bytes 524288 | tf_op jit(solution)/shard_map/all_to_all | solution.py:667
  155.4 1.4 collective-permute-done.25.refs_1_
  156.8 0.9 collective-permute-start.26
  157.7 4.0 %collective-permute-start.27 = (bf16[72,256]{1,0:T(8,128)(2,1)S(1)}, bf16[72,256]{1,0:T(8,128)(2,1)S(1)}, u32[]{:S(2)}, u32[]{:S(2)}) collective-permute-start(bf16[72,256]{1,0:T(8,128)(2,1)S(1)} %get-tuple-element.93), channel_id=1, source_target_pairs={{0,4},{1,5},{2,6},{3,7},{4,0},{5,1},{6,2},{7,3},{8,12},{9,13},{10,... | collective-permute-start | bytes 110600 | tf_op jit(solution)/shard_map/ppermute | solution.py:645
  161.7 2.3 %collective-permute-done.27.refs_2_ = bf16[72,256]{1,0:T(8,128)(2,1)S(1)} collective-permute-done((bf16[72,256]{1,0:T(8,128)(2,1)S(1)}, bf16[72,256]{1,0:T(8,128)(2,1)S(1)}, u32[]{:S(2)}, u32[]{:S(2)}) %collective-permute-start.27) | collective-permute-done | bytes 36896 | tf_op jit(solution)/shard_map/ppermute | solution.py:645
  164.0 2.8 %collective-permute-done.28.refs_3_ = bf16[72,256]{1,0:T(8,128)(2,1)S(1)} collective-permute-done((bf16[72,256]{1,0:T(8,128)(2,1)S(1)}, bf16[72,256]{1,0:T(8,128)(2,1)S(1)}, u32[]{:S(2)}, u32[]{:S(2)}) %collective-permute-start.28) | collective-permute-done | bytes 36896 | tf_op jit(solution)/shard_map/ppermute | solution.py:645
  166.9 4.6 %collective-permute-start.29 = (f32[64,128]{1,0:T(8,128)S(1)}, f32[64,128]{1,0:T(8,128)S(1)}, u32[]{:S(2)}, u32[]{:S(2)}) collective-permute-start(f32[64,128]{1,0:T(8,128)S(1)} %get-tuple-element.97), channel_id=1, source_target_pairs={{8,0},{16,8},{24,16},{32,24},{40,32},{48,40},{56,48},{64,56},{72,6... | collective-permute-start | bytes 98312 | tf_op jit(solution)/shard_map/ppermute | solution.py:724
  171.7 1.9 %collective-permute-start.30 = (f32[64,64]{1,0:T(8,128)S(1)}, f32[64,64]{1,0:T(8,128)S(1)}, u32[]{:S(2)}, u32[]{:S(2)}) collective-permute-start(f32[64,64]{1,0:T(8,128)S(1)} %shard_map.188), channel_id=1, source_target_pairs={{0,0},{1,32},{2,64},{3,96},{4,128},{5,160},{6,192},{7,224},{32,1},... | collective-permute-start | bytes 49160 | tf_op jit(solution)/shard_map/ppermute | solution.py:728
  173.7 1.0 shard_map.186.refs_0_
  174.7 1.4 shard_map.187
  176.1 7.8 %collective-permute-done.30 = f32[64,64]{1,0:T(8,128)S(1)} collective-permute-done((f32[64,64]{1,0:T(8,128)S(1)}, f32[64,64]{1,0:T(8,128)S(1)}, u32[]{:S(2)}, u32[]{:S(2)}) %collective-permute-start.30) | collective-permute-done | bytes 16416 | tf_op jit(solution)/shard_map/ppermute | solution.py:728
  (105 shorter events, 6.3 us)
Async XLA Ops:
  1.3 20.8 %copy-start.27 = (f32[256,2]{0,1:T(2,128)S(1)}, f32[256,2]{0,1:T(2,128)}, u32[]{:S(2)}) copy-start(f32[256,2]{0,1:T(2,128)} %param.15) | copy-start | bytes 6148
  3.4 27.1 %all-to-all-start = ((bf16[32,16,512]{2,1,0:T(8,128)(2,1)}), bf16[32,16,512]{2,1,0:T(8,128)(2,1)S(1)}, u32[]{:S(2)}, u32[]{:S(2)}) async-start(bf16[32,16,512]{2,1,0:T(8,128)(2,1)} %bitcast.62), calls=%async_computation | async-start | bytes 1048576 | tf_op jit(solution)/shard_map/all_to_all | solution.py:667
  14.3 1.5 collective-permute-start.4
  17.4 7.3 %collective-permute-start.5 = (bf16[4,64,256]{2,1,0:T(8,128)(2,1)S(1)}, bf16[4,64,256]{2,1,0:T(8,128)(2,1)S(1)}, u32[]{:S(2)}, u32[]{:S(2)}) collective-permute-start(bf16[4,64,256]{2,1,0:T(8,128)(2,1)S(1)} %get-tuple-element.59), channel_id=1, source_target_pairs={{0,2},{1,3},{2,0},{3,1},{4,6},{5,7},{6,4},{7,5},{8,10},{9,11},{10,... | collective-permute-start | bytes 393224 | tf_op jit(solution)/shard_map/ppermute | solution.py:645
  19.0 9.3 %collective-permute-start.6 = (bf16[4,64,256]{2,1,0:T(8,128)(2,1)S(1)}, bf16[4,64,256]{2,1,0:T(8,128)(2,1)S(1)}, u32[]{:S(2)}, u32[]{:S(2)}) collective-permute-start(bf16[4,64,256]{2,1,0:T(8,128)(2,1)S(1)} %get-tuple-element.60), channel_id=1, source_target_pairs={{0,4},{1,5},{2,6},{3,7},{4,0},{5,1},{6,2},{7,3},{8,12},{9,13},{10,... | collective-permute-start | bytes 393224 | tf_op jit(solution)/shard_map/ppermute | solution.py:645
  21.9 8.7 %collective-permute-start.7 = (bf16[4,64,256]{2,1,0:T(8,128)(2,1)S(1)}, bf16[4,64,256]{2,1,0:T(8,128)(2,1)S(1)}, u32[]{:S(2)}, u32[]{:S(2)}) collective-permute-start(bf16[4,64,256]{2,1,0:T(8,128)(2,1)S(1)} %get-tuple-element.61), channel_id=1, source_target_pairs={{0,6},{1,7},{2,4},{3,5},{4,2},{5,3},{6,0},{7,1},{8,14},{9,15},{10,... | collective-permute-start | bytes 393224 | tf_op jit(solution)/shard_map/ppermute | solution.py:645
  22.1 22.2 %copy-start.28 = (bf16[1,256,2048]{2,1,0:T(8,128)(2,1)S(1)}, bf16[1,256,2048]{2,1,0:T(8,128)(2,1)}, u32[]{:S(2)}) copy-start(bf16[1,256,2048]{2,1,0:T(8,128)(2,1)} %param.23) | copy-start | bytes 3145732
  24.7 16.2 %copy-start.18 = (bf16[4,64,256]{2,1,0:T(8,128)(2,1)}, bf16[4,64,256]{2,1,0:T(8,128)(2,1)S(1)}, u32[]{:S(2)}) copy-start(bf16[4,64,256]{2,1,0:T(8,128)(2,1)S(1)} %collective-permute-done.5.refs_3_) | copy-start | bytes 393220
  30.6 52.0 %copy-start.1 = (bf16[32,16,512]{2,1,0:T(8,128)(2,1)}, bf16[32,16,512]{2,1,0:T(8,128)(2,1)S(1)}, u32[]{:S(2)}) copy-start(bf16[32,16,512]{2,1,0:T(8,128)(2,1)S(1)} %all-to-all-done) | copy-start | bytes 1572868
  30.6 23.3 %all-to-all-start.1 = ((bf16[32,16,512]{2,1,0:T(8,128)(2,1)}), bf16[32,16,512]{2,1,0:T(8,128)(2,1)S(1)}, u32[]{:S(2)}, u32[]{:S(2)}) async-start(bf16[32,16,512]{2,1,0:T(8,128)(2,1)} %bitcast.63), calls=%async_computation.1 | async-start | bytes 1048576 | tf_op jit(solution)/shard_map/all_to_all | solution.py:667
  40.4 19.2 %collective-permute-start.15 = (bf16[2048,256]{1,0:T(8,128)(2,1)}, bf16[2048,256]{1,0:T(8,128)(2,1)}, u32[]{:S(2)}, u32[]{:S(2)}) collective-permute-start(bf16[2048,256]{1,0:T(8,128)(2,1)} %bitcast.54), channel_id=1, source_target_pairs={{0,1},{1,0},{2,3},{3,2},{4,5},{5,4},{6,7},{7,6},{8,9},{9,8},{10,11... | collective-permute-start | bytes 3145736 | tf_op jit(solution)/shard_map/ppermute | solution.py:645
  40.5 19.2 %collective-permute-start.16 = (bf16[2048,256]{1,0:T(8,128)(2,1)}, bf16[2048,256]{1,0:T(8,128)(2,1)}, u32[]{:S(2)}, u32[]{:S(2)}) collective-permute-start(bf16[2048,256]{1,0:T(8,128)(2,1)} %bitcast.58), channel_id=1, source_target_pairs={{0,1},{1,0},{2,3},{3,2},{4,5},{5,4},{6,7},{7,6},{8,9},{9,8},{10,11... | collective-permute-start | bytes 3145736 | tf_op jit(solution)/shard_map/ppermute | solution.py:645
  41.0 15.2 %collective-permute-start = (bf16[512,512]{1,0:T(8,128)(2,1)S(1)}, bf16[512,512]{1,0:T(8,128)(2,1)S(1)}, u32[]{:S(2)}, u32[]{:S(2)}) collective-permute-start(bf16[512,512]{1,0:T(8,128)(2,1)S(1)} %bitcast.34), channel_id=1, source_target_pairs={{0,2},{1,3},{2,4},{3,5},{4,6},{5,7},{6,0},{7,1},{8,10},{9,11},{10,... | collective-permute-start | bytes 1572872 | tf_op jit(solution)/shard_map/ppermute | solution.py:641
  41.1 15.2 %collective-permute-start.1 = (bf16[512,512]{1,0:T(8,128)(2,1)S(1)}, bf16[512,512]{1,0:T(8,128)(2,1)S(1)}, u32[]{:S(2)}, u32[]{:S(2)}) collective-permute-start(bf16[512,512]{1,0:T(8,128)(2,1)S(1)} %bitcast.35), channel_id=1, source_target_pairs={{0,6},{1,7},{2,0},{3,1},{4,2},{5,3},{6,4},{7,5},{8,14},{9,15},{10,... | collective-permute-start | bytes 1572872 | tf_op jit(solution)/shard_map/ppermute | solution.py:641
  44.3 38.3 %collective-permute-start.14 = (bf16[256,2048]{1,0:T(8,128)(2,1)S(1)}, bf16[256,2048]{1,0:T(8,128)(2,1)}, u32[]{:S(2)}, u32[]{:S(2)}) collective-permute-start(bf16[256,2048]{1,0:T(8,128)(2,1)S(1)} %bitcast.53), channel_id=1, source_target_pairs={{0,1},{1,0},{2,3},{3,2},{4,5},{5,4},{6,7},{7,6},{8,9},{9,8},{10,11... | collective-permute-start | bytes 3145736 | tf_op jit(solution)/shard_map/ppermute | solution.py:645
  53.9 28.8 %copy-start = (bf16[32,16,512]{2,1,0:T(8,128)(2,1)}, bf16[32,16,512]{2,1,0:T(8,128)(2,1)S(1)}, u32[]{:S(2)}) copy-start(bf16[32,16,512]{2,1,0:T(8,128)(2,1)S(1)} %all-to-all-done.1) | copy-start | bytes 1572868
  56.2 26.4 %copy-start.2 = (bf16[512,512]{1,0:T(8,128)(2,1)}, bf16[512,512]{1,0:T(8,128)(2,1)S(1)}, u32[]{:S(2)}) copy-start(bf16[512,512]{1,0:T(8,128)(2,1)S(1)} %collective-permute-done.refs_1_) | copy-start | bytes 1572868
  56.2 10.4 %collective-permute-start.8 = (bf16[256,512]{1,0:T(8,128)(2,1)S(1)}, bf16[256,512]{1,0:T(8,128)(2,1)S(1)}, u32[]{:S(2)}, u32[]{:S(2)}) collective-permute-start(bf16[256,512]{1,0:T(8,128)(2,1)S(1)} %bitcast.66), channel_id=1, source_target_pairs={{0,2},{1,3},{2,4},{3,5},{4,6},{5,7},{6,0},{7,1},{8,10},{9,11},{10,... | collective-permute-start | bytes 786440 | tf_op jit(solution)/shard_map/ppermute | solution.py:641
  56.2 26.4 %copy-start.3 = (bf16[512,512]{1,0:T(8,128)(2,1)}, bf16[512,512]{1,0:T(8,128)(2,1)S(1)}, u32[]{:S(2)}) copy-start(bf16[512,512]{1,0:T(8,128)(2,1)S(1)} %collective-permute-done.1.refs_2_) | copy-start | bytes 1572868
  56.2 10.3 %collective-permute-start.11 = (bf16[256,512]{1,0:T(8,128)(2,1)S(1)}, bf16[256,512]{1,0:T(8,128)(2,1)S(1)}, u32[]{:S(2)}, u32[]{:S(2)}) collective-permute-start(bf16[256,512]{1,0:T(8,128)(2,1)S(1)} %bitcast.64), channel_id=1, source_target_pairs={{0,6},{1,7},{2,0},{3,1},{4,2},{5,3},{6,4},{7,5},{8,14},{9,15},{10,... | collective-permute-start | bytes 786440 | tf_op jit(solution)/shard_map/ppermute | solution.py:641
  59.6 12.6 %collective-permute-start.2 = (bf16[256,512]{1,0:T(8,128)(2,1)S(1)}, bf16[256,512]{1,0:T(8,128)(2,1)S(1)}, u32[]{:S(2)}, u32[]{:S(2)}) collective-permute-start(bf16[256,512]{1,0:T(8,128)(2,1)S(1)} %slice.24), channel_id=1, source_target_pairs={{0,2},{1,3},{2,4},{3,5},{4,6},{5,7},{6,0},{7,1},{8,10},{9,11},{10,... | collective-permute-start | bytes 786440 | tf_op jit(solution)/shard_map/ppermute | solution.py:641
  59.7 12.5 %collective-permute-start.3 = (bf16[256,512]{1,0:T(8,128)(2,1)S(1)}, bf16[256,512]{1,0:T(8,128)(2,1)S(1)}, u32[]{:S(2)}, u32[]{:S(2)}) collective-permute-start(bf16[256,512]{1,0:T(8,128)(2,1)S(1)} %slice.25), channel_id=1, source_target_pairs={{0,6},{1,7},{2,0},{3,1},{4,2},{5,3},{6,4},{7,5},{8,14},{9,15},{10,... | collective-permute-start | bytes 786440 | tf_op jit(solution)/shard_map/ppermute | solution.py:641
  66.6 16.2 %copy-start.4 = (bf16[256,512]{1,0:T(8,128)(2,1)}, bf16[256,512]{1,0:T(8,128)(2,1)S(1)}, u32[]{:S(2)}) copy-start(bf16[256,512]{1,0:T(8,128)(2,1)S(1)} %collective-permute-done.8.refs_1_.refs_6_) | copy-start | bytes 786436
  66.6 16.1 %collective-permute-start.10 = (bf16[256,512]{1,0:T(8,128)(2,1)S(1)}, bf16[256,512]{1,0:T(8,128)(2,1)S(1)}, u32[]{:S(2)}, u32[]{:S(2)}) collective-permute-start(bf16[256,512]{1,0:T(8,128)(2,1)S(1)} %bitcast.67), channel_id=1, source_target_pairs={{0,6},{1,7},{2,0},{3,1},{4,2},{5,3},{6,4},{7,5},{8,14},{9,15},{10,... | collective-permute-start | bytes 786440 | tf_op jit(solution)/shard_map/ppermute | solution.py:641
  66.6 16.1 %copy-start.5 = (bf16[256,512]{1,0:T(8,128)(2,1)}, bf16[256,512]{1,0:T(8,128)(2,1)S(1)}, u32[]{:S(2)}) copy-start(bf16[256,512]{1,0:T(8,128)(2,1)S(1)} %collective-permute-done.11.refs_4_.refs_9_) | copy-start | bytes 786436
  66.6 16.1 %collective-permute-start.9 = (bf16[256,512]{1,0:T(8,128)(2,1)S(1)}, bf16[256,512]{1,0:T(8,128)(2,1)S(1)}, u32[]{:S(2)}, u32[]{:S(2)}) collective-permute-start(bf16[256,512]{1,0:T(8,128)(2,1)S(1)} %bitcast.65), channel_id=1, source_target_pairs={{0,2},{1,3},{2,4},{3,5},{4,6},{5,7},{6,0},{7,1},{8,10},{9,11},{10,... | collective-permute-start | bytes 786440 | tf_op jit(solution)/shard_map/ppermute | solution.py:641
  72.2 10.5 %collective-permute-start.12 = (bf16[256,512]{1,0:T(8,128)(2,1)S(1)}, bf16[256,512]{1,0:T(8,128)(2,1)S(1)}, u32[]{:S(2)}, u32[]{:S(2)}) collective-permute-start(bf16[256,512]{1,0:T(8,128)(2,1)S(1)} %collective-permute-done.8.refs_1_.refs_6_), channel_id=1, source_target_pairs={{0,2},{1,3},{2,4},{3,5},{4,6},{5,7},{6,0},{7,1},{8,10},{9,11},{10,... | collective-permute-start | bytes 786440 | tf_op jit(solution)/shard_map/ppermute | solution.py:641
  72.2 10.5 %collective-permute-start.13 = (bf16[256,512]{1,0:T(8,128)(2,1)S(1)}, bf16[256,512]{1,0:T(8,128)(2,1)S(1)}, u32[]{:S(2)}, u32[]{:S(2)}) collective-permute-start(bf16[256,512]{1,0:T(8,128)(2,1)S(1)} %collective-permute-done.11.refs_4_.refs_9_), channel_id=1, source_target_pairs={{0,6},{1,7},{2,0},{3,1},{4,2},{5,3},{6,4},{7,5},{8,14},{9,15},{10,... | collective-permute-start | bytes 786440 | tf_op jit(solution)/shard_map/ppermute | solution.py:641
  88.1 7.7 %collective-permute-start.17 = (bf16[2,256,256]{2,1,0:T(8,128)(2,1)S(1)}, bf16[2,256,256]{2,1,0:T(8,128)(2,1)S(1)}, u32[]{:S(2)}, u32[]{:S(2)}) collective-permute-start(bf16[2,256,256]{2,1,0:T(8,128)(2,1)S(1)} %get-tuple-element.68), channel_id=1, source_target_pairs={{0,2},{1,3},{2,4},{3,5},{4,6},{5,7},{6,0},{7,1},{8,10},{9,11},{10,... | collective-permute-start | bytes 786440 | tf_op jit(solution)/shard_map/ppermute | solution.py:641
  88.2 7.6 %collective-permute-start.18 = (bf16[2,256,256]{2,1,0:T(8,128)(2,1)S(1)}, bf16[2,256,256]{2,1,0:T(8,128)(2,1)S(1)}, u32[]{:S(2)}, u32[]{:S(2)}) collective-permute-start(bf16[2,256,256]{2,1,0:T(8,128)(2,1)S(1)} %get-tuple-element.69), channel_id=1, source_target_pairs={{0,6},{1,7},{2,0},{3,1},{4,2},{5,3},{6,4},{7,5},{8,14},{9,15},{10,... | collective-permute-start | bytes 786440 | tf_op jit(solution)/shard_map/ppermute | solution.py:641
  101.1 26.3 %copy-start.16 = (bf16[5,64,256]{2,1,0:T(8,128)(2,1)S(1)}, bf16[5,64,256]{2,1,0:T(8,128)(2,1)}, u32[]{:S(2)}) copy-start(bf16[5,64,256]{2,1,0:T(8,128)(2,1)} %copy-done.15) | copy-start | bytes 491524
  101.2 31.2 %collective-permute-start.19 = (bf16[12,512,256]{2,1,0:T(8,128)(2,1)S(1)}, bf16[12,512,256]{2,1,0:T(8,128)(2,1)}, u32[]{:S(2)}, u32[]{:S(2)}) collective-permute-start(bf16[12,512,256]{2,1,0:T(8,128)(2,1)S(1)} %shard_map.179), channel_id=1, source_target_pairs={{0,1},{1,0},{2,3},{3,2},{4,5},{5,4},{6,7},{7,6},{8,9},{9,8},{10,11... | collective-permute-start | bytes 9437192 | tf_op jit(solution)/shard_map/ppermute | solution.py:645
  101.3 6.0 %collective-permute-start.22 = (bf16[512,256]{1,0:T(8,128)(2,1)S(1)}, bf16[512,256]{1,0:T(8,128)(2,1)S(1)}, u32[]{:S(2)}, u32[]{:S(2)}) collective-permute-start(bf16[512,256]{1,0:T(8,128)(2,1)S(1)} %get-tuple-element.81), channel_id=1, source_target_pairs={{0,1},{1,0},{2,3},{3,2},{4,5},{5,4},{6,7},{7,6},{8,9},{9,8},{10,11... | collective-permute-start | bytes 786440 | tf_op jit(solution)/shard_map/ppermute | solution.py:645
  101.8 10.4 %collective-permute-start.20 = (bf16[512,256]{1,0:T(8,128)(2,1)S(1)}, bf16[512,256]{1,0:T(8,128)(2,1)S(1)}, u32[]{:S(2)}, u32[]{:S(2)}) collective-permute-start(bf16[512,256]{1,0:T(8,128)(2,1)S(1)} %get-tuple-element.74), channel_id=1, source_target_pairs={{0,2},{1,3},{2,4},{3,5},{4,6},{5,7},{6,0},{7,1},{8,10},{9,11},{10,... | collective-permute-start | bytes 786440 | tf_op jit(solution)/shard_map/ppermute | solution.py:641
  101.8 10.4 %collective-permute-start.21 = (bf16[512,256]{1,0:T(8,128)(2,1)S(1)}, bf16[512,256]{1,0:T(8,128)(2,1)S(1)}, u32[]{:S(2)}, u32[]{:S(2)}) collective-permute-start(bf16[512,256]{1,0:T(8,128)(2,1)S(1)} %get-tuple-element.80), channel_id=1, source_target_pairs={{0,6},{1,7},{2,0},{3,1},{4,2},{5,3},{6,4},{7,5},{8,14},{9,15},{10,... | collective-permute-start | bytes 786440 | tf_op jit(solution)/shard_map/ppermute | solution.py:641
  105.0 11.6 %collective-permute-start.23 = (bf16[512,256]{1,0:T(8,128)(2,1)S(1)}, bf16[512,256]{1,0:T(8,128)(2,1)S(1)}, u32[]{:S(2)}, u32[]{:S(2)}) collective-permute-start(bf16[512,256]{1,0:T(8,128)(2,1)S(1)} %get-tuple-element.82), channel_id=1, source_target_pairs={{0,3},{1,2},{2,5},{3,4},{4,7},{5,6},{6,1},{7,0},{8,11},{9,10},{10,... | collective-permute-start | bytes 786440 | tf_op jit(solution)/shard_map/ppermute | solution.py:649
  107.3 9.4 %collective-permute-start.24 = (bf16[512,256]{1,0:T(8,128)(2,1)S(1)}, bf16[512,256]{1,0:T(8,128)(2,1)S(1)}, u32[]{:S(2)}, u32[]{:S(2)}) collective-permute-start(bf16[512,256]{1,0:T(8,128)(2,1)S(1)} %get-tuple-element.83), channel_id=1, source_target_pairs={{0,7},{1,6},{2,1},{3,0},{4,3},{5,2},{6,5},{7,4},{8,15},{9,14},{10,... | collective-permute-start | bytes 786440 | tf_op jit(solution)/shard_map/ppermute | solution.py:649
  117.6 24.3 %all-to-all-start.2 = ((bf16[32,32,256]{2,1,0:T(8,128)(2,1)}), bf16[32,32,256]{2,1,0:T(8,128)(2,1)}, u32[]{:S(2)}, u32[]{:S(2)}) async-start(bf16[32,32,256]{2,1,0:T(8,128)(2,1)} %shard_map.181), calls=%async_computation.2 | async-start | bytes 1048576 | tf_op jit(solution)/shard_map/all_to_all | solution.py:667
  141.9 29.6 %copy-start.29 = (f32[31,64]{1,0:T(8,128)S(1)}, f32[31,64]{1,0:T(8,128)}, u32[]{:S(2)}) copy-start(f32[31,64]{1,0:T(8,128)} %param.18) | copy-start | bytes 23812
  141.9 32.8 %copy-start.24 = (bf16[256,64]{0,1:T(8,128)(2,1)S(1)}, bf16[256,64]{0,1:T(8,128)(2,1)}, u32[]{:S(2)}) copy-start(bf16[256,64]{0,1:T(8,128)(2,1)} %param.16) | copy-start | bytes 98308
  141.9 32.8 %copy-start.25 = (bf16[256,64]{0,1:T(8,128)(2,1)S(1)}, bf16[256,64]{0,1:T(8,128)(2,1)}, u32[]{:S(2)}) copy-start(bf16[256,64]{0,1:T(8,128)(2,1)} %param.17) | copy-start | bytes 98308
  146.1 25.6 %all-to-all-start.3 = ((bf16[32,32,128]{2,1,0:T(8,128)(2,1)}), bf16[32,32,128]{2,1,0:T(8,128)(2,1)S(1)}, u32[]{:S(2)}, u32[]{:S(2)}) async-start(bf16[32,32,128]{2,1,0:T(8,128)(2,1)} %get-tuple-element.100), calls=%async_computation.3 | async-start | bytes 524288 | tf_op jit(solution)/shard_map/all_to_all | solution.py:667
  155.3 1.5 collective-permute-start.25
  156.8 4.9 %collective-permute-start.26 = (bf16[72,256]{1,0:T(8,128)(2,1)S(1)}, bf16[72,256]{1,0:T(8,128)(2,1)S(1)}, u32[]{:S(2)}, u32[]{:S(2)}) collective-permute-start(bf16[72,256]{1,0:T(8,128)(2,1)S(1)} %get-tuple-element.92), channel_id=1, source_target_pairs={{0,2},{1,3},{2,0},{3,1},{4,6},{5,7},{6,4},{7,5},{8,10},{9,11},{10,... | collective-permute-start | bytes 110600 | tf_op jit(solution)/shard_map/ppermute | solution.py:645
  157.7 6.4 %collective-permute-start.27 = (bf16[72,256]{1,0:T(8,128)(2,1)S(1)}, bf16[72,256]{1,0:T(8,128)(2,1)S(1)}, u32[]{:S(2)}, u32[]{:S(2)}) collective-permute-start(bf16[72,256]{1,0:T(8,128)(2,1)S(1)} %get-tuple-element.93), channel_id=1, source_target_pairs={{0,4},{1,5},{2,6},{3,7},{4,0},{5,1},{6,2},{7,3},{8,12},{9,13},{10,... | collective-permute-start | bytes 110600 | tf_op jit(solution)/shard_map/ppermute | solution.py:645
  161.7 5.2 %collective-permute-start.28 = (bf16[72,256]{1,0:T(8,128)(2,1)S(1)}, bf16[72,256]{1,0:T(8,128)(2,1)S(1)}, u32[]{:S(2)}, u32[]{:S(2)}) collective-permute-start(bf16[72,256]{1,0:T(8,128)(2,1)S(1)} %get-tuple-element.94), channel_id=1, source_target_pairs={{0,6},{1,7},{2,4},{3,5},{4,2},{5,3},{6,0},{7,1},{8,14},{9,15},{10,... | collective-permute-start | bytes 110600 | tf_op jit(solution)/shard_map/ppermute | solution.py:645
  166.9 7.7 %collective-permute-start.29 = (f32[64,128]{1,0:T(8,128)S(1)}, f32[64,128]{1,0:T(8,128)S(1)}, u32[]{:S(2)}, u32[]{:S(2)}) collective-permute-start(f32[64,128]{1,0:T(8,128)S(1)} %get-tuple-element.97), channel_id=1, source_target_pairs={{8,0},{16,8},{24,16},{32,24},{40,32},{48,40},{56,48},{64,56},{72,6... | collective-permute-start | bytes 98312 | tf_op jit(solution)/shard_map/ppermute | solution.py:724
  171.7 12.1 %collective-permute-start.30 = (f32[64,64]{1,0:T(8,128)S(1)}, f32[64,64]{1,0:T(8,128)S(1)}, u32[]{:S(2)}, u32[]{:S(2)}) collective-permute-start(f32[64,64]{1,0:T(8,128)S(1)} %shard_map.188), channel_id=1, source_target_pairs={{0,0},{1,32},{2,64},{3,96},{4,128},{5,160},{6,192},{7,224},{32,1},... | collective-permute-start | bytes 49160 | tf_op jit(solution)/shard_map/ppermute | solution.py:728
  (17 other events, 101.6 us)

commit v2 on v1

--- a/solution.py
+++ b/solution.py
@@ -210,7 +210,7 @@
         (shape((ROWS, 512), BF), shape((ROWS, 512), F32), shape((ROWS, 512), F32)),
         tp,
         (*blocks, *weights),
-        staged=(5, 7, 6, 8),
+        staged=(5, 3, 4, 7, 6, 8),
         scratch=[pltpu.VMEM((ROWS, 512), F32)] * 2,
         flops=2 * 10**9,
     )
@@ -226,35 +226,64 @@
     )
 
 
+def down_columns(d, quarter):
+    return d[:, pl.ds(pl.multiple_of(quarter * 512, 512), 512)]
+
+
+def three_body(t, ins, outs, scr):
+    q = quarters(t)
+    own = ins[0][...]
+    sides = [(q[1], ins[1], ins[2]), (q[2], ins[3], ins[4])]
+    for j in range(2):
+        d = now(ins[5 + j])
+        cols = slice(256 * j, 256 * j + 256)
+        outs[0][:, cols] = dot(own, down_columns(d, q[0]), 1, 1)
+        for at, upper, lower in sides:
+            part = down_columns(d, at)
+            outs[0][0:256, cols] += dot(upper[...], part, 1, 1)
+            outs[0][256:512, cols] += dot(lower[...], part, 1, 1)
+
+
+def three(tp, blocks, downs):
+    return call(
+        three_body,
+        shape((ROWS, 512), F32),
+        tp,
+        (*blocks, *downs),
+        staged=(5, 6),
+        flops=10**9,
+        limit=32,
+    )
+
+
 def backward_body(t, ins, outs, scr):
     top_ref, bottom_ref, gg_ref, gu_ref = outs
-    ga = scr[0]
-    a1, a2 = ins[9], ins[10]
-    q = quarters(t)
-    x = joined(ins[0:7])
+    top, bottom, ga, a1, a2 = ins[0:5]
+    far = scr[0]
     for j in range(2):
-        d = now(ins[7 + j])
-        ga[:, 256 * j : 256 * j + 256] = sum(
-            dot(x[i], d[:, pl.ds(pl.multiple_of(q[i] * 512, 512), 512)], 1, 1) for i in range(4)
-        )
+        d = now(ins[5 + j])[...]
+        cols = slice(256 * j, 256 * j + 256)
+        far[0:256, cols] = dot(top[...], d, 1, 1)
+        far[256:512, cols] = dot(bottom[...], d, 1, 1)
 
     @pl.loop(0, ROWS // 32)
     def _(i):
         at = pl.ds(pl.multiple_of(i * 32, 32), 32)
-        grad = ga[at, :]
+        grad = ga[at, :] + far[at, :]
         gg_ref[at, :] = (grad * a1[at, :]).astype(BF)
         gu_ref[at, :] = (grad * a2[at, :]).astype(BF)
 
     g, u = gg_ref[...], gu_ref[...]
-    weights = [now(w) for w in ins[11:15]]
+    weights = [now(w) for w in ins[7:11]]
     for half in range(2):
         part = partial_of(g, u, weights, half).astype(BF)
         top_ref[half] = part[0:256]
         bottom_ref[half] = part[256:512]
 
 
-def backward(tp, blocks, downs, a1, a2, weights):
-    far = ((2, 256, 256), lambda t: (pl.ds(2 * ((t // 2 + 2) % 4), 2),))
+def backward(tp, far, ga, downs, a1, a2, weights):
+    pieces = ((2, 256, 256), lambda t: (pl.ds(2 * ((t // 2 + 2) % 4), 2),))
+    columns = ((256, 512), columns_of(512, lambda t: (t // 2 + 2) % 4))
     return call(
         backward_body,
         (
@@ -264,11 +293,12 @@
             shape((ROWS, 512), BF),
         ),
         tp,
-        (*blocks, *downs, a1, a2, *weights),
-        staged=(7, 8, 11, 12, 13, 14),
-        cuts={11: far, 12: far, 13: far, 14: far},
+        (*far, ga, a1, a2, *downs, *weights),
+        staged=(5, 6, 7, 8, 9, 10),
+        cuts={5: columns, 6: columns} | {i: pieces for i in range(7, 11)},
         scratch=[pltpu.VMEM((ROWS, 512), F32)],
         flops=2 * 10**9,
+        limit=32,
     )
 
 
@@ -481,7 +511,7 @@
 
 def tokens_body(t, ins, outs, scr):
     gs_ref, outer_ref, own_ref, lent_ref = outs
-    routed = dot(now(ins[0])[...], ins[2][...])
+    routed = dot(now(ins[0])[...], now(ins[2])[...])
     gs = (now(ins[1])[...].astype(F32) + routed).astype(BF)
     gs_ref[...] = gs
     outer = dot(gs, now(ins[4])[...], 0, 1)
@@ -551,7 +581,7 @@
         ),
         tp,
         (back, upstream, ret, proj, mixed, slope, slope_n),
-        staged=(0, 1, 4, 3, 5, 6),
+        staged=(0, 2, 1, 4, 3, 5, 6),
         cuts={1: ((TOK, 256), columns_of(256, lambda t: t))},
         scratch=[pltpu.VMEM((CW, TOK), F32)],
         flops=10**9,
@@ -698,7 +728,9 @@
     act, a1, a2 = forward(tp, xs, by_quarter)
 
     cs = around_in_halves(cot_in)
-    far_top, far_bottom, gg, gu = backward(tp, cs, (down_own, down_par), a1, a2, by_piece)
+    downs = (down_own, down_par)
+    ga = three(tp, cs[:5], downs)
+    far_top, far_bottom, gg, gu = backward(tp, cs[5:], ga, downs, a1, a2, by_piece)
     got_top, got_bottom = moved(far_top, 2), moved(far_bottom, -2)
     parts = near(tp, gg, gu, by_piece)
     rs, rc, ls, lc = merge(tp, got_top, got_bottom, parts[:4])

time: 185 us -> 186 us (level)
  starting transfers between devices: 81 us -> 76.5 us
  waiting for transfers between devices: 50.2 us -> 54.2 us
    ppermute x14, starting transfers between devices: 21.8 us -> 17.2 us  [moved(): return lax.ppermute(x, 'tp', [(i, (i + by) % TP) for i in range(TP)])]
    ppermute x14, waiting for transfers between devices: 11.7 us -> 15.7 us  [moved(): return lax.ppermute(x, 'tp', [(i, (i + by) % TP) for i in range(TP)])]
    pallas_call x18 -> x19, Pallas kernels: 47.1 us -> 47.3 us  [call(): pl.pallas_call(kernel, out_shape=outs, in_specs=[SMEM] + [HBM if i in sta...]
  transfers between devices with their start and end apart: 35 -> 35, of which waited for: 17 -> 19; matrix products, arithmetic and copies ran while one was open for 0% -> 0% of each run, Pallas kernels for 16% -> 18%
where the time goes in v2:
time: 186 us; the launch traced here: 185 us
  starting transfers between devices  76.5 us (41%)
  waiting for transfers between devices  54.2 us (29%)
  Pallas kernels  47.3 us (25%)
  local copies, waits for them, and re-layouts  5.68 us (3%)
    pallas_call x19, Pallas kernels, call(): pl.pallas_call(kernel, out_shape=outs, in_specs=[SMEM] + [HBM if i in sta...  47.3 us
    all_to_all x4, starting transfers between devices, exchange(): return lax.all_to_all(x, 'sp', 0, 0, tiled=True)  38.7 us
    ppermute x14, starting transfers between devices, moved(): return lax.ppermute(x, 'tp', [(i, (i + by) % TP) for i in range(TP)])  17.2 us
    ppermute x13, waiting for transfers between devices, swapped(): return lax.ppermute(x, 'tp', [(i, i ^ by) for i in range(TP)])  16 us
    ppermute x14, waiting for transfers between devices, moved(): return lax.ppermute(x, 'tp', [(i, (i + by) % TP) for i in range(TP)])  15.7 us
    ppermute x13, starting transfers between devices, swapped(): return lax.ppermute(x, 'tp', [(i, i ^ by) for i in range(TP)])  11.1 us
    all_to_all x4, waiting for transfers between devices, exchange(): return lax.all_to_all(x, 'sp', 0, 0, tiled=True)  10.1 us
    ppermute x1, waiting for transfers between devices, step(): lax.ppermute(total(tp, outer_in), ('sp', 'tp'), [((4 * u + i) * TP + t, (...  7.81 us
  transfers between devices with their start and end apart: 35, of which 19 were waited for; matrix products, arithmetic and copies ran while one was open for 0% of the time, Pallas kernels for 18%

profile of v2, /device:TPU:128, one launch (start us, length us, event | category | flops | bytes accessed | tf_op | source)
XLA Modules:
  0.0 184.8 jit_solution(7859967564680738899)
XLA Ops:
  1.3 2.1 %shard_map.171 = (bf16[512,512]{1,0:T(8,128)(2,1)}, s32[8,256]{1,0:T(8,128)S(1)}) custom-call(s32[1]{0:T(128)} %bitcast.t_ref, s32[2,256]{1,0:T(2,128)S(1)} %bitcast.47, bf16[256,2048]{1,0:T(8,128)(2,1)} %refs_1_.2), custom_call_target="tpu_custom_call" | custom-call | flops 1000000000 | bytes 1048576 | tf_op jit(solution)/shard_map/pallas_call | solution.py:81
  3.4 9.9 %all-to-all-start = ((bf16[32,16,512]{2,1,0:T(8,128)(2,1)}), bf16[32,16,512]{2,1,0:T(8,128)(2,1)S(1)}, u32[]{:S(2)}, u32[]{:S(2)}) async-start(bf16[32,16,512]{2,1,0:T(8,128)(2,1)} %bitcast.63), calls=%async_computation | async-start | bytes 1048576 | tf_op jit(solution)/shard_map/all_to_all | solution.py:697
  13.3 1.0 shard_map.173
  14.4 1.4 collective-permute-done.4.refs_2_
  15.8 1.0 shard_map.174
  17.4 1.6 collective-permute-start.5
  19.0 2.9 %collective-permute-start.6 = (bf16[4,64,256]{2,1,0:T(8,128)(2,1)S(1)}, bf16[4,64,256]{2,1,0:T(8,128)(2,1)S(1)}, u32[]{:S(2)}, u32[]{:S(2)}) collective-permute-start(bf16[4,64,256]{2,1,0:T(8,128)(2,1)S(1)} %get-tuple-element.60), channel_id=1, source_target_pairs={{0,4},{1,5},{2,6},{3,7},{4,0},{5,1},{6,2},{7,3},{8,12},{9,13},{10,... | collective-permute-start | bytes 393224 | tf_op jit(solution)/shard_map/ppermute | solution.py:675
  22.1 2.6 %shard_map.172 = (bf16[512,512]{1,0:T(8,128)(2,1)}, bf16[256,1024]{1,0:T(8,128)(2,1)}) custom-call(s32[1]{0:T(128)} %bitcast.t_ref, s32[8,256]{1,0:T(8,128)S(1)} %get-tuple-element.55.refs_0_, f32[2,256]{1,0:T(2,128)S(1)} %bitcast.48, bf16[256,2048]{1,0:T(8,128)(2,1)} %refs_1_.3), custom_call_target="tpu_custom_call" | custom-call | flops 1000000000 | bytes 1048576 | tf_op jit(solution)/shard_map/pallas_call | solution.py:81
  24.7 3.6 %collective-permute-done.6.refs_4_ = bf16[4,64,256]{2,1,0:T(8,128)(2,1)S(1)} collective-permute-done((bf16[4,64,256]{2,1,0:T(8,128)(2,1)S(1)}, bf16[4,64,256]{2,1,0:T(8,128)(2,1)S(1)}, u32[]{:S(2)}, u32[]{:S(2)}) %collective-permute-start.6) | collective-permute-done | bytes 131104 | tf_op jit(solution)/shard_map/ppermute | solution.py:675
  28.3 2.2 %collective-permute-done.7.refs_5_ = bf16[4,64,256]{2,1,0:T(8,128)(2,1)S(1)} collective-permute-done((bf16[4,64,256]{2,1,0:T(8,128)(2,1)S(1)}, bf16[4,64,256]{2,1,0:T(8,128)(2,1)S(1)}, u32[]{:S(2)}, u32[]{:S(2)}) %collective-permute-start.7) | collective-permute-done | bytes 131104 | tf_op jit(solution)/shard_map/ppermute | solution.py:675
  30.6 9.8 %all-to-all-start.1 = ((bf16[32,16,512]{2,1,0:T(8,128)(2,1)}), bf16[32,16,512]{2,1,0:T(8,128)(2,1)S(1)}, u32[]{:S(2)}, u32[]{:S(2)}) async-start(bf16[32,16,512]{2,1,0:T(8,128)(2,1)} %bitcast.64), calls=%async_computation.1 | async-start | bytes 1048576 | tf_op jit(solution)/shard_map/all_to_all | solution.py:697
  41.2 3.2 %collective-permute-start.1 = (bf16[512,512]{1,0:T(8,128)(2,1)S(1)}, bf16[512,512]{1,0:T(8,128)(2,1)S(1)}, u32[]{:S(2)}, u32[]{:S(2)}) collective-permute-start(bf16[512,512]{1,0:T(8,128)(2,1)S(1)} %bitcast.35), channel_id=1, source_target_pairs={{0,6},{1,7},{2,0},{3,1},{4,2},{5,3},{6,4},{7,5},{8,14},{9,15},{10,... | collective-permute-start | bytes 1572872 | tf_op jit(solution)/shard_map/ppermute | solution.py:671
  44.4 9.5 %all-to-all-done.1 = bf16[32,16,512]{2,1,0:T(8,128)(2,1)S(1)} async-done(((bf16[32,16,512]{2,1,0:T(8,128)(2,1)}), bf16[32,16,512]{2,1,0:T(8,128)(2,1)S(1)}, u32[]{:S(2)}, u32[]{:S(2)}) %all-to-all-start.1) | async-done | bytes 524320 | tf_op jit(solution)/shard_map/all_to_all | solution.py:697
  54.7 1.9 %collective-permute-done.refs_1_ = bf16[512,512]{1,0:T(8,128)(2,1)S(1)} collective-permute-done((bf16[512,512]{1,0:T(8,128)(2,1)S(1)}, bf16[512,512]{1,0:T(8,128)(2,1)S(1)}, u32[]{:S(2)}, u32[]{:S(2)}) %collective-permute-start) | collective-permute-done | bytes 524320 | tf_op jit(solution)/shard_map/ppermute | solution.py:671
  56.7 1.4 collective-permute-start.9
  58.2 5.1 %collective-permute-done.10.refs_3_.refs_8_ = bf16[256,512]{1,0:T(8,128)(2,1)S(1)} collective-permute-done((bf16[256,512]{1,0:T(8,128)(2,1)S(1)}, bf16[256,512]{1,0:T(8,128)(2,1)S(1)}, u32[]{:S(2)}, u32[]{:S(2)}) %collective-permute-start.10) | collective-permute-done | bytes 262176 | tf_op jit(solution)/shard_map/ppermute | solution.py:671
  63.2 3.9 %collective-permute-done.11.refs_4_.refs_9_ = bf16[256,512]{1,0:T(8,128)(2,1)S(1)} collective-permute-done((bf16[256,512]{1,0:T(8,128)(2,1)S(1)}, bf16[256,512]{1,0:T(8,128)(2,1)S(1)}, u32[]{:S(2)}, u32[]{:S(2)}) %collective-permute-start.11) | collective-permute-done | bytes 262176 | tf_op jit(solution)/shard_map/ppermute | solution.py:671
  67.1 3.7 %collective-permute-start.3 = (bf16[256,512]{1,0:T(8,128)(2,1)S(1)}, bf16[256,512]{1,0:T(8,128)(2,1)S(1)}, u32[]{:S(2)}, u32[]{:S(2)}) collective-permute-start(bf16[256,512]{1,0:T(8,128)(2,1)S(1)} %slice.25), channel_id=1, source_target_pairs={{0,6},{1,7},{2,0},{3,1},{4,2},{5,3},{6,4},{7,5},{8,14},{9,15},{10,... | collective-permute-start | bytes 786440 | tf_op jit(solution)/shard_map/ppermute | solution.py:671
  70.8 1.8 collective-permute-done.9.refs_2_.refs_7_
  72.6 1.4 collective-permute-start.13
  74.1 3.2 %shard_map.175.refs_2_ = f32[512,512]{1,0:T(8,128)S(1)} custom-call(s32[1]{0:T(128)} %bitcast.t_ref, bf16[512,512]{1,0:T(8,128)(2,1)S(1)} %bitcast.31, bf16[256,512]{1,0:T(8,128)(2,1)S(1)} %collective-permute-done.8.refs_1_.refs_6_, bf16[256,512]{1,0:T(8,128)(2,1)S(1)} %collective-permute-done.9.refs_2_.refs_7_, ...), custom_call_target="tpu_custom_call" | custom-call | flops 1000000000 | bytes 1048576 | tf_op jit(solution)/shard_map/pallas_call | solution.py:81
  79.0 7.2 %shard_map.176 = (bf16[512,512]{1,0:T(8,128)(2,1)S(1)}, f32[512,512]{1,0:T(8,128)S(1)}, f32[512,512]{1,0:T(8,128)S(1)}) custom-call(s32[1]{0:T(128)} %bitcast.t_ref, bf16[512,512]{1,0:T(8,128)(2,1)S(1)} %bitcast.36, bf16[512,512]{1,0:T(8,128)(2,1)S(1)} %collective-permute-done.refs_1_, bf16[512,512]{1,0:T(8,128)(2,1)S(1)} %collective-permute-done.1.refs_2_, ...), custom_call_target="tpu_custom_call" | custom-call | flops 2000000000 | bytes 1048576 | tf_op jit(solution)/shard_map/pallas_call | solution.py:81
  86.3 3.0 %shard_map.177 = (bf16[2,256,256]{2,1,0:T(8,128)(2,1)S(1)}, bf16[2,256,256]{2,1,0:T(8,128)(2,1)S(1)}, bf16[512,512]{1,0:T(8,128)(2,1)S(1)}, bf16[512,512]{1,0:T(8,128)(2,1)S(1)}) custom-call(s32[1]{0:T(128)} %bitcast.t_ref, bf16[256,512]{1,0:T(8,128)(2,1)S(1)} %collective-permute-done.12.refs_0_.refs_10_, ...), custom_call_target="tpu_custom_call" | custom-call | flops 2000000000 | bytes 1048576 | tf_op jit(solution)/shard_map/pallas_call | solution.py:81
  89.4 3.2 %collective-permute-start.18 = (bf16[2,256,256]{2,1,0:T(8,128)(2,1)S(1)}, bf16[2,256,256]{2,1,0:T(8,128)(2,1)S(1)}, u32[]{:S(2)}, u32[]{:S(2)}) collective-permute-start(bf16[2,256,256]{2,1,0:T(8,128)(2,1)S(1)} %get-tuple-element.69), channel_id=1, source_target_pairs={{0,6},{1,7},{2,0},{3,1},{4,2},{5,3},{6,4},{7,5},{8,14},{9,15},{10,... | collective-permute-start | bytes 786440 | tf_op jit(solution)/shard_map/ppermute | solution.py:671
  92.6 4.0 %shard_map.178 = (bf16[512,256]{1,0:T(8,128)(2,1)S(1)}, bf16[512,256]{1,0:T(8,128)(2,1)S(1)}, bf16[512,256]{1,0:T(8,128)(2,1)S(1)}, bf16[512,256]{1,0:T(8,128)(2...) custom-call(s32[1]{0:T(128)} %bitcast.t_ref, ...), custom_call_target="tpu_custom_call" | custom-call | flops 3000000000 | bytes 1048576 | tf_op jit(solution)/shard_map/pallas_call | solution.py:81
  97.1 5.2 %shard_map.180 = bf16[12,512,256]{2,1,0:T(8,128)(2,1)S(1)} custom-call(s32[1]{0:T(128)} %bitcast.t_ref, bf16[512,512]{1,0:T(8,128)(2,1)} %bitcast.37, bf16[512,512]{1,0:T(8,128)(2,1)} %copy-done.2, bf16[512,512]{1,0:T(8,128)(2,1)} %copy-done.3, bf16[256,512]{1,0:T(8,128)(2,1)} %copy-done.27, bf16[256,512]{1,0:T(8,128)(2,1)} %copy-done.28, ...), custom_call_target="tpu_custom_call" | custom-call | flops 2000000000 | bytes 1048576 | tf_op jit(solution)/shard_map/pallas_call | solution.py:81
  103.0 1.1 collective-permute-start.20
  104.0 2.2 %collective-permute-start.21 = (bf16[512,256]{1,0:T(8,128)(2,1)S(1)}, bf16[512,256]{1,0:T(8,128)(2,1)S(1)}, u32[]{:S(2)}, u32[]{:S(2)}) collective-permute-start(bf16[512,256]{1,0:T(8,128)(2,1)S(1)} %get-tuple-element.80), channel_id=1, source_target_pairs={{0,6},{1,7},{2,0},{3,1},{4,2},{5,3},{6,4},{7,5},{8,14},{9,15},{10,... | collective-permute-start | bytes 786440 | tf_op jit(solution)/shard_map/ppermute | solution.py:671
  106.2 2.3 %collective-permute-done.22.refs_3_ = bf16[512,256]{1,0:T(8,128)(2,1)S(1)} collective-permute-done((bf16[512,256]{1,0:T(8,128)(2,1)S(1)}, bf16[512,256]{1,0:T(8,128)(2,1)S(1)}, u32[]{:S(2)}, u32[]{:S(2)}) %collective-permute-start.22) | collective-permute-done | bytes 262176 | tf_op jit(solution)/shard_map/ppermute | solution.py:675
  108.5 3.0 %collective-permute-start.24 = (bf16[512,256]{1,0:T(8,128)(2,1)S(1)}, bf16[512,256]{1,0:T(8,128)(2,1)S(1)}, u32[]{:S(2)}, u32[]{:S(2)}) collective-permute-start(bf16[512,256]{1,0:T(8,128)(2,1)S(1)} %get-tuple-element.83), channel_id=1, source_target_pairs={{0,7},{1,6},{2,1},{3,0},{4,3},{5,2},{6,5},{7,4},{8,15},{9,14},{10,... | collective-permute-start | bytes 786440 | tf_op jit(solution)/shard_map/ppermute | solution.py:679
  111.5 1.9 %collective-permute-done.20.refs_1_ = bf16[512,256]{1,0:T(8,128)(2,1)S(1)} collective-permute-done((bf16[512,256]{1,0:T(8,128)(2,1)S(1)}, bf16[512,256]{1,0:T(8,128)(2,1)S(1)}, u32[]{:S(2)}, u32[]{:S(2)}) %collective-permute-start.20) | collective-permute-done | bytes 262176 | tf_op jit(solution)/shard_map/ppermute | solution.py:671
  113.3 4.4 %collective-permute-done.23.refs_4_ = bf16[512,256]{1,0:T(8,128)(2,1)S(1)} collective-permute-done((bf16[512,256]{1,0:T(8,128)(2,1)S(1)}, bf16[512,256]{1,0:T(8,128)(2,1)S(1)}, u32[]{:S(2)}, u32[]{:S(2)}) %collective-permute-start.23) | collective-permute-done | bytes 262176 | tf_op jit(solution)/shard_map/ppermute | solution.py:679
  117.8 1.0 shard_map.182
  118.8 9.8 %all-to-all-start.2 = ((bf16[32,32,256]{2,1,0:T(8,128)(2,1)}), bf16[32,32,256]{2,1,0:T(8,128)(2,1)}, u32[]{:S(2)}, u32[]{:S(2)}) async-start(bf16[32,32,256]{2,1,0:T(8,128)(2,1)} %shard_map.182), calls=%async_computation.2 | async-start | bytes 1048576 | tf_op jit(solution)/shard_map/all_to_all | solution.py:697
  130.5 0.9 copy-done.21
  131.4 2.2 %shard_map.183 = (bf16[512,256]{1,0:T(8,128)(2,1)}, bf16[512,256]{1,0:T(8,128)(2,1)}, f32[512,256]{1,0:T(8,128)}, f32[512,256]{1,0:T(8,128)}, f32[8,256]{1,0:T(8,128)S(1)}) custom-call(s32[1]{0:T(128)} %bitcast.t_ref, bf16[64,2048]{1,0:T(8,128)(2,1)} %bitcast.54, bf16[64,256]{1,0:T(8,128)(2,1)S(1)} %bitcast.41, bf16[5,64,256]{2,1,0:T(8,128)(2,1)S(1)} %copy-done.14, ...), custom_call_target="tpu_custom_call" | custom-call | flops 100000000 | bytes 1048576 | tf_op jit(solution)/shard_map/pallas_call | solution.py:81
  133.6 8.9 %shard_map.181 = (f32[4,512,256]{2,1,0:T(8,128)}, f32[4,512,256]{2,1,0:T(8,128)}, f32[256,2048]{1,0:T(8,128)}) custom-call(s32[1]{0:T(128)} %bitcast.t_ref, bf16[512,512]{1,0:T(8,128)(2,1)} %bitcast.38, bf16[512,512]{1,0:T(8,128)(2,1)} %copy-done.2, bf16[512,512]{1,0:T(8,128)(2,1)} %copy-done.3, bf16[256,512]{1,0:T(8,128)(2,1)} %copy-done.27, ...), custom_call_target="tpu_custom_call" | custom-call | flops 2000000000 | bytes 1048576 | tf_op jit(solution)/shard_map/pallas_call | solution.py:81
  143.1 3.3 %shard_map.184 = (bf16[256,256]{1,0:T(8,128)(2,1)}, bf16[32,32,128]{2,1,0:T(8,128)(2,1)}, f32[4,72,256]{2,1,0:T(8,128)S(1)}, bf16[4,72,256]{2,1,0:T(8,128)(2,1)S(1)}) custom-call(s32[1]{0:T(128)} %bitcast.t_ref, bf16[256,1024]{1,0:T(8,128)(2,1)} %get-tuple-element.77.refs_0_, bf16[256,2048]{1,0:T(8,128)(2,1)} %refs_1_.3, bf16[1024,256]{1,0:T(8,128)(2,1)} %bitcast.22.refs_2_, ...), custom_call_target="tpu_custom_call" | custom-call | flops 1000000000 | bytes 1048576 | tf_op jit(solution)/shard_map/pallas_call | solution.py:81
  146.4 9.2 %all-to-all-start.3 = ((bf16[32,32,128]{2,1,0:T(8,128)(2,1)}), bf16[32,32,128]{2,1,0:T(8,128)(2,1)S(1)}, u32[]{:S(2)}, u32[]{:S(2)}) async-start(bf16[32,32,128]{2,1,0:T(8,128)(2,1)} %get-tuple-element.100), calls=%async_computation.3 | async-start | bytes 524288 | tf_op jit(solution)/shard_map/all_to_all | solution.py:697
  155.7 1.4 collective-permute-done.25.refs_1_
  157.9 4.1 %collective-permute-start.27 = (bf16[72,256]{1,0:T(8,128)(2,1)S(1)}, bf16[72,256]{1,0:T(8,128)(2,1)S(1)}, u32[]{:S(2)}, u32[]{:S(2)}) collective-permute-start(bf16[72,256]{1,0:T(8,128)(2,1)S(1)} %get-tuple-element.93), channel_id=1, source_target_pairs={{0,4},{1,5},{2,6},{3,7},{4,0},{5,1},{6,2},{7,3},{8,12},{9,13},{10,... | collective-permute-start | bytes 110600 | tf_op jit(solution)/shard_map/ppermute | solution.py:675
  162.0 2.3 %collective-permute-done.27.refs_2_ = bf16[72,256]{1,0:T(8,128)(2,1)S(1)} collective-permute-done((bf16[72,256]{1,0:T(8,128)(2,1)S(1)}, bf16[72,256]{1,0:T(8,128)(2,1)S(1)}, u32[]{:S(2)}, u32[]{:S(2)}) %collective-permute-start.27) | collective-permute-done | bytes 36896 | tf_op jit(solution)/shard_map/ppermute | solution.py:675
  164.4 2.8 %collective-permute-done.28.refs_3_ = bf16[72,256]{1,0:T(8,128)(2,1)S(1)} collective-permute-done((bf16[72,256]{1,0:T(8,128)(2,1)S(1)}, bf16[72,256]{1,0:T(8,128)(2,1)S(1)}, u32[]{:S(2)}, u32[]{:S(2)}) %collective-permute-start.28) | collective-permute-done | bytes 36896 | tf_op jit(solution)/shard_map/ppermute | solution.py:675
  167.3 4.6 %collective-permute-start.29 = (f32[64,128]{1,0:T(8,128)S(1)}, f32[64,128]{1,0:T(8,128)S(1)}, u32[]{:S(2)}, u32[]{:S(2)}) collective-permute-start(f32[64,128]{1,0:T(8,128)S(1)} %get-tuple-element.97), channel_id=1, source_target_pairs={{8,0},{16,8},{24,16},{32,24},{40,32},{48,40},{56,48},{64,56},{72,6... | collective-permute-start | bytes 98312 | tf_op jit(solution)/shard_map/ppermute | solution.py:756
  172.1 1.9 %collective-permute-start.30 = (f32[64,64]{1,0:T(8,128)S(1)}, f32[64,64]{1,0:T(8,128)S(1)}, u32[]{:S(2)}, u32[]{:S(2)}) collective-permute-start(f32[64,64]{1,0:T(8,128)S(1)} %shard_map.189), channel_id=1, source_target_pairs={{0,0},{1,32},{2,64},{3,96},{4,128},{5,160},{6,192},{7,224},{32,1},... | collective-permute-start | bytes 49160 | tf_op jit(solution)/shard_map/ppermute | solution.py:760
  174.0 1.0 shard_map.187.refs_0_
  175.0 1.4 shard_map.188
  176.4 7.8 %collective-permute-done.30 = f32[64,64]{1,0:T(8,128)S(1)} collective-permute-done((f32[64,64]{1,0:T(8,128)S(1)}, f32[64,64]{1,0:T(8,128)S(1)}, u32[]{:S(2)}, u32[]{:S(2)}) %collective-permute-start.30) | collective-permute-done | bytes 16416 | tf_op jit(solution)/shard_map/ppermute | solution.py:760
  (106 shorter events, 10.5 us)
Async XLA Ops:
  1.3 20.8 %copy-start.25 = (f32[256,2]{0,1:T(2,128)S(1)}, f32[256,2]{0,1:T(2,128)}, u32[]{:S(2)}) copy-start(f32[256,2]{0,1:T(2,128)} %param.15) | copy-start | bytes 6148
  3.4 27.1 %all-to-all-start = ((bf16[32,16,512]{2,1,0:T(8,128)(2,1)}), bf16[32,16,512]{2,1,0:T(8,128)(2,1)S(1)}, u32[]{:S(2)}, u32[]{:S(2)}) async-start(bf16[32,16,512]{2,1,0:T(8,128)(2,1)} %bitcast.63), calls=%async_computation | async-start | bytes 1048576 | tf_op jit(solution)/shard_map/all_to_all | solution.py:697
  14.3 1.5 collective-permute-start.4
  17.4 7.3 %collective-permute-start.5 = (bf16[4,64,256]{2,1,0:T(8,128)(2,1)S(1)}, bf16[4,64,256]{2,1,0:T(8,128)(2,1)S(1)}, u32[]{:S(2)}, u32[]{:S(2)}) collective-permute-start(bf16[4,64,256]{2,1,0:T(8,128)(2,1)S(1)} %get-tuple-element.59), channel_id=1, source_target_pairs={{0,2},{1,3},{2,0},{3,1},{4,6},{5,7},{6,4},{7,5},{8,10},{9,11},{10,... | collective-permute-start | bytes 393224 | tf_op jit(solution)/shard_map/ppermute | solution.py:675
  19.0 9.3 %collective-permute-start.6 = (bf16[4,64,256]{2,1,0:T(8,128)(2,1)S(1)}, bf16[4,64,256]{2,1,0:T(8,128)(2,1)S(1)}, u32[]{:S(2)}, u32[]{:S(2)}) collective-permute-start(bf16[4,64,256]{2,1,0:T(8,128)(2,1)S(1)} %get-tuple-element.60), channel_id=1, source_target_pairs={{0,4},{1,5},{2,6},{3,7},{4,0},{5,1},{6,2},{7,3},{8,12},{9,13},{10,... | collective-permute-start | bytes 393224 | tf_op jit(solution)/shard_map/ppermute | solution.py:675
  21.9 8.7 %collective-permute-start.7 = (bf16[4,64,256]{2,1,0:T(8,128)(2,1)S(1)}, bf16[4,64,256]{2,1,0:T(8,128)(2,1)S(1)}, u32[]{:S(2)}, u32[]{:S(2)}) collective-permute-start(bf16[4,64,256]{2,1,0:T(8,128)(2,1)S(1)} %get-tuple-element.61), channel_id=1, source_target_pairs={{0,6},{1,7},{2,4},{3,5},{4,2},{5,3},{6,0},{7,1},{8,14},{9,15},{10,... | collective-permute-start | bytes 393224 | tf_op jit(solution)/shard_map/ppermute | solution.py:675
  22.1 18.2 %copy-start.26 = (bf16[1,256,2048]{2,1,0:T(8,128)(2,1)S(1)}, bf16[1,256,2048]{2,1,0:T(8,128)(2,1)}, u32[]{:S(2)}) copy-start(bf16[1,256,2048]{2,1,0:T(8,128)(2,1)} %param.23) | copy-start | bytes 3145732
  24.7 16.3 %copy-start.16 = (bf16[4,64,256]{2,1,0:T(8,128)(2,1)}, bf16[4,64,256]{2,1,0:T(8,128)(2,1)S(1)}, u32[]{:S(2)}) copy-start(bf16[4,64,256]{2,1,0:T(8,128)(2,1)S(1)} %collective-permute-done.5.refs_3_) | copy-start | bytes 393220
  28.3 12.7 %copy-start.18 = (bf16[4,64,256]{2,1,0:T(8,128)(2,1)}, bf16[4,64,256]{2,1,0:T(8,128)(2,1)S(1)}, u32[]{:S(2)}) copy-start(bf16[4,64,256]{2,1,0:T(8,128)(2,1)S(1)} %collective-permute-done.6.refs_4_) | copy-start | bytes 393220
  30.6 47.7 %copy-start.1 = (bf16[32,16,512]{2,1,0:T(8,128)(2,1)}, bf16[32,16,512]{2,1,0:T(8,128)(2,1)S(1)}, u32[]{:S(2)}) copy-start(bf16[32,16,512]{2,1,0:T(8,128)(2,1)S(1)} %all-to-all-done) | copy-start | bytes 1572868
  30.6 23.3 %all-to-all-start.1 = ((bf16[32,16,512]{2,1,0:T(8,128)(2,1)}), bf16[32,16,512]{2,1,0:T(8,128)(2,1)S(1)}, u32[]{:S(2)}, u32[]{:S(2)}) async-start(bf16[32,16,512]{2,1,0:T(8,128)(2,1)} %bitcast.64), calls=%async_computation.1 | async-start | bytes 1048576 | tf_op jit(solution)/shard_map/all_to_all | solution.py:697
  40.4 13.6 %collective-permute-start.14 = (bf16[256,2048]{1,0:T(8,128)(2,1)S(1)}, bf16[256,2048]{1,0:T(8,128)(2,1)}, u32[]{:S(2)}, u32[]{:S(2)}) collective-permute-start(bf16[256,2048]{1,0:T(8,128)(2,1)S(1)} %bitcast.51), channel_id=1, source_target_pairs={{0,1},{1,0},{2,3},{3,2},{4,5},{5,4},{6,7},{7,6},{8,9},{9,8},{10,11... | collective-permute-start | bytes 3145736 | tf_op jit(solution)/shard_map/ppermute | solution.py:675
  40.5 14.2 %collective-permute-start.15 = (bf16[2048,256]{1,0:T(8,128)(2,1)}, bf16[2048,256]{1,0:T(8,128)(2,1)}, u32[]{:S(2)}, u32[]{:S(2)}) collective-permute-start(bf16[2048,256]{1,0:T(8,128)(2,1)} %bitcast.55), channel_id=1, source_target_pairs={{0,1},{1,0},{2,3},{3,2},{4,5},{5,4},{6,7},{7,6},{8,9},{9,8},{10,11... | collective-permute-start | bytes 3145736 | tf_op jit(solution)/shard_map/ppermute | solution.py:675
  41.0 36.4 %collective-permute-start.16 = (bf16[2048,256]{1,0:T(8,128)(2,1)}, bf16[2048,256]{1,0:T(8,128)(2,1)}, u32[]{:S(2)}, u32[]{:S(2)}) collective-permute-start(bf16[2048,256]{1,0:T(8,128)(2,1)} %bitcast.59), channel_id=1, source_target_pairs={{0,1},{1,0},{2,3},{3,2},{4,5},{5,4},{6,7},{7,6},{8,9},{9,8},{10,11... | collective-permute-start | bytes 3145736 | tf_op jit(solution)/shard_map/ppermute | solution.py:675
  41.1 15.5 %collective-permute-start = (bf16[512,512]{1,0:T(8,128)(2,1)S(1)}, bf16[512,512]{1,0:T(8,128)(2,1)S(1)}, u32[]{:S(2)}, u32[]{:S(2)}) collective-permute-start(bf16[512,512]{1,0:T(8,128)(2,1)S(1)} %bitcast.34), channel_id=1, source_target_pairs={{0,2},{1,3},{2,4},{3,5},{4,6},{5,7},{6,0},{7,1},{8,10},{9,11},{10,... | collective-permute-start | bytes 1572872 | tf_op jit(solution)/shard_map/ppermute | solution.py:671
  41.2 15.5 %collective-permute-start.1 = (bf16[512,512]{1,0:T(8,128)(2,1)S(1)}, bf16[512,512]{1,0:T(8,128)(2,1)S(1)}, u32[]{:S(2)}, u32[]{:S(2)}) collective-permute-start(bf16[512,512]{1,0:T(8,128)(2,1)S(1)} %bitcast.35), channel_id=1, source_target_pairs={{0,6},{1,7},{2,0},{3,1},{4,2},{5,3},{6,4},{7,5},{8,14},{9,15},{10,... | collective-permute-start | bytes 1572872 | tf_op jit(solution)/shard_map/ppermute | solution.py:671
  53.9 23.4 %copy-start = (bf16[32,16,512]{2,1,0:T(8,128)(2,1)}, bf16[32,16,512]{2,1,0:T(8,128)(2,1)S(1)}, u32[]{:S(2)}) copy-start(bf16[32,16,512]{2,1,0:T(8,128)(2,1)S(1)} %all-to-all-done.1) | copy-start | bytes 1572868
  54.0 9.3 %collective-permute-start.10 = (bf16[256,512]{1,0:T(8,128)(2,1)S(1)}, bf16[256,512]{1,0:T(8,128)(2,1)S(1)}, u32[]{:S(2)}, u32[]{:S(2)}) collective-permute-start(bf16[256,512]{1,0:T(8,128)(2,1)S(1)} %bitcast.67), channel_id=1, source_target_pairs={{0,6},{1,7},{2,0},{3,1},{4,2},{5,3},{6,4},{7,5},{8,14},{9,15},{10,... | collective-permute-start | bytes 786440 | tf_op jit(solution)/shard_map/ppermute | solution.py:671
  54.6 12.5 %collective-permute-start.11 = (bf16[256,512]{1,0:T(8,128)(2,1)S(1)}, bf16[256,512]{1,0:T(8,128)(2,1)S(1)}, u32[]{:S(2)}, u32[]{:S(2)}) collective-permute-start(bf16[256,512]{1,0:T(8,128)(2,1)S(1)} %bitcast.65), channel_id=1, source_target_pairs={{0,6},{1,7},{2,0},{3,1},{4,2},{5,3},{6,4},{7,5},{8,14},{9,15},{10,... | collective-permute-start | bytes 786440 | tf_op jit(solution)/shard_map/ppermute | solution.py:671
  56.6 21.6 %copy-start.2 = (bf16[512,512]{1,0:T(8,128)(2,1)}, bf16[512,512]{1,0:T(8,128)(2,1)S(1)}, u32[]{:S(2)}) copy-start(bf16[512,512]{1,0:T(8,128)(2,1)S(1)} %collective-permute-done.refs_1_) | copy-start | bytes 1572868
  56.6 14.2 %collective-permute-start.8 = (bf16[256,512]{1,0:T(8,128)(2,1)S(1)}, bf16[256,512]{1,0:T(8,128)(2,1)S(1)}, u32[]{:S(2)}, u32[]{:S(2)}) collective-permute-start(bf16[256,512]{1,0:T(8,128)(2,1)S(1)} %bitcast.68), channel_id=1, source_target_pairs={{0,2},{1,3},{2,4},{3,5},{4,6},{5,7},{6,0},{7,1},{8,10},{9,11},{10,... | collective-permute-start | bytes 786440 | tf_op jit(solution)/shard_map/ppermute | solution.py:671
  56.7 21.5 %copy-start.3 = (bf16[512,512]{1,0:T(8,128)(2,1)}, bf16[512,512]{1,0:T(8,128)(2,1)S(1)}, u32[]{:S(2)}) copy-start(bf16[512,512]{1,0:T(8,128)(2,1)S(1)} %collective-permute-done.1.refs_2_) | copy-start | bytes 1572868
  56.7 15.9 %collective-permute-start.9 = (bf16[256,512]{1,0:T(8,128)(2,1)S(1)}, bf16[256,512]{1,0:T(8,128)(2,1)S(1)}, u32[]{:S(2)}, u32[]{:S(2)}) collective-permute-start(bf16[256,512]{1,0:T(8,128)(2,1)S(1)} %bitcast.66), channel_id=1, source_target_pairs={{0,2},{1,3},{2,4},{3,5},{4,6},{5,7},{6,0},{7,1},{8,10},{9,11},{10,... | collective-permute-start | bytes 786440 | tf_op jit(solution)/shard_map/ppermute | solution.py:671
  63.2 14.1 %copy-start.4 = (bf16[256,512]{1,0:T(8,128)(2,1)}, bf16[256,512]{1,0:T(8,128)(2,1)S(1)}, u32[]{:S(2)}) copy-start(bf16[256,512]{1,0:T(8,128)(2,1)S(1)} %collective-permute-done.10.refs_3_.refs_8_) | copy-start | bytes 786436
  63.2 15.0 %collective-permute-start.2 = (bf16[256,512]{1,0:T(8,128)(2,1)S(1)}, bf16[256,512]{1,0:T(8,128)(2,1)S(1)}, u32[]{:S(2)}, u32[]{:S(2)}) collective-permute-start(bf16[256,512]{1,0:T(8,128)(2,1)S(1)} %slice.24), channel_id=1, source_target_pairs={{0,2},{1,3},{2,4},{3,5},{4,6},{5,7},{6,0},{7,1},{8,10},{9,11},{10,... | collective-permute-start | bytes 786440 | tf_op jit(solution)/shard_map/ppermute | solution.py:671
  67.1 11.1 %collective-permute-start.3 = (bf16[256,512]{1,0:T(8,128)(2,1)S(1)}, bf16[256,512]{1,0:T(8,128)(2,1)S(1)}, u32[]{:S(2)}, u32[]{:S(2)}) collective-permute-start(bf16[256,512]{1,0:T(8,128)(2,1)S(1)} %slice.25), channel_id=1, source_target_pairs={{0,6},{1,7},{2,0},{3,1},{4,2},{5,3},{6,4},{7,5},{8,14},{9,15},{10,... | collective-permute-start | bytes 786440 | tf_op jit(solution)/shard_map/ppermute | solution.py:671
  70.8 15.4 %collective-permute-start.12 = (bf16[256,512]{1,0:T(8,128)(2,1)S(1)}, bf16[256,512]{1,0:T(8,128)(2,1)S(1)}, u32[]{:S(2)}, u32[]{:S(2)}) collective-permute-start(bf16[256,512]{1,0:T(8,128)(2,1)S(1)} %collective-permute-done.8.refs_1_.refs_6_), channel_id=1, source_target_pairs={{0,2},{1,3},{2,4},{3,5},{4,6},{5,7},{6,0},{7,1},{8,10},{9,11},{10,... | collective-permute-start | bytes 786440 | tf_op jit(solution)/shard_map/ppermute | solution.py:671
  72.6 13.6 %collective-permute-start.13 = (bf16[256,512]{1,0:T(8,128)(2,1)S(1)}, bf16[256,512]{1,0:T(8,128)(2,1)S(1)}, u32[]{:S(2)}, u32[]{:S(2)}) collective-permute-start(bf16[256,512]{1,0:T(8,128)(2,1)S(1)} %collective-permute-done.11.refs_4_.refs_9_), channel_id=1, source_target_pairs={{0,6},{1,7},{2,0},{3,1},{4,2},{5,3},{6,4},{7,5},{8,14},{9,15},{10,... | collective-permute-start | bytes 786440 | tf_op jit(solution)/shard_map/ppermute | solution.py:671
  89.3 7.7 %collective-permute-start.17 = (bf16[2,256,256]{2,1,0:T(8,128)(2,1)S(1)}, bf16[2,256,256]{2,1,0:T(8,128)(2,1)S(1)}, u32[]{:S(2)}, u32[]{:S(2)}) collective-permute-start(bf16[2,256,256]{2,1,0:T(8,128)(2,1)S(1)} %get-tuple-element.68), channel_id=1, source_target_pairs={{0,2},{1,3},{2,4},{3,5},{4,6},{5,7},{6,0},{7,1},{8,10},{9,11},{10,... | collective-permute-start | bytes 786440 | tf_op jit(solution)/shard_map/ppermute | solution.py:671
  89.4 7.6 %collective-permute-start.18 = (bf16[2,256,256]{2,1,0:T(8,128)(2,1)S(1)}, bf16[2,256,256]{2,1,0:T(8,128)(2,1)S(1)}, u32[]{:S(2)}, u32[]{:S(2)}) collective-permute-start(bf16[2,256,256]{2,1,0:T(8,128)(2,1)S(1)} %get-tuple-element.69), channel_id=1, source_target_pairs={{0,6},{1,7},{2,0},{3,1},{4,2},{5,3},{6,4},{7,5},{8,14},{9,15},{10,... | collective-permute-start | bytes 786440 | tf_op jit(solution)/shard_map/ppermute | solution.py:671
  102.3 26.3 %copy-start.14 = (bf16[5,64,256]{2,1,0:T(8,128)(2,1)S(1)}, bf16[5,64,256]{2,1,0:T(8,128)(2,1)}, u32[]{:S(2)}) copy-start(bf16[5,64,256]{2,1,0:T(8,128)(2,1)} %copy-done.13) | copy-start | bytes 491524
  102.4 31.2 %collective-permute-start.19 = (bf16[12,512,256]{2,1,0:T(8,128)(2,1)S(1)}, bf16[12,512,256]{2,1,0:T(8,128)(2,1)}, u32[]{:S(2)}, u32[]{:S(2)}) collective-permute-start(bf16[12,512,256]{2,1,0:T(8,128)(2,1)S(1)} %shard_map.180), channel_id=1, source_target_pairs={{0,1},{1,0},{2,3},{3,2},{4,5},{5,4},{6,7},{7,6},{8,9},{9,8},{10,11... | collective-permute-start | bytes 9437192 | tf_op jit(solution)/shard_map/ppermute | solution.py:675
  102.5 6.0 %collective-permute-start.22 = (bf16[512,256]{1,0:T(8,128)(2,1)S(1)}, bf16[512,256]{1,0:T(8,128)(2,1)S(1)}, u32[]{:S(2)}, u32[]{:S(2)}) collective-permute-start(bf16[512,256]{1,0:T(8,128)(2,1)S(1)} %get-tuple-element.81), channel_id=1, source_target_pairs={{0,1},{1,0},{2,3},{3,2},{4,5},{5,4},{6,7},{7,6},{8,9},{9,8},{10,11... | collective-permute-start | bytes 786440 | tf_op jit(solution)/shard_map/ppermute | solution.py:675
  103.0 10.4 %collective-permute-start.20 = (bf16[512,256]{1,0:T(8,128)(2,1)S(1)}, bf16[512,256]{1,0:T(8,128)(2,1)S(1)}, u32[]{:S(2)}, u32[]{:S(2)}) collective-permute-start(bf16[512,256]{1,0:T(8,128)(2,1)S(1)} %get-tuple-element.74), channel_id=1, source_target_pairs={{0,2},{1,3},{2,4},{3,5},{4,6},{5,7},{6,0},{7,1},{8,10},{9,11},{10,... | collective-permute-start | bytes 786440 | tf_op jit(solution)/shard_map/ppermute | solution.py:671
  104.0 9.3 %collective-permute-start.21 = (bf16[512,256]{1,0:T(8,128)(2,1)S(1)}, bf16[512,256]{1,0:T(8,128)(2,1)S(1)}, u32[]{:S(2)}, u32[]{:S(2)}) collective-permute-start(bf16[512,256]{1,0:T(8,128)(2,1)S(1)} %get-tuple-element.80), channel_id=1, source_target_pairs={{0,6},{1,7},{2,0},{3,1},{4,2},{5,3},{6,4},{7,5},{8,14},{9,15},{10,... | collective-permute-start | bytes 786440 | tf_op jit(solution)/shard_map/ppermute | solution.py:671
  106.2 11.6 %collective-permute-start.23 = (bf16[512,256]{1,0:T(8,128)(2,1)S(1)}, bf16[512,256]{1,0:T(8,128)(2,1)S(1)}, u32[]{:S(2)}, u32[]{:S(2)}) collective-permute-start(bf16[512,256]{1,0:T(8,128)(2,1)S(1)} %get-tuple-element.82), channel_id=1, source_target_pairs={{0,3},{1,2},{2,5},{3,4},{4,7},{5,6},{6,1},{7,0},{8,11},{9,10},{10,... | collective-permute-start | bytes 786440 | tf_op jit(solution)/shard_map/ppermute | solution.py:679
  108.5 9.4 %collective-permute-start.24 = (bf16[512,256]{1,0:T(8,128)(2,1)S(1)}, bf16[512,256]{1,0:T(8,128)(2,1)S(1)}, u32[]{:S(2)}, u32[]{:S(2)}) collective-permute-start(bf16[512,256]{1,0:T(8,128)(2,1)S(1)} %get-tuple-element.83), channel_id=1, source_target_pairs={{0,7},{1,6},{2,1},{3,0},{4,3},{5,2},{6,5},{7,4},{8,15},{9,14},{10,... | collective-permute-start | bytes 786440 | tf_op jit(solution)/shard_map/ppermute | solution.py:679
  118.8 24.3 %all-to-all-start.2 = ((bf16[32,32,256]{2,1,0:T(8,128)(2,1)}), bf16[32,32,256]{2,1,0:T(8,128)(2,1)}, u32[]{:S(2)}, u32[]{:S(2)}) async-start(bf16[32,32,256]{2,1,0:T(8,128)(2,1)} %shard_map.182), calls=%async_computation.2 | async-start | bytes 1048576 | tf_op jit(solution)/shard_map/all_to_all | solution.py:697
  143.1 28.8 %copy-start.29 = (f32[31,64]{1,0:T(8,128)S(1)}, f32[31,64]{1,0:T(8,128)}, u32[]{:S(2)}) copy-start(f32[31,64]{1,0:T(8,128)} %param.18) | copy-start | bytes 23812
  143.1 31.9 %copy-start.22 = (bf16[256,64]{0,1:T(8,128)(2,1)S(1)}, bf16[256,64]{0,1:T(8,128)(2,1)}, u32[]{:S(2)}) copy-start(bf16[256,64]{0,1:T(8,128)(2,1)} %param.16) | copy-start | bytes 98308
  143.1 31.9 %copy-start.23 = (bf16[256,64]{0,1:T(8,128)(2,1)S(1)}, bf16[256,64]{0,1:T(8,128)(2,1)}, u32[]{:S(2)}) copy-start(bf16[256,64]{0,1:T(8,128)(2,1)} %param.17) | copy-start | bytes 98308
  146.4 25.6 %all-to-all-start.3 = ((bf16[32,32,128]{2,1,0:T(8,128)(2,1)}), bf16[32,32,128]{2,1,0:T(8,128)(2,1)S(1)}, u32[]{:S(2)}, u32[]{:S(2)}) async-start(bf16[32,32,128]{2,1,0:T(8,128)(2,1)} %get-tuple-element.100), calls=%async_computation.3 | async-start | bytes 524288 | tf_op jit(solution)/shard_map/all_to_all | solution.py:697
  155.6 1.5 collective-permute-start.25
  157.1 4.9 %collective-permute-start.26 = (bf16[72,256]{1,0:T(8,128)(2,1)S(1)}, bf16[72,256]{1,0:T(8,128)(2,1)S(1)}, u32[]{:S(2)}, u32[]{:S(2)}) collective-permute-start(bf16[72,256]{1,0:T(8,128)(2,1)S(1)} %get-tuple-element.92), channel_id=1, source_target_pairs={{0,2},{1,3},{2,0},{3,1},{4,6},{5,7},{6,4},{7,5},{8,10},{9,11},{10,... | collective-permute-start | bytes 110600 | tf_op jit(solution)/shard_map/ppermute | solution.py:675
  157.9 6.5 %collective-permute-start.27 = (bf16[72,256]{1,0:T(8,128)(2,1)S(1)}, bf16[72,256]{1,0:T(8,128)(2,1)S(1)}, u32[]{:S(2)}, u32[]{:S(2)}) collective-permute-start(bf16[72,256]{1,0:T(8,128)(2,1)S(1)} %get-tuple-element.93), channel_id=1, source_target_pairs={{0,4},{1,5},{2,6},{3,7},{4,0},{5,1},{6,2},{7,3},{8,12},{9,13},{10,... | collective-permute-start | bytes 110600 | tf_op jit(solution)/shard_map/ppermute | solution.py:675
  162.0 5.2 %collective-permute-start.28 = (bf16[72,256]{1,0:T(8,128)(2,1)S(1)}, bf16[72,256]{1,0:T(8,128)(2,1)S(1)}, u32[]{:S(2)}, u32[]{:S(2)}) collective-permute-start(bf16[72,256]{1,0:T(8,128)(2,1)S(1)} %get-tuple-element.94), channel_id=1, source_target_pairs={{0,6},{1,7},{2,4},{3,5},{4,2},{5,3},{6,0},{7,1},{8,14},{9,15},{10,... | collective-permute-start | bytes 110600 | tf_op jit(solution)/shard_map/ppermute | solution.py:675
  167.3 7.7 %collective-permute-start.29 = (f32[64,128]{1,0:T(8,128)S(1)}, f32[64,128]{1,0:T(8,128)S(1)}, u32[]{:S(2)}, u32[]{:S(2)}) collective-permute-start(f32[64,128]{1,0:T(8,128)S(1)} %get-tuple-element.97), channel_id=1, source_target_pairs={{8,0},{16,8},{24,16},{32,24},{40,32},{48,40},{56,48},{64,56},{72,6... | collective-permute-start | bytes 98312 | tf_op jit(solution)/shard_map/ppermute | solution.py:756
  172.1 12.1 %collective-permute-start.30 = (f32[64,64]{1,0:T(8,128)S(1)}, f32[64,64]{1,0:T(8,128)S(1)}, u32[]{:S(2)}, u32[]{:S(2)}) collective-permute-start(f32[64,64]{1,0:T(8,128)S(1)} %shard_map.189), channel_id=1, source_target_pairs={{0,0},{1,32},{2,64},{3,96},{4,128},{5,160},{6,192},{7,224},{32,1},... | collective-permute-start | bytes 49160 | tf_op jit(solution)/shard_map/ppermute | solution.py:760
  (17 other events, 73.4 us)

commit v3 on v2

--- a/solution.py
+++ b/solution.py
@@ -15,6 +15,9 @@
 TP = 8
 TOK = 256
 ROWS = SP * HALF
+EARLY = 128
+LATE = 512 - EARLY
+FIRST = 512 + EARLY
 BF = jnp.bfloat16
 F32 = jnp.float32
 MIB = 1 << 20
@@ -33,14 +36,15 @@
 
 
 class Later:
-    def __init__(self, source, buffer, sem):
-        self.copy, self.buffer, self.waiting = pltpu.make_async_copy(source, buffer, sem), buffer, True
-        self.copy.start()
+    def __init__(self, copies, buffer):
+        self.copies, self.buffer = copies, buffer
+        for copy in copies:
+            copy.start()
 
     def now(self):
-        if self.waiting:
-            self.copy.wait()
-            self.waiting = False
+        for copy in self.copies:
+            copy.wait()
+        self.copies = []
         return self.buffer
 
 
@@ -51,6 +55,7 @@
 def call(body, outs, tp, args, staged=(), cuts=None, into=None, scratch=(), flops=0, limit=40):
     cuts, into = cuts or {}, into or {}
     own = tuple(i for i in staged if i not in into)
+    n_copies = sum(len(into[i]) if i in into else 1 for i in staged)
     single = not isinstance(outs, tuple)
     outs = (outs,) if single else outs
     n_in, n_out, n_scr = len(args), len(outs), len(scratch)
@@ -58,13 +63,18 @@
     def kernel(t_ref, *refs):
         ins, rest = list(refs[:n_in]), refs[n_in:]
         made, scr, buffers = rest[:n_out], rest[n_out : n_out + n_scr], rest[n_out + n_scr :]
-        for n, i in enumerate(staged):
-            source = ins[i].at[cuts[i][1](t_ref[0])] if i in cuts else ins[i]
+        t, sems = t_ref[0], iter(range(n_copies))
+        for i in staged:
             if i in into:
-                target = scr[into[i][0]].at[into[i][1](t_ref[0])]
+                pairs = [(ins[i].at[cut], scr[k].at[to(t)]) for cut, k, to in into[i]]
             else:
-                target = buffers[own.index(i)]
-            ins[i] = Later(source, target, buffers[-1].at[n])
+                source = ins[i].at[cuts[i][1](t)] if i in cuts else ins[i]
+                pairs = [(source, buffers[own.index(i)])]
+            copies = [
+                pltpu.make_async_copy(source, target, buffers[-1].at[next(sems)])
+                for source, target in pairs
+            ]
+            ins[i] = Later(copies, pairs[0][1])
         body(t_ref[0], ins, made, scr)
         for i in staged:
             now(ins[i])
@@ -73,7 +83,7 @@
         pltpu.VMEM(cuts[i][0] if i in cuts else args[i].shape, args[i].dtype) for i in own
     ]
     if staged:
-        extra.append(pltpu.SemaphoreType.DMA((len(staged),)))
+        extra.append(pltpu.SemaphoreType.DMA((n_copies,)))
     args = tuple(
         pltpu.with_memory_space_constraint(x, pltpu.HBM) if i in staged else x
         for i, x in enumerate(args)
@@ -120,18 +130,26 @@
     b1 = r1 * CAP + (slot1 + HALF * core) % CAP
     outs[1][...] = jnp.concatenate([l0, l1, b0, b1, l0, l1, b0, b1], axis=0)
     place = iota((ROWS, TOK), 0)
-    pick = flag((place == l0) | (place == l1)).astype(BF)
-    outs[0][...] = dot(pick, now(ins[1])[...]).astype(BF)
-
-
-def pick_rows(tp, routes, stream):
+    at0, at1 = place == l0, place == l1
+    pick = flag(at0 | at1).astype(BF)
+    w = ins[2][...]
+    scale = jnp.where(at0, w[0:1, :], 0.0) + jnp.where(at1, w[1:2, :], 0.0)
+    scale = jnp.sum(scale, axis=1, keepdims=True)
+    outs[0][:, 0:512] = dot(pick, now(ins[1])[...]).astype(BF)
+    outs[0][:, 512:FIRST] = (scale * dot(pick, now(ins[3])[...])).astype(BF)
+
+
+def pick_rows(tp, routes, stream, weights, upstream):
     return call(
         pick_rows_body,
-        (pltpu.HBM((ROWS, 512), BF), shape((8, TOK), jnp.int32)),
-        tp,
-        (routes, stream),
-        staged=(1,),
-        cuts={1: ((TOK, 512), columns_of(512, lambda t: t // 2))},
+        (pltpu.HBM((ROWS, FIRST), BF), shape((8, TOK), jnp.int32)),
+        tp,
+        (routes, stream, weights, upstream),
+        staged=(1, 3),
+        cuts={
+            1: ((TOK, 512), columns_of(512, lambda t: t // 2)),
+            3: ((TOK, EARLY), columns_of(EARLY, lambda t: t // 2 * (512 // EARLY))),
+        },
         flops=10**9,
     )
 
@@ -156,11 +174,16 @@
 def pick_cot(tp, target, weights, upstream):
     return call(
         pick_cot_body,
-        (pltpu.HBM((ROWS, 512), BF), pltpu.HBM((TOK, SP * CAP), BF)),
+        (pltpu.HBM((ROWS, LATE), BF), pltpu.HBM((TOK, SP * CAP), BF)),
         tp,
         (target, weights, upstream),
         staged=(2,),
-        cuts={2: ((TOK, 512), columns_of(512, lambda t: t // 2))},
+        cuts={
+            2: (
+                (TOK, LATE),
+                lambda t: (slice(None), pl.ds(pl.multiple_of(t // 2 * 512 + EARLY, 128), LATE)),
+            )
+        },
         flops=10**9,
     )
 
@@ -171,11 +194,8 @@
 
 
 def joined(refs):
-    refs = [now(r)[...] for r in refs]
-    own, sides, far = refs[0], refs[1:-2], jnp.concatenate(refs[-2:], axis=0)
-    if len(sides) == 4:
-        sides = [jnp.concatenate(sides[0:2], axis=0), jnp.concatenate(sides[2:4], axis=0)]
-    return own, *sides, far
+    own, left, right, top, bottom = [now(r)[:, 0:512] for r in refs]
+    return own, left, right, jnp.concatenate([top, bottom], axis=0)
 
 
 def forward_body(t, ins, outs, scr):
@@ -211,6 +231,10 @@
         tp,
         (*blocks, *weights),
         staged=(5, 3, 4, 7, 6, 8),
+        cuts={
+            3: ((256, 512), lambda t: (slice(None), pl.ds(0, 512))),
+            4: ((256, 512), lambda t: (slice(None), pl.ds(0, 512))),
+        },
         scratch=[pltpu.VMEM((ROWS, 512), F32)] * 2,
         flops=2 * 10**9,
     )
@@ -232,25 +256,36 @@
 
 def three_body(t, ins, outs, scr):
     q = quarters(t)
-    own = ins[0][...]
-    sides = [(q[1], ins[1], ins[2]), (q[2], ins[3], ins[4])]
+    early = [now(x) for x in ins[0:3]]
+    upper, lower = slice(0, 256), slice(256, 512)
+
+    def beside(block, rows, late):
+        return jnp.concatenate([early[block][rows, :], late[...]], axis=1)
+
+    own = beside(0, slice(None), ins[3])
+    parts = [
+        (q[1], upper, beside(1, upper, ins[4])),
+        (q[1], lower, beside(1, lower, ins[5])),
+        (q[2], upper, beside(2, upper, ins[6])),
+        (q[2], lower, beside(2, lower, ins[7])),
+    ]
     for j in range(2):
-        d = now(ins[5 + j])
+        d = now(ins[8 + j])
         cols = slice(256 * j, 256 * j + 256)
         outs[0][:, cols] = dot(own, down_columns(d, q[0]), 1, 1)
-        for at, upper, lower in sides:
-            part = down_columns(d, at)
-            outs[0][0:256, cols] += dot(upper[...], part, 1, 1)
-            outs[0][256:512, cols] += dot(lower[...], part, 1, 1)
-
-
-def three(tp, blocks, downs):
+        for at, rows, part in parts:
+            outs[0][rows, cols] += dot(part, down_columns(d, at), 1, 1)
+
+
+def three(tp, first, late, downs):
+    early = ((ROWS, EARLY), lambda t: (slice(None), pl.ds(512, EARLY)))
     return call(
         three_body,
         shape((ROWS, 512), F32),
         tp,
-        (*blocks, *downs),
-        staged=(5, 6),
+        (*first, *late, *downs),
+        staged=(0, 1, 2, 8, 9),
+        cuts={0: early, 1: early, 2: early},
         flops=10**9,
         limit=32,
     )
@@ -258,13 +293,15 @@
 
 def backward_body(t, ins, outs, scr):
     top_ref, bottom_ref, gg_ref, gu_ref = outs
-    top, bottom, ga, a1, a2 = ins[0:5]
+    ga, a1, a2 = ins[4:7]
+    top = jnp.concatenate([now(ins[0])[...], ins[2][...]], axis=1)
+    bottom = jnp.concatenate([now(ins[1])[...], ins[3][...]], axis=1)
     far = scr[0]
     for j in range(2):
-        d = now(ins[5 + j])[...]
+        d = now(ins[7 + j])[...]
         cols = slice(256 * j, 256 * j + 256)
-        far[0:256, cols] = dot(top[...], d, 1, 1)
-        far[256:512, cols] = dot(bottom[...], d, 1, 1)
+        far[0:256, cols] = dot(top, d, 1, 1)
+        far[256:512, cols] = dot(bottom, d, 1, 1)
 
     @pl.loop(0, ROWS // 32)
     def _(i):
@@ -274,7 +311,7 @@
         gu_ref[at, :] = (grad * a2[at, :]).astype(BF)
 
     g, u = gg_ref[...], gu_ref[...]
-    weights = [now(w) for w in ins[7:11]]
+    weights = [now(w) for w in ins[9:13]]
     for half in range(2):
         part = partial_of(g, u, weights, half).astype(BF)
         top_ref[half] = part[0:256]
@@ -284,6 +321,7 @@
 def backward(tp, far, ga, downs, a1, a2, weights):
     pieces = ((2, 256, 256), lambda t: (pl.ds(2 * ((t // 2 + 2) % 4), 2),))
     columns = ((256, 512), columns_of(512, lambda t: (t // 2 + 2) % 4))
+    early = ((256, EARLY), lambda t: (slice(None), pl.ds(512, EARLY)))
     return call(
         backward_body,
         (
@@ -294,8 +332,8 @@
         ),
         tp,
         (*far, ga, a1, a2, *downs, *weights),
-        staged=(5, 6, 7, 8, 9, 10),
-        cuts={5: columns, 6: columns} | {i: pieces for i in range(7, 11)},
+        staged=(0, 1, 7, 8, 9, 10, 11, 12),
+        cuts={0: early, 1: early, 7: columns, 8: columns} | {i: pieces for i in range(9, 13)},
         scratch=[pltpu.VMEM((ROWS, 512), F32)],
         flops=2 * 10**9,
         limit=32,
@@ -353,14 +391,23 @@
     return call(settle_body, pltpu.HBM((SP, CAP, 256), BF), tp, parts, flops=10**7, limit=16)
 
 
-def by_column(scr_index, first, halves):
-    whole, upper, lower = slice(None), slice(0, 256), slice(256, 512)
-    sides = ((3, upper), (3, lower), (1, upper), (1, lower)) if halves else ((3, whole), (1, whole))
-    places = ((0, whole), *sides, (2, upper), (2, lower))
-    return {
-        first + n: (scr_index, lambda t, by=by, rows=rows: ((t // 2 + by) % 4, rows))
-        for n, (by, rows) in enumerate(places)
-    }
+def by_column():
+    whole, upper, lower = slice(0, 512), slice(0, 256), slice(256, 512)
+    every = slice(None)
+
+    def place(by, rows, cols):
+        return lambda t: ((t // 2 + by) % 4, rows, cols)
+
+    into = {}
+    for n, (by, rows) in enumerate(((0, whole), (3, whole), (1, whole), (2, upper), (2, lower))):
+        into[n] = [
+            ((every, pl.ds(0, 512)), 0, place(by, rows, every)),
+            ((every, pl.ds(512, EARLY)), 1, place(by, rows, slice(0, EARLY))),
+        ]
+    places = ((0, whole), (3, upper), (3, lower), (1, upper), (1, lower), (2, upper), (2, lower))
+    for n, (by, rows) in enumerate(places):
+        into[5 + n] = [((every, every), 1, place(by, rows, slice(EARLY, 512)))]
+    return into
 
 
 def weights_call(body, outs, tp, args):
@@ -370,7 +417,7 @@
         tp,
         args,
         staged=tuple(range(len(args))),
-        into=by_column(0, 0, False) | by_column(1, 5, True),
+        into=by_column(),
         scratch=[pltpu.VMEM((4, ROWS, 512), BF)] * 2,
         flops=2 * 10**9,
     )
@@ -706,8 +753,9 @@
     out_proj, expert_gate, expert_up, expert_down,
 ):
     tp = lax.axis_index("tp").reshape(1)
-    rows_out, target = pick_rows(tp, routes.T, stream)
-    rows_in = exchange(rows_out.reshape(SP, HALF, 512)).reshape(ROWS, 512)
+    weights = route_weights.T
+    rows_out, target = pick_rows(tp, routes.T, stream, weights, upstream)
+    rows_in = exchange(rows_out.reshape(SP, HALF, FIRST)).reshape(ROWS, FIRST)
 
     saved, proj = conv_saved.T, out_proj.T
     near_early = swapped(hand_out(tp, proj, saved), 1)
@@ -716,10 +764,10 @@
     gate_own, up_own, down_own = expert_gate[0], expert_up[0], expert_down[0]
     gate_par, up_par, down_par = (swapped(w, 1) for w in (gate_own, up_own, down_own))
 
-    cot_out, back = pick_cot(tp, target, route_weights.T, upstream)
+    cot_out, back = pick_cot(tp, target, weights, upstream)
     cot_out = after(cot_out, *early)
-    cot_in = exchange(cot_out.reshape(SP, HALF, 512))
-    cot_in = cot_in.reshape(ROWS, 512)
+    cot_in = exchange(cot_out.reshape(SP, HALF, LATE))
+    cot_in = cot_in.reshape(ROWS, LATE)
     proj_all, mixed, slope, slope_n, stat = prepare(tp, proj, saved, early)
 
     xs = around(rows_in)
@@ -729,8 +777,8 @@
 
     cs = around_in_halves(cot_in)
     downs = (down_own, down_par)
-    ga = three(tp, cs[:5], downs)
-    far_top, far_bottom, gg, gu = backward(tp, cs[5:], ga, downs, a1, a2, by_piece)
+    ga = three(tp, xs[:3], cs[:5], downs)
+    far_top, far_bottom, gg, gu = backward(tp, (*xs[3:], *cs[5:]), ga, downs, a1, a2, by_piece)
     got_top, got_bottom = moved(far_top, 2), moved(far_bottom, -2)
     parts = near(tp, gg, gu, by_piece)
     rs, rc, ls, lc = merge(tp, got_top, got_bottom, parts[:4])

time: 186 us -> 198 us (1.065)
  waiting for transfers between devices: 54.2 us -> 63.2 us
  local copies, waits for them, and re-layouts: 5.68 us -> 10.7 us
  starting transfers between devices: 76.5 us -> 73.7 us
    ppermute x14, waiting for transfers between devices: 15.7 us -> 28.2 us  [moved(): return lax.ppermute(x, 'tp', [(i, (i + by) % TP) for i in range(TP)])]
    unnamed x62 -> x72, local copies, waits for them, and re-layouts: 5.61 us -> 10.6 us
  transfers between devices with their start and end apart: 35 -> 35, of which waited for: 19 -> 20; matrix products, arithmetic and copies ran while one was open for 0% -> 0% of each run, Pallas kernels for 18% -> 17%
where the time goes in v3:
time: 198 us; the launch traced here: 197 us
  starting transfers between devices  73.7 us (37%)
  waiting for transfers between devices  63.2 us (32%)
  Pallas kernels  48.4 us (24%)
  local copies, waits for them, and re-layouts  10.7 us (5%)
    pallas_call x19, Pallas kernels, call(): pl.pallas_call(kernel, out_shape=outs, in_specs=[SMEM] + [HBM if i in sta...  48.4 us
    all_to_all x4, starting transfers between devices, exchange(): return lax.all_to_all(x, 'sp', 0, 0, tiled=True)  38.1 us
    ppermute x14, waiting for transfers between devices, moved(): return lax.ppermute(x, 'tp', [(i, (i + by) % TP) for i in range(TP)])  28.2 us
    ppermute x14, starting transfers between devices, moved(): return lax.ppermute(x, 'tp', [(i, (i + by) % TP) for i in range(TP)])  16 us
    ppermute x13, waiting for transfers between devices, swapped(): return lax.ppermute(x, 'tp', [(i, i ^ by) for i in range(TP)])  14.6 us
    ppermute x13, starting transfers between devices, swapped(): return lax.ppermute(x, 'tp', [(i, i ^ by) for i in range(TP)])  10.8 us
    unnamed x72, local copies, waits for them, and re-layouts  10.6 us
    all_to_all x4, waiting for transfers between devices, exchange(): return lax.all_to_all(x, 'sp', 0, 0, tiled=True)  8.6 us
  transfers between devices with their start and end apart: 35, of which 20 were waited for; matrix products, arithmetic and copies ran while one was open for 0% of the time, Pallas kernels for 17%

profile of v3, /device:TPU:128, one launch (start us, length us, event | category | flops | bytes accessed | tf_op | source)
XLA Modules:
  0.0 197.2 jit_solution(16349981826825335996)
XLA Ops:
  2.0 2.7 %shard_map.171 = (bf16[512,640]{1,0:T(8,128)(2,1)}, s32[8,256]{1,0:T(8,128)S(1)}) custom-call(s32[1]{0:T(128)} %bitcast.t_ref, s32[2,256]{1,0:T(2,128)S(1)} %bitcast.48, bf16[256,2048]{1,0:T(8,128)(2,1)} %refs_1_.2, f32[2,256]{1,0:T(2,128)S(1)} %bitcast.49, bf16[256,2048]{1,0:T(8,128)(2,1)} %refs_1_.3), custom_call_target="tpu_custom_call" | custom-call | flops 1000000000 | bytes 1048576 | tf_op jit(solution)/shard_map/pallas_call | solution.py:91
  4.7 9.8 %all-to-all-start = ((bf16[32,16,640]{2,1,0:T(8,128)(2,1)}), bf16[32,16,640]{2,1,0:T(8,128)(2,1)S(1)}, u32[]{:S(2)}, u32[]{:S(2)}) async-start(bf16[32,16,640]{2,1,0:T(8,128)(2,1)} %bitcast.62), calls=%async_computation | async-start | bytes 1310720 | tf_op jit(solution)/shard_map/all_to_all | solution.py:744
  15.7 1.4 collective-permute-done.4.refs_2_
  18.7 1.6 collective-permute-start.5
  20.3 2.9 %collective-permute-start.6 = (bf16[4,64,256]{2,1,0:T(8,128)(2,1)S(1)}, bf16[4,64,256]{2,1,0:T(8,128)(2,1)S(1)}, u32[]{:S(2)}, u32[]{:S(2)}) collective-permute-start(bf16[4,64,256]{2,1,0:T(8,128)(2,1)S(1)} %get-tuple-element.60), channel_id=1, source_target_pairs={{0,4},{1,5},{2,6},{3,7},{4,0},{5,1},{6,2},{7,3},{8,12},{9,13},{10,... | collective-permute-start | bytes 393224 | tf_op jit(solution)/shard_map/ppermute | solution.py:722
  23.4 2.5 %shard_map.172 = (bf16[512,384]{1,0:T(8,128)(2,1)}, bf16[256,1024]{1,0:T(8,128)(2,1)}) custom-call(s32[1]{0:T(128)} %bitcast.t_ref, s32[8,256]{1,0:T(8,128)S(1)} %get-tuple-element.55.refs_0_, f32[2,256]{1,0:T(2,128)S(1)} %bitcast.50, bf16[256,2048]{1,0:T(8,128)(2,1)} %refs_1_.3), custom_call_target="tpu_custom_call" | custom-call | flops 1000000000 | bytes 1048576 | tf_op jit(solution)/shard_map/pallas_call | solution.py:91
  26.6 3.0 %collective-permute-done.6.refs_4_ = bf16[4,64,256]{2,1,0:T(8,128)(2,1)S(1)} collective-permute-done((bf16[4,64,256]{2,1,0:T(8,128)(2,1)S(1)}, bf16[4,64,256]{2,1,0:T(8,128)(2,1)S(1)}, u32[]{:S(2)}, u32[]{:S(2)}) %collective-permute-start.6) | collective-permute-done | bytes 131104 | tf_op jit(solution)/shard_map/ppermute | solution.py:722
  30.3 1.6 collective-permute-done.7.refs_5_
  32.5 9.8 %all-to-all-start.1 = ((bf16[32,16,384]{2,1,0:T(8,128)(2,1)}), bf16[32,16,384]{2,1,0:T(8,128)(2,1)S(1)}, u32[]{:S(2)}, u32[]{:S(2)}) async-start(bf16[32,16,384]{2,1,0:T(8,128)(2,1)} %bitcast.63), calls=%async_computation.1 | async-start | bytes 786432 | tf_op jit(solution)/shard_map/all_to_all | solution.py:744
  42.9 3.2 %collective-permute-start.1 = (bf16[512,640]{1,0:T(8,128)(2,1)S(1)}, bf16[512,640]{1,0:T(8,128)(2,1)S(1)}, u32[]{:S(2)}, u32[]{:S(2)}) collective-permute-start(bf16[512,640]{1,0:T(8,128)(2,1)S(1)} %bitcast.32), channel_id=1, source_target_pairs={{0,6},{1,7},{2,0},{3,1},{4,2},{5,3},{6,4},{7,5},{8,14},{9,15},{10,... | collective-permute-start | bytes 1966088 | tf_op jit(solution)/shard_map/ppermute | solution.py:718
  46.1 7.0 %all-to-all-done.1 = bf16[32,16,384]{2,1,0:T(8,128)(2,1)S(1)} async-done(((bf16[32,16,384]{2,1,0:T(8,128)(2,1)}), bf16[32,16,384]{2,1,0:T(8,128)(2,1)S(1)}, u32[]{:S(2)}, u32[]{:S(2)}) %all-to-all-start.1) | async-done | bytes 393248 | tf_op jit(solution)/shard_map/all_to_all | solution.py:744
  53.2 7.7 %collective-permute-done.refs_1_ = bf16[512,640]{1,0:T(8,128)(2,1)S(1)} collective-permute-done((bf16[512,640]{1,0:T(8,128)(2,1)S(1)}, bf16[512,640]{1,0:T(8,128)(2,1)S(1)}, u32[]{:S(2)}, u32[]{:S(2)}) %collective-permute-start) | collective-permute-done | bytes 655392 | tf_op jit(solution)/shard_map/ppermute | solution.py:718
  60.9 2.9 %collective-permute-start.11 = (bf16[256,384]{1,0:T(8,128)(2,1)S(1)}, bf16[256,384]{1,0:T(8,128)(2,1)S(1)}, u32[]{:S(2)}, u32[]{:S(2)}) collective-permute-start(bf16[256,384]{1,0:T(8,128)(2,1)S(1)} %bitcast.64), channel_id=1, source_target_pairs={{0,6},{1,7},{2,0},{3,1},{4,2},{5,3},{6,4},{7,5},{8,14},{9,15},{10,... | collective-permute-start | bytes 589832 | tf_op jit(solution)/shard_map/ppermute | solution.py:718
  64.0 3.2 %collective-permute-start.3 = (bf16[256,640]{1,0:T(8,128)(2,1)S(1)}, bf16[256,640]{1,0:T(8,128)(2,1)S(1)}, u32[]{:S(2)}, u32[]{:S(2)}) collective-permute-start(bf16[256,640]{1,0:T(8,128)(2,1)S(1)} %slice.25), channel_id=1, source_target_pairs={{0,6},{1,7},{2,0},{3,1},{4,2},{5,3},{6,4},{7,5},{8,14},{9,15},{10,... | collective-permute-start | bytes 983048 | tf_op jit(solution)/shard_map/ppermute | solution.py:718
  67.2 1.4 collective-permute-done.10.refs_6_.refs_8_
  68.6 4.2 %collective-permute-done.11.refs_7_.refs_9_ = bf16[256,384]{1,0:T(8,128)(2,1)S(1)} collective-permute-done((bf16[256,384]{1,0:T(8,128)(2,1)S(1)}, bf16[256,384]{1,0:T(8,128)(2,1)S(1)}, u32[]{:S(2)}, u32[]{:S(2)}) %collective-permute-start.11) | collective-permute-done | bytes 196640 | tf_op jit(solution)/shard_map/ppermute | solution.py:718
  72.9 7.1 %collective-permute-done.8.refs_4_.refs_6_ = bf16[256,384]{1,0:T(8,128)(2,1)S(1)} collective-permute-done((bf16[256,384]{1,0:T(8,128)(2,1)S(1)}, bf16[256,384]{1,0:T(8,128)(2,1)S(1)}, u32[]{:S(2)}, u32[]{:S(2)}) %collective-permute-start.8) | collective-permute-done | bytes 196640 | tf_op jit(solution)/shard_map/ppermute | solution.py:718
  80.0 4.0 %collective-permute-done.9.refs_5_.refs_7_ = bf16[256,384]{1,0:T(8,128)(2,1)S(1)} collective-permute-done((bf16[256,384]{1,0:T(8,128)(2,1)S(1)}, bf16[256,384]{1,0:T(8,128)(2,1)S(1)}, u32[]{:S(2)}, u32[]{:S(2)}) %collective-permute-start.9) | collective-permute-done | bytes 196640 | tf_op jit(solution)/shard_map/ppermute | solution.py:718
  84.1 3.5 %shard_map.175.refs_4_ = f32[512,512]{1,0:T(8,128)S(1)} custom-call(s32[1]{0:T(128)} %bitcast.t_ref, bf16[512,640]{1,0:T(8,128)(2,1)} %bitcast.33, bf16[512,640]{1,0:T(8,128)(2,1)} %copy-done.3, bf16[512,640]{1,0:T(8,128)(2,1)} %copy-done.5, bf16[512,384]{1,0:T(8,128)(2,1)S(1)} %bitcast.37, bf16[256,384]{1,0:T(8,128)(2,1)S(1)} %collective-permute-done.8.refs_4_.refs_6_, ...), custom_call_target="tpu_custom_call" | custom-call | flops 1000000000 | bytes 1048576 | tf_op jit(solution)/shard_map/pallas_call | solution.py:91
  88.5 1.1 copy-done.1
  89.6 1.1 copy-done.4
  90.7 1.1 copy-done.6
  91.8 7.2 %shard_map.176 = (bf16[512,512]{1,0:T(8,128)(2,1)S(1)}, f32[512,512]{1,0:T(8,128)S(1)}, f32[512,512]{1,0:T(8,128)S(1)}) custom-call(s32[1]{0:T(128)} %bitcast.t_ref, bf16[512,640]{1,0:T(8,128)(2,1)S(1)} %bitcast.36, bf16[512,640]{1,0:T(8,128)(2,1)S(1)} %copy-done.4, bf16[512,640]{1,0:T(8,128)(2,1)S(1)} %copy-done.6, bf16[256,640]{1,0:T(8,128)(2,1)} %copy-done.31, ...), custom_call_target="tpu_custom_call" | custom-call | flops 2000000000 | bytes 1048576 | tf_op jit(solution)/shard_map/pallas_call | solution.py:91
  99.0 3.2 %shard_map.177 = (bf16[2,256,256]{2,1,0:T(8,128)(2,1)S(1)}, bf16[2,256,256]{2,1,0:T(8,128)(2,1)S(1)}, bf16[512,512]{1,0:T(8,128)(2,1)S(1)}, bf16[512,512]{1,0:T(8,128)(2,1)S(1)}) custom-call(s32[1]{0:T(128)} %bitcast.t_ref, bf16[256,640]{1,0:T(8,128)(2,1)} %copy-done.31, bf16[256,640]{1,0:T(8,128)(2,1)} %copy-done.32, ...), custom_call_target="tpu_custom_call" | custom-call | flops 2000000000 | bytes 1048576 | tf_op jit(solution)/shard_map/pallas_call | solution.py:91
  102.2 2.0 %collective-permute-start.17 = (bf16[2,256,256]{2,1,0:T(8,128)(2,1)S(1)}, bf16[2,256,256]{2,1,0:T(8,128)(2,1)S(1)}, u32[]{:S(2)}, u32[]{:S(2)}) collective-permute-start(bf16[2,256,256]{2,1,0:T(8,128)(2,1)S(1)} %get-tuple-element.68), channel_id=1, source_target_pairs={{0,2},{1,3},{2,4},{3,5},{4,6},{5,7},{6,0},{7,1},{8,10},{9,11},{10,... | collective-permute-start | bytes 786440 | tf_op jit(solution)/shard_map/ppermute | solution.py:718
  104.2 1.3 collective-permute-start.18
  105.5 4.0 %shard_map.178 = (bf16[512,256]{1,0:T(8,128)(2,1)S(1)}, bf16[512,256]{1,0:T(8,128)(2,1)S(1)}, bf16[512,256]{1,0:T(8,128)(2,1)S(1)}, bf16[512,256]{1,0:T(8,128)(2...) custom-call(s32[1]{0:T(128)} %bitcast.t_ref, ...), custom_call_target="tpu_custom_call" | custom-call | flops 3000000000 | bytes 1048576 | tf_op jit(solution)/shard_map/pallas_call | solution.py:91
  110.7 5.3 %shard_map.180 = bf16[12,512,256]{2,1,0:T(8,128)(2,1)S(1)} custom-call(s32[1]{0:T(128)} %bitcast.t_ref, bf16[512,640]{1,0:T(8,128)(2,1)} %bitcast.34, bf16[512,640]{1,0:T(8,128)(2,1)} %copy-done.3, bf16[512,640]{1,0:T(8,128)(2,1)} %copy-done.5, bf16[256,640]{1,0:T(8,128)(2,1)} %copy-done.31, bf16[256,640]{1,0:T(8,128)(2,1)} %copy-done.32, ...), custom_call_target="tpu_custom_call" | custom-call | flops 2000000000 | bytes 1048576 | tf_op jit(solution)/shard_map/pallas_call | solution.py:91
  116.8 3.1 %collective-permute-start.21 = (bf16[512,256]{1,0:T(8,128)(2,1)S(1)}, bf16[512,256]{1,0:T(8,128)(2,1)S(1)}, u32[]{:S(2)}, u32[]{:S(2)}) collective-permute-start(bf16[512,256]{1,0:T(8,128)(2,1)S(1)} %get-tuple-element.80), channel_id=1, source_target_pairs={{0,6},{1,7},{2,0},{3,1},{4,2},{5,3},{6,4},{7,5},{8,14},{9,15},{10,... | collective-permute-start | bytes 786440 | tf_op jit(solution)/shard_map/ppermute | solution.py:718
  119.9 2.3 %collective-permute-done.22.refs_3_ = bf16[512,256]{1,0:T(8,128)(2,1)S(1)} collective-permute-done((bf16[512,256]{1,0:T(8,128)(2,1)S(1)}, bf16[512,256]{1,0:T(8,128)(2,1)S(1)}, u32[]{:S(2)}, u32[]{:S(2)}) %collective-permute-start.22) | collective-permute-done | bytes 262176 | tf_op jit(solution)/shard_map/ppermute | solution.py:722
  122.2 2.2 %collective-permute-start.24 = (bf16[512,256]{1,0:T(8,128)(2,1)S(1)}, bf16[512,256]{1,0:T(8,128)(2,1)S(1)}, u32[]{:S(2)}, u32[]{:S(2)}) collective-permute-start(bf16[512,256]{1,0:T(8,128)(2,1)S(1)} %get-tuple-element.83), channel_id=1, source_target_pairs={{0,7},{1,6},{2,1},{3,0},{4,3},{5,2},{6,5},{7,4},{8,15},{9,14},{10,... | collective-permute-start | bytes 786440 | tf_op jit(solution)/shard_map/ppermute | solution.py:726
  124.4 2.6 %collective-permute-done.20.refs_1_ = bf16[512,256]{1,0:T(8,128)(2,1)S(1)} collective-permute-done((bf16[512,256]{1,0:T(8,128)(2,1)S(1)}, bf16[512,256]{1,0:T(8,128)(2,1)S(1)}, u32[]{:S(2)}, u32[]{:S(2)}) %collective-permute-start.20) | collective-permute-done | bytes 262176 | tf_op jit(solution)/shard_map/ppermute | solution.py:718
  127.1 3.9 %collective-permute-done.23.refs_4_ = bf16[512,256]{1,0:T(8,128)(2,1)S(1)} collective-permute-done((bf16[512,256]{1,0:T(8,128)(2,1)S(1)}, bf16[512,256]{1,0:T(8,128)(2,1)S(1)}, u32[]{:S(2)}, u32[]{:S(2)}) %collective-permute-start.23) | collective-permute-done | bytes 262176 | tf_op jit(solution)/shard_map/ppermute | solution.py:726
  131.1 1.0 shard_map.182
  132.1 9.8 %all-to-all-start.2 = ((bf16[32,32,256]{2,1,0:T(8,128)(2,1)}), bf16[32,32,256]{2,1,0:T(8,128)(2,1)}, u32[]{:S(2)}, u32[]{:S(2)}) async-start(bf16[32,32,256]{2,1,0:T(8,128)(2,1)} %shard_map.182), calls=%async_computation.2 | async-start | bytes 1048576 | tf_op jit(solution)/shard_map/all_to_all | solution.py:744
  143.7 2.2 %shard_map.183 = (bf16[512,256]{1,0:T(8,128)(2,1)}, bf16[512,256]{1,0:T(8,128)(2,1)}, f32[512,256]{1,0:T(8,128)}, f32[512,256]{1,0:T(8,128)}, f32[8,256]{1,0:T(8,128)S(1)}) custom-call(s32[1]{0:T(128)} %bitcast.t_ref, bf16[64,2048]{1,0:T(8,128)(2,1)} %bitcast.53, bf16[64,256]{1,0:T(8,128)(2,1)S(1)} %bitcast.42, bf16[5,64,256]{2,1,0:T(8,128)(2,1)S(1)} %copy-done.17, ...), custom_call_target="tpu_custom_call" | custom-call | flops 100000000 | bytes 1048576 | tf_op jit(solution)/shard_map/pallas_call | solution.py:91
  145.9 8.9 %shard_map.181 = (f32[4,512,256]{2,1,0:T(8,128)}, f32[4,512,256]{2,1,0:T(8,128)}, f32[256,2048]{1,0:T(8,128)}) custom-call(s32[1]{0:T(128)} %bitcast.t_ref, bf16[512,640]{1,0:T(8,128)(2,1)} %bitcast.35, bf16[512,640]{1,0:T(8,128)(2,1)} %copy-done.3, bf16[512,640]{1,0:T(8,128)(2,1)} %copy-done.5, bf16[256,640]{1,0:T(8,128)(2,1)} %copy-done.31, ...), custom_call_target="tpu_custom_call" | custom-call | flops 2000000000 | bytes 1048576 | tf_op jit(solution)/shard_map/pallas_call | solution.py:91
  154.9 1.6 all-to-all-done.2
  156.5 3.3 %shard_map.184 = (bf16[256,256]{1,0:T(8,128)(2,1)}, bf16[32,32,128]{2,1,0:T(8,128)(2,1)}, f32[4,72,256]{2,1,0:T(8,128)S(1)}, bf16[4,72,256]{2,1,0:T(8,128)(2,1)S(1)}) custom-call(s32[1]{0:T(128)} %bitcast.t_ref, bf16[256,1024]{1,0:T(8,128)(2,1)} %get-tuple-element.77.refs_0_, bf16[256,2048]{1,0:T(8,128)(2,1)} %refs_1_.3, bf16[1024,256]{1,0:T(8,128)(2,1)} %bitcast.22.refs_2_, ...), custom_call_target="tpu_custom_call" | custom-call | flops 1000000000 | bytes 1048576 | tf_op jit(solution)/shard_map/pallas_call | solution.py:91
  159.8 8.6 %all-to-all-start.3 = ((bf16[32,32,128]{2,1,0:T(8,128)(2,1)}), bf16[32,32,128]{2,1,0:T(8,128)(2,1)S(1)}, u32[]{:S(2)}, u32[]{:S(2)}) async-start(bf16[32,32,128]{2,1,0:T(8,128)(2,1)} %get-tuple-element.100), calls=%async_computation.3 | async-start | bytes 524288 | tf_op jit(solution)/shard_map/all_to_all | solution.py:744
  168.5 1.4 collective-permute-done.25.refs_1_
  170.6 3.8 %collective-permute-start.27 = (bf16[72,256]{1,0:T(8,128)(2,1)S(1)}, bf16[72,256]{1,0:T(8,128)(2,1)S(1)}, u32[]{:S(2)}, u32[]{:S(2)}) collective-permute-start(bf16[72,256]{1,0:T(8,128)(2,1)S(1)} %get-tuple-element.93), channel_id=1, source_target_pairs={{0,4},{1,5},{2,6},{3,7},{4,0},{5,1},{6,2},{7,3},{8,12},{9,13},{10,... | collective-permute-start | bytes 110600 | tf_op jit(solution)/shard_map/ppermute | solution.py:722
  174.7 2.1 %collective-permute-done.27.refs_2_ = bf16[72,256]{1,0:T(8,128)(2,1)S(1)} collective-permute-done((bf16[72,256]{1,0:T(8,128)(2,1)S(1)}, bf16[72,256]{1,0:T(8,128)(2,1)S(1)}, u32[]{:S(2)}, u32[]{:S(2)}) %collective-permute-start.27) | collective-permute-done | bytes 36896 | tf_op jit(solution)/shard_map/ppermute | solution.py:722
  176.8 2.8 %collective-permute-done.28.refs_3_ = bf16[72,256]{1,0:T(8,128)(2,1)S(1)} collective-permute-done((bf16[72,256]{1,0:T(8,128)(2,1)S(1)}, bf16[72,256]{1,0:T(8,128)(2,1)S(1)}, u32[]{:S(2)}, u32[]{:S(2)}) %collective-permute-start.28) | collective-permute-done | bytes 36896 | tf_op jit(solution)/shard_map/ppermute | solution.py:722
  179.7 4.6 %collective-permute-start.29 = (f32[64,128]{1,0:T(8,128)S(1)}, f32[64,128]{1,0:T(8,128)S(1)}, u32[]{:S(2)}, u32[]{:S(2)}) collective-permute-start(f32[64,128]{1,0:T(8,128)S(1)} %get-tuple-element.97), channel_id=1, source_target_pairs={{8,0},{16,8},{24,16},{32,24},{40,32},{48,40},{56,48},{64,56},{72,6... | collective-permute-start | bytes 98312 | tf_op jit(solution)/shard_map/ppermute | solution.py:804
  184.5 1.9 collective-permute-start.30
  187.4 1.4 shard_map.188
  188.8 7.8 %collective-permute-done.30 = f32[64,64]{1,0:T(8,128)S(1)} collective-permute-done((f32[64,64]{1,0:T(8,128)S(1)}, f32[64,64]{1,0:T(8,128)S(1)}, u32[]{:S(2)}, u32[]{:S(2)}) %collective-permute-start.30) | collective-permute-done | bytes 16416 | tf_op jit(solution)/shard_map/ppermute | solution.py:808
  (116 shorter events, 14.7 us)
Async XLA Ops:
  2.0 21.4 %copy-start.30 = (f32[256,2]{0,1:T(2,128)S(1)}, f32[256,2]{0,1:T(2,128)}, u32[]{:S(2)}) copy-start(f32[256,2]{0,1:T(2,128)} %param.15) | copy-start | bytes 6148
  4.7 27.8 %all-to-all-start = ((bf16[32,16,640]{2,1,0:T(8,128)(2,1)}), bf16[32,16,640]{2,1,0:T(8,128)(2,1)S(1)}, u32[]{:S(2)}, u32[]{:S(2)}) async-start(bf16[32,16,640]{2,1,0:T(8,128)(2,1)} %bitcast.62), calls=%async_computation | async-start | bytes 1310720 | tf_op jit(solution)/shard_map/all_to_all | solution.py:744
  15.6 1.5 collective-permute-start.4
  18.7 7.2 %collective-permute-start.5 = (bf16[4,64,256]{2,1,0:T(8,128)(2,1)S(1)}, bf16[4,64,256]{2,1,0:T(8,128)(2,1)S(1)}, u32[]{:S(2)}, u32[]{:S(2)}) collective-permute-start(bf16[4,64,256]{2,1,0:T(8,128)(2,1)S(1)} %get-tuple-element.59), channel_id=1, source_target_pairs={{0,2},{1,3},{2,0},{3,1},{4,6},{5,7},{6,4},{7,5},{8,10},{9,11},{10,... | collective-permute-start | bytes 393224 | tf_op jit(solution)/shard_map/ppermute | solution.py:722
  20.3 9.3 %collective-permute-start.6 = (bf16[4,64,256]{2,1,0:T(8,128)(2,1)S(1)}, bf16[4,64,256]{2,1,0:T(8,128)(2,1)S(1)}, u32[]{:S(2)}, u32[]{:S(2)}) collective-permute-start(bf16[4,64,256]{2,1,0:T(8,128)(2,1)S(1)} %get-tuple-element.60), channel_id=1, source_target_pairs={{0,4},{1,5},{2,6},{3,7},{4,0},{5,1},{6,2},{7,3},{8,12},{9,13},{10,... | collective-permute-start | bytes 393224 | tf_op jit(solution)/shard_map/ppermute | solution.py:722
  23.2 8.7 %collective-permute-start.7 = (bf16[4,64,256]{2,1,0:T(8,128)(2,1)S(1)}, bf16[4,64,256]{2,1,0:T(8,128)(2,1)S(1)}, u32[]{:S(2)}, u32[]{:S(2)}) collective-permute-start(bf16[4,64,256]{2,1,0:T(8,128)(2,1)S(1)} %get-tuple-element.61), channel_id=1, source_target_pairs={{0,6},{1,7},{2,4},{3,5},{4,2},{5,3},{6,0},{7,1},{8,14},{9,15},{10,... | collective-permute-start | bytes 393224 | tf_op jit(solution)/shard_map/ppermute | solution.py:722
  23.4 19.0 %copy-start.33 = (bf16[1,2048,256]{2,1,0:T(8,128)(2,1)S(1)}, bf16[1,2048,256]{2,1,0:T(8,128)(2,1)}, u32[]{:S(2)}) copy-start(bf16[1,2048,256]{2,1,0:T(8,128)(2,1)} %param.21) | copy-start | bytes 3145732
  32.5 51.5 %copy-start = (bf16[32,16,640]{2,1,0:T(8,128)(2,1)}, bf16[32,16,640]{2,1,0:T(8,128)(2,1)S(1)}, u32[]{:S(2)}) copy-start(bf16[32,16,640]{2,1,0:T(8,128)(2,1)S(1)} %all-to-all-done) | copy-start | bytes 1966084
  32.5 20.6 %all-to-all-start.1 = ((bf16[32,16,384]{2,1,0:T(8,128)(2,1)}), bf16[32,16,384]{2,1,0:T(8,128)(2,1)S(1)}, u32[]{:S(2)}, u32[]{:S(2)}) async-start(bf16[32,16,384]{2,1,0:T(8,128)(2,1)} %bitcast.63), calls=%async_computation.1 | async-start | bytes 786432 | tf_op jit(solution)/shard_map/all_to_all | solution.py:744
  42.3 21.6 %collective-permute-start.14 = (bf16[256,2048]{1,0:T(8,128)(2,1)}, bf16[256,2048]{1,0:T(8,128)(2,1)}, u32[]{:S(2)}, u32[]{:S(2)}) collective-permute-start(bf16[256,2048]{1,0:T(8,128)(2,1)} %bitcast.11.refs_8_.refs_7_), channel_id=1, source_target_pairs={{0,1},{1,0},{2,3},{3,2},{4,5},{5,4},{6,7},{7,6},{8,9},{9,8},{10,11... | collective-permute-start | bytes 3145736 | tf_op jit(solution)/shard_map/ppermute | solution.py:722
  42.4 21.6 %collective-permute-start.15 = (bf16[2048,256]{1,0:T(8,128)(2,1)S(1)}, bf16[2048,256]{1,0:T(8,128)(2,1)}, u32[]{:S(2)}, u32[]{:S(2)}) collective-permute-start(bf16[2048,256]{1,0:T(8,128)(2,1)S(1)} %bitcast.57), channel_id=1, source_target_pairs={{0,1},{1,0},{2,3},{3,2},{4,5},{5,4},{6,7},{7,6},{8,9},{9,8},{10,11... | collective-permute-start | bytes 3145736 | tf_op jit(solution)/shard_map/ppermute | solution.py:722
  42.9 18.0 %collective-permute-start = (bf16[512,640]{1,0:T(8,128)(2,1)S(1)}, bf16[512,640]{1,0:T(8,128)(2,1)S(1)}, u32[]{:S(2)}, u32[]{:S(2)}) collective-permute-start(bf16[512,640]{1,0:T(8,128)(2,1)S(1)} %bitcast.31), channel_id=1, source_target_pairs={{0,2},{1,3},{2,4},{3,5},{4,6},{5,7},{6,0},{7,1},{8,10},{9,11},{10,... | collective-permute-start | bytes 1966088 | tf_op jit(solution)/shard_map/ppermute | solution.py:718
  42.9 18.0 %collective-permute-start.1 = (bf16[512,640]{1,0:T(8,128)(2,1)S(1)}, bf16[512,640]{1,0:T(8,128)(2,1)S(1)}, u32[]{:S(2)}, u32[]{:S(2)}) collective-permute-start(bf16[512,640]{1,0:T(8,128)(2,1)S(1)} %bitcast.32), channel_id=1, source_target_pairs={{0,6},{1,7},{2,0},{3,1},{4,2},{5,3},{6,4},{7,5},{8,14},{9,15},{10,... | collective-permute-start | bytes 1966088 | tf_op jit(solution)/shard_map/ppermute | solution.py:718
  46.1 41.5 %collective-permute-start.16 = (bf16[2048,256]{1,0:T(8,128)(2,1)}, bf16[2048,256]{1,0:T(8,128)(2,1)}, u32[]{:S(2)}, u32[]{:S(2)}) collective-permute-start(bf16[2048,256]{1,0:T(8,128)(2,1)} %bitcast.58), channel_id=1, source_target_pairs={{0,1},{1,0},{2,3},{3,2},{4,5},{5,4},{6,7},{7,6},{8,9},{9,8},{10,11... | collective-permute-start | bytes 3145736 | tf_op jit(solution)/shard_map/ppermute | solution.py:722
  53.1 34.5 %copy-start.2 = (bf16[32,16,384]{2,1,0:T(8,128)(2,1)}, bf16[32,16,384]{2,1,0:T(8,128)(2,1)S(1)}, u32[]{:S(2)}) copy-start(bf16[32,16,384]{2,1,0:T(8,128)(2,1)S(1)} %all-to-all-done.1) | copy-start | bytes 1179652
  60.9 23.2 %copy-start.3 = (bf16[512,640]{1,0:T(8,128)(2,1)}, bf16[512,640]{1,0:T(8,128)(2,1)S(1)}, u32[]{:S(2)}) copy-start(bf16[512,640]{1,0:T(8,128)(2,1)S(1)} %collective-permute-done.refs_1_) | copy-start | bytes 1966084
  60.9 7.8 %collective-permute-start.10 = (bf16[256,384]{1,0:T(8,128)(2,1)S(1)}, bf16[256,384]{1,0:T(8,128)(2,1)S(1)}, u32[]{:S(2)}, u32[]{:S(2)}) collective-permute-start(bf16[256,384]{1,0:T(8,128)(2,1)S(1)} %bitcast.66), channel_id=1, source_target_pairs={{0,6},{1,7},{2,0},{3,1},{4,2},{5,3},{6,4},{7,5},{8,14},{9,15},{10,... | collective-permute-start | bytes 589832 | tf_op jit(solution)/shard_map/ppermute | solution.py:718
  60.9 23.2 %copy-start.5 = (bf16[512,640]{1,0:T(8,128)(2,1)}, bf16[512,640]{1,0:T(8,128)(2,1)S(1)}, u32[]{:S(2)}) copy-start(bf16[512,640]{1,0:T(8,128)(2,1)S(1)} %collective-permute-done.1.refs_2_) | copy-start | bytes 1966084
  60.9 12.0 %collective-permute-start.11 = (bf16[256,384]{1,0:T(8,128)(2,1)S(1)}, bf16[256,384]{1,0:T(8,128)(2,1)S(1)}, u32[]{:S(2)}, u32[]{:S(2)}) collective-permute-start(bf16[256,384]{1,0:T(8,128)(2,1)S(1)} %bitcast.64), channel_id=1, source_target_pairs={{0,6},{1,7},{2,0},{3,1},{4,2},{5,3},{6,4},{7,5},{8,14},{9,15},{10,... | collective-permute-start | bytes 589832 | tf_op jit(solution)/shard_map/ppermute | solution.py:718
  63.9 23.8 %collective-permute-start.2 = (bf16[256,640]{1,0:T(8,128)(2,1)S(1)}, bf16[256,640]{1,0:T(8,128)(2,1)S(1)}, u32[]{:S(2)}, u32[]{:S(2)}) collective-permute-start(bf16[256,640]{1,0:T(8,128)(2,1)S(1)} %slice.24), channel_id=1, source_target_pairs={{0,2},{1,3},{2,4},{3,5},{4,6},{5,7},{6,0},{7,1},{8,10},{9,11},{10,... | collective-permute-start | bytes 983048 | tf_op jit(solution)/shard_map/ppermute | solution.py:718
  64.0 23.7 %collective-permute-start.3 = (bf16[256,640]{1,0:T(8,128)(2,1)S(1)}, bf16[256,640]{1,0:T(8,128)(2,1)S(1)}, u32[]{:S(2)}, u32[]{:S(2)}) collective-permute-start(bf16[256,640]{1,0:T(8,128)(2,1)S(1)} %slice.25), channel_id=1, source_target_pairs={{0,6},{1,7},{2,0},{3,1},{4,2},{5,3},{6,4},{7,5},{8,14},{9,15},{10,... | collective-permute-start | bytes 983048 | tf_op jit(solution)/shard_map/ppermute | solution.py:718
  68.6 19.0 %copy-start.10 = (bf16[256,384]{1,0:T(8,128)(2,1)}, bf16[256,384]{1,0:T(8,128)(2,1)S(1)}, u32[]{:S(2)}) copy-start(bf16[256,384]{1,0:T(8,128)(2,1)S(1)} %collective-permute-done.10.refs_6_.refs_8_) | copy-start | bytes 589828
  68.6 11.3 %collective-permute-start.8 = (bf16[256,384]{1,0:T(8,128)(2,1)S(1)}, bf16[256,384]{1,0:T(8,128)(2,1)S(1)}, u32[]{:S(2)}, u32[]{:S(2)}) collective-permute-start(bf16[256,384]{1,0:T(8,128)(2,1)S(1)} %bitcast.67), channel_id=1, source_target_pairs={{0,2},{1,3},{2,4},{3,5},{4,6},{5,7},{6,0},{7,1},{8,10},{9,11},{10,... | collective-permute-start | bytes 589832 | tf_op jit(solution)/shard_map/ppermute | solution.py:718
  72.9 11.2 %collective-permute-start.9 = (bf16[256,384]{1,0:T(8,128)(2,1)S(1)}, bf16[256,384]{1,0:T(8,128)(2,1)S(1)}, u32[]{:S(2)}, u32[]{:S(2)}) collective-permute-start(bf16[256,384]{1,0:T(8,128)(2,1)S(1)} %bitcast.65), channel_id=1, source_target_pairs={{0,2},{1,3},{2,4},{3,5},{4,6},{5,7},{6,0},{7,1},{8,10},{9,11},{10,... | collective-permute-start | bytes 589832 | tf_op jit(solution)/shard_map/ppermute | solution.py:718
  80.0 19.0 %collective-permute-start.12 = (bf16[256,384]{1,0:T(8,128)(2,1)S(1)}, bf16[256,384]{1,0:T(8,128)(2,1)S(1)}, u32[]{:S(2)}, u32[]{:S(2)}) collective-permute-start(bf16[256,384]{1,0:T(8,128)(2,1)S(1)} %collective-permute-done.8.refs_4_.refs_6_), channel_id=1, source_target_pairs={{0,2},{1,3},{2,4},{3,5},{4,6},{5,7},{6,0},{7,1},{8,10},{9,11},{10,... | collective-permute-start | bytes 589832 | tf_op jit(solution)/shard_map/ppermute | solution.py:718
  84.0 14.9 %collective-permute-start.13 = (bf16[256,384]{1,0:T(8,128)(2,1)S(1)}, bf16[256,384]{1,0:T(8,128)(2,1)S(1)}, u32[]{:S(2)}, u32[]{:S(2)}) collective-permute-start(bf16[256,384]{1,0:T(8,128)(2,1)S(1)} %collective-permute-done.11.refs_7_.refs_9_), channel_id=1, source_target_pairs={{0,6},{1,7},{2,0},{3,1},{4,2},{5,3},{6,4},{7,5},{8,14},{9,15},{10,... | collective-permute-start | bytes 589832 | tf_op jit(solution)/shard_map/ppermute | solution.py:718
  102.2 7.7 %collective-permute-start.17 = (bf16[2,256,256]{2,1,0:T(8,128)(2,1)S(1)}, bf16[2,256,256]{2,1,0:T(8,128)(2,1)S(1)}, u32[]{:S(2)}, u32[]{:S(2)}) collective-permute-start(bf16[2,256,256]{2,1,0:T(8,128)(2,1)S(1)} %get-tuple-element.68), channel_id=1, source_target_pairs={{0,2},{1,3},{2,4},{3,5},{4,6},{5,7},{6,0},{7,1},{8,10},{9,11},{10,... | collective-permute-start | bytes 786440 | tf_op jit(solution)/shard_map/ppermute | solution.py:718
  104.2 6.4 %collective-permute-start.18 = (bf16[2,256,256]{2,1,0:T(8,128)(2,1)S(1)}, bf16[2,256,256]{2,1,0:T(8,128)(2,1)S(1)}, u32[]{:S(2)}, u32[]{:S(2)}) collective-permute-start(bf16[2,256,256]{2,1,0:T(8,128)(2,1)S(1)} %get-tuple-element.69), channel_id=1, source_target_pairs={{0,6},{1,7},{2,0},{3,1},{4,2},{5,3},{6,4},{7,5},{8,14},{9,15},{10,... | collective-permute-start | bytes 786440 | tf_op jit(solution)/shard_map/ppermute | solution.py:718
  116.0 25.9 %copy-start.17 = (bf16[5,64,256]{2,1,0:T(8,128)(2,1)S(1)}, bf16[5,64,256]{2,1,0:T(8,128)(2,1)}, u32[]{:S(2)}) copy-start(bf16[5,64,256]{2,1,0:T(8,128)(2,1)} %copy-done.16) | copy-start | bytes 491524
  116.0 25.9 %copy-start.19 = (bf16[256,64]{0,1:T(8,128)(2,1)S(1)}, bf16[256,64]{0,1:T(8,128)(2,1)}, u32[]{:S(2)}) copy-start(bf16[256,64]{0,1:T(8,128)(2,1)} %param.19) | copy-start | bytes 98308
  116.0 25.9 %copy-start.21 = (bf16[4,64,256]{2,1,0:T(8,128)(2,1)S(1)}, bf16[4,64,256]{2,1,0:T(8,128)(2,1)}, u32[]{:S(2)}) copy-start(bf16[4,64,256]{2,1,0:T(8,128)(2,1)} %copy-done.20) | copy-start | bytes 393220
  116.1 29.9 %collective-permute-start.19 = (bf16[12,512,256]{2,1,0:T(8,128)(2,1)S(1)}, bf16[12,512,256]{2,1,0:T(8,128)(2,1)}, u32[]{:S(2)}, u32[]{:S(2)}) collective-permute-start(bf16[12,512,256]{2,1,0:T(8,128)(2,1)S(1)} %shard_map.180), channel_id=1, source_target_pairs={{0,1},{1,0},{2,3},{3,2},{4,5},{5,4},{6,7},{7,6},{8,9},{9,8},{10,11... | collective-permute-start | bytes 9437192 | tf_op jit(solution)/shard_map/ppermute | solution.py:722
  116.2 6.0 %collective-permute-start.22 = (bf16[512,256]{1,0:T(8,128)(2,1)S(1)}, bf16[512,256]{1,0:T(8,128)(2,1)S(1)}, u32[]{:S(2)}, u32[]{:S(2)}) collective-permute-start(bf16[512,256]{1,0:T(8,128)(2,1)S(1)} %get-tuple-element.81), channel_id=1, source_target_pairs={{0,1},{1,0},{2,3},{3,2},{4,5},{5,4},{6,7},{7,6},{8,9},{9,8},{10,11... | collective-permute-start | bytes 786440 | tf_op jit(solution)/shard_map/ppermute | solution.py:722
  116.7 10.4 %collective-permute-start.20 = (bf16[512,256]{1,0:T(8,128)(2,1)S(1)}, bf16[512,256]{1,0:T(8,128)(2,1)S(1)}, u32[]{:S(2)}, u32[]{:S(2)}) collective-permute-start(bf16[512,256]{1,0:T(8,128)(2,1)S(1)} %get-tuple-element.74), channel_id=1, source_target_pairs={{0,2},{1,3},{2,4},{3,5},{4,6},{5,7},{6,0},{7,1},{8,10},{9,11},{10,... | collective-permute-start | bytes 786440 | tf_op jit(solution)/shard_map/ppermute | solution.py:718
  116.8 10.3 %collective-permute-start.21 = (bf16[512,256]{1,0:T(8,128)(2,1)S(1)}, bf16[512,256]{1,0:T(8,128)(2,1)S(1)}, u32[]{:S(2)}, u32[]{:S(2)}) collective-permute-start(bf16[512,256]{1,0:T(8,128)(2,1)S(1)} %get-tuple-element.80), channel_id=1, source_target_pairs={{0,6},{1,7},{2,0},{3,1},{4,2},{5,3},{6,4},{7,5},{8,14},{9,15},{10,... | collective-permute-start | bytes 786440 | tf_op jit(solution)/shard_map/ppermute | solution.py:718
  119.9 11.0 %collective-permute-start.23 = (bf16[512,256]{1,0:T(8,128)(2,1)S(1)}, bf16[512,256]{1,0:T(8,128)(2,1)S(1)}, u32[]{:S(2)}, u32[]{:S(2)}) collective-permute-start(bf16[512,256]{1,0:T(8,128)(2,1)S(1)} %get-tuple-element.82), channel_id=1, source_target_pairs={{0,3},{1,2},{2,5},{3,4},{4,7},{5,6},{6,1},{7,0},{8,11},{9,10},{10,... | collective-permute-start | bytes 786440 | tf_op jit(solution)/shard_map/ppermute | solution.py:726
  122.2 8.9 %collective-permute-start.24 = (bf16[512,256]{1,0:T(8,128)(2,1)S(1)}, bf16[512,256]{1,0:T(8,128)(2,1)S(1)}, u32[]{:S(2)}, u32[]{:S(2)}) collective-permute-start(bf16[512,256]{1,0:T(8,128)(2,1)S(1)} %get-tuple-element.83), channel_id=1, source_target_pairs={{0,7},{1,6},{2,1},{3,0},{4,3},{5,2},{6,5},{7,4},{8,15},{9,14},{10,... | collective-permute-start | bytes 786440 | tf_op jit(solution)/shard_map/ppermute | solution.py:726
  132.1 24.4 %all-to-all-start.2 = ((bf16[32,32,256]{2,1,0:T(8,128)(2,1)}), bf16[32,32,256]{2,1,0:T(8,128)(2,1)}, u32[]{:S(2)}, u32[]{:S(2)}) async-start(bf16[32,32,256]{2,1,0:T(8,128)(2,1)} %shard_map.182), calls=%async_computation.2 | async-start | bytes 1048576 | tf_op jit(solution)/shard_map/all_to_all | solution.py:744
  156.5 27.8 %copy-start.34 = (f32[31,64]{1,0:T(8,128)S(1)}, f32[31,64]{1,0:T(8,128)}, u32[]{:S(2)}) copy-start(f32[31,64]{1,0:T(8,128)} %param.18) | copy-start | bytes 23812
  156.5 30.9 %copy-start.26 = (bf16[256,64]{0,1:T(8,128)(2,1)S(1)}, bf16[256,64]{0,1:T(8,128)(2,1)}, u32[]{:S(2)}) copy-start(bf16[256,64]{0,1:T(8,128)(2,1)} %param.16) | copy-start | bytes 98308
  156.5 30.9 %copy-start.27 = (bf16[256,64]{0,1:T(8,128)(2,1)S(1)}, bf16[256,64]{0,1:T(8,128)(2,1)}, u32[]{:S(2)}) copy-start(bf16[256,64]{0,1:T(8,128)(2,1)} %param.17) | copy-start | bytes 98308
  159.8 24.6 %all-to-all-start.3 = ((bf16[32,32,128]{2,1,0:T(8,128)(2,1)}), bf16[32,32,128]{2,1,0:T(8,128)(2,1)S(1)}, u32[]{:S(2)}, u32[]{:S(2)}) async-start(bf16[32,32,128]{2,1,0:T(8,128)(2,1)} %get-tuple-element.100), calls=%async_computation.3 | async-start | bytes 524288 | tf_op jit(solution)/shard_map/all_to_all | solution.py:744
  168.4 1.5 collective-permute-start.25
  169.9 4.8 %collective-permute-start.26 = (bf16[72,256]{1,0:T(8,128)(2,1)S(1)}, bf16[72,256]{1,0:T(8,128)(2,1)S(1)}, u32[]{:S(2)}, u32[]{:S(2)}) collective-permute-start(bf16[72,256]{1,0:T(8,128)(2,1)S(1)} %get-tuple-element.92), channel_id=1, source_target_pairs={{0,2},{1,3},{2,0},{3,1},{4,6},{5,7},{6,4},{7,5},{8,10},{9,11},{10,... | collective-permute-start | bytes 110600 | tf_op jit(solution)/shard_map/ppermute | solution.py:722
  170.6 6.2 %collective-permute-start.27 = (bf16[72,256]{1,0:T(8,128)(2,1)S(1)}, bf16[72,256]{1,0:T(8,128)(2,1)S(1)}, u32[]{:S(2)}, u32[]{:S(2)}) collective-permute-start(bf16[72,256]{1,0:T(8,128)(2,1)S(1)} %get-tuple-element.93), channel_id=1, source_target_pairs={{0,4},{1,5},{2,6},{3,7},{4,0},{5,1},{6,2},{7,3},{8,12},{9,13},{10,... | collective-permute-start | bytes 110600 | tf_op jit(solution)/shard_map/ppermute | solution.py:722
  174.5 5.2 %collective-permute-start.28 = (bf16[72,256]{1,0:T(8,128)(2,1)S(1)}, bf16[72,256]{1,0:T(8,128)(2,1)S(1)}, u32[]{:S(2)}, u32[]{:S(2)}) collective-permute-start(bf16[72,256]{1,0:T(8,128)(2,1)S(1)} %get-tuple-element.94), channel_id=1, source_target_pairs={{0,6},{1,7},{2,4},{3,5},{4,2},{5,3},{6,0},{7,1},{8,14},{9,15},{10,... | collective-permute-start | bytes 110600 | tf_op jit(solution)/shard_map/ppermute | solution.py:722
  179.7 7.7 %collective-permute-start.29 = (f32[64,128]{1,0:T(8,128)S(1)}, f32[64,128]{1,0:T(8,128)S(1)}, u32[]{:S(2)}, u32[]{:S(2)}) collective-permute-start(f32[64,128]{1,0:T(8,128)S(1)} %get-tuple-element.97), channel_id=1, source_target_pairs={{8,0},{16,8},{24,16},{32,24},{40,32},{48,40},{56,48},{64,56},{72,6... | collective-permute-start | bytes 98312 | tf_op jit(solution)/shard_map/ppermute | solution.py:804
  184.5 12.1 %collective-permute-start.30 = (f32[64,64]{1,0:T(8,128)S(1)}, f32[64,64]{1,0:T(8,128)S(1)}, u32[]{:S(2)}, u32[]{:S(2)}) collective-permute-start(f32[64,64]{1,0:T(8,128)S(1)} %shard_map.189), channel_id=1, source_target_pairs={{0,0},{1,32},{2,64},{3,96},{4,128},{5,160},{6,192},{7,224},{32,1},... | collective-permute-start | bytes 49160 | tf_op jit(solution)/shard_map/ppermute | solution.py:808
  (22 other events, 73.6 us)

commit v4 on v3

--- a/solution.py
+++ b/solution.py
@@ -193,22 +193,38 @@
     return y, (y + 3) % 4, (y + 1) % 4, (y + 2) % 4
 
 
-def joined(refs):
-    own, left, right, top, bottom = [now(r)[:, 0:512] for r in refs]
-    return own, left, right, jnp.concatenate([top, bottom], axis=0)
+def first_body(t, ins, outs, scr):
+    q = quarters(t)
+    x = [ref[:, 0:512] for ref in ins[0:3]]
+    for j in range(2):
+        cols = slice(256 * j, 256 * j + 256)
+        for out, at in ((outs[0], 3), (outs[1], 5)):
+            w = now(ins[at + j])
+            out[:, cols] = sum(dot(x[i], w[q[i]]) for i in range(3))
+
+
+def first(tp, near_blocks, weights):
+    return call(
+        first_body,
+        (shape((ROWS, 512), F32),) * 2,
+        tp,
+        (*near_blocks, *weights),
+        staged=(3, 5, 4, 6),
+        flops=10**9,
+        limit=32,
+    )
 
 
 def forward_body(t, ins, outs, scr):
     act_ref, a1_ref, a2_ref = outs
     pg, pu = scr
-    q = quarters(t)
-    x = joined(ins[0:5])
+    top, bottom = now(ins[2])[...], now(ins[3])[...]
     for j in range(2):
         cols = slice(256 * j, 256 * j + 256)
-        g = now(ins[5 + j])
-        pg[:, cols] = sum(dot(x[i], g[q[i]]) for i in range(4))
-        u = now(ins[7 + j])
-        pu[:, cols] = sum(dot(x[i], u[q[i]]) for i in range(4))
+        for near_sum, into, at in ((ins[0], pg, 4), (ins[1], pu, 6)):
+            w = now(ins[at + j])[0]
+            into[0:256, cols] = near_sum[0:256, cols] + dot(top, w)
+            into[256:512, cols] = near_sum[256:512, cols] + dot(bottom, w)
 
     @pl.loop(0, ROWS // 32)
     def _(i):
@@ -224,19 +240,19 @@
         a2_ref[at, :] = jnp.where(jnp.abs(up_pre) < CLAMP, gated, 0.0)
 
 
-def forward(tp, blocks, weights):
+def forward(tp, sums, far_blocks, weights):
+    rows = ((256, 512), lambda t: (slice(None), pl.ds(0, 512)))
+    quarter = ((1, 512, 256), lambda t: (pl.ds((t // 2 + 2) % 4, 1),))
     return call(
         forward_body,
         (shape((ROWS, 512), BF), shape((ROWS, 512), F32), shape((ROWS, 512), F32)),
         tp,
-        (*blocks, *weights),
-        staged=(5, 3, 4, 7, 6, 8),
-        cuts={
-            3: ((256, 512), lambda t: (slice(None), pl.ds(0, 512))),
-            4: ((256, 512), lambda t: (slice(None), pl.ds(0, 512))),
-        },
+        (*sums, *far_blocks, *weights),
+        staged=(2, 3, 4, 6, 5, 7),
+        cuts={2: rows, 3: rows} | {i: quarter for i in range(4, 8)},
         scratch=[pltpu.VMEM((ROWS, 512), F32)] * 2,
         flops=2 * 10**9,
+        limit=32,
     )
 
 
@@ -773,7 +789,8 @@
     xs = around(rows_in)
     by_quarter = [w.reshape(4, 512, 256) for w in (gate_own, gate_par, up_own, up_par)]
     by_piece = [w.reshape(8, 256, 256) for w in (gate_own, gate_par, up_own, up_par)]
-    act, a1, a2 = forward(tp, xs, by_quarter)
+    sums = first(tp, xs[:3], by_quarter)
+    act, a1, a2 = forward(tp, sums, xs[3:], by_quarter)
 
     cs = around_in_halves(cot_in)
     downs = (down_own, down_par)

time: 198 us -> 189 us (0.955)
  waiting for transfers between devices: 63.2 us -> 51.5 us
  starting transfers between devices: 73.7 us -> 77.5 us
  local copies, waits for them, and re-layouts: 10.7 us -> 8.25 us
    ppermute x14, waiting for transfers between devices: 28.2 us -> 16.1 us  [moved(): return lax.ppermute(x, 'tp', [(i, (i + by) % TP) for i in range(TP)])]
    ppermute x14, starting transfers between devices: 16 us -> 19 us  [moved(): return lax.ppermute(x, 'tp', [(i, (i + by) % TP) for i in range(TP)])]
    unnamed x72 -> x64, local copies, waits for them, and re-layouts: 10.6 us -> 8.15 us
    pallas_call x19 -> x20, Pallas kernels: 48.4 us -> 49.4 us  [call(): pl.pallas_call(kernel, out_shape=outs, in_specs=[SMEM] + [HBM if i in sta...]
  transfers between devices with their start and end apart: 35 -> 35, of which waited for: 20 -> 19; matrix products, arithmetic and copies ran while one was open for 0% -> 0% of each run, Pallas kernels for 17% -> 19%
where the time goes in v4:
time: 189 us; the launch traced here: 188 us
  starting transfers between devices  77.5 us (41%)
  waiting for transfers between devices  51.5 us (27%)
  Pallas kernels  49.4 us (26%)
  local copies, waits for them, and re-layouts  8.25 us (4%)
    pallas_call x20, Pallas kernels, call(): pl.pallas_call(kernel, out_shape=outs, in_specs=[SMEM] + [HBM if i in sta...  49.4 us
    all_to_all x4, starting transfers between devices, exchange(): return lax.all_to_all(x, 'sp', 0, 0, tiled=True)  38 us
    ppermute x14, starting transfers between devices, moved(): return lax.ppermute(x, 'tp', [(i, (i + by) % TP) for i in range(TP)])  19 us
    ppermute x14, waiting for transfers between devices, moved(): return lax.ppermute(x, 'tp', [(i, (i + by) % TP) for i in range(TP)])  16.1 us
    ppermute x13, waiting for transfers between devices, swapped(): return lax.ppermute(x, 'tp', [(i, i ^ by) for i in range(TP)])  14.9 us
    ppermute x13, starting transfers between devices, swapped(): return lax.ppermute(x, 'tp', [(i, i ^ by) for i in range(TP)])  11 us
    all_to_all x4, waiting for transfers between devices, exchange(): return lax.all_to_all(x, 'sp', 0, 0, tiled=True)  8.29 us
    unnamed x64, local copies, waits for them, and re-layouts  8.15 us
  transfers between devices with their start and end apart: 35, of which 19 were waited for; matrix products, arithmetic and copies ran while one was open for 0% of the time, Pallas kernels for 19%

profile of v4, /device:TPU:128, one launch (start us, length us, event | category | flops | bytes accessed | tf_op | source)
XLA Modules:
  0.0 187.9 jit_solution(15238775102924003566)
XLA Ops:
  2.0 2.7 %shard_map.171 = (bf16[512,640]{1,0:T(8,128)(2,1)}, s32[8,256]{1,0:T(8,128)S(1)}) custom-call(s32[1]{0:T(128)} %bitcast.t_ref, s32[2,256]{1,0:T(2,128)S(1)} %bitcast.48, bf16[256,2048]{1,0:T(8,128)(2,1)} %refs_1_.2, f32[2,256]{1,0:T(2,128)S(1)} %bitcast.49, bf16[256,2048]{1,0:T(8,128)(2,1)} %refs_1_.3), custom_call_target="tpu_custom_call" | custom-call | flops 1000000000 | bytes 1048576 | tf_op jit(solution)/shard_map/pallas_call | solution.py:91
  4.7 9.8 %all-to-all-start = ((bf16[32,16,640]{2,1,0:T(8,128)(2,1)}), bf16[32,16,640]{2,1,0:T(8,128)(2,1)S(1)}, u32[]{:S(2)}, u32[]{:S(2)}) async-start(bf16[32,16,640]{2,1,0:T(8,128)(2,1)} %bitcast.54), calls=%async_computation | async-start | bytes 1310720 | tf_op jit(solution)/shard_map/all_to_all | solution.py:760
  15.7 1.4 collective-permute-done.4.refs_2_
  17.1 1.0 shard_map.174
  18.7 1.6 collective-permute-start.5
  20.3 2.9 %collective-permute-start.6 = (bf16[4,64,256]{2,1,0:T(8,128)(2,1)S(1)}, bf16[4,64,256]{2,1,0:T(8,128)(2,1)S(1)}, u32[]{:S(2)}, u32[]{:S(2)}) collective-permute-start(bf16[4,64,256]{2,1,0:T(8,128)(2,1)S(1)} %get-tuple-element.62), channel_id=1, source_target_pairs={{0,4},{1,5},{2,6},{3,7},{4,0},{5,1},{6,2},{7,3},{8,12},{9,13},{10,... | collective-permute-start | bytes 393224 | tf_op jit(solution)/shard_map/ppermute | solution.py:738
  23.4 2.4 %shard_map.172 = (bf16[512,384]{1,0:T(8,128)(2,1)}, bf16[256,1024]{1,0:T(8,128)(2,1)}) custom-call(s32[1]{0:T(128)} %bitcast.t_ref, s32[8,256]{1,0:T(8,128)S(1)} %get-tuple-element.57.refs_0_, f32[2,256]{1,0:T(2,128)S(1)} %bitcast.50, bf16[256,2048]{1,0:T(8,128)(2,1)} %refs_1_.3), custom_call_target="tpu_custom_call" | custom-call | flops 1000000000 | bytes 1048576 | tf_op jit(solution)/shard_map/pallas_call | solution.py:91
  26.5 3.1 %collective-permute-done.6.refs_4_ = bf16[4,64,256]{2,1,0:T(8,128)(2,1)S(1)} collective-permute-done((bf16[4,64,256]{2,1,0:T(8,128)(2,1)S(1)}, bf16[4,64,256]{2,1,0:T(8,128)(2,1)S(1)}, u32[]{:S(2)}, u32[]{:S(2)}) %collective-permute-start.6) | collective-permute-done | bytes 131104 | tf_op jit(solution)/shard_map/ppermute | solution.py:738
  30.3 1.6 collective-permute-done.7.refs_5_
  32.5 9.8 %all-to-all-start.1 = ((bf16[32,16,384]{2,1,0:T(8,128)(2,1)}), bf16[32,16,384]{2,1,0:T(8,128)(2,1)S(1)}, u32[]{:S(2)}, u32[]{:S(2)}) async-start(bf16[32,16,384]{2,1,0:T(8,128)(2,1)} %bitcast.55), calls=%async_computation.1 | async-start | bytes 786432 | tf_op jit(solution)/shard_map/all_to_all | solution.py:760
  43.0 3.2 %collective-permute-start.1 = (bf16[512,640]{1,0:T(8,128)(2,1)S(1)}, bf16[512,640]{1,0:T(8,128)(2,1)S(1)}, u32[]{:S(2)}, u32[]{:S(2)}) collective-permute-start(bf16[512,640]{1,0:T(8,128)(2,1)S(1)} %bitcast.32), channel_id=1, source_target_pairs={{0,6},{1,7},{2,0},{3,1},{4,2},{5,3},{6,4},{7,5},{8,14},{9,15},{10,... | collective-permute-start | bytes 1966088 | tf_op jit(solution)/shard_map/ppermute | solution.py:734
  46.2 6.9 %all-to-all-done.1 = bf16[32,16,384]{2,1,0:T(8,128)(2,1)S(1)} async-done(((bf16[32,16,384]{2,1,0:T(8,128)(2,1)}), bf16[32,16,384]{2,1,0:T(8,128)(2,1)S(1)}, u32[]{:S(2)}, u32[]{:S(2)}) %all-to-all-start.1) | async-done | bytes 393248 | tf_op jit(solution)/shard_map/all_to_all | solution.py:760
  53.2 8.1 %collective-permute-done.refs_1_ = bf16[512,640]{1,0:T(8,128)(2,1)S(1)} collective-permute-done((bf16[512,640]{1,0:T(8,128)(2,1)S(1)}, bf16[512,640]{1,0:T(8,128)(2,1)S(1)}, u32[]{:S(2)}, u32[]{:S(2)}) %collective-permute-start) | collective-permute-done | bytes 655392 | tf_op jit(solution)/shard_map/ppermute | solution.py:734
  61.3 2.1 %collective-permute-start.2 = (bf16[256,640]{1,0:T(8,128)(2,1)S(1)}, bf16[256,640]{1,0:T(8,128)(2,1)S(1)}, u32[]{:S(2)}, u32[]{:S(2)}) collective-permute-start(bf16[256,640]{1,0:T(8,128)(2,1)S(1)} %slice.24), channel_id=1, source_target_pairs={{0,2},{1,3},{2,4},{3,5},{4,6},{5,7},{6,0},{7,1},{8,10},{9,11},{10,... | collective-permute-start | bytes 983048 | tf_op jit(solution)/shard_map/ppermute | solution.py:734
  63.5 1.3 collective-permute-start.3
  65.6 2.4 %collective-permute-start.11 = (bf16[256,384]{1,0:T(8,128)(2,1)S(1)}, bf16[256,384]{1,0:T(8,128)(2,1)S(1)}, u32[]{:S(2)}, u32[]{:S(2)}) collective-permute-start(bf16[256,384]{1,0:T(8,128)(2,1)S(1)} %bitcast.56), channel_id=1, source_target_pairs={{0,6},{1,7},{2,0},{3,1},{4,2},{5,3},{6,4},{7,5},{8,14},{9,15},{10,... | collective-permute-start | bytes 589832 | tf_op jit(solution)/shard_map/ppermute | solution.py:734
  68.0 1.0 collective-permute-done.10.refs_6_.refs_8_
  69.0 5.2 %shard_map.176 = (f32[512,512]{1,0:T(8,128)S(1)}, f32[512,512]{1,0:T(8,128)S(1)}) custom-call(s32[1]{0:T(128)} %bitcast.t_ref, bf16[512,640]{1,0:T(8,128)(2,1)S(1)} %bitcast.33, bf16[512,640]{1,0:T(8,128)(2,1)S(1)} %collective-permute-done.refs_1_, bf16[512,640]{1,0:T(8,128)(2,1)S(1)} %collective-permute-done.1.refs_2_, ...), custom_call_target="tpu_custom_call" | custom-call | flops 1000000000 | bytes 1048576 | tf_op jit(solution)/shard_map/pallas_call | solution.py:91
  74.3 3.2 %collective-permute-done.8.refs_4_.refs_6_ = bf16[256,384]{1,0:T(8,128)(2,1)S(1)} collective-permute-done((bf16[256,384]{1,0:T(8,128)(2,1)S(1)}, bf16[256,384]{1,0:T(8,128)(2,1)S(1)}, u32[]{:S(2)}, u32[]{:S(2)}) %collective-permute-start.8) | collective-permute-done | bytes 196640 | tf_op jit(solution)/shard_map/ppermute | solution.py:734
  78.9 1.8 collective-permute-start.13
  81.6 3.5 %shard_map.175.refs_4_ = f32[512,512]{1,0:T(8,128)S(1)} custom-call(s32[1]{0:T(128)} %bitcast.t_ref, bf16[512,640]{1,0:T(8,128)(2,1)} %bitcast.34, bf16[512,640]{1,0:T(8,128)(2,1)} %copy-done.1, bf16[512,640]{1,0:T(8,128)(2,1)} %copy-done.2, bf16[512,384]{1,0:T(8,128)(2,1)S(1)} %bitcast.37, bf16[256,384]{1,0:T(8,128)(2,1)S(1)} %collective-permute-done.8.refs_4_.refs_6_, ...), custom_call_target="tpu_custom_call" | custom-call | flops 1000000000 | bytes 1048576 | tf_op jit(solution)/shard_map/pallas_call | solution.py:91
  86.1 3.2 %shard_map.177 = (bf16[512,512]{1,0:T(8,128)(2,1)S(1)}, f32[512,512]{1,0:T(8,128)S(1)}, f32[512,512]{1,0:T(8,128)S(1)}) custom-call(s32[1]{0:T(128)} %bitcast.t_ref, f32[512,512]{1,0:T(8,128)S(1)} %get-tuple-element.65.refs_0_, f32[512,512]{1,0:T(8,128)S(1)} %get-tuple-element.66.refs_1_, bf16[256,640]{1,0:T(8,128)(2,1)} %copy-done.28, ...), custom_call_target="tpu_custom_call" | custom-call | flops 2000000000 | bytes 1048576 | tf_op jit(solution)/shard_map/pallas_call | solution.py:91
  90.1 3.0 %shard_map.178 = (bf16[2,256,256]{2,1,0:T(8,128)(2,1)S(1)}, bf16[2,256,256]{2,1,0:T(8,128)(2,1)S(1)}, bf16[512,512]{1,0:T(8,128)(2,1)S(1)}, bf16[512,512]{1,0:T(8,128)(2,1)S(1)}) custom-call(s32[1]{0:T(128)} %bitcast.t_ref, bf16[256,640]{1,0:T(8,128)(2,1)} %copy-done.28, bf16[256,640]{1,0:T(8,128)(2,1)} %copy-done.29, ...), custom_call_target="tpu_custom_call" | custom-call | flops 2000000000 | bytes 1048576 | tf_op jit(solution)/shard_map/pallas_call | solution.py:91
  94.0 2.4 %collective-permute-start.18 = (bf16[2,256,256]{2,1,0:T(8,128)(2,1)S(1)}, bf16[2,256,256]{2,1,0:T(8,128)(2,1)S(1)}, u32[]{:S(2)}, u32[]{:S(2)}) collective-permute-start(bf16[2,256,256]{2,1,0:T(8,128)(2,1)S(1)} %get-tuple-element.73), channel_id=1, source_target_pairs={{0,6},{1,7},{2,0},{3,1},{4,2},{5,3},{6,4},{7,5},{8,14},{9,15},{10,... | collective-permute-start | bytes 786440 | tf_op jit(solution)/shard_map/ppermute | solution.py:734
  96.4 4.0 %shard_map.179 = (bf16[512,256]{1,0:T(8,128)(2,1)S(1)}, bf16[512,256]{1,0:T(8,128)(2,1)S(1)}, bf16[512,256]{1,0:T(8,128)(2,1)S(1)}, bf16[512,256]{1,0:T(8,128)(2...) custom-call(s32[1]{0:T(128)} %bitcast.t_ref, ...), custom_call_target="tpu_custom_call" | custom-call | flops 3000000000 | bytes 1048576 | tf_op jit(solution)/shard_map/pallas_call | solution.py:91
  100.9 5.3 %shard_map.181 = bf16[12,512,256]{2,1,0:T(8,128)(2,1)S(1)} custom-call(s32[1]{0:T(128)} %bitcast.t_ref, bf16[512,640]{1,0:T(8,128)(2,1)} %bitcast.35, bf16[512,640]{1,0:T(8,128)(2,1)} %copy-done.1, bf16[512,640]{1,0:T(8,128)(2,1)} %copy-done.2, bf16[256,640]{1,0:T(8,128)(2,1)} %copy-done.28, bf16[256,640]{1,0:T(8,128)(2,1)} %copy-done.29, ...), custom_call_target="tpu_custom_call" | custom-call | flops 2000000000 | bytes 1048576 | tf_op jit(solution)/shard_map/pallas_call | solution.py:91
  106.8 3.2 %collective-permute-start.21 = (bf16[512,256]{1,0:T(8,128)(2,1)S(1)}, bf16[512,256]{1,0:T(8,128)(2,1)S(1)}, u32[]{:S(2)}, u32[]{:S(2)}) collective-permute-start(bf16[512,256]{1,0:T(8,128)(2,1)S(1)} %get-tuple-element.84), channel_id=1, source_target_pairs={{0,6},{1,7},{2,0},{3,1},{4,2},{5,3},{6,4},{7,5},{8,14},{9,15},{10,... | collective-permute-start | bytes 786440 | tf_op jit(solution)/shard_map/ppermute | solution.py:734
  110.1 2.3 %collective-permute-done.22.refs_3_ = bf16[512,256]{1,0:T(8,128)(2,1)S(1)} collective-permute-done((bf16[512,256]{1,0:T(8,128)(2,1)S(1)}, bf16[512,256]{1,0:T(8,128)(2,1)S(1)}, u32[]{:S(2)}, u32[]{:S(2)}) %collective-permute-start.22) | collective-permute-done | bytes 262176 | tf_op jit(solution)/shard_map/ppermute | solution.py:738
  112.4 3.0 %collective-permute-start.24 = (bf16[512,256]{1,0:T(8,128)(2,1)S(1)}, bf16[512,256]{1,0:T(8,128)(2,1)S(1)}, u32[]{:S(2)}, u32[]{:S(2)}) collective-permute-start(bf16[512,256]{1,0:T(8,128)(2,1)S(1)} %get-tuple-element.87), channel_id=1, source_target_pairs={{0,7},{1,6},{2,1},{3,0},{4,3},{5,2},{6,5},{7,4},{8,15},{9,14},{10,... | collective-permute-start | bytes 786440 | tf_op jit(solution)/shard_map/ppermute | solution.py:742
  115.3 1.9 %collective-permute-done.20.refs_1_ = bf16[512,256]{1,0:T(8,128)(2,1)S(1)} collective-permute-done((bf16[512,256]{1,0:T(8,128)(2,1)S(1)}, bf16[512,256]{1,0:T(8,128)(2,1)S(1)}, u32[]{:S(2)}, u32[]{:S(2)}) %collective-permute-start.20) | collective-permute-done | bytes 262176 | tf_op jit(solution)/shard_map/ppermute | solution.py:734
  117.2 4.4 %collective-permute-done.23.refs_4_ = bf16[512,256]{1,0:T(8,128)(2,1)S(1)} collective-permute-done((bf16[512,256]{1,0:T(8,128)(2,1)S(1)}, bf16[512,256]{1,0:T(8,128)(2,1)S(1)}, u32[]{:S(2)}, u32[]{:S(2)}) %collective-permute-start.23) | collective-permute-done | bytes 262176 | tf_op jit(solution)/shard_map/ppermute | solution.py:742
  121.7 1.0 shard_map.183
  122.7 9.8 %all-to-all-start.2 = ((bf16[32,32,256]{2,1,0:T(8,128)(2,1)}), bf16[32,32,256]{2,1,0:T(8,128)(2,1)}, u32[]{:S(2)}, u32[]{:S(2)}) async-start(bf16[32,32,256]{2,1,0:T(8,128)(2,1)} %shard_map.183), calls=%async_computation.2 | async-start | bytes 1048576 | tf_op jit(solution)/shard_map/all_to_all | solution.py:760
  134.4 2.2 %shard_map.184 = (bf16[512,256]{1,0:T(8,128)(2,1)}, bf16[512,256]{1,0:T(8,128)(2,1)}, f32[512,256]{1,0:T(8,128)}, f32[512,256]{1,0:T(8,128)}, f32[8,256]{1,0:T(8,128)S(1)}) custom-call(s32[1]{0:T(128)} %bitcast.t_ref, bf16[64,2048]{1,0:T(8,128)(2,1)} %bitcast.53, bf16[64,256]{1,0:T(8,128)(2,1)S(1)} %bitcast.42, bf16[5,64,256]{2,1,0:T(8,128)(2,1)S(1)} %copy-done.14, ...), custom_call_target="tpu_custom_call" | custom-call | flops 100000000 | bytes 1048576 | tf_op jit(solution)/shard_map/pallas_call | solution.py:91
  136.6 8.9 %shard_map.182 = (f32[4,512,256]{2,1,0:T(8,128)}, f32[4,512,256]{2,1,0:T(8,128)}, f32[256,2048]{1,0:T(8,128)}) custom-call(s32[1]{0:T(128)} %bitcast.t_ref, bf16[512,640]{1,0:T(8,128)(2,1)} %bitcast.36, bf16[512,640]{1,0:T(8,128)(2,1)} %copy-done.1, bf16[512,640]{1,0:T(8,128)(2,1)} %copy-done.2, bf16[256,640]{1,0:T(8,128)(2,1)} %copy-done.28, ...), custom_call_target="tpu_custom_call" | custom-call | flops 2000000000 | bytes 1048576 | tf_op jit(solution)/shard_map/pallas_call | solution.py:91
  145.6 1.4 all-to-all-done.2
  147.0 3.3 %shard_map.185 = (bf16[256,256]{1,0:T(8,128)(2,1)}, bf16[32,32,128]{2,1,0:T(8,128)(2,1)}, f32[4,72,256]{2,1,0:T(8,128)S(1)}, bf16[4,72,256]{2,1,0:T(8,128)(2,1)S(1)}) custom-call(s32[1]{0:T(128)} %bitcast.t_ref, bf16[256,1024]{1,0:T(8,128)(2,1)} %get-tuple-element.81.refs_0_, bf16[256,2048]{1,0:T(8,128)(2,1)} %refs_1_.3, bf16[1024,256]{1,0:T(8,128)(2,1)} %bitcast.22.refs_2_, ...), custom_call_target="tpu_custom_call" | custom-call | flops 1000000000 | bytes 1048576 | tf_op jit(solution)/shard_map/pallas_call | solution.py:91
  150.3 8.6 %all-to-all-start.3 = ((bf16[32,32,128]{2,1,0:T(8,128)(2,1)}), bf16[32,32,128]{2,1,0:T(8,128)(2,1)S(1)}, u32[]{:S(2)}, u32[]{:S(2)}) async-start(bf16[32,32,128]{2,1,0:T(8,128)(2,1)} %get-tuple-element.104), calls=%async_computation.3 | async-start | bytes 524288 | tf_op jit(solution)/shard_map/all_to_all | solution.py:760
  159.0 1.4 collective-permute-done.25.refs_1_
  160.4 1.2 collective-permute-start.26
  161.6 3.5 %collective-permute-start.27 = (bf16[72,256]{1,0:T(8,128)(2,1)S(1)}, bf16[72,256]{1,0:T(8,128)(2,1)S(1)}, u32[]{:S(2)}, u32[]{:S(2)}) collective-permute-start(bf16[72,256]{1,0:T(8,128)(2,1)S(1)} %get-tuple-element.97), channel_id=1, source_target_pairs={{0,4},{1,5},{2,6},{3,7},{4,0},{5,1},{6,2},{7,3},{8,12},{9,13},{10,... | collective-permute-start | bytes 110600 | tf_op jit(solution)/shard_map/ppermute | solution.py:738
  165.1 2.3 %collective-permute-done.27.refs_2_ = bf16[72,256]{1,0:T(8,128)(2,1)S(1)} collective-permute-done((bf16[72,256]{1,0:T(8,128)(2,1)S(1)}, bf16[72,256]{1,0:T(8,128)(2,1)S(1)}, u32[]{:S(2)}, u32[]{:S(2)}) %collective-permute-start.27) | collective-permute-done | bytes 36896 | tf_op jit(solution)/shard_map/ppermute | solution.py:738
  167.4 2.8 %collective-permute-done.28.refs_3_ = bf16[72,256]{1,0:T(8,128)(2,1)S(1)} collective-permute-done((bf16[72,256]{1,0:T(8,128)(2,1)S(1)}, bf16[72,256]{1,0:T(8,128)(2,1)S(1)}, u32[]{:S(2)}, u32[]{:S(2)}) %collective-permute-start.28) | collective-permute-done | bytes 36896 | tf_op jit(solution)/shard_map/ppermute | solution.py:738
  170.4 4.6 %collective-permute-start.29 = (f32[64,128]{1,0:T(8,128)S(1)}, f32[64,128]{1,0:T(8,128)S(1)}, u32[]{:S(2)}, u32[]{:S(2)}) collective-permute-start(f32[64,128]{1,0:T(8,128)S(1)} %get-tuple-element.101), channel_id=1, source_target_pairs={{8,0},{16,8},{24,16},{32,24},{40,32},{48,40},{56,48},{64,56},{72,6... | collective-permute-start | bytes 98312 | tf_op jit(solution)/shard_map/ppermute | solution.py:821
  175.2 1.9 %collective-permute-start.30 = (f32[64,64]{1,0:T(8,128)S(1)}, f32[64,64]{1,0:T(8,128)S(1)}, u32[]{:S(2)}, u32[]{:S(2)}) collective-permute-start(f32[64,64]{1,0:T(8,128)S(1)} %shard_map.190), channel_id=1, source_target_pairs={{0,0},{1,32},{2,64},{3,96},{4,128},{5,160},{6,192},{7,224},{32,1},... | collective-permute-start | bytes 49160 | tf_op jit(solution)/shard_map/ppermute | solution.py:825
  177.1 1.0 shard_map.188.refs_0_
  178.1 1.4 shard_map.189
  179.5 7.8 %collective-permute-done.30 = f32[64,64]{1,0:T(8,128)S(1)} collective-permute-done((f32[64,64]{1,0:T(8,128)S(1)}, f32[64,64]{1,0:T(8,128)S(1)}, u32[]{:S(2)}, u32[]{:S(2)}) %collective-permute-start.30) | collective-permute-done | bytes 16416 | tf_op jit(solution)/shard_map/ppermute | solution.py:825
  (109 shorter events, 15.8 us)
Async XLA Ops:
  2.0 12.6 %copy-start.15 = (bf16[256,64]{0,1:T(8,128)(2,1)S(1)}, bf16[256,64]{0,1:T(8,128)(2,1)}, u32[]{:S(2)}) copy-start(bf16[256,64]{0,1:T(8,128)(2,1)} %param.19) | copy-start | bytes 98308
  2.0 21.4 %copy-start.27 = (f32[256,2]{0,1:T(2,128)S(1)}, f32[256,2]{0,1:T(2,128)}, u32[]{:S(2)}) copy-start(f32[256,2]{0,1:T(2,128)} %param.15) | copy-start | bytes 6148
  4.7 27.8 %all-to-all-start = ((bf16[32,16,640]{2,1,0:T(8,128)(2,1)}), bf16[32,16,640]{2,1,0:T(8,128)(2,1)S(1)}, u32[]{:S(2)}, u32[]{:S(2)}) async-start(bf16[32,16,640]{2,1,0:T(8,128)(2,1)} %bitcast.54), calls=%async_computation | async-start | bytes 1310720 | tf_op jit(solution)/shard_map/all_to_all | solution.py:760
  15.6 1.5 collective-permute-start.4
  18.7 7.1 %collective-permute-start.5 = (bf16[4,64,256]{2,1,0:T(8,128)(2,1)S(1)}, bf16[4,64,256]{2,1,0:T(8,128)(2,1)S(1)}, u32[]{:S(2)}, u32[]{:S(2)}) collective-permute-start(bf16[4,64,256]{2,1,0:T(8,128)(2,1)S(1)} %get-tuple-element.61), channel_id=1, source_target_pairs={{0,2},{1,3},{2,0},{3,1},{4,6},{5,7},{6,4},{7,5},{8,10},{9,11},{10,... | collective-permute-start | bytes 393224 | tf_op jit(solution)/shard_map/ppermute | solution.py:738
  20.3 9.3 %collective-permute-start.6 = (bf16[4,64,256]{2,1,0:T(8,128)(2,1)S(1)}, bf16[4,64,256]{2,1,0:T(8,128)(2,1)S(1)}, u32[]{:S(2)}, u32[]{:S(2)}) collective-permute-start(bf16[4,64,256]{2,1,0:T(8,128)(2,1)S(1)} %get-tuple-element.62), channel_id=1, source_target_pairs={{0,4},{1,5},{2,6},{3,7},{4,0},{5,1},{6,2},{7,3},{8,12},{9,13},{10,... | collective-permute-start | bytes 393224 | tf_op jit(solution)/shard_map/ppermute | solution.py:738
  23.2 8.7 %collective-permute-start.7 = (bf16[4,64,256]{2,1,0:T(8,128)(2,1)S(1)}, bf16[4,64,256]{2,1,0:T(8,128)(2,1)S(1)}, u32[]{:S(2)}, u32[]{:S(2)}) collective-permute-start(bf16[4,64,256]{2,1,0:T(8,128)(2,1)S(1)} %get-tuple-element.63), channel_id=1, source_target_pairs={{0,6},{1,7},{2,4},{3,5},{4,2},{5,3},{6,0},{7,1},{8,14},{9,15},{10,... | collective-permute-start | bytes 393224 | tf_op jit(solution)/shard_map/ppermute | solution.py:738
  32.5 41.7 %copy-start = (bf16[32,16,640]{2,1,0:T(8,128)(2,1)}, bf16[32,16,640]{2,1,0:T(8,128)(2,1)S(1)}, u32[]{:S(2)}) copy-start(bf16[32,16,640]{2,1,0:T(8,128)(2,1)S(1)} %all-to-all-done) | copy-start | bytes 1966084
  32.5 20.6 %all-to-all-start.1 = ((bf16[32,16,384]{2,1,0:T(8,128)(2,1)}), bf16[32,16,384]{2,1,0:T(8,128)(2,1)S(1)}, u32[]{:S(2)}, u32[]{:S(2)}) async-start(bf16[32,16,384]{2,1,0:T(8,128)(2,1)} %bitcast.55), calls=%async_computation.1 | async-start | bytes 786432 | tf_op jit(solution)/shard_map/all_to_all | solution.py:760
  42.3 21.2 %collective-permute-start.15 = (bf16[2048,256]{1,0:T(8,128)(2,1)}, bf16[2048,256]{1,0:T(8,128)(2,1)}, u32[]{:S(2)}, u32[]{:S(2)}) collective-permute-start(bf16[2048,256]{1,0:T(8,128)(2,1)} %bitcast.13), channel_id=1, source_target_pairs={{0,1},{1,0},{2,3},{3,2},{4,5},{5,4},{6,7},{7,6},{8,9},{9,8},{10,11... | collective-permute-start | bytes 3145736 | tf_op jit(solution)/shard_map/ppermute | solution.py:738
  42.4 22.4 %collective-permute-start.16 = (bf16[2048,256]{1,0:T(8,128)(2,1)}, bf16[2048,256]{1,0:T(8,128)(2,1)}, u32[]{:S(2)}, u32[]{:S(2)}) collective-permute-start(bf16[2048,256]{1,0:T(8,128)(2,1)} %bitcast.16), channel_id=1, source_target_pairs={{0,1},{1,0},{2,3},{3,2},{4,5},{5,4},{6,7},{7,6},{8,9},{9,8},{10,11... | collective-permute-start | bytes 3145736 | tf_op jit(solution)/shard_map/ppermute | solution.py:738
  42.9 22.7 %collective-permute-start.14 = (bf16[256,2048]{1,0:T(8,128)(2,1)}, bf16[256,2048]{1,0:T(8,128)(2,1)}, u32[]{:S(2)}, u32[]{:S(2)}) collective-permute-start(bf16[256,2048]{1,0:T(8,128)(2,1)} %bitcast.11.refs_8_.refs_7_), channel_id=1, source_target_pairs={{0,1},{1,0},{2,3},{3,2},{4,5},{5,4},{6,7},{7,6},{8,9},{9,8},{10,11... | collective-permute-start | bytes 3145736 | tf_op jit(solution)/shard_map/ppermute | solution.py:738
  43.0 18.3 %collective-permute-start = (bf16[512,640]{1,0:T(8,128)(2,1)S(1)}, bf16[512,640]{1,0:T(8,128)(2,1)S(1)}, u32[]{:S(2)}, u32[]{:S(2)}) collective-permute-start(bf16[512,640]{1,0:T(8,128)(2,1)S(1)} %bitcast.31), channel_id=1, source_target_pairs={{0,2},{1,3},{2,4},{3,5},{4,6},{5,7},{6,0},{7,1},{8,10},{9,11},{10,... | collective-permute-start | bytes 1966088 | tf_op jit(solution)/shard_map/ppermute | solution.py:734
  43.0 18.3 %collective-permute-start.1 = (bf16[512,640]{1,0:T(8,128)(2,1)S(1)}, bf16[512,640]{1,0:T(8,128)(2,1)S(1)}, u32[]{:S(2)}, u32[]{:S(2)}) collective-permute-start(bf16[512,640]{1,0:T(8,128)(2,1)S(1)} %bitcast.32), channel_id=1, source_target_pairs={{0,6},{1,7},{2,0},{3,1},{4,2},{5,3},{6,4},{7,5},{8,14},{9,15},{10,... | collective-permute-start | bytes 1966088 | tf_op jit(solution)/shard_map/ppermute | solution.py:734
  53.1 28.5 %copy-start.3 = (bf16[32,16,384]{2,1,0:T(8,128)(2,1)}, bf16[32,16,384]{2,1,0:T(8,128)(2,1)S(1)}, u32[]{:S(2)}) copy-start(bf16[32,16,384]{2,1,0:T(8,128)(2,1)S(1)} %all-to-all-done.1) | copy-start | bytes 1179652
  61.3 13.0 %copy-start.1 = (bf16[512,640]{1,0:T(8,128)(2,1)}, bf16[512,640]{1,0:T(8,128)(2,1)S(1)}, u32[]{:S(2)}) copy-start(bf16[512,640]{1,0:T(8,128)(2,1)S(1)} %collective-permute-done.refs_1_) | copy-start | bytes 1966084
  61.3 7.8 %collective-permute-start.10 = (bf16[256,384]{1,0:T(8,128)(2,1)S(1)}, bf16[256,384]{1,0:T(8,128)(2,1)S(1)}, u32[]{:S(2)}, u32[]{:S(2)}) collective-permute-start(bf16[256,384]{1,0:T(8,128)(2,1)S(1)} %bitcast.58), channel_id=1, source_target_pairs={{0,6},{1,7},{2,0},{3,1},{4,2},{5,3},{6,4},{7,5},{8,14},{9,15},{10,... | collective-permute-start | bytes 589832 | tf_op jit(solution)/shard_map/ppermute | solution.py:734
  61.3 12.9 %copy-start.2 = (bf16[512,640]{1,0:T(8,128)(2,1)}, bf16[512,640]{1,0:T(8,128)(2,1)S(1)}, u32[]{:S(2)}) copy-start(bf16[512,640]{1,0:T(8,128)(2,1)S(1)} %collective-permute-done.1.refs_2_) | copy-start | bytes 1966084
  61.3 23.9 %collective-permute-start.2 = (bf16[256,640]{1,0:T(8,128)(2,1)S(1)}, bf16[256,640]{1,0:T(8,128)(2,1)S(1)}, u32[]{:S(2)}, u32[]{:S(2)}) collective-permute-start(bf16[256,640]{1,0:T(8,128)(2,1)S(1)} %slice.24), channel_id=1, source_target_pairs={{0,2},{1,3},{2,4},{3,5},{4,6},{5,7},{6,0},{7,1},{8,10},{9,11},{10,... | collective-permute-start | bytes 983048 | tf_op jit(solution)/shard_map/ppermute | solution.py:734
  63.5 21.8 %collective-permute-start.3 = (bf16[256,640]{1,0:T(8,128)(2,1)S(1)}, bf16[256,640]{1,0:T(8,128)(2,1)S(1)}, u32[]{:S(2)}, u32[]{:S(2)}) collective-permute-start(bf16[256,640]{1,0:T(8,128)(2,1)S(1)} %slice.25), channel_id=1, source_target_pairs={{0,6},{1,7},{2,0},{3,1},{4,2},{5,3},{6,4},{7,5},{8,14},{9,15},{10,... | collective-permute-start | bytes 983048 | tf_op jit(solution)/shard_map/ppermute | solution.py:734
  64.8 12.6 %collective-permute-start.8 = (bf16[256,384]{1,0:T(8,128)(2,1)S(1)}, bf16[256,384]{1,0:T(8,128)(2,1)S(1)}, u32[]{:S(2)}, u32[]{:S(2)}) collective-permute-start(bf16[256,384]{1,0:T(8,128)(2,1)S(1)} %bitcast.59), channel_id=1, source_target_pairs={{0,2},{1,3},{2,4},{3,5},{4,6},{5,7},{6,0},{7,1},{8,10},{9,11},{10,... | collective-permute-start | bytes 589832 | tf_op jit(solution)/shard_map/ppermute | solution.py:734
  65.6 13.3 %collective-permute-start.11 = (bf16[256,384]{1,0:T(8,128)(2,1)S(1)}, bf16[256,384]{1,0:T(8,128)(2,1)S(1)}, u32[]{:S(2)}, u32[]{:S(2)}) collective-permute-start(bf16[256,384]{1,0:T(8,128)(2,1)S(1)} %bitcast.56), channel_id=1, source_target_pairs={{0,6},{1,7},{2,0},{3,1},{4,2},{5,3},{6,4},{7,5},{8,14},{9,15},{10,... | collective-permute-start | bytes 589832 | tf_op jit(solution)/shard_map/ppermute | solution.py:734
  69.0 12.6 %copy-start.7 = (bf16[256,384]{1,0:T(8,128)(2,1)}, bf16[256,384]{1,0:T(8,128)(2,1)S(1)}, u32[]{:S(2)}) copy-start(bf16[256,384]{1,0:T(8,128)(2,1)S(1)} %collective-permute-done.10.refs_6_.refs_8_) | copy-start | bytes 589828
  69.0 12.6 %collective-permute-start.9 = (bf16[256,384]{1,0:T(8,128)(2,1)S(1)}, bf16[256,384]{1,0:T(8,128)(2,1)S(1)}, u32[]{:S(2)}, u32[]{:S(2)}) collective-permute-start(bf16[256,384]{1,0:T(8,128)(2,1)S(1)} %bitcast.57), channel_id=1, source_target_pairs={{0,2},{1,3},{2,4},{3,5},{4,6},{5,7},{6,0},{7,1},{8,10},{9,11},{10,... | collective-permute-start | bytes 589832 | tf_op jit(solution)/shard_map/ppermute | solution.py:734
  77.4 12.6 %collective-permute-start.12 = (bf16[256,384]{1,0:T(8,128)(2,1)S(1)}, bf16[256,384]{1,0:T(8,128)(2,1)S(1)}, u32[]{:S(2)}, u32[]{:S(2)}) collective-permute-start(bf16[256,384]{1,0:T(8,128)(2,1)S(1)} %collective-permute-done.8.refs_4_.refs_6_), channel_id=1, source_target_pairs={{0,2},{1,3},{2,4},{3,5},{4,6},{5,7},{6,0},{7,1},{8,10},{9,11},{10,... | collective-permute-start | bytes 589832 | tf_op jit(solution)/shard_map/ppermute | solution.py:734
  78.9 11.2 %collective-permute-start.13 = (bf16[256,384]{1,0:T(8,128)(2,1)S(1)}, bf16[256,384]{1,0:T(8,128)(2,1)S(1)}, u32[]{:S(2)}, u32[]{:S(2)}) collective-permute-start(bf16[256,384]{1,0:T(8,128)(2,1)S(1)} %collective-permute-done.11.refs_7_.refs_9_), channel_id=1, source_target_pairs={{0,6},{1,7},{2,0},{3,1},{4,2},{5,3},{6,4},{7,5},{8,14},{9,15},{10,... | collective-permute-start | bytes 589832 | tf_op jit(solution)/shard_map/ppermute | solution.py:734
  93.1 7.7 %collective-permute-start.17 = (bf16[2,256,256]{2,1,0:T(8,128)(2,1)S(1)}, bf16[2,256,256]{2,1,0:T(8,128)(2,1)S(1)}, u32[]{:S(2)}, u32[]{:S(2)}) collective-permute-start(bf16[2,256,256]{2,1,0:T(8,128)(2,1)S(1)} %get-tuple-element.72), channel_id=1, source_target_pairs={{0,2},{1,3},{2,4},{3,5},{4,6},{5,7},{6,0},{7,1},{8,10},{9,11},{10,... | collective-permute-start | bytes 786440 | tf_op jit(solution)/shard_map/ppermute | solution.py:734
  94.0 6.8 %collective-permute-start.18 = (bf16[2,256,256]{2,1,0:T(8,128)(2,1)S(1)}, bf16[2,256,256]{2,1,0:T(8,128)(2,1)S(1)}, u32[]{:S(2)}, u32[]{:S(2)}) collective-permute-start(bf16[2,256,256]{2,1,0:T(8,128)(2,1)S(1)} %get-tuple-element.73), channel_id=1, source_target_pairs={{0,6},{1,7},{2,0},{3,1},{4,2},{5,3},{6,4},{7,5},{8,14},{9,15},{10,... | collective-permute-start | bytes 786440 | tf_op jit(solution)/shard_map/ppermute | solution.py:734
  106.2 26.4 %copy-start.14 = (bf16[5,64,256]{2,1,0:T(8,128)(2,1)S(1)}, bf16[5,64,256]{2,1,0:T(8,128)(2,1)}, u32[]{:S(2)}) copy-start(bf16[5,64,256]{2,1,0:T(8,128)(2,1)} %copy-done.13) | copy-start | bytes 491524
  106.2 26.4 %copy-start.16 = (bf16[256,64]{0,1:T(8,128)(2,1)S(1)}, bf16[256,64]{0,1:T(8,128)(2,1)}, u32[]{:S(2)}) copy-start(bf16[256,64]{0,1:T(8,128)(2,1)} %param.19) | copy-start | bytes 98308
  106.2 26.4 %copy-start.18 = (bf16[4,64,256]{2,1,0:T(8,128)(2,1)S(1)}, bf16[4,64,256]{2,1,0:T(8,128)(2,1)}, u32[]{:S(2)}) copy-start(bf16[4,64,256]{2,1,0:T(8,128)(2,1)} %copy-done.17) | copy-start | bytes 393220
  106.2 30.4 %collective-permute-start.19 = (bf16[12,512,256]{2,1,0:T(8,128)(2,1)S(1)}, bf16[12,512,256]{2,1,0:T(8,128)(2,1)}, u32[]{:S(2)}, u32[]{:S(2)}) collective-permute-start(bf16[12,512,256]{2,1,0:T(8,128)(2,1)S(1)} %shard_map.181), channel_id=1, source_target_pairs={{0,1},{1,0},{2,3},{3,2},{4,5},{5,4},{6,7},{7,6},{8,9},{9,8},{10,11... | collective-permute-start | bytes 9437192 | tf_op jit(solution)/shard_map/ppermute | solution.py:738
  106.3 6.0 %collective-permute-start.22 = (bf16[512,256]{1,0:T(8,128)(2,1)S(1)}, bf16[512,256]{1,0:T(8,128)(2,1)S(1)}, u32[]{:S(2)}, u32[]{:S(2)}) collective-permute-start(bf16[512,256]{1,0:T(8,128)(2,1)S(1)} %get-tuple-element.85), channel_id=1, source_target_pairs={{0,1},{1,0},{2,3},{3,2},{4,5},{5,4},{6,7},{7,6},{8,9},{9,8},{10,11... | collective-permute-start | bytes 786440 | tf_op jit(solution)/shard_map/ppermute | solution.py:738
  106.8 10.4 %collective-permute-start.20 = (bf16[512,256]{1,0:T(8,128)(2,1)S(1)}, bf16[512,256]{1,0:T(8,128)(2,1)S(1)}, u32[]{:S(2)}, u32[]{:S(2)}) collective-permute-start(bf16[512,256]{1,0:T(8,128)(2,1)S(1)} %get-tuple-element.78), channel_id=1, source_target_pairs={{0,2},{1,3},{2,4},{3,5},{4,6},{5,7},{6,0},{7,1},{8,10},{9,11},{10,... | collective-permute-start | bytes 786440 | tf_op jit(solution)/shard_map/ppermute | solution.py:734
  106.8 10.4 %collective-permute-start.21 = (bf16[512,256]{1,0:T(8,128)(2,1)S(1)}, bf16[512,256]{1,0:T(8,128)(2,1)S(1)}, u32[]{:S(2)}, u32[]{:S(2)}) collective-permute-start(bf16[512,256]{1,0:T(8,128)(2,1)S(1)} %get-tuple-element.84), channel_id=1, source_target_pairs={{0,6},{1,7},{2,0},{3,1},{4,2},{5,3},{6,4},{7,5},{8,14},{9,15},{10,... | collective-permute-start | bytes 786440 | tf_op jit(solution)/shard_map/ppermute | solution.py:734
  110.1 11.6 %collective-permute-start.23 = (bf16[512,256]{1,0:T(8,128)(2,1)S(1)}, bf16[512,256]{1,0:T(8,128)(2,1)S(1)}, u32[]{:S(2)}, u32[]{:S(2)}) collective-permute-start(bf16[512,256]{1,0:T(8,128)(2,1)S(1)} %get-tuple-element.86), channel_id=1, source_target_pairs={{0,3},{1,2},{2,5},{3,4},{4,7},{5,6},{6,1},{7,0},{8,11},{9,10},{10,... | collective-permute-start | bytes 786440 | tf_op jit(solution)/shard_map/ppermute | solution.py:742
  112.4 9.4 %collective-permute-start.24 = (bf16[512,256]{1,0:T(8,128)(2,1)S(1)}, bf16[512,256]{1,0:T(8,128)(2,1)S(1)}, u32[]{:S(2)}, u32[]{:S(2)}) collective-permute-start(bf16[512,256]{1,0:T(8,128)(2,1)S(1)} %get-tuple-element.87), channel_id=1, source_target_pairs={{0,7},{1,6},{2,1},{3,0},{4,3},{5,2},{6,5},{7,4},{8,15},{9,14},{10,... | collective-permute-start | bytes 786440 | tf_op jit(solution)/shard_map/ppermute | solution.py:742
  122.7 24.3 %all-to-all-start.2 = ((bf16[32,32,256]{2,1,0:T(8,128)(2,1)}), bf16[32,32,256]{2,1,0:T(8,128)(2,1)}, u32[]{:S(2)}, u32[]{:S(2)}) async-start(bf16[32,32,256]{2,1,0:T(8,128)(2,1)} %shard_map.183), calls=%async_computation.2 | async-start | bytes 1048576 | tf_op jit(solution)/shard_map/all_to_all | solution.py:760
  147.0 27.9 %copy-start.30 = (f32[31,64]{1,0:T(8,128)S(1)}, f32[31,64]{1,0:T(8,128)}, u32[]{:S(2)}) copy-start(f32[31,64]{1,0:T(8,128)} %param.18) | copy-start | bytes 23812
  147.0 31.1 %copy-start.23 = (bf16[256,64]{0,1:T(8,128)(2,1)S(1)}, bf16[256,64]{0,1:T(8,128)(2,1)}, u32[]{:S(2)}) copy-start(bf16[256,64]{0,1:T(8,128)(2,1)} %param.16) | copy-start | bytes 98308
  147.0 31.1 %copy-start.24 = (bf16[256,64]{0,1:T(8,128)(2,1)S(1)}, bf16[256,64]{0,1:T(8,128)(2,1)}, u32[]{:S(2)}) copy-start(bf16[256,64]{0,1:T(8,128)(2,1)} %param.17) | copy-start | bytes 98308
  150.3 24.8 %all-to-all-start.3 = ((bf16[32,32,128]{2,1,0:T(8,128)(2,1)}), bf16[32,32,128]{2,1,0:T(8,128)(2,1)S(1)}, u32[]{:S(2)}, u32[]{:S(2)}) async-start(bf16[32,32,128]{2,1,0:T(8,128)(2,1)} %get-tuple-element.104), calls=%async_computation.3 | async-start | bytes 524288 | tf_op jit(solution)/shard_map/all_to_all | solution.py:760
  158.9 1.5 collective-permute-start.25
  160.4 4.8 %collective-permute-start.26 = (bf16[72,256]{1,0:T(8,128)(2,1)S(1)}, bf16[72,256]{1,0:T(8,128)(2,1)S(1)}, u32[]{:S(2)}, u32[]{:S(2)}) collective-permute-start(bf16[72,256]{1,0:T(8,128)(2,1)S(1)} %get-tuple-element.96), channel_id=1, source_target_pairs={{0,2},{1,3},{2,0},{3,1},{4,6},{5,7},{6,4},{7,5},{8,10},{9,11},{10,... | collective-permute-start | bytes 110600 | tf_op jit(solution)/shard_map/ppermute | solution.py:738
  161.6 5.9 %collective-permute-start.27 = (bf16[72,256]{1,0:T(8,128)(2,1)S(1)}, bf16[72,256]{1,0:T(8,128)(2,1)S(1)}, u32[]{:S(2)}, u32[]{:S(2)}) collective-permute-start(bf16[72,256]{1,0:T(8,128)(2,1)S(1)} %get-tuple-element.97), channel_id=1, source_target_pairs={{0,4},{1,5},{2,6},{3,7},{4,0},{5,1},{6,2},{7,3},{8,12},{9,13},{10,... | collective-permute-start | bytes 110600 | tf_op jit(solution)/shard_map/ppermute | solution.py:738
  165.1 5.2 %collective-permute-start.28 = (bf16[72,256]{1,0:T(8,128)(2,1)S(1)}, bf16[72,256]{1,0:T(8,128)(2,1)S(1)}, u32[]{:S(2)}, u32[]{:S(2)}) collective-permute-start(bf16[72,256]{1,0:T(8,128)(2,1)S(1)} %get-tuple-element.98), channel_id=1, source_target_pairs={{0,6},{1,7},{2,4},{3,5},{4,2},{5,3},{6,0},{7,1},{8,14},{9,15},{10,... | collective-permute-start | bytes 110600 | tf_op jit(solution)/shard_map/ppermute | solution.py:738
  170.4 7.7 %collective-permute-start.29 = (f32[64,128]{1,0:T(8,128)S(1)}, f32[64,128]{1,0:T(8,128)S(1)}, u32[]{:S(2)}, u32[]{:S(2)}) collective-permute-start(f32[64,128]{1,0:T(8,128)S(1)} %get-tuple-element.101), channel_id=1, source_target_pairs={{8,0},{16,8},{24,16},{32,24},{40,32},{48,40},{56,48},{64,56},{72,6... | collective-permute-start | bytes 98312 | tf_op jit(solution)/shard_map/ppermute | solution.py:821
  175.2 12.1 %collective-permute-start.30 = (f32[64,64]{1,0:T(8,128)S(1)}, f32[64,64]{1,0:T(8,128)S(1)}, u32[]{:S(2)}, u32[]{:S(2)}) collective-permute-start(f32[64,64]{1,0:T(8,128)S(1)} %shard_map.190), channel_id=1, source_target_pairs={{0,0},{1,32},{2,64},{3,96},{4,128},{5,160},{6,192},{7,224},{32,1},... | collective-permute-start | bytes 49160 | tf_op jit(solution)/shard_map/ppermute | solution.py:825
  (18 other events, 46.6 us)

commit v5 on v4

--- a/solution.py
+++ b/solution.py
@@ -206,7 +206,7 @@
 def first(tp, near_blocks, weights):
     return call(
         first_body,
-        (shape((ROWS, 512), F32),) * 2,
+        (pltpu.HBM((ROWS, 512), F32),) * 2,
         tp,
         (*near_blocks, *weights),
         staged=(3, 5, 4, 6),
@@ -221,15 +221,16 @@
     top, bottom = now(ins[2])[...], now(ins[3])[...]
     for j in range(2):
         cols = slice(256 * j, 256 * j + 256)
-        for near_sum, into, at in ((ins[0], pg, 4), (ins[1], pu, 6)):
+        for into, at in ((pg, 4), (pu, 6)):
             w = now(ins[at + j])[0]
-            into[0:256, cols] = near_sum[0:256, cols] + dot(top, w)
-            into[256:512, cols] = near_sum[256:512, cols] + dot(bottom, w)
+            into[0:256, cols] = dot(top, w)
+            into[256:512, cols] = dot(bottom, w)
+    gate_near, up_near = now(ins[0]), now(ins[1])
 
     @pl.loop(0, ROWS // 32)
     def _(i):
         at = pl.ds(pl.multiple_of(i * 32, 32), 32)
-        gate_pre, up_pre = pg[at, :], pu[at, :]
+        gate_pre, up_pre = gate_near[at, :] + pg[at, :], up_near[at, :] + pu[at, :]
         capped = jnp.minimum(gate_pre, CLAMP)
         clipped = jnp.clip(up_pre, -CLAMP, CLAMP)
         sig = jax.nn.sigmoid(ALPHA * capped)
@@ -245,10 +246,10 @@
     quarter = ((1, 512, 256), lambda t: (pl.ds((t // 2 + 2) % 4, 1),))
     return call(
         forward_body,
-        (shape((ROWS, 512), BF), shape((ROWS, 512), F32), shape((ROWS, 512), F32)),
+        (pltpu.HBM((ROWS, 512), BF), shape((ROWS, 512), F32), shape((ROWS, 512), F32)),
         tp,
         (*sums, *far_blocks, *weights),
-        staged=(2, 3, 4, 6, 5, 7),
+        staged=(2, 3, 4, 6, 5, 7, 0, 1),
         cuts={2: rows, 3: rows} | {i: quarter for i in range(4, 8)},
         scratch=[pltpu.VMEM((ROWS, 512), F32)] * 2,
         flops=2 * 10**9,

time: 189 us -> 189 us (level)
    unnamed x64 -> x62, local copies, waits for them, and re-layouts: 8.15 us -> 7.36 us
  transfers between devices with their start and end apart: 35 -> 35, of which waited for: 19 -> 19; matrix products, arithmetic and copies ran while one was open for 0% -> 0% of each run, Pallas kernels for 19% -> 20%
where the time goes in v5:
time: 189 us; the launch traced here: 188 us
  starting transfers between devices  77.5 us (41%)
  Pallas kernels  51.2 us (27%)
  waiting for transfers between devices  50.6 us (27%)
  local copies, waits for them, and re-layouts  7.45 us (4%)
    pallas_call x20, Pallas kernels, call(): pl.pallas_call(kernel, out_shape=outs, in_specs=[SMEM] + [HBM if i in sta...  51.2 us
    all_to_all x4, starting transfers between devices, exchange(): return lax.all_to_all(x, 'sp', 0, 0, tiled=True)  38 us
    ppermute x14, starting transfers between devices, moved(): return lax.ppermute(x, 'tp', [(i, (i + by) % TP) for i in range(TP)])  19 us
    ppermute x14, waiting for transfers between devices, moved(): return lax.ppermute(x, 'tp', [(i, (i + by) % TP) for i in range(TP)])  15.1 us
    ppermute x13, waiting for transfers between devices, swapped(): return lax.ppermute(x, 'tp', [(i, i ^ by) for i in range(TP)])  14.9 us
    ppermute x13, starting transfers between devices, swapped(): return lax.ppermute(x, 'tp', [(i, i ^ by) for i in range(TP)])  11 us
    all_to_all x4, waiting for transfers between devices, exchange(): return lax.all_to_all(x, 'sp', 0, 0, tiled=True)  8.3 us
    ppermute x1, waiting for transfers between devices, step(): lax.ppermute(total(tp, outer_in), ('sp', 'tp'), [((4 * u + i) * TP + t, (...  7.81 us
  transfers between devices with their start and end apart: 35, of which 19 were waited for; matrix products, arithmetic and copies ran while one was open for 0% of the time, Pallas kernels for 20%

profile of v5, /device:TPU:128, one launch (start us, length us, event | category | flops | bytes accessed | tf_op | source)
XLA Modules:
  0.0 187.9 jit_solution(14212043906676265294)
XLA Ops:
  2.0 2.7 %shard_map.171 = (bf16[512,640]{1,0:T(8,128)(2,1)}, s32[8,256]{1,0:T(8,128)S(1)}) custom-call(s32[1]{0:T(128)} %bitcast.t_ref, s32[2,256]{1,0:T(2,128)S(1)} %bitcast.48, bf16[256,2048]{1,0:T(8,128)(2,1)} %refs_1_.2, f32[2,256]{1,0:T(2,128)S(1)} %bitcast.49, bf16[256,2048]{1,0:T(8,128)(2,1)} %refs_1_.3), custom_call_target="tpu_custom_call" | custom-call | flops 1000000000 | bytes 1048576 | tf_op jit(solution)/shard_map/pallas_call | solution.py:91
  4.7 9.8 %all-to-all-start = ((bf16[32,16,640]{2,1,0:T(8,128)(2,1)}), bf16[32,16,640]{2,1,0:T(8,128)(2,1)S(1)}, u32[]{:S(2)}, u32[]{:S(2)}) async-start(bf16[32,16,640]{2,1,0:T(8,128)(2,1)} %bitcast.54), calls=%async_computation | async-start | bytes 1310720 | tf_op jit(solution)/shard_map/all_to_all | solution.py:761
  15.7 1.4 collective-permute-done.4.refs_2_
  17.1 1.0 shard_map.174
  18.7 1.6 collective-permute-start.5
  20.3 2.9 %collective-permute-start.6 = (bf16[4,64,256]{2,1,0:T(8,128)(2,1)S(1)}, bf16[4,64,256]{2,1,0:T(8,128)(2,1)S(1)}, u32[]{:S(2)}, u32[]{:S(2)}) collective-permute-start(bf16[4,64,256]{2,1,0:T(8,128)(2,1)S(1)} %get-tuple-element.62), channel_id=1, source_target_pairs={{0,4},{1,5},{2,6},{3,7},{4,0},{5,1},{6,2},{7,3},{8,12},{9,13},{10,... | collective-permute-start | bytes 393224 | tf_op jit(solution)/shard_map/ppermute | solution.py:739
  23.4 2.4 %shard_map.172 = (bf16[512,384]{1,0:T(8,128)(2,1)}, bf16[256,1024]{1,0:T(8,128)(2,1)}) custom-call(s32[1]{0:T(128)} %bitcast.t_ref, s32[8,256]{1,0:T(8,128)S(1)} %get-tuple-element.57.refs_0_, f32[2,256]{1,0:T(2,128)S(1)} %bitcast.50, bf16[256,2048]{1,0:T(8,128)(2,1)} %refs_1_.3), custom_call_target="tpu_custom_call" | custom-call | flops 1000000000 | bytes 1048576 | tf_op jit(solution)/shard_map/pallas_call | solution.py:91
  26.5 3.1 %collective-permute-done.6.refs_4_ = bf16[4,64,256]{2,1,0:T(8,128)(2,1)S(1)} collective-permute-done((bf16[4,64,256]{2,1,0:T(8,128)(2,1)S(1)}, bf16[4,64,256]{2,1,0:T(8,128)(2,1)S(1)}, u32[]{:S(2)}, u32[]{:S(2)}) %collective-permute-start.6) | collective-permute-done | bytes 131104 | tf_op jit(solution)/shard_map/ppermute | solution.py:739
  30.3 1.6 collective-permute-done.7.refs_5_
  32.5 9.8 %all-to-all-start.1 = ((bf16[32,16,384]{2,1,0:T(8,128)(2,1)}), bf16[32,16,384]{2,1,0:T(8,128)(2,1)S(1)}, u32[]{:S(2)}, u32[]{:S(2)}) async-start(bf16[32,16,384]{2,1,0:T(8,128)(2,1)} %bitcast.55), calls=%async_computation.1 | async-start | bytes 786432 | tf_op jit(solution)/shard_map/all_to_all | solution.py:761
  43.0 3.2 %collective-permute-start.1 = (bf16[512,640]{1,0:T(8,128)(2,1)S(1)}, bf16[512,640]{1,0:T(8,128)(2,1)S(1)}, u32[]{:S(2)}, u32[]{:S(2)}) collective-permute-start(bf16[512,640]{1,0:T(8,128)(2,1)S(1)} %bitcast.32), channel_id=1, source_target_pairs={{0,6},{1,7},{2,0},{3,1},{4,2},{5,3},{6,4},{7,5},{8,14},{9,15},{10,... | collective-permute-start | bytes 1966088 | tf_op jit(solution)/shard_map/ppermute | solution.py:735
  46.3 6.9 %all-to-all-done.1 = bf16[32,16,384]{2,1,0:T(8,128)(2,1)S(1)} async-done(((bf16[32,16,384]{2,1,0:T(8,128)(2,1)}), bf16[32,16,384]{2,1,0:T(8,128)(2,1)S(1)}, u32[]{:S(2)}, u32[]{:S(2)}) %all-to-all-start.1) | async-done | bytes 393248 | tf_op jit(solution)/shard_map/all_to_all | solution.py:761
  53.2 8.1 %collective-permute-done.refs_1_ = bf16[512,640]{1,0:T(8,128)(2,1)S(1)} collective-permute-done((bf16[512,640]{1,0:T(8,128)(2,1)S(1)}, bf16[512,640]{1,0:T(8,128)(2,1)S(1)}, u32[]{:S(2)}, u32[]{:S(2)}) %collective-permute-start) | collective-permute-done | bytes 655392 | tf_op jit(solution)/shard_map/ppermute | solution.py:735
  61.3 2.1 %collective-permute-start.2 = (bf16[256,640]{1,0:T(8,128)(2,1)S(1)}, bf16[256,640]{1,0:T(8,128)(2,1)S(1)}, u32[]{:S(2)}, u32[]{:S(2)}) collective-permute-start(bf16[256,640]{1,0:T(8,128)(2,1)S(1)} %slice.24), channel_id=1, source_target_pairs={{0,2},{1,3},{2,4},{3,5},{4,6},{5,7},{6,0},{7,1},{8,10},{9,11},{10,... | collective-permute-start | bytes 983048 | tf_op jit(solution)/shard_map/ppermute | solution.py:735
  63.5 1.3 collective-permute-start.3
  65.6 2.4 %collective-permute-start.11 = (bf16[256,384]{1,0:T(8,128)(2,1)S(1)}, bf16[256,384]{1,0:T(8,128)(2,1)S(1)}, u32[]{:S(2)}, u32[]{:S(2)}) collective-permute-start(bf16[256,384]{1,0:T(8,128)(2,1)S(1)} %bitcast.56), channel_id=1, source_target_pairs={{0,6},{1,7},{2,0},{3,1},{4,2},{5,3},{6,4},{7,5},{8,14},{9,15},{10,... | collective-permute-start | bytes 589832 | tf_op jit(solution)/shard_map/ppermute | solution.py:735
  68.0 1.0 collective-permute-done.10.refs_6_.refs_8_
  69.0 6.1 %shard_map.176 = (f32[512,512]{1,0:T(8,128)}, f32[512,512]{1,0:T(8,128)}) custom-call(s32[1]{0:T(128)} %bitcast.t_ref, bf16[512,640]{1,0:T(8,128)(2,1)S(1)} %bitcast.33, bf16[512,640]{1,0:T(8,128)(2,1)S(1)} %collective-permute-done.refs_1_, bf16[512,640]{1,0:T(8,128)(2,1)S(1)} %collective-permute-done.1.refs_2_, ...), custom_call_target="tpu_custom_call" | custom-call | flops 1000000000 | bytes 1048576 | tf_op jit(solution)/shard_map/pallas_call | solution.py:91
  75.2 2.2 %collective-permute-done.8.refs_4_.refs_6_ = bf16[256,384]{1,0:T(8,128)(2,1)S(1)} collective-permute-done((bf16[256,384]{1,0:T(8,128)(2,1)S(1)}, bf16[256,384]{1,0:T(8,128)(2,1)S(1)}, u32[]{:S(2)}, u32[]{:S(2)}) %collective-permute-start.8) | collective-permute-done | bytes 196640 | tf_op jit(solution)/shard_map/ppermute | solution.py:735
  78.9 1.8 collective-permute-start.13
  81.6 3.5 %shard_map.175.refs_4_ = f32[512,512]{1,0:T(8,128)S(1)} custom-call(s32[1]{0:T(128)} %bitcast.t_ref, bf16[512,640]{1,0:T(8,128)(2,1)} %bitcast.34, bf16[512,640]{1,0:T(8,128)(2,1)} %copy-done.1, bf16[512,640]{1,0:T(8,128)(2,1)} %copy-done.2, bf16[512,384]{1,0:T(8,128)(2,1)S(1)} %bitcast.37, bf16[256,384]{1,0:T(8,128)(2,1)S(1)} %collective-permute-done.8.refs_4_.refs_6_, ...), custom_call_target="tpu_custom_call" | custom-call | flops 1000000000 | bytes 1048576 | tf_op jit(solution)/shard_map/pallas_call | solution.py:91
  86.0 4.0 %shard_map.177 = (bf16[512,512]{1,0:T(8,128)(2,1)}, f32[512,512]{1,0:T(8,128)S(1)}, f32[512,512]{1,0:T(8,128)S(1)}) custom-call(s32[1]{0:T(128)} %bitcast.t_ref, f32[512,512]{1,0:T(8,128)} %get-tuple-element.65.refs_0_, f32[512,512]{1,0:T(8,128)} %get-tuple-element.66.refs_1_, bf16[256,640]{1,0:T(8,128)(2,1)} %copy-done.27, bf16[256,640]{1,0:T(8,128)(2,1)} %copy-done.28, ...), custom_call_target="tpu_custom_call" | custom-call | flops 2000000000 | bytes 1048576 | tf_op jit(solution)/shard_map/pallas_call | solution.py:91
  90.1 3.0 %shard_map.178 = (bf16[2,256,256]{2,1,0:T(8,128)(2,1)S(1)}, bf16[2,256,256]{2,1,0:T(8,128)(2,1)S(1)}, bf16[512,512]{1,0:T(8,128)(2,1)S(1)}, bf16[512,512]{1,0:T(8,128)(2,1)S(1)}) custom-call(s32[1]{0:T(128)} %bitcast.t_ref, bf16[256,640]{1,0:T(8,128)(2,1)} %copy-done.27, bf16[256,640]{1,0:T(8,128)(2,1)} %copy-done.28, ...), custom_call_target="tpu_custom_call" | custom-call | flops 2000000000 | bytes 1048576 | tf_op jit(solution)/shard_map/pallas_call | solution.py:91
  94.1 2.4 %collective-permute-start.18 = (bf16[2,256,256]{2,1,0:T(8,128)(2,1)S(1)}, bf16[2,256,256]{2,1,0:T(8,128)(2,1)S(1)}, u32[]{:S(2)}, u32[]{:S(2)}) collective-permute-start(bf16[2,256,256]{2,1,0:T(8,128)(2,1)S(1)} %get-tuple-element.73), channel_id=1, source_target_pairs={{0,6},{1,7},{2,0},{3,1},{4,2},{5,3},{6,4},{7,5},{8,14},{9,15},{10,... | collective-permute-start | bytes 786440 | tf_op jit(solution)/shard_map/ppermute | solution.py:735
  96.5 4.0 %shard_map.179 = (bf16[512,256]{1,0:T(8,128)(2,1)S(1)}, bf16[512,256]{1,0:T(8,128)(2,1)S(1)}, bf16[512,256]{1,0:T(8,128)(2,1)S(1)}, bf16[512,256]{1,0:T(8,128)(2...) custom-call(s32[1]{0:T(128)} %bitcast.t_ref, ...), custom_call_target="tpu_custom_call" | custom-call | flops 3000000000 | bytes 1048576 | tf_op jit(solution)/shard_map/pallas_call | solution.py:91
  101.0 5.3 %shard_map.181 = bf16[12,512,256]{2,1,0:T(8,128)(2,1)S(1)} custom-call(s32[1]{0:T(128)} %bitcast.t_ref, bf16[512,640]{1,0:T(8,128)(2,1)} %bitcast.35, bf16[512,640]{1,0:T(8,128)(2,1)} %copy-done.1, bf16[512,640]{1,0:T(8,128)(2,1)} %copy-done.2, bf16[256,640]{1,0:T(8,128)(2,1)} %copy-done.27, bf16[256,640]{1,0:T(8,128)(2,1)} %copy-done.28, ...), custom_call_target="tpu_custom_call" | custom-call | flops 2000000000 | bytes 1048576 | tf_op jit(solution)/shard_map/pallas_call | solution.py:91
  106.9 3.2 %collective-permute-start.21 = (bf16[512,256]{1,0:T(8,128)(2,1)S(1)}, bf16[512,256]{1,0:T(8,128)(2,1)S(1)}, u32[]{:S(2)}, u32[]{:S(2)}) collective-permute-start(bf16[512,256]{1,0:T(8,128)(2,1)S(1)} %get-tuple-element.84), channel_id=1, source_target_pairs={{0,6},{1,7},{2,0},{3,1},{4,2},{5,3},{6,4},{7,5},{8,14},{9,15},{10,... | collective-permute-start | bytes 786440 | tf_op jit(solution)/shard_map/ppermute | solution.py:735
  110.1 2.3 %collective-permute-done.22.refs_3_ = bf16[512,256]{1,0:T(8,128)(2,1)S(1)} collective-permute-done((bf16[512,256]{1,0:T(8,128)(2,1)S(1)}, bf16[512,256]{1,0:T(8,128)(2,1)S(1)}, u32[]{:S(2)}, u32[]{:S(2)}) %collective-permute-start.22) | collective-permute-done | bytes 262176 | tf_op jit(solution)/shard_map/ppermute | solution.py:739
  112.4 3.0 %collective-permute-start.24 = (bf16[512,256]{1,0:T(8,128)(2,1)S(1)}, bf16[512,256]{1,0:T(8,128)(2,1)S(1)}, u32[]{:S(2)}, u32[]{:S(2)}) collective-permute-start(bf16[512,256]{1,0:T(8,128)(2,1)S(1)} %get-tuple-element.87), channel_id=1, source_target_pairs={{0,7},{1,6},{2,1},{3,0},{4,3},{5,2},{6,5},{7,4},{8,15},{9,14},{10,... | collective-permute-start | bytes 786440 | tf_op jit(solution)/shard_map/ppermute | solution.py:743
  115.4 1.9 %collective-permute-done.20.refs_1_ = bf16[512,256]{1,0:T(8,128)(2,1)S(1)} collective-permute-done((bf16[512,256]{1,0:T(8,128)(2,1)S(1)}, bf16[512,256]{1,0:T(8,128)(2,1)S(1)}, u32[]{:S(2)}, u32[]{:S(2)}) %collective-permute-start.20) | collective-permute-done | bytes 262176 | tf_op jit(solution)/shard_map/ppermute | solution.py:735
  117.3 4.4 %collective-permute-done.23.refs_4_ = bf16[512,256]{1,0:T(8,128)(2,1)S(1)} collective-permute-done((bf16[512,256]{1,0:T(8,128)(2,1)S(1)}, bf16[512,256]{1,0:T(8,128)(2,1)S(1)}, u32[]{:S(2)}, u32[]{:S(2)}) %collective-permute-start.23) | collective-permute-done | bytes 262176 | tf_op jit(solution)/shard_map/ppermute | solution.py:743
  121.8 1.0 shard_map.183
  122.8 9.8 %all-to-all-start.2 = ((bf16[32,32,256]{2,1,0:T(8,128)(2,1)}), bf16[32,32,256]{2,1,0:T(8,128)(2,1)}, u32[]{:S(2)}, u32[]{:S(2)}) async-start(bf16[32,32,256]{2,1,0:T(8,128)(2,1)} %shard_map.183), calls=%async_computation.2 | async-start | bytes 1048576 | tf_op jit(solution)/shard_map/all_to_all | solution.py:761
  134.5 2.2 %shard_map.184 = (bf16[512,256]{1,0:T(8,128)(2,1)}, bf16[512,256]{1,0:T(8,128)(2,1)}, f32[512,256]{1,0:T(8,128)}, f32[512,256]{1,0:T(8,128)}, f32[8,256]{1,0:T(8,128)S(1)}) custom-call(s32[1]{0:T(128)} %bitcast.t_ref, bf16[64,2048]{1,0:T(8,128)(2,1)} %bitcast.53, bf16[64,256]{1,0:T(8,128)(2,1)S(1)} %bitcast.42, bf16[5,64,256]{2,1,0:T(8,128)(2,1)S(1)} %copy-done.13, ...), custom_call_target="tpu_custom_call" | custom-call | flops 100000000 | bytes 1048576 | tf_op jit(solution)/shard_map/pallas_call | solution.py:91
  136.7 8.9 %shard_map.182 = (f32[4,512,256]{2,1,0:T(8,128)}, f32[4,512,256]{2,1,0:T(8,128)}, f32[256,2048]{1,0:T(8,128)}) custom-call(s32[1]{0:T(128)} %bitcast.t_ref, bf16[512,640]{1,0:T(8,128)(2,1)} %bitcast.36, bf16[512,640]{1,0:T(8,128)(2,1)} %copy-done.1, bf16[512,640]{1,0:T(8,128)(2,1)} %copy-done.2, bf16[256,640]{1,0:T(8,128)(2,1)} %copy-done.27, ...), custom_call_target="tpu_custom_call" | custom-call | flops 2000000000 | bytes 1048576 | tf_op jit(solution)/shard_map/pallas_call | solution.py:91
  145.6 1.4 all-to-all-done.2
  147.0 3.3 %shard_map.185 = (bf16[256,256]{1,0:T(8,128)(2,1)}, bf16[32,32,128]{2,1,0:T(8,128)(2,1)}, f32[4,72,256]{2,1,0:T(8,128)S(1)}, bf16[4,72,256]{2,1,0:T(8,128)(2,1)S(1)}) custom-call(s32[1]{0:T(128)} %bitcast.t_ref, bf16[256,1024]{1,0:T(8,128)(2,1)} %get-tuple-element.81.refs_0_, bf16[256,2048]{1,0:T(8,128)(2,1)} %refs_1_.3, bf16[1024,256]{1,0:T(8,128)(2,1)} %bitcast.22.refs_2_, ...), custom_call_target="tpu_custom_call" | custom-call | flops 1000000000 | bytes 1048576 | tf_op jit(solution)/shard_map/pallas_call | solution.py:91
  150.3 8.6 %all-to-all-start.3 = ((bf16[32,32,128]{2,1,0:T(8,128)(2,1)}), bf16[32,32,128]{2,1,0:T(8,128)(2,1)S(1)}, u32[]{:S(2)}, u32[]{:S(2)}) async-start(bf16[32,32,128]{2,1,0:T(8,128)(2,1)} %get-tuple-element.104), calls=%async_computation.3 | async-start | bytes 524288 | tf_op jit(solution)/shard_map/all_to_all | solution.py:761
  159.0 1.4 collective-permute-done.25.refs_1_
  160.4 1.2 collective-permute-start.26
  161.6 3.5 %collective-permute-start.27 = (bf16[72,256]{1,0:T(8,128)(2,1)S(1)}, bf16[72,256]{1,0:T(8,128)(2,1)S(1)}, u32[]{:S(2)}, u32[]{:S(2)}) collective-permute-start(bf16[72,256]{1,0:T(8,128)(2,1)S(1)} %get-tuple-element.97), channel_id=1, source_target_pairs={{0,4},{1,5},{2,6},{3,7},{4,0},{5,1},{6,2},{7,3},{8,12},{9,13},{10,... | collective-permute-start | bytes 110600 | tf_op jit(solution)/shard_map/ppermute | solution.py:739
  165.2 2.3 %collective-permute-done.27.refs_2_ = bf16[72,256]{1,0:T(8,128)(2,1)S(1)} collective-permute-done((bf16[72,256]{1,0:T(8,128)(2,1)S(1)}, bf16[72,256]{1,0:T(8,128)(2,1)S(1)}, u32[]{:S(2)}, u32[]{:S(2)}) %collective-permute-start.27) | collective-permute-done | bytes 36896 | tf_op jit(solution)/shard_map/ppermute | solution.py:739
  167.5 2.8 %collective-permute-done.28.refs_3_ = bf16[72,256]{1,0:T(8,128)(2,1)S(1)} collective-permute-done((bf16[72,256]{1,0:T(8,128)(2,1)S(1)}, bf16[72,256]{1,0:T(8,128)(2,1)S(1)}, u32[]{:S(2)}, u32[]{:S(2)}) %collective-permute-start.28) | collective-permute-done | bytes 36896 | tf_op jit(solution)/shard_map/ppermute | solution.py:739
  170.4 4.6 %collective-permute-start.29 = (f32[64,128]{1,0:T(8,128)S(1)}, f32[64,128]{1,0:T(8,128)S(1)}, u32[]{:S(2)}, u32[]{:S(2)}) collective-permute-start(f32[64,128]{1,0:T(8,128)S(1)} %get-tuple-element.101), channel_id=1, source_target_pairs={{8,0},{16,8},{24,16},{32,24},{40,32},{48,40},{56,48},{64,56},{72,6... | collective-permute-start | bytes 98312 | tf_op jit(solution)/shard_map/ppermute | solution.py:822
  175.2 1.9 %collective-permute-start.30 = (f32[64,64]{1,0:T(8,128)S(1)}, f32[64,64]{1,0:T(8,128)S(1)}, u32[]{:S(2)}, u32[]{:S(2)}) collective-permute-start(f32[64,64]{1,0:T(8,128)S(1)} %shard_map.190), channel_id=1, source_target_pairs={{0,0},{1,32},{2,64},{3,96},{4,128},{5,160},{6,192},{7,224},{32,1},... | collective-permute-start | bytes 49160 | tf_op jit(solution)/shard_map/ppermute | solution.py:826
  177.1 1.0 shard_map.188.refs_0_
  178.1 1.4 shard_map.189
  179.5 7.8 %collective-permute-done.30 = f32[64,64]{1,0:T(8,128)S(1)} collective-permute-done((f32[64,64]{1,0:T(8,128)S(1)}, f32[64,64]{1,0:T(8,128)S(1)}, u32[]{:S(2)}, u32[]{:S(2)}) %collective-permute-start.30) | collective-permute-done | bytes 16416 | tf_op jit(solution)/shard_map/ppermute | solution.py:826
  (107 shorter events, 15.0 us)
Async XLA Ops:
  2.0 12.6 %copy-start.14 = (bf16[256,64]{0,1:T(8,128)(2,1)S(1)}, bf16[256,64]{0,1:T(8,128)(2,1)}, u32[]{:S(2)}) copy-start(bf16[256,64]{0,1:T(8,128)(2,1)} %param.19) | copy-start | bytes 98308
  2.0 21.4 %copy-start.26 = (f32[256,2]{0,1:T(2,128)S(1)}, f32[256,2]{0,1:T(2,128)}, u32[]{:S(2)}) copy-start(f32[256,2]{0,1:T(2,128)} %param.15) | copy-start | bytes 6148
  4.7 27.8 %all-to-all-start = ((bf16[32,16,640]{2,1,0:T(8,128)(2,1)}), bf16[32,16,640]{2,1,0:T(8,128)(2,1)S(1)}, u32[]{:S(2)}, u32[]{:S(2)}) async-start(bf16[32,16,640]{2,1,0:T(8,128)(2,1)} %bitcast.54), calls=%async_computation | async-start | bytes 1310720 | tf_op jit(solution)/shard_map/all_to_all | solution.py:761
  15.6 1.5 collective-permute-start.4
  18.7 7.1 %collective-permute-start.5 = (bf16[4,64,256]{2,1,0:T(8,128)(2,1)S(1)}, bf16[4,64,256]{2,1,0:T(8,128)(2,1)S(1)}, u32[]{:S(2)}, u32[]{:S(2)}) collective-permute-start(bf16[4,64,256]{2,1,0:T(8,128)(2,1)S(1)} %get-tuple-element.61), channel_id=1, source_target_pairs={{0,2},{1,3},{2,0},{3,1},{4,6},{5,7},{6,4},{7,5},{8,10},{9,11},{10,... | collective-permute-start | bytes 393224 | tf_op jit(solution)/shard_map/ppermute | solution.py:739
  20.3 9.3 %collective-permute-start.6 = (bf16[4,64,256]{2,1,0:T(8,128)(2,1)S(1)}, bf16[4,64,256]{2,1,0:T(8,128)(2,1)S(1)}, u32[]{:S(2)}, u32[]{:S(2)}) collective-permute-start(bf16[4,64,256]{2,1,0:T(8,128)(2,1)S(1)} %get-tuple-element.62), channel_id=1, source_target_pairs={{0,4},{1,5},{2,6},{3,7},{4,0},{5,1},{6,2},{7,3},{8,12},{9,13},{10,... | collective-permute-start | bytes 393224 | tf_op jit(solution)/shard_map/ppermute | solution.py:739
  23.2 8.7 %collective-permute-start.7 = (bf16[4,64,256]{2,1,0:T(8,128)(2,1)S(1)}, bf16[4,64,256]{2,1,0:T(8,128)(2,1)S(1)}, u32[]{:S(2)}, u32[]{:S(2)}) collective-permute-start(bf16[4,64,256]{2,1,0:T(8,128)(2,1)S(1)} %get-tuple-element.63), channel_id=1, source_target_pairs={{0,6},{1,7},{2,4},{3,5},{4,2},{5,3},{6,0},{7,1},{8,14},{9,15},{10,... | collective-permute-start | bytes 393224 | tf_op jit(solution)/shard_map/ppermute | solution.py:739
  32.5 42.7 %copy-start = (bf16[32,16,640]{2,1,0:T(8,128)(2,1)}, bf16[32,16,640]{2,1,0:T(8,128)(2,1)S(1)}, u32[]{:S(2)}) copy-start(bf16[32,16,640]{2,1,0:T(8,128)(2,1)S(1)} %all-to-all-done) | copy-start | bytes 1966084
  32.5 20.6 %all-to-all-start.1 = ((bf16[32,16,384]{2,1,0:T(8,128)(2,1)}), bf16[32,16,384]{2,1,0:T(8,128)(2,1)S(1)}, u32[]{:S(2)}, u32[]{:S(2)}) async-start(bf16[32,16,384]{2,1,0:T(8,128)(2,1)} %bitcast.55), calls=%async_computation.1 | async-start | bytes 786432 | tf_op jit(solution)/shard_map/all_to_all | solution.py:761
  42.3 21.2 %collective-permute-start.15 = (bf16[2048,256]{1,0:T(8,128)(2,1)}, bf16[2048,256]{1,0:T(8,128)(2,1)}, u32[]{:S(2)}, u32[]{:S(2)}) collective-permute-start(bf16[2048,256]{1,0:T(8,128)(2,1)} %bitcast.13), channel_id=1, source_target_pairs={{0,1},{1,0},{2,3},{3,2},{4,5},{5,4},{6,7},{7,6},{8,9},{9,8},{10,11... | collective-permute-start | bytes 3145736 | tf_op jit(solution)/shard_map/ppermute | solution.py:739
  42.4 22.4 %collective-permute-start.16 = (bf16[2048,256]{1,0:T(8,128)(2,1)}, bf16[2048,256]{1,0:T(8,128)(2,1)}, u32[]{:S(2)}, u32[]{:S(2)}) collective-permute-start(bf16[2048,256]{1,0:T(8,128)(2,1)} %bitcast.16), channel_id=1, source_target_pairs={{0,1},{1,0},{2,3},{3,2},{4,5},{5,4},{6,7},{7,6},{8,9},{9,8},{10,11... | collective-permute-start | bytes 3145736 | tf_op jit(solution)/shard_map/ppermute | solution.py:739
  42.9 22.7 %collective-permute-start.14 = (bf16[256,2048]{1,0:T(8,128)(2,1)}, bf16[256,2048]{1,0:T(8,128)(2,1)}, u32[]{:S(2)}, u32[]{:S(2)}) collective-permute-start(bf16[256,2048]{1,0:T(8,128)(2,1)} %bitcast.11.refs_8_.refs_7_), channel_id=1, source_target_pairs={{0,1},{1,0},{2,3},{3,2},{4,5},{5,4},{6,7},{7,6},{8,9},{9,8},{10,11... | collective-permute-start | bytes 3145736 | tf_op jit(solution)/shard_map/ppermute | solution.py:739
  43.0 18.3 %collective-permute-start = (bf16[512,640]{1,0:T(8,128)(2,1)S(1)}, bf16[512,640]{1,0:T(8,128)(2,1)S(1)}, u32[]{:S(2)}, u32[]{:S(2)}) collective-permute-start(bf16[512,640]{1,0:T(8,128)(2,1)S(1)} %bitcast.31), channel_id=1, source_target_pairs={{0,2},{1,3},{2,4},{3,5},{4,6},{5,7},{6,0},{7,1},{8,10},{9,11},{10,... | collective-permute-start | bytes 1966088 | tf_op jit(solution)/shard_map/ppermute | solution.py:735
  43.0 18.3 %collective-permute-start.1 = (bf16[512,640]{1,0:T(8,128)(2,1)S(1)}, bf16[512,640]{1,0:T(8,128)(2,1)S(1)}, u32[]{:S(2)}, u32[]{:S(2)}) collective-permute-start(bf16[512,640]{1,0:T(8,128)(2,1)S(1)} %bitcast.32), channel_id=1, source_target_pairs={{0,6},{1,7},{2,0},{3,1},{4,2},{5,3},{6,4},{7,5},{8,14},{9,15},{10,... | collective-permute-start | bytes 1966088 | tf_op jit(solution)/shard_map/ppermute | solution.py:735
  53.1 28.5 %copy-start.3 = (bf16[32,16,384]{2,1,0:T(8,128)(2,1)}, bf16[32,16,384]{2,1,0:T(8,128)(2,1)S(1)}, u32[]{:S(2)}) copy-start(bf16[32,16,384]{2,1,0:T(8,128)(2,1)S(1)} %all-to-all-done.1) | copy-start | bytes 1179652
  61.3 13.9 %copy-start.1 = (bf16[512,640]{1,0:T(8,128)(2,1)}, bf16[512,640]{1,0:T(8,128)(2,1)S(1)}, u32[]{:S(2)}) copy-start(bf16[512,640]{1,0:T(8,128)(2,1)S(1)} %collective-permute-done.refs_1_) | copy-start | bytes 1966084
  61.3 7.8 %collective-permute-start.10 = (bf16[256,384]{1,0:T(8,128)(2,1)S(1)}, bf16[256,384]{1,0:T(8,128)(2,1)S(1)}, u32[]{:S(2)}, u32[]{:S(2)}) collective-permute-start(bf16[256,384]{1,0:T(8,128)(2,1)S(1)} %bitcast.58), channel_id=1, source_target_pairs={{0,6},{1,7},{2,0},{3,1},{4,2},{5,3},{6,4},{7,5},{8,14},{9,15},{10,... | collective-permute-start | bytes 589832 | tf_op jit(solution)/shard_map/ppermute | solution.py:735
  61.3 13.9 %copy-start.2 = (bf16[512,640]{1,0:T(8,128)(2,1)}, bf16[512,640]{1,0:T(8,128)(2,1)S(1)}, u32[]{:S(2)}) copy-start(bf16[512,640]{1,0:T(8,128)(2,1)S(1)} %collective-permute-done.1.refs_2_) | copy-start | bytes 1966084
  61.3 23.9 %collective-permute-start.2 = (bf16[256,640]{1,0:T(8,128)(2,1)S(1)}, bf16[256,640]{1,0:T(8,128)(2,1)S(1)}, u32[]{:S(2)}, u32[]{:S(2)}) collective-permute-start(bf16[256,640]{1,0:T(8,128)(2,1)S(1)} %slice.24), channel_id=1, source_target_pairs={{0,2},{1,3},{2,4},{3,5},{4,6},{5,7},{6,0},{7,1},{8,10},{9,11},{10,... | collective-permute-start | bytes 983048 | tf_op jit(solution)/shard_map/ppermute | solution.py:735
  63.5 21.8 %collective-permute-start.3 = (bf16[256,640]{1,0:T(8,128)(2,1)S(1)}, bf16[256,640]{1,0:T(8,128)(2,1)S(1)}, u32[]{:S(2)}, u32[]{:S(2)}) collective-permute-start(bf16[256,640]{1,0:T(8,128)(2,1)S(1)} %slice.25), channel_id=1, source_target_pairs={{0,6},{1,7},{2,0},{3,1},{4,2},{5,3},{6,4},{7,5},{8,14},{9,15},{10,... | collective-permute-start | bytes 983048 | tf_op jit(solution)/shard_map/ppermute | solution.py:735
  64.8 12.6 %collective-permute-start.8 = (bf16[256,384]{1,0:T(8,128)(2,1)S(1)}, bf16[256,384]{1,0:T(8,128)(2,1)S(1)}, u32[]{:S(2)}, u32[]{:S(2)}) collective-permute-start(bf16[256,384]{1,0:T(8,128)(2,1)S(1)} %bitcast.59), channel_id=1, source_target_pairs={{0,2},{1,3},{2,4},{3,5},{4,6},{5,7},{6,0},{7,1},{8,10},{9,11},{10,... | collective-permute-start | bytes 589832 | tf_op jit(solution)/shard_map/ppermute | solution.py:735
  65.6 13.3 %collective-permute-start.11 = (bf16[256,384]{1,0:T(8,128)(2,1)S(1)}, bf16[256,384]{1,0:T(8,128)(2,1)S(1)}, u32[]{:S(2)}, u32[]{:S(2)}) collective-permute-start(bf16[256,384]{1,0:T(8,128)(2,1)S(1)} %bitcast.56), channel_id=1, source_target_pairs={{0,6},{1,7},{2,0},{3,1},{4,2},{5,3},{6,4},{7,5},{8,14},{9,15},{10,... | collective-permute-start | bytes 589832 | tf_op jit(solution)/shard_map/ppermute | solution.py:735
  69.0 12.6 %copy-start.6 = (bf16[256,384]{1,0:T(8,128)(2,1)}, bf16[256,384]{1,0:T(8,128)(2,1)S(1)}, u32[]{:S(2)}) copy-start(bf16[256,384]{1,0:T(8,128)(2,1)S(1)} %collective-permute-done.10.refs_6_.refs_8_) | copy-start | bytes 589828
  69.0 12.6 %collective-permute-start.9 = (bf16[256,384]{1,0:T(8,128)(2,1)S(1)}, bf16[256,384]{1,0:T(8,128)(2,1)S(1)}, u32[]{:S(2)}, u32[]{:S(2)}) collective-permute-start(bf16[256,384]{1,0:T(8,128)(2,1)S(1)} %bitcast.57), channel_id=1, source_target_pairs={{0,2},{1,3},{2,4},{3,5},{4,6},{5,7},{6,0},{7,1},{8,10},{9,11},{10,... | collective-permute-start | bytes 589832 | tf_op jit(solution)/shard_map/ppermute | solution.py:735
  77.4 12.7 %collective-permute-start.12 = (bf16[256,384]{1,0:T(8,128)(2,1)S(1)}, bf16[256,384]{1,0:T(8,128)(2,1)S(1)}, u32[]{:S(2)}, u32[]{:S(2)}) collective-permute-start(bf16[256,384]{1,0:T(8,128)(2,1)S(1)} %collective-permute-done.8.refs_4_.refs_6_), channel_id=1, source_target_pairs={{0,2},{1,3},{2,4},{3,5},{4,6},{5,7},{6,0},{7,1},{8,10},{9,11},{10,... | collective-permute-start | bytes 589832 | tf_op jit(solution)/shard_map/ppermute | solution.py:735
  78.9 11.3 %collective-permute-start.13 = (bf16[256,384]{1,0:T(8,128)(2,1)S(1)}, bf16[256,384]{1,0:T(8,128)(2,1)S(1)}, u32[]{:S(2)}, u32[]{:S(2)}) collective-permute-start(bf16[256,384]{1,0:T(8,128)(2,1)S(1)} %collective-permute-done.11.refs_7_.refs_9_), channel_id=1, source_target_pairs={{0,6},{1,7},{2,0},{3,1},{4,2},{5,3},{6,4},{7,5},{8,14},{9,15},{10,... | collective-permute-start | bytes 589832 | tf_op jit(solution)/shard_map/ppermute | solution.py:735
  93.2 7.7 %collective-permute-start.17 = (bf16[2,256,256]{2,1,0:T(8,128)(2,1)S(1)}, bf16[2,256,256]{2,1,0:T(8,128)(2,1)S(1)}, u32[]{:S(2)}, u32[]{:S(2)}) collective-permute-start(bf16[2,256,256]{2,1,0:T(8,128)(2,1)S(1)} %get-tuple-element.72), channel_id=1, source_target_pairs={{0,2},{1,3},{2,4},{3,5},{4,6},{5,7},{6,0},{7,1},{8,10},{9,11},{10,... | collective-permute-start | bytes 786440 | tf_op jit(solution)/shard_map/ppermute | solution.py:735
  94.1 6.8 %collective-permute-start.18 = (bf16[2,256,256]{2,1,0:T(8,128)(2,1)S(1)}, bf16[2,256,256]{2,1,0:T(8,128)(2,1)S(1)}, u32[]{:S(2)}, u32[]{:S(2)}) collective-permute-start(bf16[2,256,256]{2,1,0:T(8,128)(2,1)S(1)} %get-tuple-element.73), channel_id=1, source_target_pairs={{0,6},{1,7},{2,0},{3,1},{4,2},{5,3},{6,4},{7,5},{8,14},{9,15},{10,... | collective-permute-start | bytes 786440 | tf_op jit(solution)/shard_map/ppermute | solution.py:735
  106.3 26.4 %copy-start.13 = (bf16[5,64,256]{2,1,0:T(8,128)(2,1)S(1)}, bf16[5,64,256]{2,1,0:T(8,128)(2,1)}, u32[]{:S(2)}) copy-start(bf16[5,64,256]{2,1,0:T(8,128)(2,1)} %copy-done.12) | copy-start | bytes 491524
  106.3 26.4 %copy-start.15 = (bf16[256,64]{0,1:T(8,128)(2,1)S(1)}, bf16[256,64]{0,1:T(8,128)(2,1)}, u32[]{:S(2)}) copy-start(bf16[256,64]{0,1:T(8,128)(2,1)} %param.19) | copy-start | bytes 98308
  106.3 26.4 %copy-start.17 = (bf16[4,64,256]{2,1,0:T(8,128)(2,1)S(1)}, bf16[4,64,256]{2,1,0:T(8,128)(2,1)}, u32[]{:S(2)}) copy-start(bf16[4,64,256]{2,1,0:T(8,128)(2,1)} %copy-done.16) | copy-start | bytes 393220
  106.3 30.4 %collective-permute-start.19 = (bf16[12,512,256]{2,1,0:T(8,128)(2,1)S(1)}, bf16[12,512,256]{2,1,0:T(8,128)(2,1)}, u32[]{:S(2)}, u32[]{:S(2)}) collective-permute-start(bf16[12,512,256]{2,1,0:T(8,128)(2,1)S(1)} %shard_map.181), channel_id=1, source_target_pairs={{0,1},{1,0},{2,3},{3,2},{4,5},{5,4},{6,7},{7,6},{8,9},{9,8},{10,11... | collective-permute-start | bytes 9437192 | tf_op jit(solution)/shard_map/ppermute | solution.py:739
  106.4 6.0 %collective-permute-start.22 = (bf16[512,256]{1,0:T(8,128)(2,1)S(1)}, bf16[512,256]{1,0:T(8,128)(2,1)S(1)}, u32[]{:S(2)}, u32[]{:S(2)}) collective-permute-start(bf16[512,256]{1,0:T(8,128)(2,1)S(1)} %get-tuple-element.85), channel_id=1, source_target_pairs={{0,1},{1,0},{2,3},{3,2},{4,5},{5,4},{6,7},{7,6},{8,9},{9,8},{10,11... | collective-permute-start | bytes 786440 | tf_op jit(solution)/shard_map/ppermute | solution.py:739
  106.9 10.4 %collective-permute-start.20 = (bf16[512,256]{1,0:T(8,128)(2,1)S(1)}, bf16[512,256]{1,0:T(8,128)(2,1)S(1)}, u32[]{:S(2)}, u32[]{:S(2)}) collective-permute-start(bf16[512,256]{1,0:T(8,128)(2,1)S(1)} %get-tuple-element.78), channel_id=1, source_target_pairs={{0,2},{1,3},{2,4},{3,5},{4,6},{5,7},{6,0},{7,1},{8,10},{9,11},{10,... | collective-permute-start | bytes 786440 | tf_op jit(solution)/shard_map/ppermute | solution.py:735
  106.9 10.4 %collective-permute-start.21 = (bf16[512,256]{1,0:T(8,128)(2,1)S(1)}, bf16[512,256]{1,0:T(8,128)(2,1)S(1)}, u32[]{:S(2)}, u32[]{:S(2)}) collective-permute-start(bf16[512,256]{1,0:T(8,128)(2,1)S(1)} %get-tuple-element.84), channel_id=1, source_target_pairs={{0,6},{1,7},{2,0},{3,1},{4,2},{5,3},{6,4},{7,5},{8,14},{9,15},{10,... | collective-permute-start | bytes 786440 | tf_op jit(solution)/shard_map/ppermute | solution.py:735
  110.1 11.6 %collective-permute-start.23 = (bf16[512,256]{1,0:T(8,128)(2,1)S(1)}, bf16[512,256]{1,0:T(8,128)(2,1)S(1)}, u32[]{:S(2)}, u32[]{:S(2)}) collective-permute-start(bf16[512,256]{1,0:T(8,128)(2,1)S(1)} %get-tuple-element.86), channel_id=1, source_target_pairs={{0,3},{1,2},{2,5},{3,4},{4,7},{5,6},{6,1},{7,0},{8,11},{9,10},{10,... | collective-permute-start | bytes 786440 | tf_op jit(solution)/shard_map/ppermute | solution.py:743
  112.4 9.4 %collective-permute-start.24 = (bf16[512,256]{1,0:T(8,128)(2,1)S(1)}, bf16[512,256]{1,0:T(8,128)(2,1)S(1)}, u32[]{:S(2)}, u32[]{:S(2)}) collective-permute-start(bf16[512,256]{1,0:T(8,128)(2,1)S(1)} %get-tuple-element.87), channel_id=1, source_target_pairs={{0,7},{1,6},{2,1},{3,0},{4,3},{5,2},{6,5},{7,4},{8,15},{9,14},{10,... | collective-permute-start | bytes 786440 | tf_op jit(solution)/shard_map/ppermute | solution.py:743
  122.8 24.2 %all-to-all-start.2 = ((bf16[32,32,256]{2,1,0:T(8,128)(2,1)}), bf16[32,32,256]{2,1,0:T(8,128)(2,1)}, u32[]{:S(2)}, u32[]{:S(2)}) async-start(bf16[32,32,256]{2,1,0:T(8,128)(2,1)} %shard_map.183), calls=%async_computation.2 | async-start | bytes 1048576 | tf_op jit(solution)/shard_map/all_to_all | solution.py:761
  147.0 27.9 %copy-start.29 = (f32[31,64]{1,0:T(8,128)S(1)}, f32[31,64]{1,0:T(8,128)}, u32[]{:S(2)}) copy-start(f32[31,64]{1,0:T(8,128)} %param.18) | copy-start | bytes 23812
  147.0 31.1 %copy-start.22 = (bf16[256,64]{0,1:T(8,128)(2,1)S(1)}, bf16[256,64]{0,1:T(8,128)(2,1)}, u32[]{:S(2)}) copy-start(bf16[256,64]{0,1:T(8,128)(2,1)} %param.16) | copy-start | bytes 98308
  147.0 31.1 %copy-start.23 = (bf16[256,64]{0,1:T(8,128)(2,1)S(1)}, bf16[256,64]{0,1:T(8,128)(2,1)}, u32[]{:S(2)}) copy-start(bf16[256,64]{0,1:T(8,128)(2,1)} %param.17) | copy-start | bytes 98308
  150.3 24.8 %all-to-all-start.3 = ((bf16[32,32,128]{2,1,0:T(8,128)(2,1)}), bf16[32,32,128]{2,1,0:T(8,128)(2,1)S(1)}, u32[]{:S(2)}, u32[]{:S(2)}) async-start(bf16[32,32,128]{2,1,0:T(8,128)(2,1)} %get-tuple-element.104), calls=%async_computation.3 | async-start | bytes 524288 | tf_op jit(solution)/shard_map/all_to_all | solution.py:761
  158.9 1.5 collective-permute-start.25
  160.4 4.8 %collective-permute-start.26 = (bf16[72,256]{1,0:T(8,128)(2,1)S(1)}, bf16[72,256]{1,0:T(8,128)(2,1)S(1)}, u32[]{:S(2)}, u32[]{:S(2)}) collective-permute-start(bf16[72,256]{1,0:T(8,128)(2,1)S(1)} %get-tuple-element.96), channel_id=1, source_target_pairs={{0,2},{1,3},{2,0},{3,1},{4,6},{5,7},{6,4},{7,5},{8,10},{9,11},{10,... | collective-permute-start | bytes 110600 | tf_op jit(solution)/shard_map/ppermute | solution.py:739
  161.6 5.9 %collective-permute-start.27 = (bf16[72,256]{1,0:T(8,128)(2,1)S(1)}, bf16[72,256]{1,0:T(8,128)(2,1)S(1)}, u32[]{:S(2)}, u32[]{:S(2)}) collective-permute-start(bf16[72,256]{1,0:T(8,128)(2,1)S(1)} %get-tuple-element.97), channel_id=1, source_target_pairs={{0,4},{1,5},{2,6},{3,7},{4,0},{5,1},{6,2},{7,3},{8,12},{9,13},{10,... | collective-permute-start | bytes 110600 | tf_op jit(solution)/shard_map/ppermute | solution.py:739
  165.1 5.2 %collective-permute-start.28 = (bf16[72,256]{1,0:T(8,128)(2,1)S(1)}, bf16[72,256]{1,0:T(8,128)(2,1)S(1)}, u32[]{:S(2)}, u32[]{:S(2)}) collective-permute-start(bf16[72,256]{1,0:T(8,128)(2,1)S(1)} %get-tuple-element.98), channel_id=1, source_target_pairs={{0,6},{1,7},{2,4},{3,5},{4,2},{5,3},{6,0},{7,1},{8,14},{9,15},{10,... | collective-permute-start | bytes 110600 | tf_op jit(solution)/shard_map/ppermute | solution.py:739
  170.4 7.7 %collective-permute-start.29 = (f32[64,128]{1,0:T(8,128)S(1)}, f32[64,128]{1,0:T(8,128)S(1)}, u32[]{:S(2)}, u32[]{:S(2)}) collective-permute-start(f32[64,128]{1,0:T(8,128)S(1)} %get-tuple-element.101), channel_id=1, source_target_pairs={{8,0},{16,8},{24,16},{32,24},{40,32},{48,40},{56,48},{64,56},{72,6... | collective-permute-start | bytes 98312 | tf_op jit(solution)/shard_map/ppermute | solution.py:822
  175.2 12.1 %collective-permute-start.30 = (f32[64,64]{1,0:T(8,128)S(1)}, f32[64,64]{1,0:T(8,128)S(1)}, u32[]{:S(2)}, u32[]{:S(2)}) collective-permute-start(f32[64,64]{1,0:T(8,128)S(1)} %shard_map.190), channel_id=1, source_target_pairs={{0,0},{1,32},{2,64},{3,96},{4,128},{5,160},{6,192},{7,224},{32,1},... | collective-permute-start | bytes 49160 | tf_op jit(solution)/shard_map/ppermute | solution.py:826
  (17 other events, 45.8 us)

commit v6 on v2

--- a/solution.py
+++ b/solution.py
@@ -170,30 +170,44 @@
     return y, (y + 3) % 4, (y + 1) % 4, (y + 2) % 4
 
 
-def joined(refs):
-    refs = [now(r)[...] for r in refs]
-    own, sides, far = refs[0], refs[1:-2], jnp.concatenate(refs[-2:], axis=0)
-    if len(sides) == 4:
-        sides = [jnp.concatenate(sides[0:2], axis=0), jnp.concatenate(sides[2:4], axis=0)]
-    return own, *sides, far
+def first_body(t, ins, outs, scr):
+    q = quarters(t)
+    x = [ref[:, 0:512] for ref in ins[0:3]]
+    for j in range(2):
+        cols = slice(256 * j, 256 * j + 256)
+        for out, at in ((outs[0], 3), (outs[1], 5)):
+            w = now(ins[at + j])
+            out[:, cols] = sum(dot(x[i], w[q[i]]) for i in range(3))
+
+
+def first(tp, near_blocks, weights):
+    return call(
+        first_body,
+        (pltpu.HBM((ROWS, 512), F32),) * 2,
+        tp,
+        (*near_blocks, *weights),
+        staged=(3, 5, 4, 6),
+        flops=10**9,
+        limit=32,
+    )
 
 
 def forward_body(t, ins, outs, scr):
     act_ref, a1_ref, a2_ref = outs
     pg, pu = scr
-    q = quarters(t)
-    x = joined(ins[0:5])
+    top, bottom = now(ins[2])[...], now(ins[3])[...]
     for j in range(2):
         cols = slice(256 * j, 256 * j + 256)
-        g = now(ins[5 + j])
-        pg[:, cols] = sum(dot(x[i], g[q[i]]) for i in range(4))
-        u = now(ins[7 + j])
-        pu[:, cols] = sum(dot(x[i], u[q[i]]) for i in range(4))
+        for into, at in ((pg, 4), (pu, 6)):
+            w = now(ins[at + j])[0]
+            into[0:256, cols] = dot(top, w)
+            into[256:512, cols] = dot(bottom, w)
+    gate_near, up_near = now(ins[0]), now(ins[1])
 
     @pl.loop(0, ROWS // 32)
     def _(i):
         at = pl.ds(pl.multiple_of(i * 32, 32), 32)
-        gate_pre, up_pre = pg[at, :], pu[at, :]
+        gate_pre, up_pre = gate_near[at, :] + pg[at, :], up_near[at, :] + pu[at, :]
         capped = jnp.minimum(gate_pre, CLAMP)
         clipped = jnp.clip(up_pre, -CLAMP, CLAMP)
         sig = jax.nn.sigmoid(ALPHA * capped)
@@ -204,15 +218,19 @@
         a2_ref[at, :] = jnp.where(jnp.abs(up_pre) < CLAMP, gated, 0.0)
 
 
-def forward(tp, blocks, weights):
+def forward(tp, sums, far_blocks, weights):
+    rows = ((256, 512), lambda t: (slice(None), pl.ds(0, 512)))
+    quarter = ((1, 512, 256), lambda t: (pl.ds((t // 2 + 2) % 4, 1),))
     return call(
         forward_body,
-        (shape((ROWS, 512), BF), shape((ROWS, 512), F32), shape((ROWS, 512), F32)),
-        tp,
-        (*blocks, *weights),
-        staged=(5, 3, 4, 7, 6, 8),
+        (pltpu.HBM((ROWS, 512), BF), shape((ROWS, 512), F32), shape((ROWS, 512), F32)),
+        tp,
+        (*sums, *far_blocks, *weights),
+        staged=(2, 3, 4, 6, 5, 7, 0, 1),
+        cuts={2: rows, 3: rows} | {i: quarter for i in range(4, 8)},
         scratch=[pltpu.VMEM((ROWS, 512), F32)] * 2,
         flops=2 * 10**9,
+        limit=32,
     )
 
 
@@ -725,7 +743,8 @@
     xs = around(rows_in)
     by_quarter = [w.reshape(4, 512, 256) for w in (gate_own, gate_par, up_own, up_par)]
     by_piece = [w.reshape(8, 256, 256) for w in (gate_own, gate_par, up_own, up_par)]
-    act, a1, a2 = forward(tp, xs, by_quarter)
+    sums = first(tp, xs[:3], by_quarter)
+    act, a1, a2 = forward(tp, sums, xs[3:], by_quarter)
 
     cs = around_in_halves(cot_in)
     downs = (down_own, down_par)

time: 186 us -> 183 us (0.984)
  waiting for transfers between devices: 54.2 us -> 45.6 us
  Pallas kernels: 47.3 us -> 50.3 us
  starting transfers between devices: 76.5 us -> 79.4 us
    ppermute x14, waiting for transfers between devices: 15.7 us -> 7.16 us  [moved(): return lax.ppermute(x, 'tp', [(i, (i + by) % TP) for i in range(TP)])]
    pallas_call x19 -> x20, Pallas kernels: 47.3 us -> 50.3 us  [call(): pl.pallas_call(kernel, out_shape=outs, in_specs=[SMEM] + [HBM if i in sta...]
    ppermute x14, starting transfers between devices: 17.2 us -> 20.2 us  [moved(): return lax.ppermute(x, 'tp', [(i, (i + by) % TP) for i in range(TP)])]
    unnamed x62 -> x60, local copies, waits for them, and re-layouts: 5.61 us -> 5.61 us
  transfers between devices with their start and end apart: 35 -> 35, of which waited for: 19 -> 16; matrix products, arithmetic and copies ran while one was open for 0% -> 0% of each run, Pallas kernels for 18% -> 20%
where the time goes in v6:
time: 183 us; the launch traced here: 182 us
  starting transfers between devices  79.4 us (43%)
  Pallas kernels  50.3 us (27%)
  waiting for transfers between devices  45.6 us (25%)
  local copies, waits for them, and re-layouts  5.68 us (3%)
    pallas_call x20, Pallas kernels, call(): pl.pallas_call(kernel, out_shape=outs, in_specs=[SMEM] + [HBM if i in sta...  50.3 us
    all_to_all x4, starting transfers between devices, exchange(): return lax.all_to_all(x, 'sp', 0, 0, tiled=True)  38.7 us
    ppermute x14, starting transfers between devices, moved(): return lax.ppermute(x, 'tp', [(i, (i + by) % TP) for i in range(TP)])  20.2 us
    ppermute x13, waiting for transfers between devices, swapped(): return lax.ppermute(x, 'tp', [(i, i ^ by) for i in range(TP)])  16 us
    ppermute x13, starting transfers between devices, swapped(): return lax.ppermute(x, 'tp', [(i, i ^ by) for i in range(TP)])  11.1 us
    all_to_all x4, waiting for transfers between devices, exchange(): return lax.all_to_all(x, 'sp', 0, 0, tiled=True)  10.1 us
    ppermute x1, waiting for transfers between devices, step(): lax.ppermute(total(tp, outer_in), ('sp', 'tp'), [((4 * u + i) * TP + t, (...  7.81 us
    ppermute x14, waiting for transfers between devices, moved(): return lax.ppermute(x, 'tp', [(i, (i + by) % TP) for i in range(TP)])  7.16 us
  transfers between devices with their start and end apart: 35, of which 16 were waited for; matrix products, arithmetic and copies ran while one was open for 0% of the time, Pallas kernels for 20%

profile of v6, /device:TPU:128, one launch (start us, length us, event | category | flops | bytes accessed | tf_op | source)
XLA Modules:
  0.0 182.2 jit_solution(9212630534579421788)
XLA Ops:
  1.3 2.1 %shard_map.171 = (bf16[512,512]{1,0:T(8,128)(2,1)}, s32[8,256]{1,0:T(8,128)S(1)}) custom-call(s32[1]{0:T(128)} %bitcast.t_ref, s32[2,256]{1,0:T(2,128)S(1)} %bitcast.47, bf16[256,2048]{1,0:T(8,128)(2,1)} %refs_1_.2), custom_call_target="tpu_custom_call" | custom-call | flops 1000000000 | bytes 1048576 | tf_op jit(solution)/shard_map/pallas_call | solution.py:81
  3.4 9.9 %all-to-all-start = ((bf16[32,16,512]{2,1,0:T(8,128)(2,1)}), bf16[32,16,512]{2,1,0:T(8,128)(2,1)S(1)}, u32[]{:S(2)}, u32[]{:S(2)}) async-start(bf16[32,16,512]{2,1,0:T(8,128)(2,1)} %bitcast.65), calls=%async_computation | async-start | bytes 1048576 | tf_op jit(solution)/shard_map/all_to_all | solution.py:715
  13.3 1.0 shard_map.173
  14.4 1.4 collective-permute-done.4.refs_2_
  15.8 1.0 shard_map.174
  17.4 1.6 collective-permute-start.5
  19.0 2.9 %collective-permute-start.6 = (bf16[4,64,256]{2,1,0:T(8,128)(2,1)S(1)}, bf16[4,64,256]{2,1,0:T(8,128)(2,1)S(1)}, u32[]{:S(2)}, u32[]{:S(2)}) collective-permute-start(bf16[4,64,256]{2,1,0:T(8,128)(2,1)S(1)} %get-tuple-element.62), channel_id=1, source_target_pairs={{0,4},{1,5},{2,6},{3,7},{4,0},{5,1},{6,2},{7,3},{8,12},{9,13},{10,... | collective-permute-start | bytes 393224 | tf_op jit(solution)/shard_map/ppermute | solution.py:693
  22.1 2.6 %shard_map.172 = (bf16[512,512]{1,0:T(8,128)(2,1)}, bf16[256,1024]{1,0:T(8,128)(2,1)}) custom-call(s32[1]{0:T(128)} %bitcast.t_ref, s32[8,256]{1,0:T(8,128)S(1)} %get-tuple-element.57.refs_0_, f32[2,256]{1,0:T(2,128)S(1)} %bitcast.48, bf16[256,2048]{1,0:T(8,128)(2,1)} %refs_1_.3), custom_call_target="tpu_custom_call" | custom-call | flops 1000000000 | bytes 1048576 | tf_op jit(solution)/shard_map/pallas_call | solution.py:81
  24.7 3.6 %collective-permute-done.6.refs_4_ = bf16[4,64,256]{2,1,0:T(8,128)(2,1)S(1)} collective-permute-done((bf16[4,64,256]{2,1,0:T(8,128)(2,1)S(1)}, bf16[4,64,256]{2,1,0:T(8,128)(2,1)S(1)}, u32[]{:S(2)}, u32[]{:S(2)}) %collective-permute-start.6) | collective-permute-done | bytes 131104 | tf_op jit(solution)/shard_map/ppermute | solution.py:693
  28.3 2.2 %collective-permute-done.7.refs_5_ = bf16[4,64,256]{2,1,0:T(8,128)(2,1)S(1)} collective-permute-done((bf16[4,64,256]{2,1,0:T(8,128)(2,1)S(1)}, bf16[4,64,256]{2,1,0:T(8,128)(2,1)S(1)}, u32[]{:S(2)}, u32[]{:S(2)}) %collective-permute-start.7) | collective-permute-done | bytes 131104 | tf_op jit(solution)/shard_map/ppermute | solution.py:693
  30.6 9.8 %all-to-all-start.1 = ((bf16[32,16,512]{2,1,0:T(8,128)(2,1)}), bf16[32,16,512]{2,1,0:T(8,128)(2,1)S(1)}, u32[]{:S(2)}, u32[]{:S(2)}) async-start(bf16[32,16,512]{2,1,0:T(8,128)(2,1)} %bitcast.66), calls=%async_computation.1 | async-start | bytes 1048576 | tf_op jit(solution)/shard_map/all_to_all | solution.py:715
  41.2 3.2 %collective-permute-start.1 = (bf16[512,512]{1,0:T(8,128)(2,1)S(1)}, bf16[512,512]{1,0:T(8,128)(2,1)S(1)}, u32[]{:S(2)}, u32[]{:S(2)}) collective-permute-start(bf16[512,512]{1,0:T(8,128)(2,1)S(1)} %bitcast.35), channel_id=1, source_target_pairs={{0,6},{1,7},{2,0},{3,1},{4,2},{5,3},{6,4},{7,5},{8,14},{9,15},{10,... | collective-permute-start | bytes 1572872 | tf_op jit(solution)/shard_map/ppermute | solution.py:689
  44.4 9.5 %all-to-all-done.1 = bf16[32,16,512]{2,1,0:T(8,128)(2,1)S(1)} async-done(((bf16[32,16,512]{2,1,0:T(8,128)(2,1)}), bf16[32,16,512]{2,1,0:T(8,128)(2,1)S(1)}, u32[]{:S(2)}, u32[]{:S(2)}) %all-to-all-start.1) | async-done | bytes 524320 | tf_op jit(solution)/shard_map/all_to_all | solution.py:715
  54.6 1.4 collective-permute-start.8
  56.8 1.1 collective-permute-start.11
  57.9 1.0 collective-permute-start.9
  59.0 4.2 %collective-permute-done.10.refs_3_.refs_8_ = bf16[256,512]{1,0:T(8,128)(2,1)S(1)} collective-permute-done((bf16[256,512]{1,0:T(8,128)(2,1)S(1)}, bf16[256,512]{1,0:T(8,128)(2,1)S(1)}, u32[]{:S(2)}, u32[]{:S(2)}) %collective-permute-start.10) | collective-permute-done | bytes 262176 | tf_op jit(solution)/shard_map/ppermute | solution.py:689
  63.2 2.8 %collective-permute-start.3 = (bf16[256,512]{1,0:T(8,128)(2,1)S(1)}, bf16[256,512]{1,0:T(8,128)(2,1)S(1)}, u32[]{:S(2)}, u32[]{:S(2)}) collective-permute-start(bf16[256,512]{1,0:T(8,128)(2,1)S(1)} %slice.25), channel_id=1, source_target_pairs={{0,6},{1,7},{2,0},{3,1},{4,2},{5,3},{6,4},{7,5},{8,14},{9,15},{10,... | collective-permute-start | bytes 786440 | tf_op jit(solution)/shard_map/ppermute | solution.py:689
  66.0 6.1 %shard_map.176 = (f32[512,512]{1,0:T(8,128)}, f32[512,512]{1,0:T(8,128)}) custom-call(s32[1]{0:T(128)} %bitcast.t_ref, bf16[512,512]{1,0:T(8,128)(2,1)S(1)} %bitcast.36, bf16[512,512]{1,0:T(8,128)(2,1)S(1)} %collective-permute-done.refs_1_, bf16[512,512]{1,0:T(8,128)(2,1)S(1)} %collective-permute-done.1.refs_2_, bf16[4,512,256]{2,1,0:T(8,128)(2,1)} %bitcast.53, ...), custom_call_target="tpu_custom_call" | custom-call | flops 1000000000 | bytes 1048576 | tf_op jit(solution)/shard_map/pallas_call | solution.py:81
  72.3 3.2 %collective-permute-start.13 = (bf16[256,512]{1,0:T(8,128)(2,1)S(1)}, bf16[256,512]{1,0:T(8,128)(2,1)S(1)}, u32[]{:S(2)}, u32[]{:S(2)}) collective-permute-start(bf16[256,512]{1,0:T(8,128)(2,1)S(1)} %collective-permute-done.11.refs_4_.refs_9_), channel_id=1, source_target_pairs={{0,6},{1,7},{2,0},{3,1},{4,2},{5,3},{6,4},{7,5},{8,14},{9,15},{10,... | collective-permute-start | bytes 786440 | tf_op jit(solution)/shard_map/ppermute | solution.py:689
  75.5 3.3 %shard_map.175.refs_2_ = f32[512,512]{1,0:T(8,128)S(1)} custom-call(s32[1]{0:T(128)} %bitcast.t_ref, bf16[512,512]{1,0:T(8,128)(2,1)S(1)} %bitcast.31, bf16[256,512]{1,0:T(8,128)(2,1)S(1)} %collective-permute-done.8.refs_1_.refs_6_, bf16[256,512]{1,0:T(8,128)(2,1)S(1)} %collective-permute-done.9.refs_2_.refs_7_, ...), custom_call_target="tpu_custom_call" | custom-call | flops 1000000000 | bytes 1048576 | tf_op jit(solution)/shard_map/pallas_call | solution.py:81
  79.7 4.1 %shard_map.177 = (bf16[512,512]{1,0:T(8,128)(2,1)}, f32[512,512]{1,0:T(8,128)S(1)}, f32[512,512]{1,0:T(8,128)S(1)}) custom-call(s32[1]{0:T(128)} %bitcast.t_ref, f32[512,512]{1,0:T(8,128)} %get-tuple-element.65.refs_0_, f32[512,512]{1,0:T(8,128)} %get-tuple-element.66.refs_1_, bf16[256,512]{1,0:T(8,128)(2,1)} %copy-done.26, bf16[256,512]{1,0:T(8,128)(2,1)} %copy-done.27, ...), custom_call_target="tpu_custom_call" | custom-call | flops 2000000000 | bytes 1048576 | tf_op jit(solution)/shard_map/pallas_call | solution.py:81
  83.8 2.9 %shard_map.178 = (bf16[2,256,256]{2,1,0:T(8,128)(2,1)S(1)}, bf16[2,256,256]{2,1,0:T(8,128)(2,1)S(1)}, bf16[512,512]{1,0:T(8,128)(2,1)S(1)}, bf16[512,512]{1,0:T(8,128)(2,1)S(1)}) custom-call(s32[1]{0:T(128)} %bitcast.t_ref, bf16[256,512]{1,0:T(8,128)(2,1)S(1)} %collective-permute-done.12.refs_0_.refs_10_, ...), custom_call_target="tpu_custom_call" | custom-call | flops 2000000000 | bytes 1048576 | tf_op jit(solution)/shard_map/pallas_call | solution.py:81
  86.9 3.2 %collective-permute-start.18 = (bf16[2,256,256]{2,1,0:T(8,128)(2,1)S(1)}, bf16[2,256,256]{2,1,0:T(8,128)(2,1)S(1)}, u32[]{:S(2)}, u32[]{:S(2)}) collective-permute-start(bf16[2,256,256]{2,1,0:T(8,128)(2,1)S(1)} %get-tuple-element.73), channel_id=1, source_target_pairs={{0,6},{1,7},{2,0},{3,1},{4,2},{5,3},{6,4},{7,5},{8,14},{9,15},{10,... | collective-permute-start | bytes 786440 | tf_op jit(solution)/shard_map/ppermute | solution.py:689
  90.1 4.0 %shard_map.179 = (bf16[512,256]{1,0:T(8,128)(2,1)S(1)}, bf16[512,256]{1,0:T(8,128)(2,1)S(1)}, bf16[512,256]{1,0:T(8,128)(2,1)S(1)}, bf16[512,256]{1,0:T(8,128)(2...) custom-call(s32[1]{0:T(128)} %bitcast.t_ref, ...), custom_call_target="tpu_custom_call" | custom-call | flops 3000000000 | bytes 1048576 | tf_op jit(solution)/shard_map/pallas_call | solution.py:81
  94.6 5.2 %shard_map.181 = bf16[12,512,256]{2,1,0:T(8,128)(2,1)S(1)} custom-call(s32[1]{0:T(128)} %bitcast.t_ref, bf16[512,512]{1,0:T(8,128)(2,1)} %bitcast.37, bf16[512,512]{1,0:T(8,128)(2,1)} %copy-done.2, bf16[512,512]{1,0:T(8,128)(2,1)} %copy-done.3, bf16[256,512]{1,0:T(8,128)(2,1)} %copy-done.26, bf16[256,512]{1,0:T(8,128)(2,1)} %copy-done.27, ...), custom_call_target="tpu_custom_call" | custom-call | flops 2000000000 | bytes 1048576 | tf_op jit(solution)/shard_map/pallas_call | solution.py:81
  100.4 3.2 %collective-permute-start.21 = (bf16[512,256]{1,0:T(8,128)(2,1)S(1)}, bf16[512,256]{1,0:T(8,128)(2,1)S(1)}, u32[]{:S(2)}, u32[]{:S(2)}) collective-permute-start(bf16[512,256]{1,0:T(8,128)(2,1)S(1)} %get-tuple-element.84), channel_id=1, source_target_pairs={{0,6},{1,7},{2,0},{3,1},{4,2},{5,3},{6,4},{7,5},{8,14},{9,15},{10,... | collective-permute-start | bytes 786440 | tf_op jit(solution)/shard_map/ppermute | solution.py:689
  103.6 2.3 %collective-permute-done.22.refs_3_ = bf16[512,256]{1,0:T(8,128)(2,1)S(1)} collective-permute-done((bf16[512,256]{1,0:T(8,128)(2,1)S(1)}, bf16[512,256]{1,0:T(8,128)(2,1)S(1)}, u32[]{:S(2)}, u32[]{:S(2)}) %collective-permute-start.22) | collective-permute-done | bytes 262176 | tf_op jit(solution)/shard_map/ppermute | solution.py:693
  105.9 3.0 %collective-permute-start.24 = (bf16[512,256]{1,0:T(8,128)(2,1)S(1)}, bf16[512,256]{1,0:T(8,128)(2,1)S(1)}, u32[]{:S(2)}, u32[]{:S(2)}) collective-permute-start(bf16[512,256]{1,0:T(8,128)(2,1)S(1)} %get-tuple-element.87), channel_id=1, source_target_pairs={{0,7},{1,6},{2,1},{3,0},{4,3},{5,2},{6,5},{7,4},{8,15},{9,14},{10,... | collective-permute-start | bytes 786440 | tf_op jit(solution)/shard_map/ppermute | solution.py:697
  108.9 1.9 %collective-permute-done.20.refs_1_ = bf16[512,256]{1,0:T(8,128)(2,1)S(1)} collective-permute-done((bf16[512,256]{1,0:T(8,128)(2,1)S(1)}, bf16[512,256]{1,0:T(8,128)(2,1)S(1)}, u32[]{:S(2)}, u32[]{:S(2)}) %collective-permute-start.20) | collective-permute-done | bytes 262176 | tf_op jit(solution)/shard_map/ppermute | solution.py:689
  110.8 4.4 %collective-permute-done.23.refs_4_ = bf16[512,256]{1,0:T(8,128)(2,1)S(1)} collective-permute-done((bf16[512,256]{1,0:T(8,128)(2,1)S(1)}, bf16[512,256]{1,0:T(8,128)(2,1)S(1)}, u32[]{:S(2)}, u32[]{:S(2)}) %collective-permute-start.23) | collective-permute-done | bytes 262176 | tf_op jit(solution)/shard_map/ppermute | solution.py:697
  115.3 1.0 shard_map.183
  116.3 9.8 %all-to-all-start.2 = ((bf16[32,32,256]{2,1,0:T(8,128)(2,1)}), bf16[32,32,256]{2,1,0:T(8,128)(2,1)}, u32[]{:S(2)}, u32[]{:S(2)}) async-start(bf16[32,32,256]{2,1,0:T(8,128)(2,1)} %shard_map.183), calls=%async_computation.2 | async-start | bytes 1048576 | tf_op jit(solution)/shard_map/all_to_all | solution.py:715
  127.9 0.9 copy-done.20
  128.8 2.2 %shard_map.184 = (bf16[512,256]{1,0:T(8,128)(2,1)}, bf16[512,256]{1,0:T(8,128)(2,1)}, f32[512,256]{1,0:T(8,128)}, f32[512,256]{1,0:T(8,128)}, f32[8,256]{1,0:T(8,128)S(1)}) custom-call(s32[1]{0:T(128)} %bitcast.t_ref, bf16[64,2048]{1,0:T(8,128)(2,1)} %bitcast.64, bf16[64,256]{1,0:T(8,128)(2,1)S(1)} %bitcast.41, bf16[5,64,256]{2,1,0:T(8,128)(2,1)S(1)} %copy-done.13, ...), custom_call_target="tpu_custom_call" | custom-call | flops 100000000 | bytes 1048576 | tf_op jit(solution)/shard_map/pallas_call | solution.py:81
  131.0 8.9 %shard_map.182 = (f32[4,512,256]{2,1,0:T(8,128)}, f32[4,512,256]{2,1,0:T(8,128)}, f32[256,2048]{1,0:T(8,128)}) custom-call(s32[1]{0:T(128)} %bitcast.t_ref, bf16[512,512]{1,0:T(8,128)(2,1)} %bitcast.38, bf16[512,512]{1,0:T(8,128)(2,1)} %copy-done.2, bf16[512,512]{1,0:T(8,128)(2,1)} %copy-done.3, bf16[256,512]{1,0:T(8,128)(2,1)} %copy-done.26, ...), custom_call_target="tpu_custom_call" | custom-call | flops 2000000000 | bytes 1048576 | tf_op jit(solution)/shard_map/pallas_call | solution.py:81
  140.5 3.3 %shard_map.185 = (bf16[256,256]{1,0:T(8,128)(2,1)}, bf16[32,32,128]{2,1,0:T(8,128)(2,1)}, f32[4,72,256]{2,1,0:T(8,128)S(1)}, bf16[4,72,256]{2,1,0:T(8,128)(2,1)S(1)}) custom-call(s32[1]{0:T(128)} %bitcast.t_ref, bf16[256,1024]{1,0:T(8,128)(2,1)} %get-tuple-element.81.refs_0_, bf16[256,2048]{1,0:T(8,128)(2,1)} %refs_1_.3, bf16[1024,256]{1,0:T(8,128)(2,1)} %bitcast.22.refs_2_, ...), custom_call_target="tpu_custom_call" | custom-call | flops 1000000000 | bytes 1048576 | tf_op jit(solution)/shard_map/pallas_call | solution.py:81
  143.8 9.2 %all-to-all-start.3 = ((bf16[32,32,128]{2,1,0:T(8,128)(2,1)}), bf16[32,32,128]{2,1,0:T(8,128)(2,1)S(1)}, u32[]{:S(2)}, u32[]{:S(2)}) async-start(bf16[32,32,128]{2,1,0:T(8,128)(2,1)} %get-tuple-element.104), calls=%async_computation.3 | async-start | bytes 524288 | tf_op jit(solution)/shard_map/all_to_all | solution.py:715
  153.2 1.4 collective-permute-done.25.refs_1_
  154.6 0.9 collective-permute-start.26
  155.5 4.0 %collective-permute-start.27 = (bf16[72,256]{1,0:T(8,128)(2,1)S(1)}, bf16[72,256]{1,0:T(8,128)(2,1)S(1)}, u32[]{:S(2)}, u32[]{:S(2)}) collective-permute-start(bf16[72,256]{1,0:T(8,128)(2,1)S(1)} %get-tuple-element.97), channel_id=1, source_target_pairs={{0,4},{1,5},{2,6},{3,7},{4,0},{5,1},{6,2},{7,3},{8,12},{9,13},{10,... | collective-permute-start | bytes 110600 | tf_op jit(solution)/shard_map/ppermute | solution.py:693
  159.5 2.3 %collective-permute-done.27.refs_2_ = bf16[72,256]{1,0:T(8,128)(2,1)S(1)} collective-permute-done((bf16[72,256]{1,0:T(8,128)(2,1)S(1)}, bf16[72,256]{1,0:T(8,128)(2,1)S(1)}, u32[]{:S(2)}, u32[]{:S(2)}) %collective-permute-start.27) | collective-permute-done | bytes 36896 | tf_op jit(solution)/shard_map/ppermute | solution.py:693
  161.8 2.8 %collective-permute-done.28.refs_3_ = bf16[72,256]{1,0:T(8,128)(2,1)S(1)} collective-permute-done((bf16[72,256]{1,0:T(8,128)(2,1)S(1)}, bf16[72,256]{1,0:T(8,128)(2,1)S(1)}, u32[]{:S(2)}, u32[]{:S(2)}) %collective-permute-start.28) | collective-permute-done | bytes 36896 | tf_op jit(solution)/shard_map/ppermute | solution.py:693
  164.7 4.6 %collective-permute-start.29 = (f32[64,128]{1,0:T(8,128)S(1)}, f32[64,128]{1,0:T(8,128)S(1)}, u32[]{:S(2)}, u32[]{:S(2)}) collective-permute-start(f32[64,128]{1,0:T(8,128)S(1)} %get-tuple-element.101), channel_id=1, source_target_pairs={{8,0},{16,8},{24,16},{32,24},{40,32},{48,40},{56,48},{64,56},{72,6... | collective-permute-start | bytes 98312 | tf_op jit(solution)/shard_map/ppermute | solution.py:775
  169.5 1.9 %collective-permute-start.30 = (f32[64,64]{1,0:T(8,128)S(1)}, f32[64,64]{1,0:T(8,128)S(1)}, u32[]{:S(2)}, u32[]{:S(2)}) collective-permute-start(f32[64,64]{1,0:T(8,128)S(1)} %shard_map.190), channel_id=1, source_target_pairs={{0,0},{1,32},{2,64},{3,96},{4,128},{5,160},{6,192},{7,224},{32,1},... | collective-permute-start | bytes 49160 | tf_op jit(solution)/shard_map/ppermute | solution.py:779
  171.4 1.0 shard_map.188.refs_0_
  172.5 1.4 shard_map.189
  173.8 7.8 %collective-permute-done.30 = f32[64,64]{1,0:T(8,128)S(1)} collective-permute-done((f32[64,64]{1,0:T(8,128)S(1)}, f32[64,64]{1,0:T(8,128)S(1)}, u32[]{:S(2)}, u32[]{:S(2)}) %collective-permute-start.30) | collective-permute-done | bytes 16416 | tf_op jit(solution)/shard_map/ppermute | solution.py:779
  (105 shorter events, 9.6 us)
Async XLA Ops:
  1.3 20.8 %copy-start.24 = (f32[256,2]{0,1:T(2,128)S(1)}, f32[256,2]{0,1:T(2,128)}, u32[]{:S(2)}) copy-start(f32[256,2]{0,1:T(2,128)} %param.15) | copy-start | bytes 6148
  3.4 27.1 %all-to-all-start = ((bf16[32,16,512]{2,1,0:T(8,128)(2,1)}), bf16[32,16,512]{2,1,0:T(8,128)(2,1)S(1)}, u32[]{:S(2)}, u32[]{:S(2)}) async-start(bf16[32,16,512]{2,1,0:T(8,128)(2,1)} %bitcast.65), calls=%async_computation | async-start | bytes 1048576 | tf_op jit(solution)/shard_map/all_to_all | solution.py:715
  14.3 1.5 collective-permute-start.4
  17.4 7.3 %collective-permute-start.5 = (bf16[4,64,256]{2,1,0:T(8,128)(2,1)S(1)}, bf16[4,64,256]{2,1,0:T(8,128)(2,1)S(1)}, u32[]{:S(2)}, u32[]{:S(2)}) collective-permute-start(bf16[4,64,256]{2,1,0:T(8,128)(2,1)S(1)} %get-tuple-element.61), channel_id=1, source_target_pairs={{0,2},{1,3},{2,0},{3,1},{4,6},{5,7},{6,4},{7,5},{8,10},{9,11},{10,... | collective-permute-start | bytes 393224 | tf_op jit(solution)/shard_map/ppermute | solution.py:693
  19.0 9.3 %collective-permute-start.6 = (bf16[4,64,256]{2,1,0:T(8,128)(2,1)S(1)}, bf16[4,64,256]{2,1,0:T(8,128)(2,1)S(1)}, u32[]{:S(2)}, u32[]{:S(2)}) collective-permute-start(bf16[4,64,256]{2,1,0:T(8,128)(2,1)S(1)} %get-tuple-element.62), channel_id=1, source_target_pairs={{0,4},{1,5},{2,6},{3,7},{4,0},{5,1},{6,2},{7,3},{8,12},{9,13},{10,... | collective-permute-start | bytes 393224 | tf_op jit(solution)/shard_map/ppermute | solution.py:693
  21.9 8.7 %collective-permute-start.7 = (bf16[4,64,256]{2,1,0:T(8,128)(2,1)S(1)}, bf16[4,64,256]{2,1,0:T(8,128)(2,1)S(1)}, u32[]{:S(2)}, u32[]{:S(2)}) collective-permute-start(bf16[4,64,256]{2,1,0:T(8,128)(2,1)S(1)} %get-tuple-element.63), channel_id=1, source_target_pairs={{0,6},{1,7},{2,4},{3,5},{4,2},{5,3},{6,0},{7,1},{8,14},{9,15},{10,... | collective-permute-start | bytes 393224 | tf_op jit(solution)/shard_map/ppermute | solution.py:693
  22.1 18.8 %copy-start.25 = (bf16[1,256,2048]{2,1,0:T(8,128)(2,1)S(1)}, bf16[1,256,2048]{2,1,0:T(8,128)(2,1)}, u32[]{:S(2)}) copy-start(bf16[1,256,2048]{2,1,0:T(8,128)(2,1)} %param.23) | copy-start | bytes 3145732
  24.7 16.3 %copy-start.15 = (bf16[4,64,256]{2,1,0:T(8,128)(2,1)}, bf16[4,64,256]{2,1,0:T(8,128)(2,1)S(1)}, u32[]{:S(2)}) copy-start(bf16[4,64,256]{2,1,0:T(8,128)(2,1)S(1)} %collective-permute-done.5.refs_3_) | copy-start | bytes 393220
  28.3 12.7 %copy-start.17 = (bf16[4,64,256]{2,1,0:T(8,128)(2,1)}, bf16[4,64,256]{2,1,0:T(8,128)(2,1)S(1)}, u32[]{:S(2)}) copy-start(bf16[4,64,256]{2,1,0:T(8,128)(2,1)S(1)} %collective-permute-done.6.refs_4_) | copy-start | bytes 393220
  30.6 41.5 %copy-start.1 = (bf16[32,16,512]{2,1,0:T(8,128)(2,1)}, bf16[32,16,512]{2,1,0:T(8,128)(2,1)S(1)}, u32[]{:S(2)}) copy-start(bf16[32,16,512]{2,1,0:T(8,128)(2,1)S(1)} %all-to-all-done) | copy-start | bytes 1572868
  30.6 23.3 %all-to-all-start.1 = ((bf16[32,16,512]{2,1,0:T(8,128)(2,1)}), bf16[32,16,512]{2,1,0:T(8,128)(2,1)S(1)}, u32[]{:S(2)}, u32[]{:S(2)}) async-start(bf16[32,16,512]{2,1,0:T(8,128)(2,1)} %bitcast.66), calls=%async_computation.1 | async-start | bytes 1048576 | tf_op jit(solution)/shard_map/all_to_all | solution.py:715
  40.4 13.6 %collective-permute-start.15 = (bf16[2048,256]{1,0:T(8,128)(2,1)}, bf16[2048,256]{1,0:T(8,128)(2,1)}, u32[]{:S(2)}, u32[]{:S(2)}) collective-permute-start(bf16[2048,256]{1,0:T(8,128)(2,1)} %bitcast.52), channel_id=1, source_target_pairs={{0,1},{1,0},{2,3},{3,2},{4,5},{5,4},{6,7},{7,6},{8,9},{9,8},{10,11... | collective-permute-start | bytes 3145736 | tf_op jit(solution)/shard_map/ppermute | solution.py:693
  40.5 14.2 %collective-permute-start.16 = (bf16[2048,256]{1,0:T(8,128)(2,1)}, bf16[2048,256]{1,0:T(8,128)(2,1)}, u32[]{:S(2)}, u32[]{:S(2)}) collective-permute-start(bf16[2048,256]{1,0:T(8,128)(2,1)} %bitcast.57), channel_id=1, source_target_pairs={{0,1},{1,0},{2,3},{3,2},{4,5},{5,4},{6,7},{7,6},{8,9},{9,8},{10,11... | collective-permute-start | bytes 3145736 | tf_op jit(solution)/shard_map/ppermute | solution.py:693
  41.0 17.9 %collective-permute-start.14 = (bf16[256,2048]{1,0:T(8,128)(2,1)S(1)}, bf16[256,2048]{1,0:T(8,128)(2,1)}, u32[]{:S(2)}, u32[]{:S(2)}) collective-permute-start(bf16[256,2048]{1,0:T(8,128)(2,1)S(1)} %bitcast.51), channel_id=1, source_target_pairs={{0,1},{1,0},{2,3},{3,2},{4,5},{5,4},{6,7},{7,6},{8,9},{9,8},{10,11... | collective-permute-start | bytes 3145736 | tf_op jit(solution)/shard_map/ppermute | solution.py:693
  41.1 15.7 %collective-permute-start = (bf16[512,512]{1,0:T(8,128)(2,1)S(1)}, bf16[512,512]{1,0:T(8,128)(2,1)S(1)}, u32[]{:S(2)}, u32[]{:S(2)}) collective-permute-start(bf16[512,512]{1,0:T(8,128)(2,1)S(1)} %bitcast.34), channel_id=1, source_target_pairs={{0,2},{1,3},{2,4},{3,5},{4,6},{5,7},{6,0},{7,1},{8,10},{9,11},{10,... | collective-permute-start | bytes 1572872 | tf_op jit(solution)/shard_map/ppermute | solution.py:689
  41.2 16.7 %collective-permute-start.1 = (bf16[512,512]{1,0:T(8,128)(2,1)S(1)}, bf16[512,512]{1,0:T(8,128)(2,1)S(1)}, u32[]{:S(2)}, u32[]{:S(2)}) collective-permute-start(bf16[512,512]{1,0:T(8,128)(2,1)S(1)} %bitcast.35), channel_id=1, source_target_pairs={{0,6},{1,7},{2,0},{3,1},{4,2},{5,3},{6,4},{7,5},{8,14},{9,15},{10,... | collective-permute-start | bytes 1572872 | tf_op jit(solution)/shard_map/ppermute | solution.py:689
  53.9 21.6 %copy-start = (bf16[32,16,512]{2,1,0:T(8,128)(2,1)}, bf16[32,16,512]{2,1,0:T(8,128)(2,1)S(1)}, u32[]{:S(2)}) copy-start(bf16[32,16,512]{2,1,0:T(8,128)(2,1)S(1)} %all-to-all-done.1) | copy-start | bytes 1572868
  54.0 9.3 %collective-permute-start.10 = (bf16[256,512]{1,0:T(8,128)(2,1)S(1)}, bf16[256,512]{1,0:T(8,128)(2,1)S(1)}, u32[]{:S(2)}, u32[]{:S(2)}) collective-permute-start(bf16[256,512]{1,0:T(8,128)(2,1)S(1)} %bitcast.69), channel_id=1, source_target_pairs={{0,6},{1,7},{2,0},{3,1},{4,2},{5,3},{6,4},{7,5},{8,14},{9,15},{10,... | collective-permute-start | bytes 786440 | tf_op jit(solution)/shard_map/ppermute | solution.py:689
  54.6 17.5 %collective-permute-start.8 = (bf16[256,512]{1,0:T(8,128)(2,1)S(1)}, bf16[256,512]{1,0:T(8,128)(2,1)S(1)}, u32[]{:S(2)}, u32[]{:S(2)}) collective-permute-start(bf16[256,512]{1,0:T(8,128)(2,1)S(1)} %bitcast.70), channel_id=1, source_target_pairs={{0,2},{1,3},{2,4},{3,5},{4,6},{5,7},{6,0},{7,1},{8,10},{9,11},{10,... | collective-permute-start | bytes 786440 | tf_op jit(solution)/shard_map/ppermute | solution.py:689
  56.8 15.3 %copy-start.2 = (bf16[512,512]{1,0:T(8,128)(2,1)}, bf16[512,512]{1,0:T(8,128)(2,1)S(1)}, u32[]{:S(2)}) copy-start(bf16[512,512]{1,0:T(8,128)(2,1)S(1)} %collective-permute-done.refs_1_) | copy-start | bytes 1572868
  56.8 15.4 %collective-permute-start.11 = (bf16[256,512]{1,0:T(8,128)(2,1)S(1)}, bf16[256,512]{1,0:T(8,128)(2,1)S(1)}, u32[]{:S(2)}, u32[]{:S(2)}) collective-permute-start(bf16[256,512]{1,0:T(8,128)(2,1)S(1)} %bitcast.67), channel_id=1, source_target_pairs={{0,6},{1,7},{2,0},{3,1},{4,2},{5,3},{6,4},{7,5},{8,14},{9,15},{10,... | collective-permute-start | bytes 786440 | tf_op jit(solution)/shard_map/ppermute | solution.py:689
  57.9 14.2 %copy-start.3 = (bf16[512,512]{1,0:T(8,128)(2,1)}, bf16[512,512]{1,0:T(8,128)(2,1)S(1)}, u32[]{:S(2)}) copy-start(bf16[512,512]{1,0:T(8,128)(2,1)S(1)} %collective-permute-done.1.refs_2_) | copy-start | bytes 1572868
  57.9 17.6 %collective-permute-start.9 = (bf16[256,512]{1,0:T(8,128)(2,1)S(1)}, bf16[256,512]{1,0:T(8,128)(2,1)S(1)}, u32[]{:S(2)}, u32[]{:S(2)}) collective-permute-start(bf16[256,512]{1,0:T(8,128)(2,1)S(1)} %bitcast.68), channel_id=1, source_target_pairs={{0,2},{1,3},{2,4},{3,5},{4,6},{5,7},{6,0},{7,1},{8,10},{9,11},{10,... | collective-permute-start | bytes 786440 | tf_op jit(solution)/shard_map/ppermute | solution.py:689
  58.9 19.9 %collective-permute-start.2 = (bf16[256,512]{1,0:T(8,128)(2,1)S(1)}, bf16[256,512]{1,0:T(8,128)(2,1)S(1)}, u32[]{:S(2)}, u32[]{:S(2)}) collective-permute-start(bf16[256,512]{1,0:T(8,128)(2,1)S(1)} %slice.24), channel_id=1, source_target_pairs={{0,2},{1,3},{2,4},{3,5},{4,6},{5,7},{6,0},{7,1},{8,10},{9,11},{10,... | collective-permute-start | bytes 786440 | tf_op jit(solution)/shard_map/ppermute | solution.py:689
  63.2 12.3 %copy-start.4 = (bf16[256,512]{1,0:T(8,128)(2,1)}, bf16[256,512]{1,0:T(8,128)(2,1)S(1)}, u32[]{:S(2)}) copy-start(bf16[256,512]{1,0:T(8,128)(2,1)S(1)} %collective-permute-done.10.refs_3_.refs_8_) | copy-start | bytes 786436
  63.2 15.6 %collective-permute-start.3 = (bf16[256,512]{1,0:T(8,128)(2,1)S(1)}, bf16[256,512]{1,0:T(8,128)(2,1)S(1)}, u32[]{:S(2)}, u32[]{:S(2)}) collective-permute-start(bf16[256,512]{1,0:T(8,128)(2,1)S(1)} %slice.25), channel_id=1, source_target_pairs={{0,6},{1,7},{2,0},{3,1},{4,2},{5,3},{6,4},{7,5},{8,14},{9,15},{10,... | collective-permute-start | bytes 786440 | tf_op jit(solution)/shard_map/ppermute | solution.py:689
  72.2 11.6 %collective-permute-start.12 = (bf16[256,512]{1,0:T(8,128)(2,1)S(1)}, bf16[256,512]{1,0:T(8,128)(2,1)S(1)}, u32[]{:S(2)}, u32[]{:S(2)}) collective-permute-start(bf16[256,512]{1,0:T(8,128)(2,1)S(1)} %collective-permute-done.8.refs_1_.refs_6_), channel_id=1, source_target_pairs={{0,2},{1,3},{2,4},{3,5},{4,6},{5,7},{6,0},{7,1},{8,10},{9,11},{10,... | collective-permute-start | bytes 786440 | tf_op jit(solution)/shard_map/ppermute | solution.py:689
  72.3 11.5 %collective-permute-start.13 = (bf16[256,512]{1,0:T(8,128)(2,1)S(1)}, bf16[256,512]{1,0:T(8,128)(2,1)S(1)}, u32[]{:S(2)}, u32[]{:S(2)}) collective-permute-start(bf16[256,512]{1,0:T(8,128)(2,1)S(1)} %collective-permute-done.11.refs_4_.refs_9_), channel_id=1, source_target_pairs={{0,6},{1,7},{2,0},{3,1},{4,2},{5,3},{6,4},{7,5},{8,14},{9,15},{10,... | collective-permute-start | bytes 786440 | tf_op jit(solution)/shard_map/ppermute | solution.py:689
  86.8 7.7 %collective-permute-start.17 = (bf16[2,256,256]{2,1,0:T(8,128)(2,1)S(1)}, bf16[2,256,256]{2,1,0:T(8,128)(2,1)S(1)}, u32[]{:S(2)}, u32[]{:S(2)}) collective-permute-start(bf16[2,256,256]{2,1,0:T(8,128)(2,1)S(1)} %get-tuple-element.72), channel_id=1, source_target_pairs={{0,2},{1,3},{2,4},{3,5},{4,6},{5,7},{6,0},{7,1},{8,10},{9,11},{10,... | collective-permute-start | bytes 786440 | tf_op jit(solution)/shard_map/ppermute | solution.py:689
  86.9 7.6 %collective-permute-start.18 = (bf16[2,256,256]{2,1,0:T(8,128)(2,1)S(1)}, bf16[2,256,256]{2,1,0:T(8,128)(2,1)S(1)}, u32[]{:S(2)}, u32[]{:S(2)}) collective-permute-start(bf16[2,256,256]{2,1,0:T(8,128)(2,1)S(1)} %get-tuple-element.73), channel_id=1, source_target_pairs={{0,6},{1,7},{2,0},{3,1},{4,2},{5,3},{6,4},{7,5},{8,14},{9,15},{10,... | collective-permute-start | bytes 786440 | tf_op jit(solution)/shard_map/ppermute | solution.py:689
  99.8 26.3 %copy-start.13 = (bf16[5,64,256]{2,1,0:T(8,128)(2,1)S(1)}, bf16[5,64,256]{2,1,0:T(8,128)(2,1)}, u32[]{:S(2)}) copy-start(bf16[5,64,256]{2,1,0:T(8,128)(2,1)} %copy-done.12) | copy-start | bytes 491524
  99.8 31.2 %collective-permute-start.19 = (bf16[12,512,256]{2,1,0:T(8,128)(2,1)S(1)}, bf16[12,512,256]{2,1,0:T(8,128)(2,1)}, u32[]{:S(2)}, u32[]{:S(2)}) collective-permute-start(bf16[12,512,256]{2,1,0:T(8,128)(2,1)S(1)} %shard_map.181), channel_id=1, source_target_pairs={{0,1},{1,0},{2,3},{3,2},{4,5},{5,4},{6,7},{7,6},{8,9},{9,8},{10,11... | collective-permute-start | bytes 9437192 | tf_op jit(solution)/shard_map/ppermute | solution.py:693
  99.9 6.0 %collective-permute-start.22 = (bf16[512,256]{1,0:T(8,128)(2,1)S(1)}, bf16[512,256]{1,0:T(8,128)(2,1)S(1)}, u32[]{:S(2)}, u32[]{:S(2)}) collective-permute-start(bf16[512,256]{1,0:T(8,128)(2,1)S(1)} %get-tuple-element.85), channel_id=1, source_target_pairs={{0,1},{1,0},{2,3},{3,2},{4,5},{5,4},{6,7},{7,6},{8,9},{9,8},{10,11... | collective-permute-start | bytes 786440 | tf_op jit(solution)/shard_map/ppermute | solution.py:693
  100.4 10.4 %collective-permute-start.20 = (bf16[512,256]{1,0:T(8,128)(2,1)S(1)}, bf16[512,256]{1,0:T(8,128)(2,1)S(1)}, u32[]{:S(2)}, u32[]{:S(2)}) collective-permute-start(bf16[512,256]{1,0:T(8,128)(2,1)S(1)} %get-tuple-element.78), channel_id=1, source_target_pairs={{0,2},{1,3},{2,4},{3,5},{4,6},{5,7},{6,0},{7,1},{8,10},{9,11},{10,... | collective-permute-start | bytes 786440 | tf_op jit(solution)/shard_map/ppermute | solution.py:689
  100.4 10.4 %collective-permute-start.21 = (bf16[512,256]{1,0:T(8,128)(2,1)S(1)}, bf16[512,256]{1,0:T(8,128)(2,1)S(1)}, u32[]{:S(2)}, u32[]{:S(2)}) collective-permute-start(bf16[512,256]{1,0:T(8,128)(2,1)S(1)} %get-tuple-element.84), channel_id=1, source_target_pairs={{0,6},{1,7},{2,0},{3,1},{4,2},{5,3},{6,4},{7,5},{8,14},{9,15},{10,... | collective-permute-start | bytes 786440 | tf_op jit(solution)/shard_map/ppermute | solution.py:689
  103.6 11.6 %collective-permute-start.23 = (bf16[512,256]{1,0:T(8,128)(2,1)S(1)}, bf16[512,256]{1,0:T(8,128)(2,1)S(1)}, u32[]{:S(2)}, u32[]{:S(2)}) collective-permute-start(bf16[512,256]{1,0:T(8,128)(2,1)S(1)} %get-tuple-element.86), channel_id=1, source_target_pairs={{0,3},{1,2},{2,5},{3,4},{4,7},{5,6},{6,1},{7,0},{8,11},{9,10},{10,... | collective-permute-start | bytes 786440 | tf_op jit(solution)/shard_map/ppermute | solution.py:697
  105.9 9.4 %collective-permute-start.24 = (bf16[512,256]{1,0:T(8,128)(2,1)S(1)}, bf16[512,256]{1,0:T(8,128)(2,1)S(1)}, u32[]{:S(2)}, u32[]{:S(2)}) collective-permute-start(bf16[512,256]{1,0:T(8,128)(2,1)S(1)} %get-tuple-element.87), channel_id=1, source_target_pairs={{0,7},{1,6},{2,1},{3,0},{4,3},{5,2},{6,5},{7,4},{8,15},{9,14},{10,... | collective-permute-start | bytes 786440 | tf_op jit(solution)/shard_map/ppermute | solution.py:697
  116.3 24.3 %all-to-all-start.2 = ((bf16[32,32,256]{2,1,0:T(8,128)(2,1)}), bf16[32,32,256]{2,1,0:T(8,128)(2,1)}, u32[]{:S(2)}, u32[]{:S(2)}) async-start(bf16[32,32,256]{2,1,0:T(8,128)(2,1)} %shard_map.183), calls=%async_computation.2 | async-start | bytes 1048576 | tf_op jit(solution)/shard_map/all_to_all | solution.py:715
  140.5 28.8 %copy-start.28 = (f32[31,64]{1,0:T(8,128)S(1)}, f32[31,64]{1,0:T(8,128)}, u32[]{:S(2)}) copy-start(f32[31,64]{1,0:T(8,128)} %param.18) | copy-start | bytes 23812
  140.5 31.9 %copy-start.21 = (bf16[256,64]{0,1:T(8,128)(2,1)S(1)}, bf16[256,64]{0,1:T(8,128)(2,1)}, u32[]{:S(2)}) copy-start(bf16[256,64]{0,1:T(8,128)(2,1)} %param.16) | copy-start | bytes 98308
  140.5 31.9 %copy-start.22 = (bf16[256,64]{0,1:T(8,128)(2,1)S(1)}, bf16[256,64]{0,1:T(8,128)(2,1)}, u32[]{:S(2)}) copy-start(bf16[256,64]{0,1:T(8,128)(2,1)} %param.17) | copy-start | bytes 98308
  143.8 25.6 %all-to-all-start.3 = ((bf16[32,32,128]{2,1,0:T(8,128)(2,1)}), bf16[32,32,128]{2,1,0:T(8,128)(2,1)S(1)}, u32[]{:S(2)}, u32[]{:S(2)}) async-start(bf16[32,32,128]{2,1,0:T(8,128)(2,1)} %get-tuple-element.104), calls=%async_computation.3 | async-start | bytes 524288 | tf_op jit(solution)/shard_map/all_to_all | solution.py:715
  153.1 1.5 collective-permute-start.25
  154.6 4.9 %collective-permute-start.26 = (bf16[72,256]{1,0:T(8,128)(2,1)S(1)}, bf16[72,256]{1,0:T(8,128)(2,1)S(1)}, u32[]{:S(2)}, u32[]{:S(2)}) collective-permute-start(bf16[72,256]{1,0:T(8,128)(2,1)S(1)} %get-tuple-element.96), channel_id=1, source_target_pairs={{0,2},{1,3},{2,0},{3,1},{4,6},{5,7},{6,4},{7,5},{8,10},{9,11},{10,... | collective-permute-start | bytes 110600 | tf_op jit(solution)/shard_map/ppermute | solution.py:693
  155.5 6.4 %collective-permute-start.27 = (bf16[72,256]{1,0:T(8,128)(2,1)S(1)}, bf16[72,256]{1,0:T(8,128)(2,1)S(1)}, u32[]{:S(2)}, u32[]{:S(2)}) collective-permute-start(bf16[72,256]{1,0:T(8,128)(2,1)S(1)} %get-tuple-element.97), channel_id=1, source_target_pairs={{0,4},{1,5},{2,6},{3,7},{4,0},{5,1},{6,2},{7,3},{8,12},{9,13},{10,... | collective-permute-start | bytes 110600 | tf_op jit(solution)/shard_map/ppermute | solution.py:693
  159.5 5.2 %collective-permute-start.28 = (bf16[72,256]{1,0:T(8,128)(2,1)S(1)}, bf16[72,256]{1,0:T(8,128)(2,1)S(1)}, u32[]{:S(2)}, u32[]{:S(2)}) collective-permute-start(bf16[72,256]{1,0:T(8,128)(2,1)S(1)} %get-tuple-element.98), channel_id=1, source_target_pairs={{0,6},{1,7},{2,4},{3,5},{4,2},{5,3},{6,0},{7,1},{8,14},{9,15},{10,... | collective-permute-start | bytes 110600 | tf_op jit(solution)/shard_map/ppermute | solution.py:693
  164.7 7.7 %collective-permute-start.29 = (f32[64,128]{1,0:T(8,128)S(1)}, f32[64,128]{1,0:T(8,128)S(1)}, u32[]{:S(2)}, u32[]{:S(2)}) collective-permute-start(f32[64,128]{1,0:T(8,128)S(1)} %get-tuple-element.101), channel_id=1, source_target_pairs={{8,0},{16,8},{24,16},{32,24},{40,32},{48,40},{56,48},{64,56},{72,6... | collective-permute-start | bytes 98312 | tf_op jit(solution)/shard_map/ppermute | solution.py:775
  169.5 12.1 %collective-permute-start.30 = (f32[64,64]{1,0:T(8,128)S(1)}, f32[64,64]{1,0:T(8,128)S(1)}, u32[]{:S(2)}, u32[]{:S(2)}) collective-permute-start(f32[64,64]{1,0:T(8,128)S(1)} %shard_map.190), channel_id=1, source_target_pairs={{0,0},{1,32},{2,64},{3,96},{4,128},{5,160},{6,192},{7,224},{32,1},... | collective-permute-start | bytes 49160 | tf_op jit(solution)/shard_map/ppermute | solution.py:779
  (16 other events, 65.4 us)
